TPU v7x, 128 devices: a whole 4x4x4 slice. The times are simulated.
128 devices in a mesh: sp: 16 (over z, x), tp: 8 (over y, core).
Axes of the slice: x: 4, y: 4, z: 4, core: 2. Of those that a mesh axis runs over, the one named last changes fastest.
Arguments:
- queries: bfloat16 [8192, 2048], P('sp', 'tp'), may hold values from -4.5 to 4.5
- keys: bfloat16 [8192, 2048], P('sp', 'tp'), may hold values from -4.5 to 4.5
- values: bfloat16 [8192, 2048], P('sp', 'tp'), may hold values from -6 to 6
- forget_logits: float32 [8192, 16], P('sp', 'tp'), may hold values from -1 to 20
- layer_input: bfloat16 [8192, 4096], P('sp', 'tp'), may hold values from -0.09375 to 0.09375
- out_grad: bfloat16 [8192, 2048], P('sp', 'tp'), may hold values from -6 to 6
Outputs:
- query_grad: float32 [8192, 2048], P('sp', 'tp')
- key_grad: float32 [8192, 2048], P('sp', 'tp')
- value_grad: float32 [8192, 2048], P('sp', 'tp')
- weight_grad: float32 [4096, 2048], P('sp', 'tp')
All inputs are finite; a program needn't handle non-finite values.
Results may differ from a plain program's by a relative error of at most 0.04.
Values may be sent and summed in bfloat16 or wider, within the bound.
No kernel may reach another device: no remote copies, remote signals or barrier semaphores. Data moves between devices by JAX's collectives and lax.ppermute only.
A program may use at most 64 MiB of HBM per device.

v0:
```python
import functools
import math

import jax
import jax.numpy as jnp
from jax import lax
from jax.experimental import pallas as pl
from jax.experimental.pallas import tpu as pltpu
from jax.sharding import PartitionSpec as P


HEAD = 128
SIDE = 4
SCALE = HEAD ** (-0.5)
LOG2E = math.log2(math.e)
NEG_BIG = -1e30
SUB = 256


def along_z(r):
    return [(4 * z + x, 4 * ((z + r) % SIDE) + x) for z in range(SIDE) for x in range(SIDE)]


def along_x(r):
    return [(4 * z + x, 4 * z + (x + r) % SIDE) for z in range(SIDE) for x in range(SIDE)]


def fetched(array, axis_perm):
    return [array] + [lax.ppermute(array, "sp", axis_perm(-r)) for r in range(1, SIDE)]


def dot_nt(a, b):
    return lax.dot_general(a, b, (((1,), (1,)), ((), ())), preferred_element_type=jnp.float32)


def dot_nn(a, b):
    return lax.dot_general(a, b, (((1,), (0,)), ((), ())), preferred_element_type=jnp.float32)


def start_loads(z_refs, x_refs, slots, qd, kv, sems):
    copies = []
    for r, z_ref, x_ref in zip(slots, z_refs, x_refs):
        for ref, dst, half in (
            (z_ref, qd.at[0, r], 0),
            (x_ref, kv.at[0, r], 0),
            (x_ref, qd.at[1, r], 1),
            (z_ref, kv.at[1, r], 1),
        ):
            cols = pl.ds(half * 2 * HEAD, 2 * HEAD)
            copies.append(pltpu.make_async_copy(ref.at[:, cols], dst, sems.at[len(copies)]))
    for c in copies:
        c.start()
    return copies


def gates_kernel(logits_ref, out_ref):
    sums = jax.nn.log_sigmoid(logits_ref[...])
    rows, width = sums.shape
    lane = lax.broadcasted_iota(jnp.int32, sums.shape, 1)
    step = 1
    while step < width:
        sums = sums + jnp.where(lane >= step, pltpu.roll(sums, step, axis=1), 0.0)
        step *= 2
    shape = (rows, rows)
    mine, other = (lax.broadcasted_iota(jnp.int32, shape, d) for d in (0, 1))
    earlier = jnp.where((other < mine) & (other % 2 == mine % 2), 1.0, 0.0)
    totals = jnp.broadcast_to(sums[:, width - 1 :], (rows, HEAD))
    before = jnp.dot(
        earlier, totals, preferred_element_type=jnp.float32, precision=lax.Precision.HIGHEST
    )
    out_ref[...] = (sums + wide(before, width)) * LOG2E


def fill_bias(pos_ref, bias_ref, bcol, h):
    def one(r, _):
        row = bias_ref[pl.ds(2 * pos_ref[h, 1, r] + h, 1), :]
        for j in range(4):
            tile = jnp.broadcast_to(row[:, j * HEAD : (j + 1) * HEAD], (HEAD, HEAD))
            bcol[r, j * HEAD : (j + 1) * HEAD, :] = tile.T
        return 0

    lax.fori_loop(0, SIDE, one, 0)


def visible_mask(shape, first_query):
    key_at = lax.broadcasted_iota(jnp.int32, shape, 0)
    query_at = lax.broadcasted_iota(jnp.int32, shape, 1) + first_query
    return key_at <= query_at


def wide(tile, width):
    return jnp.concatenate([tile] * (width // tile.shape[1]), axis=1)


NEAR = (0, 1, 3)


def near_slot(n):
    return n + n // 2


def near_pairs(n):
    return near_slot(n // 3), near_slot(n % 3)


def far_pairs(n):
    near = near_slot(jnp.maximum(n - SIDE, 0))
    return jnp.where(n < SIDE, 2, near), jnp.where(n < SIDE, n, 2)


def stats_kernel(slots, pair_count, pair_of, pos_ref, bias_ref, *rest):
    n_slots = len(slots)
    z_refs, x_refs = rest[:n_slots], rest[n_slots : 2 * n_slots]
    rest = rest[2 * n_slots :]
    known, rest = rest[:-7], rest[-7:]
    outs = rest[:2]
    qd, kv, bcol, stats, sems = rest[2:]
    span = qd.shape[2]
    copies = start_loads(z_refs, x_refs, slots, qd, kv, sems)
    if known:
        stats[0] = known[0][...]
        stats[1] = known[1][...]
    else:
        stats[...] = jnp.zeros_like(stats)
        stats[:, :, 0:1, :] = jnp.full((2, SIDE, 1, span), NEG_BIG, jnp.float32)
    for c in copies:
        c.wait()

    def block(h, qi, ki, diagonal):
        for s in range(span // SUB):
            cols = slice(s * SUB, (s + 1) * SUB)
            q = qd[h, qi, cols, :HEAD]
            do = qd[h, qi, cols, HEAD:]
            k = kv[h, ki, :, :HEAD]
            v = kv[h, ki, :, HEAD:]
            x = dot_nt(k, q) * (SCALE * LOG2E) - wide(bcol[ki], SUB)
            if diagonal:
                x = jnp.where(visible_mask(x.shape, s * SUB), x, NEG_BIG)
            dp = dot_nt(v, do)
            old = stats[h, qi, 0:1, cols]
            new = jnp.maximum(old, jnp.max(x, axis=0, keepdims=True))
            p = jnp.exp2(x - new)
            shrink = jnp.exp2(old - new)
            stats[h, qi, 0:1, cols] = new
            stats[h, qi, 1:2, cols] = stats[h, qi, 1:2, cols] * shrink + jnp.sum(
                p, axis=0, keepdims=True
            )
            stats[h, qi, 2:3, cols] = stats[h, qi, 2:3, cols] * shrink + jnp.sum(
                p * dp, axis=0, keepdims=True
            )

    def one_head(h, _):
        fill_bias(pos_ref, bias_ref, bcol, h)

        def one_pair(n, _):
            qi, ki = pair_of(n)
            q_span, k_span = pos_ref[h, 0, qi], pos_ref[h, 1, ki]

            @pl.when(k_span < q_span)
            def _():
                block(h, qi, ki, False)

            @pl.when(k_span == q_span)
            def _():
                block(h, qi, ki, True)

            return 0

        lax.fori_loop(0, pair_count, one_pair, 0)
        return 0

    lax.fori_loop(0, 2, one_head, 0)
    outs[0][...] = stats[0]
    outs[1][...] = stats[1]


def grads_kernel(pos_ref, bias_ref, *rest):
    z_refs, x_refs = rest[:4], rest[4:8]
    stat_refs = (rest[8:12], rest[12:16])
    outs = rest[16:32]
    qd, kv, bcol, rows, kt, dqt, dkv, sems = rest[32:]
    span = qd.shape[2]
    copies = start_loads(z_refs, x_refs, range(SIDE), qd, kv, sems)
    dqt[...] = jnp.zeros_like(dqt)
    dkv[...] = jnp.zeros_like(dkv)
    for h in range(2):
        for r in range(SIDE):
            parts = [stat_refs[h][s][(r - s) % SIDE] for s in range(SIDE)]
            top = functools.reduce(jnp.maximum, [p[0:1, :] for p in parts])
            factors = [jnp.exp2(p[0:1, :] - top) for p in parts]
            total = sum(p[1:2, :] * f for p, f in zip(parts, factors))
            mixed = sum(p[2:3, :] * f for p, f in zip(parts, factors))
            rows[h, r, 0:1, :] = top + jnp.log2(total)
            rows[h, r, 1:2, :] = mixed / total
    for c in copies:
        c.wait()

    def block(h, qi, ki, diagonal):
        for s in range(span // SUB):
            cols = slice(s * SUB, (s + 1) * SUB)
            q = qd[h, qi, cols, :HEAD]
            do = qd[h, qi, cols, HEAD:]
            k = kv[h, ki, :, :HEAD]
            v = kv[h, ki, :, HEAD:]
            x = dot_nt(k, q) * (SCALE * LOG2E) - wide(bcol[ki], SUB) - rows[h, qi, 0:1, cols]
            if diagonal:
                x = jnp.where(visible_mask(x.shape, s * SUB), x, NEG_BIG)
            p = jnp.exp2(x)
            ds = (p * (dot_nt(v, do) - rows[h, qi, 1:2, cols])).astype(jnp.bfloat16)
            dkv[h, ki, :, HEAD:] += dot_nn(p.astype(jnp.bfloat16), do)
            dkv[h, ki, :, :HEAD] += dot_nn(ds, q)
            dqt[h, qi, :, cols] += dot_nn(kt[ki], ds)

    def one_head(h, _):
        fill_bias(pos_ref, bias_ref, bcol, h)

        def turn(r, _):
            kt[r] = kv[h, r, :, :HEAD].astype(jnp.float32).T.astype(jnp.bfloat16)
            return 0

        lax.fori_loop(0, SIDE, turn, 0)

        def one_pair(n, _):
            ki, qi = n // SIDE, n % SIDE
            q_span, k_span = pos_ref[h, 0, qi], pos_ref[h, 1, ki]

            @pl.when(k_span < q_span)
            def _():
                block(h, qi, ki, False)

            @pl.when(k_span == q_span)
            def _():
                block(h, qi, ki, True)

            return 0

        lax.fori_loop(0, SIDE * SIDE, one_pair, 0)
        return 0

    lax.fori_loop(0, 2, one_head, 0)
    for h in range(2):
        for r in range(SIDE):
            dq_out, dkv_out = outs[SIDE * h + r], outs[8 + SIDE * h + r]
            dq_out[...] = (dqt[h, r] * SCALE).astype(dq_out.dtype)
            dkv_out[:, :HEAD] = (dkv[h, r, :, :HEAD] * SCALE).astype(dkv_out.dtype)
            dkv_out[:, HEAD:] = dkv[h, r, :, HEAD:].astype(dkv_out.dtype)


def weight_kernel(at_ref, *rest):
    dq_refs, in_refs, outs = rest[:4], rest[4:12], rest[12:16]
    dqs, inputs, sems = rest[16:]
    copies = []
    for r in range(SIDE):
        for other in range(2):
            copies.append(
                pltpu.make_async_copy(
                    in_refs[SIDE * other + r],
                    inputs.at[at_ref[3, other], at_ref[0, r]],
                    sems.at[2 * r + other],
                )
            )
        copies.append(pltpu.make_async_copy(dq_refs[r], dqs.at[at_ref[1, r]], sems.at[8 + r]))
    for c in copies:
        c.start()
    for c in copies:
        c.wait()
    width = outs[0].shape[1]
    for r in (1, 2, 3, 0):
        block = at_ref[2, r]
        cols = pl.ds(pl.multiple_of((block % 2) * width, width), width)
        total = sum(dot_nn(dqs[a], inputs[block // 2, a, :, cols]) for a in range(SIDE))
        outs[r][...] = total.astype(outs[r].dtype)


ANY = pl.BlockSpec(memory_space=pl.ANY)
VM = pl.BlockSpec(memory_space=pltpu.VMEM)
SM = pl.BlockSpec(memory_space=pltpu.SMEM)


def stats_call(pos, bias, z_parts, x_parts, known=None):
    span = z_parts[0].shape[0]
    if known is None:
        slots, pair_count, pair_of, known = NEAR, 9, near_pairs, ()
        z_parts, x_parts = ([parts[r] for r in NEAR] for parts in (z_parts, x_parts))
    else:
        slots, pair_count, pair_of = range(SIDE), 7, far_pairs
    pairs = pair_count * span * span
    return pl.pallas_call(
        functools.partial(stats_kernel, slots, pair_count, pair_of),
        out_shape=[jax.ShapeDtypeStruct((SIDE, 8, span), jnp.float32)] * 2,
        in_specs=[SM, VM] + [ANY] * (2 * len(slots)) + [VM] * len(known),
        out_specs=[VM] * 2,
        scratch_shapes=[
            pltpu.VMEM((2, SIDE, span, 2 * HEAD), jnp.bfloat16),
            pltpu.VMEM((2, SIDE, span, 2 * HEAD), jnp.bfloat16),
            pltpu.VMEM((SIDE, span, HEAD), jnp.float32),
            pltpu.VMEM((2, SIDE, 8, span), jnp.float32),
            pltpu.SemaphoreType.DMA((16,)),
        ],
        compiler_params=pltpu.CompilerParams(vmem_limit_bytes=20 << 20),
        cost_estimate=pl.CostEstimate(
            flops=4 * HEAD * pairs, bytes_accessed=4 << 20, transcendentals=pairs
        ),
        name="stats",
    )(pos, bias, *z_parts, *x_parts, *known)


def grads_call(pos, bias, z_parts, x_parts, z_stats, x_stats):
    span = z_parts[0].shape[0]
    pairs = 17 * span * span

    def shapes(*shape):
        own = jax.ShapeDtypeStruct(shape, jnp.float32)
        send = jax.ShapeDtypeStruct(shape, jnp.bfloat16)
        return ([own] + [send] * 3) * 2

    outs = pl.pallas_call(
        grads_kernel,
        out_shape=shapes(HEAD, span) + shapes(span, 2 * HEAD),
        in_specs=[SM, VM] + [ANY] * 8 + [VM] * 8,
        out_specs=[VM] * 16,
        scratch_shapes=[
            pltpu.VMEM((2, SIDE, span, 2 * HEAD), jnp.bfloat16),
            pltpu.VMEM((2, SIDE, span, 2 * HEAD), jnp.bfloat16),
            pltpu.VMEM((SIDE, span, HEAD), jnp.float32),
            pltpu.VMEM((2, SIDE, 8, span), jnp.float32),
            pltpu.VMEM((SIDE, HEAD, span), jnp.bfloat16),
            pltpu.VMEM((2, SIDE, HEAD, span), jnp.float32),
            pltpu.VMEM((2, SIDE, span, 2 * HEAD), jnp.float32),
            pltpu.SemaphoreType.DMA((16,)),
        ],
        compiler_params=pltpu.CompilerParams(vmem_limit_bytes=32 << 20),
        cost_estimate=pl.CostEstimate(
            flops=10 * HEAD * pairs, bytes_accessed=8 << 20, transcendentals=pairs
        ),
        name="grads",
    )(pos, bias, *z_parts, *x_parts, *z_stats, *x_stats)
    return outs[:4], outs[4:8], outs[8:12], outs[12:]


def weight_call(at, query_grads, inputs):
    cols, rows = query_grads[0].shape
    width = inputs[0].shape[1]
    own = jax.ShapeDtypeStruct((cols, width // 2), jnp.float32)
    send = jax.ShapeDtypeStruct((cols, width // 2), jnp.bfloat16)
    return pl.pallas_call(
        weight_kernel,
        out_shape=[own] + [send] * 3,
        in_specs=[SM] + [ANY] * 12,
        out_specs=[VM] * 4,
        scratch_shapes=[
            pltpu.VMEM((SIDE, cols, rows), jnp.bfloat16),
            pltpu.VMEM((2, SIDE, rows, width), jnp.bfloat16),
            pltpu.SemaphoreType.DMA((12,)),
        ],
        compiler_params=pltpu.CompilerParams(vmem_limit_bytes=32 << 20),
        cost_estimate=pl.CostEstimate(
            flops=16 * rows * width * cols, bytes_accessed=6 << 20, transcendentals=0
        ),
        name="weight",
    )(at, *query_grads, *inputs)


def head_of(array, h):
    return array[:, h * HEAD : (h + 1) * HEAD]


def local(queries, keys, values, forget_logits, layer_input, out_grad):
    here = lax.axis_index("sp")
    z, x = here // SIDE, here % SIDE
    part = lax.axis_index("tp")
    y, core = part // 2, part % 2
    steps = jnp.arange(SIDE, dtype=jnp.int32)
    z_spans = 4 * ((z + steps) % SIDE) + x
    x_spans = 4 * z + (x + steps) % SIDE
    pos = jnp.stack([jnp.stack([z_spans, x_spans]), jnp.stack([x_spans, z_spans])]).astype(
        jnp.int32
    )
    cores = jnp.stack([core, 1 - core, core, 1 - core])
    at = jnp.stack([(y + steps) % SIDE, (z + steps) % SIDE, (x + steps) % SIDE, cores]).astype(
        jnp.int32
    )

    gates = lax.all_to_all(jnp.tile(forget_logits.T, (16, 1)), "sp", 0, 0, tiled=True)

    for_z = jnp.concatenate(
        [head_of(queries, 0), head_of(out_grad, 0), head_of(keys, 1), head_of(values, 1)], axis=1
    )
    for_x = jnp.concatenate(
        [head_of(keys, 0), head_of(values, 0), head_of(queries, 1), head_of(out_grad, 1)], axis=1
    )
    z_parts = fetched(for_z, along_z)
    x_parts = fetched(for_x, along_x)

    bias = pl.pallas_call(
        gates_kernel,
        out_shape=jax.ShapeDtypeStruct(gates.shape, jnp.float32),
        in_specs=[VM],
        out_specs=VM,
        cost_estimate=pl.CostEstimate(flops=10**6, bytes_accessed=1 << 17, transcendentals=0),
        name="gate_sums",
    )(gates)

    swap = [
        (((a * SIDE + b) * SIDE + c) * 2 + d, ((c * SIDE + b) * SIDE + a) * 2 + d)
        for a in range(SIDE)
        for b in range(SIDE)
        for c in range(SIDE)
        for d in range(2)
    ]
    moved = lax.ppermute(layer_input, ("sp", "tp"), swap)
    inputs = [moved]
    for r in range(1, SIDE):
        inputs.append(lax.ppermute(moved, "tp", [(p, (p - 2 * r) % 8) for p in range(8)]))
    for part in list(inputs):
        inputs.append(lax.ppermute(part, "tp", [(p, p ^ 1) for p in range(8)]))

    known = stats_call(pos, bias, z_parts, x_parts)
    stats_z, stats_x = stats_call(pos, bias, z_parts, x_parts, known)
    z_stats = fetched(stats_z, along_z)
    x_stats = fetched(stats_x, along_x)
    dq_0, dq_1, dkv_0, dkv_1 = grads_call(pos, bias, z_parts, x_parts, z_stats, x_stats)

    def summed(parts, axis_perm):
        total = parts[0]
        for r in range(1, SIDE):
            total = total + lax.ppermute(parts[r], "sp", axis_perm(r)).astype(jnp.float32)
        return total

    query_t = jnp.concatenate([summed(dq_0, along_z), summed(dq_1, along_x)], axis=0)
    low, dkv_0, dkv_1 = lax.optimization_barrier((query_t.astype(jnp.bfloat16), dkv_0, dkv_1))
    low_parts = fetched(low, along_z)
    terms = weight_call(at, low_parts, inputs)
    weight_grad = summed(terms, along_x).T
    sum_0, sum_1 = summed(dkv_0, along_x), summed(dkv_1, along_z)
    query_grad = query_t.T
    key_grad = jnp.concatenate([head_of(sum_0, 0), head_of(sum_1, 0)], axis=1)
    value_grad = jnp.concatenate([head_of(sum_0, 1), head_of(sum_1, 1)], axis=1)
    return (query_grad, key_grad, value_grad, weight_grad)


def solution(mesh):
    placed = P("sp", "tp")

    return jax.shard_map(
        local,
        mesh=mesh,
        in_specs=(placed,) * 6,
        out_specs=(placed,) * 4,
        check_vma=False,
    )
```

profile of v0, /device:TPU:0, one launch (start us, length us, event | category | flops | bytes accessed | tf_op | source)
XLA Modules:
  0.0 204.1 jit_solution(7446524244690224571)
XLA Ops:
  0.7 1.2 fusion.7
  2.1 4.2 %collective-permute-start = (bf16[512,512]{1,0:T(8,128)(2,1)S(1)}, bf16[512,512]{1,0:T(8,128)(2,1)S(1)}, u32[]{:S(2)}, u32[]{:S(2)}) collective-permute-start(bf16[512,512]{1,0:T(8,128)(2,1)S(1)} %pad_maximum_fusion.rest_0_), channel_id=1, source_target_pairs={{0,96},{8,104},{16,112},{24,120},{32,0},{40,8},{48,16},{56,24},{64... | collective-permute-start | bytes 1572872 | tf_op jit(solution)/shard_map/ppermute | solution.py:29
  6.4 2.8 %collective-permute-start.3 = (bf16[512,512]{1,0:T(8,128)(2,1)S(1)}, bf16[512,512]{1,0:T(8,128)(2,1)S(1)}, u32[]{:S(2)}, u32[]{:S(2)}) collective-permute-start(bf16[512,512]{1,0:T(8,128)(2,1)S(1)} %pad_maximum_fusion.1.rest_3_.rest_4_), channel_id=1, source_target_pairs={{0,24},{8,0},{16,8},{24,16},{32,56},{40,32},{48,40},{56,48},{64,88... | collective-permute-start | bytes 1572872 | tf_op jit(solution)/shard_map/ppermute | solution.py:29
  9.2 1.9 collective-permute-start.1
  11.1 17.7 %collective-permute-done.rest_1_ = bf16[512,512]{1,0:T(8,128)(2,1)S(1)} collective-permute-done((bf16[512,512]{1,0:T(8,128)(2,1)S(1)}, bf16[512,512]{1,0:T(8,128)(2,1)S(1)}, u32[]{:S(2)}, u32[]{:S(2)}) %collective-permute-start) | collective-permute-done | bytes 524320 | tf_op jit(solution)/shard_map/ppermute | solution.py:29
  28.7 3.0 %collective-permute-start.4 = (bf16[512,512]{1,0:T(8,128)(2,1)S(1)}, bf16[512,512]{1,0:T(8,128)(2,1)}, u32[]{:S(2)}, u32[]{:S(2)}) collective-permute-start(bf16[512,512]{1,0:T(8,128)(2,1)S(1)} %pad_maximum_fusion.1.rest_3_.rest_4_), channel_id=1, source_target_pairs={{0,16},{8,24},{16,0},{24,8},{32,48},{40,56},{48,32},{56,40},{64,80... | collective-permute-start | bytes 1572872 | tf_op jit(solution)/shard_map/ppermute | solution.py:29
  32.4 5.6 %all-to-all-start = ((f32[16,2,512]{2,1,0:T(2,128)}), f32[16,2,512]{2,1,0:T(2,128)S(1)}, u32[]{:S(2)}, u32[]{:S(2)}) async-start(f32[16,2,512]{2,1,0:T(2,128)} %tile.2), calls=%async_computation | async-start | bytes 131072 | tf_op jit(solution)/shard_map/all_to_all | solution.py:384
  38.1 8.8 %all-to-all-done = f32[16,2,512]{2,1,0:T(2,128)S(1)} async-done(((f32[16,2,512]{2,1,0:T(2,128)}), f32[16,2,512]{2,1,0:T(2,128)S(1)}, u32[]{:S(2)}, u32[]{:S(2)}) %all-to-all-start) | async-done | bytes 65568 | tf_op jit(solution)/shard_map/all_to_all | solution.py:384
  47.6 2.3 %gate_sums.1.bias_ref = f32[32,512]{1,0:T(8,128)} custom-call(f32[32,512]{1,0:T(8,128)} %all_to_all.6.logits_ref), custom_call_target="tpu_custom_call" | custom-call | flops 1000000 | bytes 131072 | tf_op jit(solution)/shard_map/gate_sums/pallas_call | solution.py:395
  49.9 0.9 copy-done.4
  50.8 8.6 %stats.2 = (f32[4,8,512]{2,1,0:T(8,128)S(1)}, f32[4,8,512]{2,1,0:T(8,128)S(1)}) custom-call(s32[2,2,4]{2,1,0:T(2,128)S(1)} %pad_add_fusion.pos_ref, f32[32,512]{1,0:T(8,128)S(1)} %copy-done.4, bf16[512,512]{1,0:T(8,128)(2,1)S(1)} %pad_maximum_fusion.rest_0_, bf16[512,512]{1,0:T(8,128)(2,1)S(1)} %collective-permute-done.rest_1_, ...), custom_call_target="tpu_custom_call" | custom-call | flops 1207959552 | bytes 4194304 | tf_op jit(solution)/shard_map/stats/pallas_call | solution.py:288
  59.4 7.6 %stats.3 = (f32[4,8,512]{2,1,0:T(8,128)S(1)}, f32[4,8,512]{2,1,0:T(8,128)S(1)}) custom-call(s32[2,2,4]{2,1,0:T(2,128)S(1)} %pad_add_fusion.pos_ref, f32[32,512]{1,0:T(8,128)S(1)} %copy-done.4, bf16[512,512]{1,0:T(8,128)(2,1)S(1)} %pad_maximum_fusion.rest_0_, bf16[512,512]{1,0:T(8,128)(2,1)S(1)} %collective-permute-done.rest_1_, ...), custom_call_target="tpu_custom_call" | custom-call | flops 939524096 | bytes 4194304 | tf_op jit(solution)/shard_map/stats/pallas_call | solution.py:288
  67.7 2.3 %collective-permute-start.7 = (f32[4,8,512]{2,1,0:T(8,128)S(1)}, f32[4,8,512]{2,1,0:T(8,128)S(1)}, u32[]{:S(2)}, u32[]{:S(2)}) collective-permute-start(f32[4,8,512]{2,1,0:T(8,128)S(1)} %get-tuple-element.39.rest_8_), channel_id=1, source_target_pairs={{0,64},{8,72},{16,80},{24,88},{32,96},{40,104},{48,112},{56,120},{... | collective-permute-start | bytes 196616 | tf_op jit(solution)/shard_map/ppermute | solution.py:29
  70.0 2.6 %collective-permute-start.9 = (f32[4,8,512]{2,1,0:T(8,128)S(1)}, f32[4,8,512]{2,1,0:T(8,128)S(1)}, u32[]{:S(2)}, u32[]{:S(2)}) collective-permute-start(f32[4,8,512]{2,1,0:T(8,128)S(1)} %get-tuple-element.40.rest_12_), channel_id=1, source_target_pairs={{0,24},{8,0},{16,8},{24,16},{32,56},{40,32},{48,40},{56,48},{64,88... | collective-permute-start | bytes 196616 | tf_op jit(solution)/shard_map/ppermute | solution.py:29
  74.4 1.1 collective-permute-done.8.rest_11_
  75.5 3.0 %collective-permute-done.10.rest_14_ = f32[4,8,512]{2,1,0:T(8,128)S(1)} collective-permute-done((f32[4,8,512]{2,1,0:T(8,128)S(1)}, f32[4,8,512]{2,1,0:T(8,128)S(1)}, u32[]{:S(2)}, u32[]{:S(2)}) %collective-permute-start.10) | collective-permute-done | bytes 65568 | tf_op jit(solution)/shard_map/ppermute | solution.py:29
  79.2 1.0 copy-done.1
  80.2 1.0 copy-done.3
  81.2 20.0 %grads.1 = (f32[128,512]{1,0:T(8,128)S(1)}, bf16[128,512]{1,0:T(8,128)(2,1)S(1)}, bf16[128,512]{1,0:T(8,128)(2,1)S(1)}, bf16[128,512]{1,0:T(8,128)(2,1)S(1)}, f3...) custom-call(s32[2,2,4]{2,1,0:T(2,128)S(1)} %pad_add_fusion.pos_ref, ...), custom_call_target="tpu_custom_call" | custom-call | flops 5704253440 | bytes 8388608 | tf_op jit(solution)/shard_map/grads/pallas_call | solution.py:317
  101.9 1.0 collective-permute-start.16
  102.9 1.2 collective-permute-start.15
  104.1 1.7 collective-permute-start.27
  105.8 6.0 %collective-permute-start.14 = (bf16[128,512]{1,0:T(8,128)(2,1)S(1)}, bf16[128,512]{1,0:T(8,128)(2,1)S(1)}, u32[]{:S(2)}, u32[]{:S(2)}) collective-permute-start(bf16[128,512]{1,0:T(8,128)(2,1)S(1)} %get-tuple-element.44), channel_id=1, source_target_pairs={{0,96},{8,104},{16,112},{24,120},{32,0},{40,8},{48,16},{56,24},{64... | collective-permute-start | bytes 393224 | tf_op jit(solution)/shard_map/ppermute | solution.py:427
  112.3 1.3 collective-permute-start.12
  113.7 3.6 %collective-permute-done.14 = bf16[128,512]{1,0:T(8,128)(2,1)S(1)} collective-permute-done((bf16[128,512]{1,0:T(8,128)(2,1)S(1)}, bf16[128,512]{1,0:T(8,128)(2,1)S(1)}, u32[]{:S(2)}, u32[]{:S(2)}) %collective-permute-start.14) | collective-permute-done | bytes 131104 | tf_op jit(solution)/shard_map/ppermute | solution.py:427
  117.3 12.8 %collective-permute-done.13 = bf16[128,512]{1,0:T(8,128)(2,1)S(1)} collective-permute-done((bf16[128,512]{1,0:T(8,128)(2,1)S(1)}, bf16[128,512]{1,0:T(8,128)(2,1)S(1)}, u32[]{:S(2)}, u32[]{:S(2)}) %collective-permute-start.13) | collective-permute-done | bytes 131104 | tf_op jit(solution)/shard_map/ppermute | solution.py:427
  130.1 2.7 %collective-permute-done.12 = bf16[128,512]{1,0:T(8,128)(2,1)S(1)} collective-permute-done((bf16[128,512]{1,0:T(8,128)(2,1)S(1)}, bf16[128,512]{1,0:T(8,128)(2,1)S(1)}, u32[]{:S(2)}, u32[]{:S(2)}) %collective-permute-start.12) | collective-permute-done | bytes 131104 | tf_op jit(solution)/shard_map/ppermute | solution.py:427
  133.6 4.5 %collective-permute-start.22 = (bf16[512,256]{1,0:T(8,128)(2,1)}, bf16[512,256]{1,0:T(8,128)(2,1)}, u32[]{:S(2)}, u32[]{:S(2)}) collective-permute-start(bf16[512,256]{1,0:T(8,128)(2,1)} %get-tuple-element.63), channel_id=1, source_target_pairs={{0,64},{8,72},{16,80},{24,88},{32,96},{40,104},{48,112},{56,120},{... | collective-permute-start | bytes 786440 | tf_op jit(solution)/shard_map/ppermute | solution.py:427
  138.2 3.0 %collective-permute-start.28 = (bf16[512,512]{1,0:T(8,128)(2,1)S(1)}, bf16[512,512]{1,0:T(8,128)(2,1)S(1)}, u32[]{:S(2)}, u32[]{:S(2)}) collective-permute-start(bf16[512,512]{1,0:T(8,128)(2,1)S(1)} %collective-permute-done.27.rest_4_), channel_id=1, source_target_pairs={{0,6},{1,7},{2,0},{3,1},{4,2},{5,3},{6,4},{7,5},{8,14},{9,15},{10,... | collective-permute-start | bytes 1572872 | tf_op jit(solution)/shard_map/ppermute | solution.py:414
  142.0 1.6 collective-permute-done.23
  143.6 6.3 %collective-permute-start.30 = (bf16[512,512]{1,0:T(8,128)(2,1)S(1)}, bf16[512,512]{1,0:T(8,128)(2,1)}, u32[]{:S(2)}, u32[]{:S(2)}) collective-permute-start(bf16[512,512]{1,0:T(8,128)(2,1)S(1)} %collective-permute-done.27.rest_4_), channel_id=1, source_target_pairs={{0,2},{1,3},{2,4},{3,5},{4,6},{5,7},{6,0},{7,1},{8,10},{9,11},{10,... | collective-permute-start | bytes 1572872 | tf_op jit(solution)/shard_map/ppermute | solution.py:414
  149.9 2.6 %collective-permute-start.20 = (bf16[512,256]{1,0:T(8,128)(2,1)}, bf16[512,256]{1,0:T(8,128)(2,1)}, u32[]{:S(2)}, u32[]{:S(2)}) collective-permute-start(bf16[512,256]{1,0:T(8,128)(2,1)} %copy-done.7), channel_id=1, source_target_pairs={{0,24},{8,0},{16,8},{24,16},{32,56},{40,32},{48,40},{56,48},{64,88... | collective-permute-start | bytes 786440 | tf_op jit(solution)/shard_map/ppermute | solution.py:427
  152.5 1.3 collective-permute-start.19
  153.9 1.8 fusion.1
  155.6 2.0 copy.10
  157.7 5.2 %collective-permute-done.20 = bf16[512,256]{1,0:T(8,128)(2,1)} collective-permute-done((bf16[512,256]{1,0:T(8,128)(2,1)}, bf16[512,256]{1,0:T(8,128)(2,1)}, u32[]{:S(2)}, u32[]{:S(2)}) %collective-permute-start.20) | collective-permute-done | bytes 262176 | tf_op jit(solution)/shard_map/ppermute | solution.py:427
  162.9 3.7 %collective-permute-start.24 = (bf16[256,512]{1,0:T(8,128)(2,1)S(1)}, bf16[256,512]{1,0:T(8,128)(2,1)S(1)}, u32[]{:S(2)}, u32[]{:S(2)}) collective-permute-start(bf16[256,512]{1,0:T(8,128)(2,1)S(1)} %fusion.rest_0_), channel_id=1, source_target_pairs={{0,96},{8,104},{16,112},{24,120},{32,0},{40,8},{48,16},{56,24},{64... | collective-permute-start | bytes 786440 | tf_op jit(solution)/shard_map/ppermute | solution.py:29
  166.6 1.2 convert_add_fusion
  167.8 3.1 %collective-permute-done.18 = bf16[512,256]{1,0:T(8,128)(2,1)S(1)} collective-permute-done((bf16[512,256]{1,0:T(8,128)(2,1)S(1)}, bf16[512,256]{1,0:T(8,128)(2,1)S(1)}, u32[]{:S(2)}, u32[]{:S(2)}) %collective-permute-start.18) | collective-permute-done | bytes 262176 | tf_op jit(solution)/shard_map/ppermute | solution.py:427
  170.9 1.5 collective-permute-start.25
  173.0 1.1 convert_add_fusion.1
  174.2 7.0 %collective-permute-done.25.rest_2_ = bf16[256,512]{1,0:T(8,128)(2,1)S(1)} collective-permute-done((bf16[256,512]{1,0:T(8,128)(2,1)S(1)}, bf16[256,512]{1,0:T(8,128)(2,1)S(1)}, u32[]{:S(2)}, u32[]{:S(2)}) %collective-permute-start.25) | collective-permute-done | bytes 262176 | tf_op jit(solution)/shard_map/ppermute | solution.py:29
  181.2 1.3 collective-permute-start.26
  182.5 8.4 %collective-permute-done.26.rest_3_ = bf16[256,512]{1,0:T(8,128)(2,1)S(1)} collective-permute-done((bf16[256,512]{1,0:T(8,128)(2,1)S(1)}, bf16[256,512]{1,0:T(8,128)(2,1)S(1)}, u32[]{:S(2)}, u32[]{:S(2)}) %collective-permute-start.26) | collective-permute-done | bytes 262176 | tf_op jit(solution)/shard_map/ppermute | solution.py:29
  191.0 3.3 %weight.1 = (f32[256,256]{1,0:T(8,128)S(1)}, bf16[256,256]{1,0:T(8,128)(2,1)S(1)}, bf16[256,256]{1,0:T(8,128)(2,1)S(1)}, bf16[256,256]{1,0:T(8,128)(2,1)S(1)}) custom-call(s32[4,4]{1,0:T(4,128)S(1)} %pad_add_fusion.1.at_ref, bf16[256,512]{1,0:T(8,128)(2,1)S(1)} %fusion.rest_0_, bf16[256,512]{1,0:T(8,128)(2,1)S(1)} %collective-permute-done.24.rest_1_, ...), custom_call_target="tpu_custom_call" | custom-call | flops 1073741824 | bytes 6291456 | tf_op jit(solution)/shard_map/weight/pallas_call | solution.py:346
  195.2 1.2 collective-permute-start.35
  198.0 2.2 %collective-permute-done.37 = bf16[256,256]{1,0:T(8,128)(2,1)S(1)} collective-permute-done((bf16[256,256]{1,0:T(8,128)(2,1)S(1)}, bf16[256,256]{1,0:T(8,128)(2,1)S(1)}, u32[]{:S(2)}, u32[]{:S(2)}) %collective-permute-start.37) | collective-permute-done | bytes 131104 | tf_op jit(solution)/shard_map/ppermute | solution.py:427
  200.2 2.3 %collective-permute-done.36 = bf16[256,256]{1,0:T(8,128)(2,1)S(1)} collective-permute-done((bf16[256,256]{1,0:T(8,128)(2,1)S(1)}, bf16[256,256]{1,0:T(8,128)(2,1)S(1)}, u32[]{:S(2)}, u32[]{:S(2)}) %collective-permute-start.36) | collective-permute-done | bytes 131104 | tf_op jit(solution)/shard_map/ppermute | solution.py:427
  (85 shorter events, 12.5 us)
Async XLA Ops:
  0.6 1.2 copy-start.9
  0.6 1.3 copy-start.10
  2.1 26.6 %collective-permute-start = (bf16[512,512]{1,0:T(8,128)(2,1)S(1)}, bf16[512,512]{1,0:T(8,128)(2,1)S(1)}, u32[]{:S(2)}, u32[]{:S(2)}) collective-permute-start(bf16[512,512]{1,0:T(8,128)(2,1)S(1)} %pad_maximum_fusion.rest_0_), channel_id=1, source_target_pairs={{0,96},{8,104},{16,112},{24,120},{32,0},{40,8},{48,16},{56,24},{64... | collective-permute-start | bytes 1572872 | tf_op jit(solution)/shard_map/ppermute | solution.py:29
  6.3 43.5 %collective-permute-start.2 = (bf16[512,512]{1,0:T(8,128)(2,1)S(1)}, bf16[512,512]{1,0:T(8,128)(2,1)S(1)}, u32[]{:S(2)}, u32[]{:S(2)}) collective-permute-start(bf16[512,512]{1,0:T(8,128)(2,1)S(1)} %pad_maximum_fusion.rest_0_), channel_id=1, source_target_pairs={{0,32},{8,40},{16,48},{24,56},{32,64},{40,72},{48,80},{56,88},{64,... | collective-permute-start | bytes 1572872 | tf_op jit(solution)/shard_map/ppermute | solution.py:29
  6.3 25.4 %copy-start.11 = (f32[512,2]{0,1:T(2,128)S(1)}, f32[512,2]{0,1:T(2,128)}, u32[]{:S(2)}) copy-start(f32[512,2]{0,1:T(2,128)} %param.9) | copy-start | bytes 12292
  6.4 43.5 %collective-permute-start.3 = (bf16[512,512]{1,0:T(8,128)(2,1)S(1)}, bf16[512,512]{1,0:T(8,128)(2,1)S(1)}, u32[]{:S(2)}, u32[]{:S(2)}) collective-permute-start(bf16[512,512]{1,0:T(8,128)(2,1)S(1)} %pad_maximum_fusion.1.rest_3_.rest_4_), channel_id=1, source_target_pairs={{0,24},{8,0},{16,8},{24,16},{32,56},{40,32},{48,40},{56,48},{64,88... | collective-permute-start | bytes 1572872 | tf_op jit(solution)/shard_map/ppermute | solution.py:29
  9.2 40.7 %collective-permute-start.5 = (bf16[512,512]{1,0:T(8,128)(2,1)S(1)}, bf16[512,512]{1,0:T(8,128)(2,1)S(1)}, u32[]{:S(2)}, u32[]{:S(2)}) collective-permute-start(bf16[512,512]{1,0:T(8,128)(2,1)S(1)} %pad_maximum_fusion.1.rest_3_.rest_4_), channel_id=1, source_target_pairs={{0,8},{8,16},{16,24},{24,0},{32,40},{40,48},{48,56},{56,32},{64,72... | collective-permute-start | bytes 1572872 | tf_op jit(solution)/shard_map/ppermute | solution.py:29
  9.2 50.2 %collective-permute-start.1 = (bf16[512,512]{1,0:T(8,128)(2,1)S(1)}, bf16[512,512]{1,0:T(8,128)(2,1)}, u32[]{:S(2)}, u32[]{:S(2)}) collective-permute-start(bf16[512,512]{1,0:T(8,128)(2,1)S(1)} %pad_maximum_fusion.rest_0_), channel_id=1, source_target_pairs={{0,64},{8,72},{16,80},{24,88},{32,96},{40,104},{48,112},{56,120},{... | collective-permute-start | bytes 1572872 | tf_op jit(solution)/shard_map/ppermute | solution.py:29
  28.7 30.7 %collective-permute-start.4 = (bf16[512,512]{1,0:T(8,128)(2,1)S(1)}, bf16[512,512]{1,0:T(8,128)(2,1)}, u32[]{:S(2)}, u32[]{:S(2)}) collective-permute-start(bf16[512,512]{1,0:T(8,128)(2,1)S(1)} %pad_maximum_fusion.1.rest_3_.rest_4_), channel_id=1, source_target_pairs={{0,16},{8,24},{16,0},{24,8},{32,48},{40,56},{48,32},{56,40},{64,80... | collective-permute-start | bytes 1572872 | tf_op jit(solution)/shard_map/ppermute | solution.py:29
  32.4 14.5 %all-to-all-start = ((f32[16,2,512]{2,1,0:T(2,128)}), f32[16,2,512]{2,1,0:T(2,128)S(1)}, u32[]{:S(2)}, u32[]{:S(2)}) async-start(f32[16,2,512]{2,1,0:T(2,128)} %tile.2), calls=%async_computation | async-start | bytes 131072 | tf_op jit(solution)/shard_map/all_to_all | solution.py:384
  49.8 9.6 %copy-start = (bf16[512,512]{1,0:T(8,128)(2,1)}, bf16[512,512]{1,0:T(8,128)(2,1)S(1)}, u32[]{:S(2)}) copy-start(bf16[512,512]{1,0:T(8,128)(2,1)S(1)} %collective-permute-done.3.rest_4_.rest_5_) | copy-start | bytes 1572868
  50.8 8.7 %copy-start.2 = (bf16[512,512]{1,0:T(8,128)(2,1)}, bf16[512,512]{1,0:T(8,128)(2,1)S(1)}, u32[]{:S(2)}) copy-start(bf16[512,512]{1,0:T(8,128)(2,1)S(1)} %collective-permute-done.5.rest_5_.rest_7_) | copy-start | bytes 1572868
  59.4 19.7 %copy-start.5 = (f32[32,512]{1,0:T(8,128)S(1)}, f32[32,512]{1,0:T(8,128)}, u32[]{:S(2)}) copy-start(f32[32,512]{1,0:T(8,128)} %gate_sums.1.bias_ref) | copy-start | bytes 196612
  67.1 6.5 %collective-permute-start.6 = (f32[4,8,512]{2,1,0:T(8,128)S(1)}, f32[4,8,512]{2,1,0:T(8,128)S(1)}, u32[]{:S(2)}, u32[]{:S(2)}) collective-permute-start(f32[4,8,512]{2,1,0:T(8,128)S(1)} %get-tuple-element.39.rest_8_), channel_id=1, source_target_pairs={{0,96},{8,104},{16,112},{24,120},{32,0},{40,8},{48,16},{56,24},{64... | collective-permute-start | bytes 196616 | tf_op jit(solution)/shard_map/ppermute | solution.py:29
  67.7 6.6 %collective-permute-start.7 = (f32[4,8,512]{2,1,0:T(8,128)S(1)}, f32[4,8,512]{2,1,0:T(8,128)S(1)}, u32[]{:S(2)}, u32[]{:S(2)}) collective-permute-start(f32[4,8,512]{2,1,0:T(8,128)S(1)} %get-tuple-element.39.rest_8_), channel_id=1, source_target_pairs={{0,64},{8,72},{16,80},{24,88},{32,96},{40,104},{48,112},{56,120},{... | collective-permute-start | bytes 196616 | tf_op jit(solution)/shard_map/ppermute | solution.py:29
  70.0 5.5 %collective-permute-start.8 = (f32[4,8,512]{2,1,0:T(8,128)S(1)}, f32[4,8,512]{2,1,0:T(8,128)S(1)}, u32[]{:S(2)}, u32[]{:S(2)}) collective-permute-start(f32[4,8,512]{2,1,0:T(8,128)S(1)} %get-tuple-element.39.rest_8_), channel_id=1, source_target_pairs={{0,32},{8,40},{16,48},{24,56},{32,64},{40,72},{48,80},{56,88},{64,... | collective-permute-start | bytes 196616 | tf_op jit(solution)/shard_map/ppermute | solution.py:29
  70.0 5.5 %collective-permute-start.9 = (f32[4,8,512]{2,1,0:T(8,128)S(1)}, f32[4,8,512]{2,1,0:T(8,128)S(1)}, u32[]{:S(2)}, u32[]{:S(2)}) collective-permute-start(f32[4,8,512]{2,1,0:T(8,128)S(1)} %get-tuple-element.40.rest_12_), channel_id=1, source_target_pairs={{0,24},{8,0},{16,8},{24,16},{32,56},{40,32},{48,40},{56,48},{64,88... | collective-permute-start | bytes 196616 | tf_op jit(solution)/shard_map/ppermute | solution.py:29
  72.7 5.8 %collective-permute-start.10 = (f32[4,8,512]{2,1,0:T(8,128)S(1)}, f32[4,8,512]{2,1,0:T(8,128)S(1)}, u32[]{:S(2)}, u32[]{:S(2)}) collective-permute-start(f32[4,8,512]{2,1,0:T(8,128)S(1)} %get-tuple-element.40.rest_12_), channel_id=1, source_target_pairs={{0,16},{8,24},{16,0},{24,8},{32,48},{40,56},{48,32},{56,40},{64,80... | collective-permute-start | bytes 196616 | tf_op jit(solution)/shard_map/ppermute | solution.py:29
  73.6 5.6 %collective-permute-start.11 = (f32[4,8,512]{2,1,0:T(8,128)S(1)}, f32[4,8,512]{2,1,0:T(8,128)S(1)}, u32[]{:S(2)}, u32[]{:S(2)}) collective-permute-start(f32[4,8,512]{2,1,0:T(8,128)S(1)} %get-tuple-element.40.rest_12_), channel_id=1, source_target_pairs={{0,8},{8,16},{16,24},{24,0},{32,40},{40,48},{48,56},{56,32},{64,72... | collective-permute-start | bytes 196616 | tf_op jit(solution)/shard_map/ppermute | solution.py:29
  79.2 1.0 copy-start.1
  101.3 31.6 %copy-start.6 = (bf16[512,256]{1,0:T(8,128)(2,1)}, bf16[512,256]{1,0:T(8,128)(2,1)S(1)}, u32[]{:S(2)}) copy-start(bf16[512,256]{1,0:T(8,128)(2,1)S(1)} %get-tuple-element.59) | copy-start | bytes 786436
  101.3 31.6 %copy-start.7 = (bf16[512,256]{1,0:T(8,128)(2,1)}, bf16[512,256]{1,0:T(8,128)(2,1)S(1)}, u32[]{:S(2)}) copy-start(bf16[512,256]{1,0:T(8,128)(2,1)S(1)} %get-tuple-element.60) | copy-start | bytes 786436
  101.3 10.5 %collective-permute-start.17 = (bf16[128,512]{1,0:T(8,128)(2,1)S(1)}, bf16[128,512]{1,0:T(8,128)(2,1)S(1)}, u32[]{:S(2)}, u32[]{:S(2)}) collective-permute-start(bf16[128,512]{1,0:T(8,128)(2,1)S(1)} %get-tuple-element.48), channel_id=1, source_target_pairs={{0,24},{8,0},{16,8},{24,16},{32,56},{40,32},{48,40},{56,48},{64,88... | collective-permute-start | bytes 393224 | tf_op jit(solution)/shard_map/ppermute | solution.py:427
  101.9 10.4 %collective-permute-start.16 = (bf16[128,512]{1,0:T(8,128)(2,1)S(1)}, bf16[128,512]{1,0:T(8,128)(2,1)S(1)}, u32[]{:S(2)}, u32[]{:S(2)}) collective-permute-start(bf16[128,512]{1,0:T(8,128)(2,1)S(1)} %get-tuple-element.47), channel_id=1, source_target_pairs={{0,16},{8,24},{16,0},{24,8},{32,48},{40,56},{48,32},{56,40},{64,80... | collective-permute-start | bytes 393224 | tf_op jit(solution)/shard_map/ppermute | solution.py:427
  102.9 10.8 %collective-permute-start.15 = (bf16[128,512]{1,0:T(8,128)(2,1)S(1)}, bf16[128,512]{1,0:T(8,128)(2,1)S(1)}, u32[]{:S(2)}, u32[]{:S(2)}) collective-permute-start(bf16[128,512]{1,0:T(8,128)(2,1)S(1)} %get-tuple-element.46), channel_id=1, source_target_pairs={{0,8},{8,16},{16,24},{24,0},{32,40},{40,48},{48,56},{56,32},{64,72... | collective-permute-start | bytes 393224 | tf_op jit(solution)/shard_map/ppermute | solution.py:427
  104.1 34.1 %collective-permute-start.27 = (bf16[512,512]{1,0:T(8,128)(2,1)}, bf16[512,512]{1,0:T(8,128)(2,1)S(1)}, u32[]{:S(2)}, u32[]{:S(2)}) collective-permute-start(bf16[512,512]{1,0:T(8,128)(2,1)} %param.10), channel_id=1, source_target_pairs={{0,0},{1,1},{2,32},{3,33},{4,64},{5,65},{6,96},{7,97},{8,8},{9,9},... | collective-permute-start | bytes 1572872 | tf_op jit(solution)/shard_map/ppermute | solution.py:411
  105.8 11.5 %collective-permute-start.14 = (bf16[128,512]{1,0:T(8,128)(2,1)S(1)}, bf16[128,512]{1,0:T(8,128)(2,1)S(1)}, u32[]{:S(2)}, u32[]{:S(2)}) collective-permute-start(bf16[128,512]{1,0:T(8,128)(2,1)S(1)} %get-tuple-element.44), channel_id=1, source_target_pairs={{0,96},{8,104},{16,112},{24,120},{32,0},{40,8},{48,16},{56,24},{64... | collective-permute-start | bytes 393224 | tf_op jit(solution)/shard_map/ppermute | solution.py:427
  111.8 18.4 %collective-permute-start.13 = (bf16[128,512]{1,0:T(8,128)(2,1)S(1)}, bf16[128,512]{1,0:T(8,128)(2,1)S(1)}, u32[]{:S(2)}, u32[]{:S(2)}) collective-permute-start(bf16[128,512]{1,0:T(8,128)(2,1)S(1)} %get-tuple-element.43), channel_id=1, source_target_pairs={{0,64},{8,72},{16,80},{24,88},{32,96},{40,104},{48,112},{56,120},{... | collective-permute-start | bytes 393224 | tf_op jit(solution)/shard_map/ppermute | solution.py:427
  112.3 20.5 %collective-permute-start.12 = (bf16[128,512]{1,0:T(8,128)(2,1)S(1)}, bf16[128,512]{1,0:T(8,128)(2,1)S(1)}, u32[]{:S(2)}, u32[]{:S(2)}) collective-permute-start(bf16[128,512]{1,0:T(8,128)(2,1)S(1)} %get-tuple-element.42), channel_id=1, source_target_pairs={{0,32},{8,40},{16,48},{24,56},{32,64},{40,72},{48,80},{56,88},{64,... | collective-permute-start | bytes 393224 | tf_op jit(solution)/shard_map/ppermute | solution.py:427
  133.6 10.0 %collective-permute-start.23 = (bf16[512,256]{1,0:T(8,128)(2,1)}, bf16[512,256]{1,0:T(8,128)(2,1)}, u32[]{:S(2)}, u32[]{:S(2)}) collective-permute-start(bf16[512,256]{1,0:T(8,128)(2,1)} %get-tuple-element.64), channel_id=1, source_target_pairs={{0,96},{8,104},{16,112},{24,120},{32,0},{40,8},{48,16},{56,24},{64... | collective-permute-start | bytes 786440 | tf_op jit(solution)/shard_map/ppermute | solution.py:427
  133.6 16.2 %collective-permute-start.22 = (bf16[512,256]{1,0:T(8,128)(2,1)}, bf16[512,256]{1,0:T(8,128)(2,1)}, u32[]{:S(2)}, u32[]{:S(2)}) collective-permute-start(bf16[512,256]{1,0:T(8,128)(2,1)} %get-tuple-element.63), channel_id=1, source_target_pairs={{0,64},{8,72},{16,80},{24,88},{32,96},{40,104},{48,112},{56,120},{... | collective-permute-start | bytes 786440 | tf_op jit(solution)/shard_map/ppermute | solution.py:427
  138.2 14.3 %collective-permute-start.21 = (bf16[512,256]{1,0:T(8,128)(2,1)}, bf16[512,256]{1,0:T(8,128)(2,1)}, u32[]{:S(2)}, u32[]{:S(2)}) collective-permute-start(bf16[512,256]{1,0:T(8,128)(2,1)} %get-tuple-element.62), channel_id=1, source_target_pairs={{0,32},{8,40},{16,48},{24,56},{32,64},{40,72},{48,80},{56,88},{64,... | collective-permute-start | bytes 786440 | tf_op jit(solution)/shard_map/ppermute | solution.py:427
  138.2 34.2 %collective-permute-start.28 = (bf16[512,512]{1,0:T(8,128)(2,1)S(1)}, bf16[512,512]{1,0:T(8,128)(2,1)S(1)}, u32[]{:S(2)}, u32[]{:S(2)}) collective-permute-start(bf16[512,512]{1,0:T(8,128)(2,1)S(1)} %collective-permute-done.27.rest_4_), channel_id=1, source_target_pairs={{0,6},{1,7},{2,0},{3,1},{4,2},{5,3},{6,4},{7,5},{8,14},{9,15},{10,... | collective-permute-start | bytes 1572872 | tf_op jit(solution)/shard_map/ppermute | solution.py:414
  141.2 31.2 %collective-permute-start.29 = (bf16[512,512]{1,0:T(8,128)(2,1)S(1)}, bf16[512,512]{1,0:T(8,128)(2,1)S(1)}, u32[]{:S(2)}, u32[]{:S(2)}) collective-permute-start(bf16[512,512]{1,0:T(8,128)(2,1)S(1)} %collective-permute-done.27.rest_4_), channel_id=1, source_target_pairs={{0,4},{1,5},{2,6},{3,7},{4,0},{5,1},{6,2},{7,3},{8,12},{9,13},{10,... | collective-permute-start | bytes 1572872 | tf_op jit(solution)/shard_map/ppermute | solution.py:414
  143.6 29.4 %collective-permute-start.30 = (bf16[512,512]{1,0:T(8,128)(2,1)S(1)}, bf16[512,512]{1,0:T(8,128)(2,1)}, u32[]{:S(2)}, u32[]{:S(2)}) collective-permute-start(bf16[512,512]{1,0:T(8,128)(2,1)S(1)} %collective-permute-done.27.rest_4_), channel_id=1, source_target_pairs={{0,2},{1,3},{2,4},{3,5},{4,6},{5,7},{6,0},{7,1},{8,10},{9,11},{10,... | collective-permute-start | bytes 1572872 | tf_op jit(solution)/shard_map/ppermute | solution.py:414
  149.9 13.1 %collective-permute-start.20 = (bf16[512,256]{1,0:T(8,128)(2,1)}, bf16[512,256]{1,0:T(8,128)(2,1)}, u32[]{:S(2)}, u32[]{:S(2)}) collective-permute-start(bf16[512,256]{1,0:T(8,128)(2,1)} %copy-done.7), channel_id=1, source_target_pairs={{0,24},{8,0},{16,8},{24,16},{32,56},{40,32},{48,40},{56,48},{64,88... | collective-permute-start | bytes 786440 | tf_op jit(solution)/shard_map/ppermute | solution.py:427
  152.5 10.5 %collective-permute-start.19 = (bf16[512,256]{1,0:T(8,128)(2,1)}, bf16[512,256]{1,0:T(8,128)(2,1)}, u32[]{:S(2)}, u32[]{:S(2)}) collective-permute-start(bf16[512,256]{1,0:T(8,128)(2,1)} %copy-done.6), channel_id=1, source_target_pairs={{0,16},{8,24},{16,0},{24,8},{32,48},{40,56},{48,32},{56,40},{64,80... | collective-permute-start | bytes 786440 | tf_op jit(solution)/shard_map/ppermute | solution.py:427
  162.9 8.0 %collective-permute-start.18 = (bf16[512,256]{1,0:T(8,128)(2,1)S(1)}, bf16[512,256]{1,0:T(8,128)(2,1)S(1)}, u32[]{:S(2)}, u32[]{:S(2)}) collective-permute-start(bf16[512,256]{1,0:T(8,128)(2,1)S(1)} %get-tuple-element.58), channel_id=1, source_target_pairs={{0,8},{8,16},{16,24},{24,0},{32,40},{40,48},{48,56},{56,32},{64,72... | collective-permute-start | bytes 786440 | tf_op jit(solution)/shard_map/ppermute | solution.py:427
  162.9 8.0 %collective-permute-start.24 = (bf16[256,512]{1,0:T(8,128)(2,1)S(1)}, bf16[256,512]{1,0:T(8,128)(2,1)S(1)}, u32[]{:S(2)}, u32[]{:S(2)}) collective-permute-start(bf16[256,512]{1,0:T(8,128)(2,1)S(1)} %fusion.rest_0_), channel_id=1, source_target_pairs={{0,96},{8,104},{16,112},{24,120},{32,0},{40,8},{48,16},{56,24},{64... | collective-permute-start | bytes 786440 | tf_op jit(solution)/shard_map/ppermute | solution.py:29
  170.9 20.0 %collective-permute-start.31 = (bf16[512,512]{1,0:T(8,128)(2,1)S(1)}, bf16[512,512]{1,0:T(8,128)(2,1)S(1)}, u32[]{:S(2)}, u32[]{:S(2)}) collective-permute-start(bf16[512,512]{1,0:T(8,128)(2,1)S(1)} %collective-permute-done.27.rest_4_), channel_id=1, source_target_pairs={{0,1},{1,0},{2,3},{3,2},{4,5},{5,4},{6,7},{7,6},{8,9},{9,8},{10,11... | collective-permute-start | bytes 1572872 | tf_op jit(solution)/shard_map/ppermute | solution.py:416
  170.9 10.2 %collective-permute-start.25 = (bf16[256,512]{1,0:T(8,128)(2,1)S(1)}, bf16[256,512]{1,0:T(8,128)(2,1)S(1)}, u32[]{:S(2)}, u32[]{:S(2)}) collective-permute-start(bf16[256,512]{1,0:T(8,128)(2,1)S(1)} %fusion.rest_0_), channel_id=1, source_target_pairs={{0,64},{8,72},{16,80},{24,88},{32,96},{40,104},{48,112},{56,120},{... | collective-permute-start | bytes 786440 | tf_op jit(solution)/shard_map/ppermute | solution.py:29
  172.4 18.5 %collective-permute-start.32 = (bf16[512,512]{1,0:T(8,128)(2,1)S(1)}, bf16[512,512]{1,0:T(8,128)(2,1)S(1)}, u32[]{:S(2)}, u32[]{:S(2)}) collective-permute-start(bf16[512,512]{1,0:T(8,128)(2,1)S(1)} %collective-permute-done.28.rest_5_), channel_id=1, source_target_pairs={{0,1},{1,0},{2,3},{3,2},{4,5},{5,4},{6,7},{7,6},{8,9},{9,8},{10,11... | collective-permute-start | bytes 1572872 | tf_op jit(solution)/shard_map/ppermute | solution.py:416
  172.4 18.5 %collective-permute-start.33 = (bf16[512,512]{1,0:T(8,128)(2,1)S(1)}, bf16[512,512]{1,0:T(8,128)(2,1)S(1)}, u32[]{:S(2)}, u32[]{:S(2)}) collective-permute-start(bf16[512,512]{1,0:T(8,128)(2,1)S(1)} %collective-permute-done.29.rest_6_), channel_id=1, source_target_pairs={{0,1},{1,0},{2,3},{3,2},{4,5},{5,4},{6,7},{7,6},{8,9},{9,8},{10,11... | collective-permute-start | bytes 1572872 | tf_op jit(solution)/shard_map/ppermute | solution.py:416
  173.0 18.0 %collective-permute-start.34 = (bf16[512,512]{1,0:T(8,128)(2,1)}, bf16[512,512]{1,0:T(8,128)(2,1)S(1)}, u32[]{:S(2)}, u32[]{:S(2)}) collective-permute-start(bf16[512,512]{1,0:T(8,128)(2,1)} %collective-permute-done.30.rest_7_), channel_id=1, source_target_pairs={{0,1},{1,0},{2,3},{3,2},{4,5},{5,4},{6,7},{7,6},{8,9},{9,8},{10,11... | collective-permute-start | bytes 1572872 | tf_op jit(solution)/shard_map/ppermute | solution.py:416
  181.2 9.8 %collective-permute-start.26 = (bf16[256,512]{1,0:T(8,128)(2,1)S(1)}, bf16[256,512]{1,0:T(8,128)(2,1)S(1)}, u32[]{:S(2)}, u32[]{:S(2)}) collective-permute-start(bf16[256,512]{1,0:T(8,128)(2,1)S(1)} %fusion.rest_0_), channel_id=1, source_target_pairs={{0,32},{8,40},{16,48},{24,56},{32,64},{40,72},{48,80},{56,88},{64,... | collective-permute-start | bytes 786440 | tf_op jit(solution)/shard_map/ppermute | solution.py:29
  194.3 5.9 %collective-permute-start.37 = (bf16[256,256]{1,0:T(8,128)(2,1)S(1)}, bf16[256,256]{1,0:T(8,128)(2,1)S(1)}, u32[]{:S(2)}, u32[]{:S(2)}) collective-permute-start(bf16[256,256]{1,0:T(8,128)(2,1)S(1)} %get-tuple-element.69), channel_id=1, source_target_pairs={{0,24},{8,0},{16,8},{24,16},{32,56},{40,32},{48,40},{56,48},{64,88... | collective-permute-start | bytes 393224 | tf_op jit(solution)/shard_map/ppermute | solution.py:427
  195.2 7.3 %collective-permute-start.36 = (bf16[256,256]{1,0:T(8,128)(2,1)S(1)}, bf16[256,256]{1,0:T(8,128)(2,1)S(1)}, u32[]{:S(2)}, u32[]{:S(2)}) collective-permute-start(bf16[256,256]{1,0:T(8,128)(2,1)S(1)} %get-tuple-element.68), channel_id=1, source_target_pairs={{0,16},{8,24},{16,0},{24,8},{32,48},{40,56},{48,32},{56,40},{64,80... | collective-permute-start | bytes 393224 | tf_op jit(solution)/shard_map/ppermute | solution.py:427
  195.2 8.1 %collective-permute-start.35 = (bf16[256,256]{1,0:T(8,128)(2,1)S(1)}, bf16[256,256]{1,0:T(8,128)(2,1)S(1)}, u32[]{:S(2)}, u32[]{:S(2)}) collective-permute-start(bf16[256,256]{1,0:T(8,128)(2,1)S(1)} %get-tuple-element.67), channel_id=1, source_target_pairs={{0,8},{8,16},{16,24},{24,0},{32,40},{40,48},{48,56},{56,32},{64,72... | collective-permute-start | bytes 393224 | tf_op jit(solution)/shard_map/ppermute | solution.py:427
  (3 other events, 2.7 us)
where the time goes:
time: 205 us; the launch traced here: 204 us
  waiting for transfers between devices  80.9 us (39%)
  starting transfers between devices  65 us (32%)
  Pallas kernels  41.8 us (20%)
  local copies, waits for them, and re-layouts  9.28 us (5%)
  other arithmetic  6.25 us (3%)
    ppermute x15, waiting for transfers between devices, fetched(): lax.ppermute(array, 'sp', axis_perm(-r))  37.9 us
    ppermute x15, waiting for transfers between devices, summed(): lax.ppermute(parts[r], 'sp', axis_perm(r)).astype(jnp.float32)  34.2 us
    ppermute x15, starting transfers between devices, fetched(): lax.ppermute(array, 'sp', axis_perm(-r))  25.7 us
    ppermute x15, starting transfers between devices, summed(): lax.ppermute(parts[r], 'sp', axis_perm(r)).astype(jnp.float32)  21.2 us
    pallas_call x1, Pallas kernels, grads_call(): pl.pallas_call(grads_kernel, out_shape=shapes(HEAD, span) + shapes(span,...  20 us
    pallas_call x2, Pallas kernels, stats_call(): pl.pallas_call(functools.partial(stats_kernel, slots, pair_count, pair_of...  16.2 us
    ppermute x3, starting transfers between devices, local(): lax.ppermute(moved, 'tp', [(p, (p - 2 * r) % 8) for p in range(8)])  10.1 us
    all_to_all x1, waiting for transfers between devices, local(): lax.all_to_all(jnp.tile(forget_logits.T, (16, 1)), 'sp', 0, 0, tiled=True)  8.78 us
  transfers between devices with their start and end apart: 39, of which 16 were waited for; matrix products, arithmetic and copies ran while one was open for 4% of the time, Pallas kernels for 5%

commit v1 on v0

--- a/solution.py
+++ b/solution.py
@@ -26,7 +26,10 @@
 
 
 def fetched(array, axis_perm):
-    return [array] + [lax.ppermute(array, "sp", axis_perm(-r)) for r in range(1, SIDE)]
+    parts = [array]
+    for r in range(1, SIDE):
+        parts.append(lax.ppermute(array, "sp", axis_perm(-r)))
+    return parts
 
 
 def dot_nt(a, b):
@@ -297,7 +300,7 @@
             pltpu.VMEM((2, SIDE, 8, span), jnp.float32),
             pltpu.SemaphoreType.DMA((16,)),
         ],
-        compiler_params=pltpu.CompilerParams(vmem_limit_bytes=20 << 20),
+        compiler_params=pltpu.CompilerParams(vmem_limit_bytes=62 << 20),
         cost_estimate=pl.CostEstimate(
             flops=4 * HEAD * pairs, bytes_accessed=4 << 20, transcendentals=pairs
         ),
@@ -329,7 +332,7 @@
             pltpu.VMEM((2, SIDE, span, 2 * HEAD), jnp.float32),
             pltpu.SemaphoreType.DMA((16,)),
         ],
-        compiler_params=pltpu.CompilerParams(vmem_limit_bytes=32 << 20),
+        compiler_params=pltpu.CompilerParams(vmem_limit_bytes=62 << 20),
         cost_estimate=pl.CostEstimate(
             flops=10 * HEAD * pairs, bytes_accessed=8 << 20, transcendentals=pairs
         ),
@@ -353,7 +356,7 @@
             pltpu.VMEM((2, SIDE, rows, width), jnp.bfloat16),
             pltpu.SemaphoreType.DMA((12,)),
         ],
-        compiler_params=pltpu.CompilerParams(vmem_limit_bytes=32 << 20),
+        compiler_params=pltpu.CompilerParams(vmem_limit_bytes=62 << 20),
         cost_estimate=pl.CostEstimate(
             flops=16 * rows * width * cols, bytes_accessed=6 << 20, transcendentals=0
         ),
@@ -377,7 +380,7 @@
         jnp.int32
     )
     cores = jnp.stack([core, 1 - core, core, 1 - core])
-    at = jnp.stack([(y + steps) % SIDE, (z + steps) % SIDE, (x + steps) % SIDE, cores]).astype(
+    at = jnp.stack([(y - z + steps) % SIDE, (z + steps) % SIDE, (x + steps) % SIDE, cores]).astype(
         jnp.int32
     )
 
@@ -401,14 +404,17 @@
         name="gate_sums",
     )(gates)
 
-    swap = [
-        (((a * SIDE + b) * SIDE + c) * 2 + d, ((c * SIDE + b) * SIDE + a) * 2 + d)
-        for a in range(SIDE)
-        for b in range(SIDE)
-        for c in range(SIDE)
-        for d in range(2)
-    ]
-    moved = lax.ppermute(layer_input, ("sp", "tp"), swap)
+    def over_zy(target):
+        pairs = []
+        for n in range(SIDE**3 * 2):
+            zxyc = (n // 32, n // 8 % SIDE, n // 2 % SIDE, n % 2)
+            new_z, new_y = target(zxyc[0], zxyc[2])
+            pairs.append((n, new_z % SIDE * 32 + zxyc[1] * 8 + new_y % SIDE * 2 + zxyc[3]))
+        return pairs
+
+    everywhere = ("sp", "tp")
+    moved = lax.ppermute(layer_input, everywhere, over_zy(lambda a, b: (a, a + b)))
+    moved = lax.ppermute(moved, everywhere, over_zy(lambda a, b: (b - a, b)))
     inputs = [moved]
     for r in range(1, SIDE):
         inputs.append(lax.ppermute(moved, "tp", [(p, (p - 2 * r) % 8) for p in range(8)]))

time: 205 us -> 206 us (level)
  Pallas kernels: 41.8 us -> 50.6 us
  waiting for transfers between devices: 80.9 us -> 73.8 us
    ppermute x15, waiting for transfers between devices: 34.2 us -> 24.6 us  [summed(): lax.ppermute(parts[r], 'sp', axis_perm(r)).astype(jnp.float32)]
    ppermute x3, starting transfers between devices: 10.1 us -> 0.94 us  [local(): lax.ppermute(moved, 'tp', [(p, (p - 2 * r) % 8) for p in range(8)])]
    ppermute x15, starting transfers between devices: 21.2 us -> 27 us  [summed(): lax.ppermute(parts[r], 'sp', axis_perm(r)).astype(jnp.float32)]
    pallas_call x2, Pallas kernels: 16.2 us -> 20.6 us  [stats_call(): pl.pallas_call(functools.partial(stats_kernel, slots, pair_count, pair_of...]
    pallas_call x1, Pallas kernels: 20 us -> 22.5 us  [grads_call(): pl.pallas_call(grads_kernel, out_shape=shapes(HEAD, span) + shapes(span,...]
    ppermute x16 -> x17, starting transfers between devices: 27.4 us -> 29.5 us  [the longest x15 26.3 us: fetched(): parts.append(lax.ppermute(array, 'sp', axis_perm(-r)))]
    ppermute x16 -> x17, waiting for transfers between devices: 37.9 us -> 39.9 us  [the longest x15 39.8 us: fetched(): parts.append(lax.ppermute(array, 'sp', axis_perm(-r)))]
    unnamed x26 -> x64, local copies, waits for them, and re-layouts: 6.61 us -> 7.49 us
  transfers between devices with their start and end apart: 39 -> 40, of which waited for: 16 -> 15; matrix products, arithmetic and copies ran while one was open for 4% -> 3% of each run, Pallas kernels for 5% -> 18%
where the time goes in v1:
time: 206 us; the launch traced here: 205 us
  waiting for transfers between devices  73.8 us (36%)
  starting transfers between devices  63.6 us (31%)
  Pallas kernels  50.6 us (25%)
  local copies, waits for them, and re-layouts  10.2 us (5%)
  other arithmetic  5.55 us (3%)
    ppermute x15, waiting for transfers between devices, fetched(): parts.append(lax.ppermute(array, 'sp', axis_perm(-r)))  39.8 us
    ppermute x15, starting transfers between devices, summed(): lax.ppermute(parts[r], 'sp', axis_perm(r)).astype(jnp.float32)  27 us
    ppermute x15, starting transfers between devices, fetched(): parts.append(lax.ppermute(array, 'sp', axis_perm(-r)))  26.3 us
    ppermute x15, waiting for transfers between devices, summed(): lax.ppermute(parts[r], 'sp', axis_perm(r)).astype(jnp.float32)  24.6 us
    pallas_call x1, Pallas kernels, grads_call(): pl.pallas_call(grads_kernel, out_shape=shapes(HEAD, span) + shapes(span,...  22.5 us
    pallas_call x2, Pallas kernels, stats_call(): pl.pallas_call(functools.partial(stats_kernel, slots, pair_count, pair_of...  20.6 us
    all_to_all x1, waiting for transfers between devices, local(): lax.all_to_all(jnp.tile(forget_logits.T, (16, 1)), 'sp', 0, 0, tiled=True)  8.2 us
    unnamed x64, local copies, waits for them, and re-layouts  7.49 us
  transfers between devices with their start and end apart: 40, of which 15 were waited for; matrix products, arithmetic and copies ran while one was open for 3% of the time, Pallas kernels for 18%

profile of v1, /device:TPU:0, one launch (start us, length us, event | category | flops | bytes accessed | tf_op | source)
XLA Modules:
  0.0 204.8 jit_solution(12177894282156159049)
XLA Ops:
  0.7 1.2 fusion.7
  2.1 4.2 %collective-permute-start = (bf16[512,512]{1,0:T(8,128)(2,1)S(1)}, bf16[512,512]{1,0:T(8,128)(2,1)S(1)}, u32[]{:S(2)}, u32[]{:S(2)}) collective-permute-start(bf16[512,512]{1,0:T(8,128)(2,1)S(1)} %pad_maximum_fusion.rest_0_), channel_id=1, source_target_pairs={{0,96},{8,104},{16,112},{24,120},{32,0},{40,8},{48,16},{56,24},{64... | collective-permute-start | bytes 1572872 | tf_op jit(solution)/shard_map/ppermute | solution.py:31
  6.4 2.8 %collective-permute-start.3 = (bf16[512,512]{1,0:T(8,128)(2,1)S(1)}, bf16[512,512]{1,0:T(8,128)(2,1)S(1)}, u32[]{:S(2)}, u32[]{:S(2)}) collective-permute-start(bf16[512,512]{1,0:T(8,128)(2,1)S(1)} %pad_maximum_fusion.1.rest_3_.rest_4_), channel_id=1, source_target_pairs={{0,24},{8,0},{16,8},{24,16},{32,56},{40,32},{48,40},{56,48},{64,88... | collective-permute-start | bytes 1572872 | tf_op jit(solution)/shard_map/ppermute | solution.py:31
  9.2 1.9 collective-permute-start.1
  11.1 17.6 %collective-permute-done.rest_1_ = bf16[512,512]{1,0:T(8,128)(2,1)S(1)} collective-permute-done((bf16[512,512]{1,0:T(8,128)(2,1)S(1)}, bf16[512,512]{1,0:T(8,128)(2,1)S(1)}, u32[]{:S(2)}, u32[]{:S(2)}) %collective-permute-start) | collective-permute-done | bytes 524320 | tf_op jit(solution)/shard_map/ppermute | solution.py:31
  28.7 3.0 %collective-permute-start.4 = (bf16[512,512]{1,0:T(8,128)(2,1)S(1)}, bf16[512,512]{1,0:T(8,128)(2,1)}, u32[]{:S(2)}, u32[]{:S(2)}) collective-permute-start(bf16[512,512]{1,0:T(8,128)(2,1)S(1)} %pad_maximum_fusion.1.rest_3_.rest_4_), channel_id=1, source_target_pairs={{0,16},{8,24},{16,0},{24,8},{32,48},{40,56},{48,32},{56,40},{64,80... | collective-permute-start | bytes 1572872 | tf_op jit(solution)/shard_map/ppermute | solution.py:31
  32.4 5.6 %all-to-all-start = ((f32[16,2,512]{2,1,0:T(2,128)}), f32[16,2,512]{2,1,0:T(2,128)S(1)}, u32[]{:S(2)}, u32[]{:S(2)}) async-start(f32[16,2,512]{2,1,0:T(2,128)} %tile.2), calls=%async_computation | async-start | bytes 131072 | tf_op jit(solution)/shard_map/all_to_all | solution.py:387
  38.7 8.2 %all-to-all-done = f32[16,2,512]{2,1,0:T(2,128)S(1)} async-done(((f32[16,2,512]{2,1,0:T(2,128)}), f32[16,2,512]{2,1,0:T(2,128)S(1)}, u32[]{:S(2)}, u32[]{:S(2)}) %all-to-all-start) | async-done | bytes 65568 | tf_op jit(solution)/shard_map/all_to_all | solution.py:387
  47.6 2.3 %gate_sums.1.bias_ref = f32[32,512]{1,0:T(8,128)} custom-call(f32[32,512]{1,0:T(8,128)} %all_to_all.6.logits_ref), custom_call_target="tpu_custom_call" | custom-call | flops 1000000 | bytes 131072 | tf_op jit(solution)/shard_map/gate_sums/pallas_call | solution.py:398
  51.4 11.1 %stats.2 = (f32[4,8,512]{2,1,0:T(8,128)}, f32[4,8,512]{2,1,0:T(8,128)}) custom-call(s32[2,2,4]{2,1,0:T(2,128)} %pad_add_fusion.pos_ref, f32[32,512]{1,0:T(8,128)} %gate_sums.1.bias_ref, bf16[512,512]{1,0:T(8,128)(2,1)} %copy-done, bf16[512,512]{1,0:T(8,128)(2,1)} %copy-done.9, bf16[512,512]{1,0:T(8,128)(2,1)} %copy-done.10, bf16[512,512]{1,0:T(8,128)(2,1)} %copy-done.1, ...), custom_call_target="tpu_custom_call" | custom-call | flops 1207959552 | bytes 4194304 | tf_op jit(solution)/shard_map/stats/pallas_call | solution.py:291
  62.6 9.5 %stats.3 = (f32[4,8,512]{2,1,0:T(8,128)}, f32[4,8,512]{2,1,0:T(8,128)}) custom-call(s32[2,2,4]{2,1,0:T(2,128)} %pad_add_fusion.pos_ref, f32[32,512]{1,0:T(8,128)} %gate_sums.1.bias_ref, bf16[512,512]{1,0:T(8,128)(2,1)} %copy-done, bf16[512,512]{1,0:T(8,128)(2,1)} %copy-done.9, bf16[512,512]{1,0:T(8,128)(2,1)} %collective-permute-done.1.rest_2_, ...), custom_call_target="tpu_custom_call" | custom-call | flops 939524096 | bytes 4194304 | tf_op jit(solution)/shard_map/stats/pallas_call | solution.py:291
  72.8 2.3 %collective-permute-start.7 = (f32[4,8,512]{2,1,0:T(8,128)}, f32[4,8,512]{2,1,0:T(8,128)S(1)}, u32[]{:S(2)}, u32[]{:S(2)}) collective-permute-start(f32[4,8,512]{2,1,0:T(8,128)} %get-tuple-element.39.rest_8_), channel_id=1, source_target_pairs={{0,64},{8,72},{16,80},{24,88},{32,96},{40,104},{48,112},{56,120},{... | collective-permute-start | bytes 196616 | tf_op jit(solution)/shard_map/ppermute | solution.py:31
  75.0 2.7 %collective-permute-start.9 = (f32[4,8,512]{2,1,0:T(8,128)}, f32[4,8,512]{2,1,0:T(8,128)S(1)}, u32[]{:S(2)}, u32[]{:S(2)}) collective-permute-start(f32[4,8,512]{2,1,0:T(8,128)} %get-tuple-element.40.rest_12_), channel_id=1, source_target_pairs={{0,24},{8,0},{16,8},{24,16},{32,56},{40,32},{48,40},{56,48},{64,88... | collective-permute-start | bytes 196616 | tf_op jit(solution)/shard_map/ppermute | solution.py:31
  77.7 0.9 collective-permute-start.10
  79.4 1.5 collective-permute-start.27
  80.9 2.8 %collective-permute-done.10.rest_14_ = f32[4,8,512]{2,1,0:T(8,128)S(1)} collective-permute-done((f32[4,8,512]{2,1,0:T(8,128)}, f32[4,8,512]{2,1,0:T(8,128)S(1)}, u32[]{:S(2)}, u32[]{:S(2)}) %collective-permute-start.10) | collective-permute-done | bytes 65568 | tf_op jit(solution)/shard_map/ppermute | solution.py:31
  85.0 22.5 %grads.1 = (f32[128,512]{1,0:T(8,128)}, bf16[128,512]{1,0:T(8,128)(2,1)}, bf16[128,512]{1,0:T(8,128)(2,1)}, bf16[128,512]{1,0:T(8,128)(2,1)}, f32[128,512]{1,0:T...) custom-call(s32[2,2,4]{2,1,0:T(2,128)} %pad_add_fusion.pos_ref, ...), custom_call_target="tpu_custom_call" | custom-call | flops 5704253440 | bytes 8388608 | tf_op jit(solution)/shard_map/grads/pallas_call | solution.py:320
  108.3 0.8 collective-permute-start.16
  109.1 1.2 collective-permute-start.15
  110.3 1.7 collective-permute-start.28
  112.0 5.4 %collective-permute-start.14 = (bf16[128,512]{1,0:T(8,128)(2,1)}, bf16[128,512]{1,0:T(8,128)(2,1)S(1)}, u32[]{:S(2)}, u32[]{:S(2)}) collective-permute-start(bf16[128,512]{1,0:T(8,128)(2,1)} %get-tuple-element.44), channel_id=1, source_target_pairs={{0,96},{8,104},{16,112},{24,120},{32,0},{40,8},{48,16},{56,24},{64... | collective-permute-start | bytes 393224 | tf_op jit(solution)/shard_map/ppermute | solution.py:433
  117.5 2.9 %collective-permute-start.13 = (bf16[128,512]{1,0:T(8,128)(2,1)}, bf16[128,512]{1,0:T(8,128)(2,1)S(1)}, u32[]{:S(2)}, u32[]{:S(2)}) collective-permute-start(bf16[128,512]{1,0:T(8,128)(2,1)} %get-tuple-element.43), channel_id=1, source_target_pairs={{0,64},{8,72},{16,80},{24,88},{32,96},{40,104},{48,112},{56,120},{... | collective-permute-start | bytes 393224 | tf_op jit(solution)/shard_map/ppermute | solution.py:433
  120.4 1.1 convert_add_fusion.2
  121.5 9.3 %collective-permute-done.14 = bf16[128,512]{1,0:T(8,128)(2,1)S(1)} collective-permute-done((bf16[128,512]{1,0:T(8,128)(2,1)}, bf16[128,512]{1,0:T(8,128)(2,1)S(1)}, u32[]{:S(2)}, u32[]{:S(2)}) %collective-permute-start.14) | collective-permute-done | bytes 131104 | tf_op jit(solution)/shard_map/ppermute | solution.py:433
  130.9 0.9 copy-done.24
  131.8 4.1 %collective-permute-start.23 = (bf16[512,256]{1,0:T(8,128)(2,1)S(1)}, bf16[512,256]{1,0:T(8,128)(2,1)S(1)}, u32[]{:S(2)}, u32[]{:S(2)}) collective-permute-start(bf16[512,256]{1,0:T(8,128)(2,1)S(1)} %copy-done.24), channel_id=1, source_target_pairs={{0,96},{8,104},{16,112},{24,120},{32,0},{40,8},{48,16},{56,24},{64... | collective-permute-start | bytes 786440 | tf_op jit(solution)/shard_map/ppermute | solution.py:433
  135.8 1.0 collective-permute-start.21
  136.9 3.0 %collective-permute-start.20 = (bf16[512,256]{1,0:T(8,128)(2,1)}, bf16[512,256]{1,0:T(8,128)(2,1)}, u32[]{:S(2)}, u32[]{:S(2)}) collective-permute-start(bf16[512,256]{1,0:T(8,128)(2,1)} %get-tuple-element.60), channel_id=1, source_target_pairs={{0,24},{8,0},{16,8},{24,16},{32,56},{40,32},{48,40},{56,48},{64,88... | collective-permute-start | bytes 786440 | tf_op jit(solution)/shard_map/ppermute | solution.py:433
  139.9 5.8 %collective-permute-done.23 = bf16[512,256]{1,0:T(8,128)(2,1)S(1)} collective-permute-done((bf16[512,256]{1,0:T(8,128)(2,1)S(1)}, bf16[512,256]{1,0:T(8,128)(2,1)S(1)}, u32[]{:S(2)}, u32[]{:S(2)}) %collective-permute-start.23) | collective-permute-done | bytes 262176 | tf_op jit(solution)/shard_map/ppermute | solution.py:433
  145.7 2.2 %collective-permute-start.19 = (bf16[512,256]{1,0:T(8,128)(2,1)}, bf16[512,256]{1,0:T(8,128)(2,1)}, u32[]{:S(2)}, u32[]{:S(2)}) collective-permute-start(bf16[512,256]{1,0:T(8,128)(2,1)} %get-tuple-element.59), channel_id=1, source_target_pairs={{0,16},{8,24},{16,0},{24,8},{32,48},{40,56},{48,32},{56,40},{64,80... | collective-permute-start | bytes 786440 | tf_op jit(solution)/shard_map/ppermute | solution.py:433
  148.1 1.2 collective-permute-done.21
  150.7 1.0 copy.10
  151.7 1.7 collective-permute-start.18
  153.9 4.5 %collective-permute-start.24 = (bf16[256,512]{1,0:T(8,128)(2,1)S(1)}, bf16[256,512]{1,0:T(8,128)(2,1)S(1)}, u32[]{:S(2)}, u32[]{:S(2)}) collective-permute-start(bf16[256,512]{1,0:T(8,128)(2,1)S(1)} %fusion.rest_0_), channel_id=1, source_target_pairs={{0,96},{8,104},{16,112},{24,120},{32,0},{40,8},{48,16},{56,24},{64... | collective-permute-start | bytes 786440 | tf_op jit(solution)/shard_map/ppermute | solution.py:31
  158.6 1.7 collective-permute-done.18
  160.5 7.4 %collective-permute-done.24.rest_1_ = bf16[256,512]{1,0:T(8,128)(2,1)S(1)} collective-permute-done((bf16[256,512]{1,0:T(8,128)(2,1)S(1)}, bf16[256,512]{1,0:T(8,128)(2,1)S(1)}, u32[]{:S(2)}, u32[]{:S(2)}) %collective-permute-start.24) | collective-permute-done | bytes 262176 | tf_op jit(solution)/shard_map/ppermute | solution.py:31
  168.6 1.2 collective-permute-done.31.rest_7_
  169.8 1.1 convert_add_fusion.1
  171.0 2.3 %collective-permute-start.26 = (bf16[256,512]{1,0:T(8,128)(2,1)S(1)}, bf16[256,512]{1,0:T(8,128)(2,1)S(1)}, u32[]{:S(2)}, u32[]{:S(2)}) collective-permute-start(bf16[256,512]{1,0:T(8,128)(2,1)S(1)} %fusion.rest_0_), channel_id=1, source_target_pairs={{0,32},{8,40},{16,48},{24,56},{32,64},{40,72},{48,80},{56,88},{64,... | collective-permute-start | bytes 786440 | tf_op jit(solution)/shard_map/ppermute | solution.py:31
  173.3 11.2 %collective-permute-done.26.rest_3_ = bf16[256,512]{1,0:T(8,128)(2,1)S(1)} collective-permute-done((bf16[256,512]{1,0:T(8,128)(2,1)S(1)}, bf16[256,512]{1,0:T(8,128)(2,1)S(1)}, u32[]{:S(2)}, u32[]{:S(2)}) %collective-permute-start.26) | collective-permute-done | bytes 262176 | tf_op jit(solution)/shard_map/ppermute | solution.py:31
  187.0 5.2 %weight.1 = (f32[256,256]{1,0:T(8,128)}, bf16[256,256]{1,0:T(8,128)(2,1)}, bf16[256,256]{1,0:T(8,128)(2,1)}, bf16[256,256]{1,0:T(8,128)(2,1)}) custom-call(s32[4,4]{1,0:T(4,128)} %pad_add_fusion.1.at_ref, bf16[256,512]{1,0:T(8,128)(2,1)} %copy-done.2, bf16[256,512]{1,0:T(8,128)(2,1)} %copy-done.13, bf16[256,512]{1,0:T(8,128)(2,1)} %copy-done.14, ...), custom_call_target="tpu_custom_call" | custom-call | flops 1073741824 | bytes 6291456 | tf_op jit(solution)/shard_map/weight/pallas_call | solution.py:349
  192.3 2.0 collective-permute-start.38
  194.3 1.8 collective-permute-start.37
  196.1 0.8 pad_maximum_fusion.3
  197.7 2.6 %collective-permute-done.38 = bf16[256,256]{1,0:T(8,128)(2,1)S(1)} collective-permute-done((bf16[256,256]{1,0:T(8,128)(2,1)}, bf16[256,256]{1,0:T(8,128)(2,1)S(1)}, u32[]{:S(2)}, u32[]{:S(2)}) %collective-permute-start.38) | collective-permute-done | bytes 131104 | tf_op jit(solution)/shard_map/ppermute | solution.py:433
  200.3 2.1 %collective-permute-done.37 = bf16[256,256]{1,0:T(8,128)(2,1)S(1)} collective-permute-done((bf16[256,256]{1,0:T(8,128)(2,1)}, bf16[256,256]{1,0:T(8,128)(2,1)S(1)}, u32[]{:S(2)}, u32[]{:S(2)}) %collective-permute-start.37) | collective-permute-done | bytes 131104 | tf_op jit(solution)/shard_map/ppermute | solution.py:433
  202.4 1.5 collective-permute-done.36
  204.0 0.8 copy.11
  (125 shorter events, 14.1 us)
Async XLA Ops:
  2.1 26.6 %collective-permute-start = (bf16[512,512]{1,0:T(8,128)(2,1)S(1)}, bf16[512,512]{1,0:T(8,128)(2,1)S(1)}, u32[]{:S(2)}, u32[]{:S(2)}) collective-permute-start(bf16[512,512]{1,0:T(8,128)(2,1)S(1)} %pad_maximum_fusion.rest_0_), channel_id=1, source_target_pairs={{0,96},{8,104},{16,112},{24,120},{32,0},{40,8},{48,16},{56,24},{64... | collective-permute-start | bytes 1572872 | tf_op jit(solution)/shard_map/ppermute | solution.py:31
  6.3 43.5 %collective-permute-start.2 = (bf16[512,512]{1,0:T(8,128)(2,1)S(1)}, bf16[512,512]{1,0:T(8,128)(2,1)S(1)}, u32[]{:S(2)}, u32[]{:S(2)}) collective-permute-start(bf16[512,512]{1,0:T(8,128)(2,1)S(1)} %pad_maximum_fusion.rest_0_), channel_id=1, source_target_pairs={{0,32},{8,40},{16,48},{24,56},{32,64},{40,72},{48,80},{56,88},{64,... | collective-permute-start | bytes 1572872 | tf_op jit(solution)/shard_map/ppermute | solution.py:31
  6.3 25.4 %copy-start.19 = (f32[512,2]{0,1:T(2,128)S(1)}, f32[512,2]{0,1:T(2,128)}, u32[]{:S(2)}) copy-start(f32[512,2]{0,1:T(2,128)} %param.9) | copy-start | bytes 12292
  6.4 45.1 %copy-start.1 = (bf16[512,512]{1,0:T(8,128)(2,1)}, bf16[512,512]{1,0:T(8,128)(2,1)S(1)}, u32[]{:S(2)}) copy-start(bf16[512,512]{1,0:T(8,128)(2,1)S(1)} %pad_maximum_fusion.1.rest_3_.rest_4_) | copy-start | bytes 1572868
  6.4 43.5 %collective-permute-start.3 = (bf16[512,512]{1,0:T(8,128)(2,1)S(1)}, bf16[512,512]{1,0:T(8,128)(2,1)S(1)}, u32[]{:S(2)}, u32[]{:S(2)}) collective-permute-start(bf16[512,512]{1,0:T(8,128)(2,1)S(1)} %pad_maximum_fusion.1.rest_3_.rest_4_), channel_id=1, source_target_pairs={{0,24},{8,0},{16,8},{24,16},{32,56},{40,32},{48,40},{56,48},{64,88... | collective-permute-start | bytes 1572872 | tf_op jit(solution)/shard_map/ppermute | solution.py:31
  9.2 42.2 %collective-permute-start.5 = (bf16[512,512]{1,0:T(8,128)(2,1)S(1)}, bf16[512,512]{1,0:T(8,128)(2,1)}, u32[]{:S(2)}, u32[]{:S(2)}) collective-permute-start(bf16[512,512]{1,0:T(8,128)(2,1)S(1)} %pad_maximum_fusion.1.rest_3_.rest_4_), channel_id=1, source_target_pairs={{0,8},{8,16},{16,24},{24,0},{32,40},{40,48},{48,56},{56,32},{64,72... | collective-permute-start | bytes 1572872 | tf_op jit(solution)/shard_map/ppermute | solution.py:31
  9.2 53.4 %collective-permute-start.1 = (bf16[512,512]{1,0:T(8,128)(2,1)S(1)}, bf16[512,512]{1,0:T(8,128)(2,1)}, u32[]{:S(2)}, u32[]{:S(2)}) collective-permute-start(bf16[512,512]{1,0:T(8,128)(2,1)S(1)} %pad_maximum_fusion.rest_0_), channel_id=1, source_target_pairs={{0,64},{8,72},{16,80},{24,88},{32,96},{40,104},{48,112},{56,120},{... | collective-permute-start | bytes 1572872 | tf_op jit(solution)/shard_map/ppermute | solution.py:31
  28.7 22.7 %copy-start.9 = (bf16[512,512]{1,0:T(8,128)(2,1)}, bf16[512,512]{1,0:T(8,128)(2,1)S(1)}, u32[]{:S(2)}) copy-start(bf16[512,512]{1,0:T(8,128)(2,1)S(1)} %collective-permute-done.rest_1_) | copy-start | bytes 1572868
  28.7 33.9 %collective-permute-start.4 = (bf16[512,512]{1,0:T(8,128)(2,1)S(1)}, bf16[512,512]{1,0:T(8,128)(2,1)}, u32[]{:S(2)}, u32[]{:S(2)}) collective-permute-start(bf16[512,512]{1,0:T(8,128)(2,1)S(1)} %pad_maximum_fusion.1.rest_3_.rest_4_), channel_id=1, source_target_pairs={{0,16},{8,24},{16,0},{24,8},{32,48},{40,56},{48,32},{56,40},{64,80... | collective-permute-start | bytes 1572872 | tf_op jit(solution)/shard_map/ppermute | solution.py:31
  32.4 14.5 %all-to-all-start = ((f32[16,2,512]{2,1,0:T(2,128)}), f32[16,2,512]{2,1,0:T(2,128)S(1)}, u32[]{:S(2)}, u32[]{:S(2)}) async-start(f32[16,2,512]{2,1,0:T(2,128)} %tile.2), calls=%async_computation | async-start | bytes 131072 | tf_op jit(solution)/shard_map/all_to_all | solution.py:387
  62.6 16.8 %copy-start.20 = (bf16[512,512]{1,0:T(8,128)(2,1)S(1)}, bf16[512,512]{1,0:T(8,128)(2,1)}, u32[]{:S(2)}) copy-start(bf16[512,512]{1,0:T(8,128)(2,1)} %param.10) | copy-start | bytes 1572868
  72.1 6.5 %collective-permute-start.6 = (f32[4,8,512]{2,1,0:T(8,128)}, f32[4,8,512]{2,1,0:T(8,128)S(1)}, u32[]{:S(2)}, u32[]{:S(2)}) collective-permute-start(f32[4,8,512]{2,1,0:T(8,128)} %get-tuple-element.39.rest_8_), channel_id=1, source_target_pairs={{0,96},{8,104},{16,112},{24,120},{32,0},{40,8},{48,16},{56,24},{64... | collective-permute-start | bytes 196616 | tf_op jit(solution)/shard_map/ppermute | solution.py:31
  72.8 6.6 %collective-permute-start.7 = (f32[4,8,512]{2,1,0:T(8,128)}, f32[4,8,512]{2,1,0:T(8,128)S(1)}, u32[]{:S(2)}, u32[]{:S(2)}) collective-permute-start(f32[4,8,512]{2,1,0:T(8,128)} %get-tuple-element.39.rest_8_), channel_id=1, source_target_pairs={{0,64},{8,72},{16,80},{24,88},{32,96},{40,104},{48,112},{56,120},{... | collective-permute-start | bytes 196616 | tf_op jit(solution)/shard_map/ppermute | solution.py:31
  75.0 5.8 %collective-permute-start.8 = (f32[4,8,512]{2,1,0:T(8,128)}, f32[4,8,512]{2,1,0:T(8,128)S(1)}, u32[]{:S(2)}, u32[]{:S(2)}) collective-permute-start(f32[4,8,512]{2,1,0:T(8,128)} %get-tuple-element.39.rest_8_), channel_id=1, source_target_pairs={{0,32},{8,40},{16,48},{24,56},{32,64},{40,72},{48,80},{56,88},{64,... | collective-permute-start | bytes 196616 | tf_op jit(solution)/shard_map/ppermute | solution.py:31
  75.0 5.8 %collective-permute-start.9 = (f32[4,8,512]{2,1,0:T(8,128)}, f32[4,8,512]{2,1,0:T(8,128)S(1)}, u32[]{:S(2)}, u32[]{:S(2)}) collective-permute-start(f32[4,8,512]{2,1,0:T(8,128)} %get-tuple-element.40.rest_12_), channel_id=1, source_target_pairs={{0,24},{8,0},{16,8},{24,16},{32,56},{40,32},{48,40},{56,48},{64,88... | collective-permute-start | bytes 196616 | tf_op jit(solution)/shard_map/ppermute | solution.py:31
  77.7 6.0 %collective-permute-start.10 = (f32[4,8,512]{2,1,0:T(8,128)}, f32[4,8,512]{2,1,0:T(8,128)S(1)}, u32[]{:S(2)}, u32[]{:S(2)}) collective-permute-start(f32[4,8,512]{2,1,0:T(8,128)} %get-tuple-element.40.rest_12_), channel_id=1, source_target_pairs={{0,16},{8,24},{16,0},{24,8},{32,48},{40,56},{48,32},{56,40},{64,80... | collective-permute-start | bytes 196616 | tf_op jit(solution)/shard_map/ppermute | solution.py:31
  78.6 5.8 %collective-permute-start.11 = (f32[4,8,512]{2,1,0:T(8,128)}, f32[4,8,512]{2,1,0:T(8,128)S(1)}, u32[]{:S(2)}, u32[]{:S(2)}) collective-permute-start(f32[4,8,512]{2,1,0:T(8,128)} %get-tuple-element.40.rest_12_), channel_id=1, source_target_pairs={{0,8},{8,16},{16,24},{24,0},{32,40},{40,48},{48,56},{56,32},{64,72... | collective-permute-start | bytes 196616 | tf_op jit(solution)/shard_map/ppermute | solution.py:31
  79.4 30.9 %collective-permute-start.27 = (bf16[512,512]{1,0:T(8,128)(2,1)S(1)}, bf16[512,512]{1,0:T(8,128)(2,1)}, u32[]{:S(2)}, u32[]{:S(2)}) collective-permute-start(bf16[512,512]{1,0:T(8,128)(2,1)S(1)} %copy-done.20), channel_id=1, source_target_pairs={{0,0},{1,1},{2,2},{3,3},{4,4},{5,5},{6,6},{7,7},{8,8},{9,9},{10,10... | collective-permute-start | bytes 1572872 | tf_op jit(solution)/shard_map/ppermute | solution.py:416
  107.5 10.0 %collective-permute-start.17 = (bf16[128,512]{1,0:T(8,128)(2,1)}, bf16[128,512]{1,0:T(8,128)(2,1)S(1)}, u32[]{:S(2)}, u32[]{:S(2)}) collective-permute-start(bf16[128,512]{1,0:T(8,128)(2,1)} %get-tuple-element.48), channel_id=1, source_target_pairs={{0,24},{8,0},{16,8},{24,16},{32,56},{40,32},{48,40},{56,48},{64,88... | collective-permute-start | bytes 393224 | tf_op jit(solution)/shard_map/ppermute | solution.py:433
  108.3 12.1 %collective-permute-start.16 = (bf16[128,512]{1,0:T(8,128)(2,1)}, bf16[128,512]{1,0:T(8,128)(2,1)S(1)}, u32[]{:S(2)}, u32[]{:S(2)}) collective-permute-start(bf16[128,512]{1,0:T(8,128)(2,1)} %get-tuple-element.47), channel_id=1, source_target_pairs={{0,16},{8,24},{16,0},{24,8},{32,48},{40,56},{48,32},{56,40},{64,80... | collective-permute-start | bytes 393224 | tf_op jit(solution)/shard_map/ppermute | solution.py:433
  109.1 11.3 %collective-permute-start.15 = (bf16[128,512]{1,0:T(8,128)(2,1)}, bf16[128,512]{1,0:T(8,128)(2,1)S(1)}, u32[]{:S(2)}, u32[]{:S(2)}) collective-permute-start(bf16[128,512]{1,0:T(8,128)(2,1)} %get-tuple-element.46), channel_id=1, source_target_pairs={{0,8},{8,16},{16,24},{24,0},{32,40},{40,48},{48,56},{56,32},{64,72... | collective-permute-start | bytes 393224 | tf_op jit(solution)/shard_map/ppermute | solution.py:433
  110.3 37.6 %collective-permute-start.28 = (bf16[512,512]{1,0:T(8,128)(2,1)}, bf16[512,512]{1,0:T(8,128)(2,1)S(1)}, u32[]{:S(2)}, u32[]{:S(2)}) collective-permute-start(bf16[512,512]{1,0:T(8,128)(2,1)} %collective-permute-done.27), channel_id=1, source_target_pairs={{0,0},{1,1},{2,34},{3,35},{4,68},{5,69},{6,102},{7,103},{8,8},{9,9... | collective-permute-start | bytes 1572872 | tf_op jit(solution)/shard_map/ppermute | solution.py:417
  112.0 18.7 %collective-permute-start.14 = (bf16[128,512]{1,0:T(8,128)(2,1)}, bf16[128,512]{1,0:T(8,128)(2,1)S(1)}, u32[]{:S(2)}, u32[]{:S(2)}) collective-permute-start(bf16[128,512]{1,0:T(8,128)(2,1)} %get-tuple-element.44), channel_id=1, source_target_pairs={{0,96},{8,104},{16,112},{24,120},{32,0},{40,8},{48,16},{56,24},{64... | collective-permute-start | bytes 393224 | tf_op jit(solution)/shard_map/ppermute | solution.py:433
  117.5 13.3 %collective-permute-start.13 = (bf16[128,512]{1,0:T(8,128)(2,1)}, bf16[128,512]{1,0:T(8,128)(2,1)S(1)}, u32[]{:S(2)}, u32[]{:S(2)}) collective-permute-start(bf16[128,512]{1,0:T(8,128)(2,1)} %get-tuple-element.43), channel_id=1, source_target_pairs={{0,64},{8,72},{16,80},{24,88},{32,96},{40,104},{48,112},{56,120},{... | collective-permute-start | bytes 393224 | tf_op jit(solution)/shard_map/ppermute | solution.py:433
  120.4 10.3 %collective-permute-start.12 = (bf16[128,512]{1,0:T(8,128)(2,1)}, bf16[128,512]{1,0:T(8,128)(2,1)S(1)}, u32[]{:S(2)}, u32[]{:S(2)}) collective-permute-start(bf16[128,512]{1,0:T(8,128)(2,1)} %get-tuple-element.42), channel_id=1, source_target_pairs={{0,32},{8,40},{16,48},{24,56},{32,64},{40,72},{48,80},{56,88},{64,... | collective-permute-start | bytes 393224 | tf_op jit(solution)/shard_map/ppermute | solution.py:433
  120.4 10.3 %copy-start.12 = (f32[128,512]{1,0:T(8,128)S(1)}, f32[128,512]{1,0:T(8,128)}, u32[]{:S(2)}) copy-start(f32[128,512]{1,0:T(8,128)} %get-tuple-element.41) | copy-start | bytes 786436
  130.9 40.1 %copy-start.2 = (bf16[256,512]{1,0:T(8,128)(2,1)}, bf16[256,512]{1,0:T(8,128)(2,1)S(1)}, u32[]{:S(2)}) copy-start(bf16[256,512]{1,0:T(8,128)(2,1)S(1)} %fusion.rest_0_) | copy-start | bytes 786436
  131.8 14.0 %collective-permute-start.23 = (bf16[512,256]{1,0:T(8,128)(2,1)S(1)}, bf16[512,256]{1,0:T(8,128)(2,1)S(1)}, u32[]{:S(2)}, u32[]{:S(2)}) collective-permute-start(bf16[512,256]{1,0:T(8,128)(2,1)S(1)} %copy-done.24), channel_id=1, source_target_pairs={{0,96},{8,104},{16,112},{24,120},{32,0},{40,8},{48,16},{56,24},{64... | collective-permute-start | bytes 786440 | tf_op jit(solution)/shard_map/ppermute | solution.py:433
  135.8 12.1 %collective-permute-start.22 = (bf16[512,256]{1,0:T(8,128)(2,1)S(1)}, bf16[512,256]{1,0:T(8,128)(2,1)S(1)}, u32[]{:S(2)}, u32[]{:S(2)}) collective-permute-start(bf16[512,256]{1,0:T(8,128)(2,1)S(1)} %copy-done.23), channel_id=1, source_target_pairs={{0,64},{8,72},{16,80},{24,88},{32,96},{40,104},{48,112},{56,120},{... | collective-permute-start | bytes 786440 | tf_op jit(solution)/shard_map/ppermute | solution.py:433
  135.8 13.4 %collective-permute-start.21 = (bf16[512,256]{1,0:T(8,128)(2,1)S(1)}, bf16[512,256]{1,0:T(8,128)(2,1)S(1)}, u32[]{:S(2)}, u32[]{:S(2)}) collective-permute-start(bf16[512,256]{1,0:T(8,128)(2,1)S(1)} %copy-done.22), channel_id=1, source_target_pairs={{0,32},{8,40},{16,48},{24,56},{32,64},{40,72},{48,80},{56,88},{64,... | collective-permute-start | bytes 786440 | tf_op jit(solution)/shard_map/ppermute | solution.py:433
  136.9 14.8 %collective-permute-start.20 = (bf16[512,256]{1,0:T(8,128)(2,1)}, bf16[512,256]{1,0:T(8,128)(2,1)}, u32[]{:S(2)}, u32[]{:S(2)}) collective-permute-start(bf16[512,256]{1,0:T(8,128)(2,1)} %get-tuple-element.60), channel_id=1, source_target_pairs={{0,24},{8,0},{16,8},{24,16},{32,56},{40,32},{48,40},{56,48},{64,88... | collective-permute-start | bytes 786440 | tf_op jit(solution)/shard_map/ppermute | solution.py:433
  145.7 8.2 %collective-permute-start.19 = (bf16[512,256]{1,0:T(8,128)(2,1)}, bf16[512,256]{1,0:T(8,128)(2,1)}, u32[]{:S(2)}, u32[]{:S(2)}) collective-permute-start(bf16[512,256]{1,0:T(8,128)(2,1)} %get-tuple-element.59), channel_id=1, source_target_pairs={{0,16},{8,24},{16,0},{24,8},{32,48},{40,56},{48,32},{56,40},{64,80... | collective-permute-start | bytes 786440 | tf_op jit(solution)/shard_map/ppermute | solution.py:433
  147.9 20.1 %copy-start.3 = (bf16[512,512]{1,0:T(8,128)(2,1)}, bf16[512,512]{1,0:T(8,128)(2,1)S(1)}, u32[]{:S(2)}) copy-start(bf16[512,512]{1,0:T(8,128)(2,1)S(1)} %collective-permute-done.28.rest_4_) | copy-start | bytes 1572868
  147.9 20.1 %collective-permute-start.29 = (bf16[512,512]{1,0:T(8,128)(2,1)S(1)}, bf16[512,512]{1,0:T(8,128)(2,1)}, u32[]{:S(2)}, u32[]{:S(2)}) collective-permute-start(bf16[512,512]{1,0:T(8,128)(2,1)S(1)} %collective-permute-done.28.rest_4_), channel_id=1, source_target_pairs={{0,6},{1,7},{2,0},{3,1},{4,2},{5,3},{6,4},{7,5},{8,14},{9,15},{10,... | collective-permute-start | bytes 1572872 | tf_op jit(solution)/shard_map/ppermute | solution.py:420
  147.9 20.6 %collective-permute-start.30 = (bf16[512,512]{1,0:T(8,128)(2,1)S(1)}, bf16[512,512]{1,0:T(8,128)(2,1)}, u32[]{:S(2)}, u32[]{:S(2)}) collective-permute-start(bf16[512,512]{1,0:T(8,128)(2,1)S(1)} %collective-permute-done.28.rest_4_), channel_id=1, source_target_pairs={{0,4},{1,5},{2,6},{3,7},{4,0},{5,1},{6,2},{7,3},{8,12},{9,13},{10,... | collective-permute-start | bytes 1572872 | tf_op jit(solution)/shard_map/ppermute | solution.py:420
  149.2 20.6 %collective-permute-start.31 = (bf16[512,512]{1,0:T(8,128)(2,1)S(1)}, bf16[512,512]{1,0:T(8,128)(2,1)}, u32[]{:S(2)}, u32[]{:S(2)}) collective-permute-start(bf16[512,512]{1,0:T(8,128)(2,1)S(1)} %collective-permute-done.28.rest_4_), channel_id=1, source_target_pairs={{0,2},{1,3},{2,4},{3,5},{4,6},{5,7},{6,0},{7,1},{8,10},{9,11},{10,... | collective-permute-start | bytes 1572872 | tf_op jit(solution)/shard_map/ppermute | solution.py:420
  151.7 18.1 %copy-start.4 = (f32[512,256]{1,0:T(8,128)S(1)}, f32[512,256]{1,0:T(8,128)}, u32[]{:S(2)}) copy-start(f32[512,256]{1,0:T(8,128)} %get-tuple-element.57) | copy-start | bytes 1572868
  151.7 8.5 %collective-permute-start.18 = (bf16[512,256]{1,0:T(8,128)(2,1)S(1)}, bf16[512,256]{1,0:T(8,128)(2,1)S(1)}, u32[]{:S(2)}, u32[]{:S(2)}) collective-permute-start(bf16[512,256]{1,0:T(8,128)(2,1)S(1)} %copy-done.21), channel_id=1, source_target_pairs={{0,8},{8,16},{16,24},{24,0},{32,40},{40,48},{48,56},{56,32},{64,72... | collective-permute-start | bytes 786440 | tf_op jit(solution)/shard_map/ppermute | solution.py:433
  153.9 14.1 %collective-permute-start.24 = (bf16[256,512]{1,0:T(8,128)(2,1)S(1)}, bf16[256,512]{1,0:T(8,128)(2,1)S(1)}, u32[]{:S(2)}, u32[]{:S(2)}) collective-permute-start(bf16[256,512]{1,0:T(8,128)(2,1)S(1)} %fusion.rest_0_), channel_id=1, source_target_pairs={{0,96},{8,104},{16,112},{24,120},{32,0},{40,8},{48,16},{56,24},{64... | collective-permute-start | bytes 786440 | tf_op jit(solution)/shard_map/ppermute | solution.py:31
  160.2 10.7 %collective-permute-start.25 = (bf16[256,512]{1,0:T(8,128)(2,1)S(1)}, bf16[256,512]{1,0:T(8,128)(2,1)S(1)}, u32[]{:S(2)}, u32[]{:S(2)}) collective-permute-start(bf16[256,512]{1,0:T(8,128)(2,1)S(1)} %fusion.rest_0_), channel_id=1, source_target_pairs={{0,64},{8,72},{16,80},{24,88},{32,96},{40,104},{48,112},{56,120},{... | collective-permute-start | bytes 786440 | tf_op jit(solution)/shard_map/ppermute | solution.py:31
  168.0 16.6 %collective-permute-start.32 = (bf16[512,512]{1,0:T(8,128)(2,1)S(1)}, bf16[512,512]{1,0:T(8,128)(2,1)S(1)}, u32[]{:S(2)}, u32[]{:S(2)}) collective-permute-start(bf16[512,512]{1,0:T(8,128)(2,1)S(1)} %collective-permute-done.28.rest_4_), channel_id=1, source_target_pairs={{0,1},{1,0},{2,3},{3,2},{4,5},{5,4},{6,7},{7,6},{8,9},{9,8},{10,11... | collective-permute-start | bytes 1572872 | tf_op jit(solution)/shard_map/ppermute | solution.py:422
  168.0 17.4 %collective-permute-start.33 = (bf16[512,512]{1,0:T(8,128)(2,1)}, bf16[512,512]{1,0:T(8,128)(2,1)S(1)}, u32[]{:S(2)}, u32[]{:S(2)}) collective-permute-start(bf16[512,512]{1,0:T(8,128)(2,1)} %collective-permute-done.29.rest_5_), channel_id=1, source_target_pairs={{0,1},{1,0},{2,3},{3,2},{4,5},{5,4},{6,7},{7,6},{8,9},{9,8},{10,11... | collective-permute-start | bytes 1572872 | tf_op jit(solution)/shard_map/ppermute | solution.py:422
  168.5 17.7 %collective-permute-start.34 = (bf16[512,512]{1,0:T(8,128)(2,1)}, bf16[512,512]{1,0:T(8,128)(2,1)S(1)}, u32[]{:S(2)}, u32[]{:S(2)}) collective-permute-start(bf16[512,512]{1,0:T(8,128)(2,1)} %collective-permute-done.30.rest_6_), channel_id=1, source_target_pairs={{0,1},{1,0},{2,3},{3,2},{4,5},{5,4},{6,7},{7,6},{8,9},{9,8},{10,11... | collective-permute-start | bytes 1572872 | tf_op jit(solution)/shard_map/ppermute | solution.py:422
  169.8 17.2 %collective-permute-start.35 = (bf16[512,512]{1,0:T(8,128)(2,1)}, bf16[512,512]{1,0:T(8,128)(2,1)}, u32[]{:S(2)}, u32[]{:S(2)}) collective-permute-start(bf16[512,512]{1,0:T(8,128)(2,1)} %collective-permute-done.31.rest_7_), channel_id=1, source_target_pairs={{0,1},{1,0},{2,3},{3,2},{4,5},{5,4},{6,7},{7,6},{8,9},{9,8},{10,11... | collective-permute-start | bytes 1572872 | tf_op jit(solution)/shard_map/ppermute | solution.py:422
  171.0 13.6 %collective-permute-start.26 = (bf16[256,512]{1,0:T(8,128)(2,1)S(1)}, bf16[256,512]{1,0:T(8,128)(2,1)S(1)}, u32[]{:S(2)}, u32[]{:S(2)}) collective-permute-start(bf16[256,512]{1,0:T(8,128)(2,1)S(1)} %fusion.rest_0_), channel_id=1, source_target_pairs={{0,32},{8,40},{16,48},{24,56},{32,64},{40,72},{48,80},{56,88},{64,... | collective-permute-start | bytes 786440 | tf_op jit(solution)/shard_map/ppermute | solution.py:31
  192.3 8.0 %collective-permute-start.38 = (bf16[256,256]{1,0:T(8,128)(2,1)}, bf16[256,256]{1,0:T(8,128)(2,1)S(1)}, u32[]{:S(2)}, u32[]{:S(2)}) collective-permute-start(bf16[256,256]{1,0:T(8,128)(2,1)} %get-tuple-element.69), channel_id=1, source_target_pairs={{0,24},{8,0},{16,8},{24,16},{32,56},{40,32},{48,40},{56,48},{64,88... | collective-permute-start | bytes 393224 | tf_op jit(solution)/shard_map/ppermute | solution.py:433
  194.3 8.1 %collective-permute-start.37 = (bf16[256,256]{1,0:T(8,128)(2,1)}, bf16[256,256]{1,0:T(8,128)(2,1)S(1)}, u32[]{:S(2)}, u32[]{:S(2)}) collective-permute-start(bf16[256,256]{1,0:T(8,128)(2,1)} %get-tuple-element.68), channel_id=1, source_target_pairs={{0,16},{8,24},{16,0},{24,8},{32,48},{40,56},{48,32},{56,40},{64,80... | collective-permute-start | bytes 393224 | tf_op jit(solution)/shard_map/ppermute | solution.py:433
  196.1 7.8 %collective-permute-start.36 = (bf16[256,256]{1,0:T(8,128)(2,1)}, bf16[256,256]{1,0:T(8,128)(2,1)S(1)}, u32[]{:S(2)}, u32[]{:S(2)}) collective-permute-start(bf16[256,256]{1,0:T(8,128)(2,1)} %get-tuple-element.67), channel_id=1, source_target_pairs={{0,8},{8,16},{16,24},{24,0},{32,40},{40,48},{48,56},{56,32},{64,72... | collective-permute-start | bytes 393224 | tf_op jit(solution)/shard_map/ppermute | solution.py:433
  (23 other events, 66.4 us)

commit v2 on v1

v2 whole, which is shorter than its diff:
```python
import functools
import math

import jax
import jax.numpy as jnp
from jax import lax
from jax.experimental import pallas as pl
from jax.experimental.pallas import tpu as pltpu
from jax.sharding import PartitionSpec as P


HEAD = 128
SIDE = 4
SCALE = HEAD ** (-0.5)
LOG2E = math.log2(math.e)
NEG_BIG = -1e30
SUB = 256


def along_z(r):
    return [(4 * z + x, 4 * ((z + r) % SIDE) + x) for z in range(SIDE) for x in range(SIDE)]


def along_x(r):
    return [(4 * z + x, 4 * z + (x + r) % SIDE) for z in range(SIDE) for x in range(SIDE)]


def fetched(array, axis_perm):
    parts = [array]
    for r in range(1, SIDE):
        parts.append(lax.ppermute(array, "sp", axis_perm(-r)))
    return parts


def dot_nt(a, b):
    return lax.dot_general(a, b, (((1,), (1,)), ((), ())), preferred_element_type=jnp.float32)


def dot_nn(a, b):
    return lax.dot_general(a, b, (((1,), (0,)), ((), ())), preferred_element_type=jnp.float32)


def copy_list(sems):
    made = []

    def begin(src, dst):
        copy = pltpu.make_async_copy(src, dst, sems.at[len(made)])
        made.append(copy)
        copy.start()
        return copy

    return begin


def wait_all(copies):
    for c in copies:
        c.wait()


def start_loads(begin, h, z_refs, x_refs, slots, qd, kv):
    cols = pl.ds(h * 2 * HEAD, 2 * HEAD)
    q_refs, k_refs = (z_refs, x_refs) if h == 0 else (x_refs, z_refs)
    copies = []
    for r, q_ref, k_ref in zip(slots, q_refs, k_refs):
        copies.append(begin(q_ref.at[:, cols], qd.at[h, r]))
        copies.append(begin(k_ref.at[:, cols], kv.at[h, r]))
    return copies


def span_at(h, keys, r):
    here = lax.axis_index("sp")
    z, x = here // SIDE, here % SIDE
    if (h == 0) != keys:
        return SIDE * ((z + r) % SIDE) + x
    return SIDE * z + (x + r) % SIDE


def gates_kernel(logits_ref, out_ref):
    sums = jax.nn.log_sigmoid(logits_ref[...])
    rows, width = sums.shape
    lane = lax.broadcasted_iota(jnp.int32, sums.shape, 1)
    step = 1
    while step < width:
        sums = sums + jnp.where(lane >= step, pltpu.roll(sums, step, axis=1), 0.0)
        step *= 2
    shape = (rows, rows)
    mine, other = (lax.broadcasted_iota(jnp.int32, shape, d) for d in (0, 1))
    earlier = jnp.where((other < mine) & (other % 2 == mine % 2), 1.0, 0.0)
    totals = jnp.broadcast_to(sums[:, width - 1 :], (rows, HEAD))
    before = jnp.dot(
        earlier, totals, preferred_element_type=jnp.float32, precision=lax.Precision.HIGHEST
    )
    out_ref[...] = (sums + wide(before, width)) * LOG2E


def fill_bias(bias, bcol, h):
    def one(r, _):
        row = bias[pl.ds(2 * span_at(h, True, r) + h, 1), :]
        for j in range(4):
            tile = jnp.broadcast_to(row[:, j * HEAD : (j + 1) * HEAD], (HEAD, HEAD))
            bcol[r, j * HEAD : (j + 1) * HEAD, :] = tile.T
        return 0

    lax.fori_loop(0, SIDE, one, 0)


def for_visible(h, qi, ki, block):
    q_span, k_span = span_at(h, False, qi), span_at(h, True, ki)

    @pl.when(k_span < q_span)
    def _():
        block(h, qi, ki, False)

    @pl.when(k_span == q_span)
    def _():
        block(h, qi, ki, True)


def visible_mask(shape, first_query):
    key_at = lax.broadcasted_iota(jnp.int32, shape, 0)
    query_at = lax.broadcasted_iota(jnp.int32, shape, 1) + first_query
    return key_at <= query_at


def wide(tile, width):
    return jnp.concatenate([tile] * (width // tile.shape[1]), axis=1)


NEAR = (0, 1, 3)


def near_slot(n):
    return n + n // 2


def near_pairs(n):
    return near_slot(n // 3), near_slot(n % 3)


def far_pairs(n):
    near = near_slot(jnp.maximum(n - SIDE, 0))
    return jnp.where(n < SIDE, 2, near), jnp.where(n < SIDE, n, 2)


def stats_kernel(slots, pair_count, pair_of, bias_ref, *rest):
    n_slots = len(slots)
    z_refs, x_refs = rest[:n_slots], rest[n_slots : 2 * n_slots]
    rest = rest[2 * n_slots :]
    known, rest = rest[:-8], rest[-8:]
    outs = rest[:2]
    bias, qd, kv, bcol, stats, sems = rest[2:]
    span = qd.shape[2]
    begin = copy_list(sems)
    bias_copy = begin(bias_ref, bias)
    loads = []
    for h in range(2):
        loads.append(start_loads(begin, h, z_refs, x_refs, slots, qd, kv))
        if known:
            loads[h].append(begin(known[h], stats.at[h]))
        else:
            stats[h] = jnp.zeros((SIDE, 8, span), jnp.float32)
            stats[h, :, 0:1, :] = jnp.full((SIDE, 1, span), NEG_BIG, jnp.float32)

    def block(h, qi, ki, diagonal):
        for s in range(span // SUB):
            cols = slice(s * SUB, (s + 1) * SUB)
            q = qd[h, qi, cols, :HEAD]
            do = qd[h, qi, cols, HEAD:]
            k = kv[h, ki, :, :HEAD]
            v = kv[h, ki, :, HEAD:]
            x = dot_nt(k, q) * (SCALE * LOG2E) - wide(bcol[ki], SUB)
            if diagonal:
                x = jnp.where(visible_mask(x.shape, s * SUB), x, NEG_BIG)
            dp = dot_nt(v, do)
            old = stats[h, qi, 0:1, cols]
            new = jnp.maximum(old, jnp.max(x, axis=0, keepdims=True))
            p = jnp.exp2(x - new)
            shrink = jnp.exp2(old - new)
            stats[h, qi, 0:1, cols] = new
            stats[h, qi, 1:2, cols] = stats[h, qi, 1:2, cols] * shrink + jnp.sum(
                p, axis=0, keepdims=True
            )
            stats[h, qi, 2:3, cols] = stats[h, qi, 2:3, cols] * shrink + jnp.sum(
                p * dp, axis=0, keepdims=True
            )

    bias_copy.wait()
    stores = []
    for h in range(2):
        fill_bias(bias, bcol, h)
        wait_all(loads[h])

        def one_pair(n, _, h=h):
            qi, ki = pair_of(n)
            for_visible(h, qi, ki, block)
            return 0

        lax.fori_loop(0, pair_count, one_pair, 0)
        stores.append(begin(stats.at[h], outs[h]))
    wait_all(stores)


def grads_kernel(bias_ref, *rest):
    z_refs, x_refs = rest[:4], rest[4:8]
    stat_refs = (rest[8:12], rest[12:16])
    outs = rest[16:32]
    bias, qd, kv, bcol, parts, rows, kt, dqt, dkv, dq_send, dkv_send, sems = rest[32:]
    span = qd.shape[2]
    begin = copy_list(sems)
    bias_copy = begin(bias_ref, bias)
    loads = []
    for h in range(2):
        stat_copies = [begin(stat_refs[h][s], parts.at[h, s]) for s in range(SIDE)]
        loads.append(stat_copies + start_loads(begin, h, z_refs, x_refs, range(SIDE), qd, kv))

    def combine(h):
        for r in range(SIDE):
            found = [parts[h, s, (r - s) % SIDE] for s in range(SIDE)]
            top = functools.reduce(jnp.maximum, [p[0:1, :] for p in found])
            factors = [jnp.exp2(p[0:1, :] - top) for p in found]
            total = sum(p[1:2, :] * f for p, f in zip(found, factors))
            mixed = sum(p[2:3, :] * f for p, f in zip(found, factors))
            rows[h, r, 0:1, :] = top + jnp.log2(total)
            rows[h, r, 1:2, :] = mixed / total

    def block(h, qi, ki, diagonal):
        for s in range(span // SUB):
            cols = slice(s * SUB, (s + 1) * SUB)
            q = qd[h, qi, cols, :HEAD]
            do = qd[h, qi, cols, HEAD:]
            k = kv[h, ki, :, :HEAD]
            v = kv[h, ki, :, HEAD:]
            x = dot_nt(k, q) * (SCALE * LOG2E) - wide(bcol[ki], SUB) - rows[h, qi, 0:1, cols]
            if diagonal:
                x = jnp.where(visible_mask(x.shape, s * SUB), x, NEG_BIG)
            p = jnp.exp2(x)
            ds = (p * (dot_nt(v, do) - rows[h, qi, 1:2, cols])).astype(jnp.bfloat16)
            dkv[h, ki, :, HEAD:] += dot_nn(p.astype(jnp.bfloat16), do)
            dkv[h, ki, :, :HEAD] += dot_nn(ds, q)
            dqt[h, qi, :, cols] += dot_nn(kt[ki], ds)

    bias_copy.wait()
    stores = []
    for h in range(2):
        dqt[h] = jnp.zeros((SIDE, HEAD, span), jnp.float32)
        dkv[h] = jnp.zeros((SIDE, span, 2 * HEAD), jnp.float32)
        fill_bias(bias, bcol, h)
        wait_all(loads[h])
        combine(h)
        key_outs = outs[8 + SIDE * h : 8 + SIDE * (h + 1)]
        key_sources = [dkv.at[h, 0]] + [dkv_send.at[h, r] for r in range(1, SIDE)]
        key_stores = [
            pltpu.make_async_copy(source, out, sems.at[40 + SIDE * h + r])
            for r, (source, out) in enumerate(zip(key_sources, key_outs))
        ]

        def turn(r, _, h=h):
            kt[r] = kv[h, r, :, :HEAD].astype(jnp.float32).T.astype(jnp.bfloat16)
            return 0

        lax.fori_loop(0, SIDE, turn, 0)

        def one_key_span(ki, _, h=h, key_stores=key_stores):
            def one_query_span(qi, _):
                for_visible(h, qi, ki, block)
                return 0

            lax.fori_loop(0, SIDE, one_query_span, 0)
            scaled = dkv[h, ki, :, :HEAD] * SCALE
            dkv[h, ki, :, :HEAD] = scaled
            dkv_send[h, ki, :, :HEAD] = scaled.astype(jnp.bfloat16)
            dkv_send[h, ki, :, HEAD:] = dkv[h, ki, :, HEAD:].astype(jnp.bfloat16)
            for r in range(SIDE):
                pl.when(ki == r)(key_stores[r].start)
            return 0

        lax.fori_loop(0, SIDE, one_key_span, 0)
        stores += key_stores
        dqt[h, 0] = dqt[h, 0] * SCALE
        stores.append(begin(dqt.at[h, 0], outs[SIDE * h]))
        for r in range(1, SIDE):
            dq_send[h, r] = (dqt[h, r] * SCALE).astype(jnp.bfloat16)
            stores.append(begin(dq_send.at[h, r], outs[SIDE * h + r]))
    wait_all(stores)


def weight_kernel(*rest):
    dq_refs, in_refs, outs = rest[:4], rest[4:12], rest[12:16]
    dqs, inputs, sems = rest[16:]
    here, part = lax.axis_index("sp"), lax.axis_index("tp")
    z, x, y, core = here // SIDE, here % SIDE, part // 2, part % 2
    begin = copy_list(sems)
    copies = []
    for r in range(SIDE):
        of_span = (y - z + r + SIDE) % SIDE
        for other in range(2):
            held_by = core if other == 0 else 1 - core
            copies.append(begin(in_refs[SIDE * other + r], inputs.at[held_by, of_span]))
        copies.append(begin(dq_refs[r], dqs.at[(z + r) % SIDE]))
    wait_all(copies)
    width = outs[0].shape[1]
    for r in (1, 2, 3, 0):
        block = (x + r) % SIDE
        cols = pl.ds(pl.multiple_of((block % 2) * width, width), width)
        total = sum(dot_nn(dqs[a], inputs[block // 2, a, :, cols]) for a in range(SIDE))
        outs[r][...] = total.astype(outs[r].dtype)


ANY = pl.BlockSpec(memory_space=pl.ANY)
VM = pl.BlockSpec(memory_space=pltpu.VMEM)


def stats_call(bias, z_parts, x_parts, known=None):
    span = z_parts[0].shape[0]
    if known is None:
        slots, pair_count, pair_of, known = NEAR, 9, near_pairs, ()
        z_parts, x_parts = ([parts[r] for r in NEAR] for parts in (z_parts, x_parts))
    else:
        slots, pair_count, pair_of = range(SIDE), 7, far_pairs
    pairs = pair_count * span * span
    return pl.pallas_call(
        functools.partial(stats_kernel, slots, pair_count, pair_of),
        out_shape=[jax.ShapeDtypeStruct((SIDE, 8, span), jnp.float32)] * 2,
        in_specs=[ANY] * (1 + 2 * len(slots) + len(known)),
        out_specs=[ANY] * 2,
        scratch_shapes=[
            pltpu.VMEM(bias.shape, jnp.float32),
            pltpu.VMEM((2, SIDE, span, 2 * HEAD), jnp.bfloat16),
            pltpu.VMEM((2, SIDE, span, 2 * HEAD), jnp.bfloat16),
            pltpu.VMEM((SIDE, span, HEAD), jnp.float32),
            pltpu.VMEM((2, SIDE, 8, span), jnp.float32),
            pltpu.SemaphoreType.DMA((24,)),
        ],
        compiler_params=pltpu.CompilerParams(vmem_limit_bytes=62 << 20),
        cost_estimate=pl.CostEstimate(
            flops=4 * HEAD * pairs, bytes_accessed=4 << 20, transcendentals=pairs
        ),
        name="stats",
    )(bias, *z_parts, *x_parts, *known)


def grads_call(bias, z_parts, x_parts, z_stats, x_stats):
    span = z_parts[0].shape[0]
    pairs = 17 * span * span

    def shapes(*shape):
        own = jax.ShapeDtypeStruct(shape, jnp.float32)
        send = jax.ShapeDtypeStruct(shape, jnp.bfloat16)
        return ([own] + [send] * 3) * 2

    outs = pl.pallas_call(
        grads_kernel,
        out_shape=shapes(HEAD, span) + shapes(span, 2 * HEAD),
        in_specs=[ANY] * 17,
        out_specs=[ANY] * 16,
        scratch_shapes=[
            pltpu.VMEM(bias.shape, jnp.float32),
            pltpu.VMEM((2, SIDE, span, 2 * HEAD), jnp.bfloat16),
            pltpu.VMEM((2, SIDE, span, 2 * HEAD), jnp.bfloat16),
            pltpu.VMEM((SIDE, span, HEAD), jnp.float32),
            pltpu.VMEM((2, SIDE, SIDE, 8, span), jnp.float32),
            pltpu.VMEM((2, SIDE, 8, span), jnp.float32),
            pltpu.VMEM((SIDE, HEAD, span), jnp.bfloat16),
            pltpu.VMEM((2, SIDE, HEAD, span), jnp.float32),
            pltpu.VMEM((2, SIDE, span, 2 * HEAD), jnp.float32),
            pltpu.VMEM((2, SIDE, HEAD, span), jnp.bfloat16),
            pltpu.VMEM((2, SIDE, span, 2 * HEAD), jnp.bfloat16),
            pltpu.SemaphoreType.DMA((48,)),
        ],
        compiler_params=pltpu.CompilerParams(vmem_limit_bytes=62 << 20),
        cost_estimate=pl.CostEstimate(
            flops=10 * HEAD * pairs, bytes_accessed=8 << 20, transcendentals=pairs
        ),
        name="grads",
    )(bias, *z_parts, *x_parts, *z_stats, *x_stats)
    return outs[:4], outs[4:8], outs[8:12], outs[12:]


def weight_call(query_grads, inputs):
    cols, rows = query_grads[0].shape
    width = inputs[0].shape[1]
    own = jax.ShapeDtypeStruct((cols, width // 2), jnp.float32)
    send = jax.ShapeDtypeStruct((cols, width // 2), jnp.bfloat16)
    return pl.pallas_call(
        weight_kernel,
        out_shape=[own] + [send] * 3,
        in_specs=[ANY] * 12,
        out_specs=[VM] * 4,
        scratch_shapes=[
            pltpu.VMEM((SIDE, cols, rows), jnp.bfloat16),
            pltpu.VMEM((2, SIDE, rows, width), jnp.bfloat16),
            pltpu.SemaphoreType.DMA((12,)),
        ],
        compiler_params=pltpu.CompilerParams(vmem_limit_bytes=16 << 20),
        cost_estimate=pl.CostEstimate(
            flops=16 * rows * width * cols, bytes_accessed=6 << 20, transcendentals=0
        ),
        name="weight",
    )(*query_grads, *inputs)


def head_of(array, h):
    return array[:, h * HEAD : (h + 1) * HEAD]


def local(queries, keys, values, forget_logits, layer_input, out_grad):
    gates = lax.all_to_all(jnp.tile(forget_logits.T, (16, 1)), "sp", 0, 0, tiled=True)

    for_z = jnp.concatenate(
        [head_of(queries, 0), head_of(out_grad, 0), head_of(keys, 1), head_of(values, 1)], axis=1
    )
    for_x = jnp.concatenate(
        [head_of(keys, 0), head_of(values, 0), head_of(queries, 1), head_of(out_grad, 1)], axis=1
    )
    z_parts = fetched(for_z, along_z)
    x_parts = fetched(for_x, along_x)

    bias = pl.pallas_call(
        gates_kernel,
        out_shape=jax.ShapeDtypeStruct(gates.shape, jnp.float32),
        in_specs=[VM],
        out_specs=VM,
        cost_estimate=pl.CostEstimate(flops=10**6, bytes_accessed=1 << 17, transcendentals=0),
        name="gate_sums",
    )(gates)

    def over_zy(target):
        pairs = []
        for n in range(SIDE**3 * 2):
            zxyc = (n // 32, n // 8 % SIDE, n // 2 % SIDE, n % 2)
            new_z, new_y = target(zxyc[0], zxyc[2])
            pairs.append((n, new_z % SIDE * 32 + zxyc[1] * 8 + new_y % SIDE * 2 + zxyc[3]))
        return pairs

    everywhere = ("sp", "tp")
    moved = lax.ppermute(layer_input, everywhere, over_zy(lambda a, b: (a, a + b)))
    moved = lax.ppermute(moved, everywhere, over_zy(lambda a, b: (b - a, b)))
    inputs = [moved]
    for r in range(1, SIDE):
        inputs.append(lax.ppermute(moved, "tp", [(p, (p - 2 * r) % 8) for p in range(8)]))
    for part in list(inputs):
        inputs.append(lax.ppermute(part, "tp", [(p, p ^ 1) for p in range(8)]))

    known = stats_call(bias, z_parts, x_parts)
    stats_z, stats_x = stats_call(bias, z_parts, x_parts, known)
    z_stats = fetched(stats_z, along_z)
    x_stats = fetched(stats_x, along_x)
    dq_0, dq_1, dkv_0, dkv_1 = grads_call(bias, z_parts, x_parts, z_stats, x_stats)

    def summed(parts, axis_perm):
        total = parts[0]
        for r in range(1, SIDE):
            total = total + lax.ppermute(parts[r], "sp", axis_perm(r)).astype(jnp.float32)
        return total

    query_t = jnp.concatenate([summed(dq_0, along_z), summed(dq_1, along_x)], axis=0)
    low, dkv_0, dkv_1 = lax.optimization_barrier((query_t.astype(jnp.bfloat16), dkv_0, dkv_1))
    low_parts = fetched(low, along_z)
    terms = weight_call(low_parts, inputs)
    weight_grad = summed(terms, along_x).T
    sum_0, sum_1 = summed(dkv_0, along_x), summed(dkv_1, along_z)
    query_grad = query_t.T
    key_grad = jnp.concatenate([head_of(sum_0, 0), head_of(sum_1, 0)], axis=1)
    value_grad = jnp.concatenate([head_of(sum_0, 1), head_of(sum_1, 1)], axis=1)
    return (query_grad, key_grad, value_grad, weight_grad)


def solution(mesh):
    placed = P("sp", "tp")

    return jax.shard_map(
        local,
        mesh=mesh,
        in_specs=(placed,) * 6,
        out_specs=(placed,) * 4,
        check_vma=False,
    )
```

time: 206 us -> 169 us (0.82)
  waiting for transfers between devices: 73.8 us -> 27.5 us
  blocking collectives: 0 us -> 22.5 us
  Pallas kernels: 50.6 us -> 41.9 us
  starting transfers between devices: 63.6 us -> 60.4 us
  local copies, waits for them, and re-layouts: 10.2 us -> 7.78 us
    ppermute x15, waiting for transfers between devices: 39.8 us -> 17.1 us  [fetched(): parts.append(lax.ppermute(array, 'sp', axis_perm(-r)))]
    all_to_all x0 -> x1, blocking collectives: none -> 22.5 us  [local(): lax.all_to_all(jnp.tile(forget_logits.T, (16, 1)), 'sp', 0, 0, tiled=True)]
    ppermute x15, waiting for transfers between devices: 24.6 us -> 10.3 us  [summed(): lax.ppermute(parts[r], 'sp', axis_perm(r)).astype(jnp.float32)]
    all_to_all x1 -> x0, waiting for transfers between devices: 8.2 us -> none  [local(): lax.all_to_all(jnp.tile(forget_logits.T, (16, 1)), 'sp', 0, 0, tiled=True)]
    all_to_all x1 -> x0, starting transfers between devices: 5.65 us -> none  [local(): lax.all_to_all(jnp.tile(forget_logits.T, (16, 1)), 'sp', 0, 0, tiled=True)]
    ppermute x3, starting transfers between devices: 0.94 us -> 6.44 us  [local(): lax.ppermute(moved, 'tp', [(p, (p - 2 * r) % 8) for p in range(8)])]
    pallas_call x2, Pallas kernels: 20.6 us -> 17.1 us  [stats_call(): pl.pallas_call(functools.partial(stats_kernel, slots, pair_count, pair_of...]
    pallas_call x1, Pallas kernels: 5.24 us -> 1.83 us  [weight_call(): pl.pallas_call(weight_kernel, out_shape=[own] + [send] * 3, in_specs=[ANY...]
  transfers between devices with their start and end apart: 40 -> 39, of which waited for: 15 -> 14; matrix products, arithmetic and copies ran while one was open for 3% -> 4% of each run, Pallas kernels for 18% -> 19%
where the time goes in v2:
time: 169 us; the launch traced here: 166 us
  starting transfers between devices  60.4 us (36%)
  Pallas kernels  41.9 us (25%)
  waiting for transfers between devices  27.5 us (16%)
  blocking collectives  22.5 us (13%)
  local copies, waits for them, and re-layouts  7.78 us (5%)
  other arithmetic  5.37 us (3%)
    ppermute x15, starting transfers between devices, summed(): lax.ppermute(parts[r], 'sp', axis_perm(r)).astype(jnp.float32)  26.4 us
    ppermute x15, starting transfers between devices, fetched(): parts.append(lax.ppermute(array, 'sp', axis_perm(-r)))  25 us
    all_to_all x1, blocking collectives, local(): lax.all_to_all(jnp.tile(forget_logits.T, (16, 1)), 'sp', 0, 0, tiled=True)  22.5 us
    pallas_call x1, Pallas kernels, grads_call(): pl.pallas_call(grads_kernel, out_shape=shapes(HEAD, span) + shapes(span,...  20.7 us
    pallas_call x2, Pallas kernels, stats_call(): pl.pallas_call(functools.partial(stats_kernel, slots, pair_count, pair_of...  17.1 us
    ppermute x15, waiting for transfers between devices, fetched(): parts.append(lax.ppermute(array, 'sp', axis_perm(-r)))  17.1 us
    ppermute x15, waiting for transfers between devices, summed(): lax.ppermute(parts[r], 'sp', axis_perm(r)).astype(jnp.float32)  10.3 us
    ppermute x3, starting transfers between devices, local(): lax.ppermute(moved, 'tp', [(p, (p - 2 * r) % 8) for p in range(8)])  6.44 us
  transfers between devices with their start and end apart: 39, of which 14 were waited for; matrix products, arithmetic and copies ran while one was open for 4% of the time, Pallas kernels for 19%

profile of v2, /device:TPU:0, one launch (start us, length us, event | category | flops | bytes accessed | tf_op | source)
XLA Modules:
  0.0 166.5 jit_solution(7518737047290115564)
XLA Ops:
  0.7 1.2 fusion.6
  2.1 2.1 %collective-permute-start.2 = (bf16[512,512]{1,0:T(8,128)(2,1)S(1)}, bf16[512,512]{1,0:T(8,128)(2,1)S(1)}, u32[]{:S(2)}, u32[]{:S(2)}) collective-permute-start(bf16[512,512]{1,0:T(8,128)(2,1)S(1)} %pad_maximum_fusion.rest_0_), channel_id=1, source_target_pairs={{0,32},{8,40},{16,48},{24,56},{32,64},{40,72},{48,80},{56,88},{64,... | collective-permute-start | bytes 1572872 | tf_op jit(solution)/shard_map/ppermute | solution.py:31
  4.2 2.2 %collective-permute-start = (bf16[512,512]{1,0:T(8,128)(2,1)S(1)}, bf16[512,512]{1,0:T(8,128)(2,1)S(1)}, u32[]{:S(2)}, u32[]{:S(2)}) collective-permute-start(bf16[512,512]{1,0:T(8,128)(2,1)S(1)} %pad_maximum_fusion.rest_0_), channel_id=1, source_target_pairs={{0,96},{8,104},{16,112},{24,120},{32,0},{40,8},{48,16},{56,24},{64... | collective-permute-start | bytes 1572872 | tf_op jit(solution)/shard_map/ppermute | solution.py:31
  6.5 1.6 collective-permute-start.5
  8.0 1.7 %collective-permute-start.3 = (bf16[512,512]{1,0:T(8,128)(2,1)S(1)}, bf16[512,512]{1,0:T(8,128)(2,1)}, u32[]{:S(2)}, u32[]{:S(2)}) collective-permute-start(bf16[512,512]{1,0:T(8,128)(2,1)S(1)} %pad_maximum_fusion.1.rest_3_.rest_4_), channel_id=1, source_target_pairs={{0,24},{8,0},{16,8},{24,16},{32,56},{40,32},{48,40},{56,48},{64,88... | collective-permute-start | bytes 1572872 | tf_op jit(solution)/shard_map/ppermute | solution.py:31
  9.8 1.8 %collective-permute-start.1 = (bf16[512,512]{1,0:T(8,128)(2,1)S(1)}, bf16[512,512]{1,0:T(8,128)(2,1)}, u32[]{:S(2)}, u32[]{:S(2)}) collective-permute-start(bf16[512,512]{1,0:T(8,128)(2,1)S(1)} %pad_maximum_fusion.rest_0_), channel_id=1, source_target_pairs={{0,64},{8,72},{16,80},{24,88},{32,96},{40,104},{48,112},{56,120},{... | collective-permute-start | bytes 1572872 | tf_op jit(solution)/shard_map/ppermute | solution.py:31
  11.6 6.7 %collective-permute-done.2.rest_2_.rest_3_ = bf16[512,512]{1,0:T(8,128)(2,1)S(1)} collective-permute-done((bf16[512,512]{1,0:T(8,128)(2,1)S(1)}, bf16[512,512]{1,0:T(8,128)(2,1)S(1)}, u32[]{:S(2)}, u32[]{:S(2)}) %collective-permute-start.2) | collective-permute-done | bytes 524320 | tf_op jit(solution)/shard_map/ppermute | solution.py:31
  18.2 3.0 %collective-permute-start.4 = (bf16[512,512]{1,0:T(8,128)(2,1)S(1)}, bf16[512,512]{1,0:T(8,128)(2,1)}, u32[]{:S(2)}, u32[]{:S(2)}) collective-permute-start(bf16[512,512]{1,0:T(8,128)(2,1)S(1)} %pad_maximum_fusion.1.rest_3_.rest_4_), channel_id=1, source_target_pairs={{0,16},{8,24},{16,0},{24,8},{32,48},{40,56},{48,32},{56,40},{64,80... | collective-permute-start | bytes 1572872 | tf_op jit(solution)/shard_map/ppermute | solution.py:31
  21.3 22.5 %all_to_all.8 = f32[16,2,512]{2,1,0:T(2,128)S(1)} all-to-all(f32[16,2,512]{2,1,0:T(2,128)S(1)} %tile.2), channel_id=1, replica_groups=mesh['sp'=16,'tp'=8] {'sp'}, dimensions={0} | all-to-all | bytes 131072 | tf_op jit(solution)/shard_map/all_to_all | solution.py:407
  44.5 2.3 %gate_sums.1.bias_ref = f32[32,512]{1,0:T(8,128)} custom-call(f32[32,512]{1,0:T(8,128)} %all_to_all.6.logits_ref), custom_call_target="tpu_custom_call" | custom-call | flops 1000000 | bytes 131072 | tf_op jit(solution)/shard_map/gate_sums/pallas_call | solution.py:418
  48.3 9.5 %stats.2 = (f32[4,8,512]{2,1,0:T(8,128)}, f32[4,8,512]{2,1,0:T(8,128)}) custom-call(f32[32,512]{1,0:T(8,128)} %gate_sums.1.bias_ref, bf16[512,512]{1,0:T(8,128)(2,1)} %copy-done, bf16[512,512]{1,0:T(8,128)(2,1)} %copy-done.5, bf16[512,512]{1,0:T(8,128)(2,1)} %copy-done.4, bf16[512,512]{1,0:T(8,128)(2,1)} %copy-done.1, ...), custom_call_target="tpu_custom_call" | custom-call | flops 1207959552 | bytes 4194304 | tf_op jit(solution)/shard_map/stats/pallas_call | solution.py:321
  57.9 7.6 %stats.3 = (f32[4,8,512]{2,1,0:T(8,128)}, f32[4,8,512]{2,1,0:T(8,128)}) custom-call(f32[32,512]{1,0:T(8,128)} %gate_sums.1.bias_ref, bf16[512,512]{1,0:T(8,128)(2,1)} %copy-done, bf16[512,512]{1,0:T(8,128)(2,1)} %copy-done.5, bf16[512,512]{1,0:T(8,128)(2,1)} %collective-permute-done.1.rest_2_, bf16[512,512]{1,0:T(8,128)(2,1)} %copy-done.4, ...), custom_call_target="tpu_custom_call" | custom-call | flops 939524096 | bytes 4194304 | tf_op jit(solution)/shard_map/stats/pallas_call | solution.py:321
  66.1 2.0 %collective-permute-start.7 = (f32[4,8,512]{2,1,0:T(8,128)}, f32[4,8,512]{2,1,0:T(8,128)S(1)}, u32[]{:S(2)}, u32[]{:S(2)}) collective-permute-start(f32[4,8,512]{2,1,0:T(8,128)} %get-tuple-element.39.rest_8_), channel_id=1, source_target_pairs={{0,64},{8,72},{16,80},{24,88},{32,96},{40,104},{48,112},{56,120},{... | collective-permute-start | bytes 196616 | tf_op jit(solution)/shard_map/ppermute | solution.py:31
  68.1 1.2 collective-permute-start.6
  69.9 2.1 %collective-permute-start.10 = (f32[4,8,512]{2,1,0:T(8,128)}, f32[4,8,512]{2,1,0:T(8,128)S(1)}, u32[]{:S(2)}, u32[]{:S(2)}) collective-permute-start(f32[4,8,512]{2,1,0:T(8,128)} %get-tuple-element.40.rest_12_), channel_id=1, source_target_pairs={{0,16},{8,24},{16,0},{24,8},{32,48},{40,56},{48,32},{56,40},{64,80... | collective-permute-start | bytes 196616 | tf_op jit(solution)/shard_map/ppermute | solution.py:31
  72.0 1.3 collective-permute-start.9
  73.3 0.9 collective-permute-start.27
  77.2 20.7 %grads.1 = (f32[128,512]{1,0:T(8,128)}, bf16[128,512]{1,0:T(8,128)(2,1)}, bf16[128,512]{1,0:T(8,128)(2,1)}, bf16[128,512]{1,0:T(8,128)(2,1)}, f32[128,512]{1,0:T...) custom-call(f32[32,512]{1,0:T(8,128)} %gate_sums.1.bias_ref, ...), custom_call_target="tpu_custom_call" | custom-call | flops 5704253440 | bytes 8388608 | tf_op jit(solution)/shard_map/grads/pallas_call | solution.py:351
  97.9 2.0 %collective-permute-start.12 = (bf16[128,512]{1,0:T(8,128)(2,1)}, bf16[128,512]{1,0:T(8,128)(2,1)S(1)}, u32[]{:S(2)}, u32[]{:S(2)}) collective-permute-start(bf16[128,512]{1,0:T(8,128)(2,1)} %get-tuple-element.42), channel_id=1, source_target_pairs={{0,32},{8,40},{16,48},{24,56},{32,64},{40,72},{48,80},{56,88},{64,... | collective-permute-start | bytes 393224 | tf_op jit(solution)/shard_map/ppermute | solution.py:453
  99.9 3.6 %collective-permute-start.13 = (bf16[128,512]{1,0:T(8,128)(2,1)}, bf16[128,512]{1,0:T(8,128)(2,1)S(1)}, u32[]{:S(2)}, u32[]{:S(2)}) collective-permute-start(bf16[128,512]{1,0:T(8,128)(2,1)} %get-tuple-element.43), channel_id=1, source_target_pairs={{0,64},{8,72},{16,80},{24,88},{32,96},{40,104},{48,112},{56,120},{... | collective-permute-start | bytes 393224 | tf_op jit(solution)/shard_map/ppermute | solution.py:453
  103.5 2.2 %collective-permute-start.14 = (bf16[128,512]{1,0:T(8,128)(2,1)}, bf16[128,512]{1,0:T(8,128)(2,1)S(1)}, u32[]{:S(2)}, u32[]{:S(2)}) collective-permute-start(bf16[128,512]{1,0:T(8,128)(2,1)} %get-tuple-element.44), channel_id=1, source_target_pairs={{0,96},{8,104},{16,112},{24,120},{32,0},{40,8},{48,16},{56,24},{64... | collective-permute-start | bytes 393224 | tf_op jit(solution)/shard_map/ppermute | solution.py:453
  107.2 1.6 collective-permute-start.16
  108.8 2.5 %collective-permute-start.17 = (bf16[128,512]{1,0:T(8,128)(2,1)}, bf16[128,512]{1,0:T(8,128)(2,1)S(1)}, u32[]{:S(2)}, u32[]{:S(2)}) collective-permute-start(bf16[128,512]{1,0:T(8,128)(2,1)} %get-tuple-element.48), channel_id=1, source_target_pairs={{0,24},{8,0},{16,8},{24,16},{32,56},{40,32},{48,40},{56,48},{64,88... | collective-permute-start | bytes 393224 | tf_op jit(solution)/shard_map/ppermute | solution.py:453
  111.4 1.1 convert_add_fusion.3
  112.4 3.2 %collective-permute-done.15 = bf16[128,512]{1,0:T(8,128)(2,1)S(1)} collective-permute-done((bf16[128,512]{1,0:T(8,128)(2,1)}, bf16[128,512]{1,0:T(8,128)(2,1)S(1)}, u32[]{:S(2)}, u32[]{:S(2)}) %collective-permute-start.15) | collective-permute-done | bytes 131104 | tf_op jit(solution)/shard_map/ppermute | solution.py:453
  115.8 0.9 copy-done.17
  116.6 1.1 collective-permute-start.18
  117.8 2.5 %collective-permute-start.19 = (bf16[512,256]{1,0:T(8,128)(2,1)S(1)}, bf16[512,256]{1,0:T(8,128)(2,1)S(1)}, u32[]{:S(2)}, u32[]{:S(2)}) collective-permute-start(bf16[512,256]{1,0:T(8,128)(2,1)S(1)} %copy-done.16), channel_id=1, source_target_pairs={{0,16},{8,24},{16,0},{24,8},{32,48},{40,56},{48,32},{56,40},{64,80... | collective-permute-start | bytes 786440 | tf_op jit(solution)/shard_map/ppermute | solution.py:453
  121.0 2.1 %collective-permute-start.21 = (bf16[512,256]{1,0:T(8,128)(2,1)}, bf16[512,256]{1,0:T(8,128)(2,1)}, u32[]{:S(2)}, u32[]{:S(2)}) collective-permute-start(bf16[512,256]{1,0:T(8,128)(2,1)} %get-tuple-element.62), channel_id=1, source_target_pairs={{0,32},{8,40},{16,48},{24,56},{32,64},{40,72},{48,80},{56,88},{64,... | collective-permute-start | bytes 786440 | tf_op jit(solution)/shard_map/ppermute | solution.py:453
  123.1 1.1 collective-permute-done.18
  124.2 1.6 collective-permute-start.22
  125.9 1.6 collective-permute-start.31
  127.5 2.8 %collective-permute-start.30 = (bf16[512,512]{1,0:T(8,128)(2,1)S(1)}, bf16[512,512]{1,0:T(8,128)(2,1)S(1)}, u32[]{:S(2)}, u32[]{:S(2)}) collective-permute-start(bf16[512,512]{1,0:T(8,128)(2,1)S(1)} %collective-permute-done.28.rest_4_), channel_id=1, source_target_pairs={{0,4},{1,5},{2,6},{3,7},{4,0},{5,1},{6,2},{7,3},{8,12},{9,13},{10,... | collective-permute-start | bytes 1572872 | tf_op jit(solution)/shard_map/ppermute | solution.py:440
  131.0 2.0 %collective-permute-start.29 = (bf16[512,512]{1,0:T(8,128)(2,1)S(1)}, bf16[512,512]{1,0:T(8,128)(2,1)S(1)}, u32[]{:S(2)}, u32[]{:S(2)}) collective-permute-start(bf16[512,512]{1,0:T(8,128)(2,1)S(1)} %collective-permute-done.28.rest_4_), channel_id=1, source_target_pairs={{0,6},{1,7},{2,0},{3,1},{4,2},{5,3},{6,4},{7,5},{8,14},{9,15},{10,... | collective-permute-start | bytes 1572872 | tf_op jit(solution)/shard_map/ppermute | solution.py:440
  133.1 1.0 copy.10
  134.1 1.3 collective-permute-start.23
  137.0 1.2 convert_add_fusion.1
  138.2 2.5 %collective-permute-done.23 = bf16[512,256]{1,0:T(8,128)(2,1)S(1)} collective-permute-done((bf16[512,256]{1,0:T(8,128)(2,1)}, bf16[512,256]{1,0:T(8,128)(2,1)S(1)}, u32[]{:S(2)}, u32[]{:S(2)}) %collective-permute-start.23) | collective-permute-done | bytes 262176 | tf_op jit(solution)/shard_map/ppermute | solution.py:453
  140.7 1.4 collective-permute-start.25
  142.1 1.6 collective-permute-done.26.rest_3_
  144.8 1.1 convert_add_fusion
  145.9 2.6 %collective-permute-done.25.rest_2_ = bf16[256,512]{1,0:T(8,128)(2,1)S(1)} collective-permute-done((bf16[256,512]{1,0:T(8,128)(2,1)S(1)}, bf16[256,512]{1,0:T(8,128)(2,1)S(1)}, u32[]{:S(2)}, u32[]{:S(2)}) %collective-permute-start.25) | collective-permute-done | bytes 262176 | tf_op jit(solution)/shard_map/ppermute | solution.py:31
  148.6 2.5 %collective-permute-start.24 = (bf16[256,512]{1,0:T(8,128)(2,1)S(1)}, bf16[256,512]{1,0:T(8,128)(2,1)S(1)}, u32[]{:S(2)}, u32[]{:S(2)}) collective-permute-start(bf16[256,512]{1,0:T(8,128)(2,1)S(1)} %fusion.rest_0_), channel_id=1, source_target_pairs={{0,96},{8,104},{16,112},{24,120},{32,0},{40,8},{48,16},{56,24},{64... | collective-permute-start | bytes 786440 | tf_op jit(solution)/shard_map/ppermute | solution.py:31
  151.2 3.8 %collective-permute-done.24.rest_1_ = bf16[256,512]{1,0:T(8,128)(2,1)S(1)} collective-permute-done((bf16[256,512]{1,0:T(8,128)(2,1)S(1)}, bf16[256,512]{1,0:T(8,128)(2,1)S(1)}, u32[]{:S(2)}, u32[]{:S(2)}) %collective-permute-start.24) | collective-permute-done | bytes 262176 | tf_op jit(solution)/shard_map/ppermute | solution.py:31
  155.0 1.8 %weight.1 = (f32[256,256]{1,0:T(8,128)S(1)}, bf16[256,256]{1,0:T(8,128)(2,1)S(1)}, bf16[256,256]{1,0:T(8,128)(2,1)S(1)}, bf16[256,256]{1,0:T(8,128)(2,1)S(1)}) custom-call(bf16[256,512]{1,0:T(8,128)(2,1)S(1)} %fusion.rest_0_, bf16[256,512]{1,0:T(8,128)(2,1)S(1)} %collective-permute-done.24.rest_1_, bf16[256,512]{1,0:T(8,128)(2,1)S(1)} %collective-permute-done.25.rest_2_, ...), custom_call_target="tpu_custom_call" | custom-call | flops 1073741824 | bytes 6291456 | tf_op jit(solution)/shard_map/weight/pallas_call | solution.py:384
  156.9 1.2 collective-permute-start.36
  158.1 2.5 %collective-permute-start.37 = (bf16[256,256]{1,0:T(8,128)(2,1)S(1)}, bf16[256,256]{1,0:T(8,128)(2,1)S(1)}, u32[]{:S(2)}, u32[]{:S(2)}) collective-permute-start(bf16[256,256]{1,0:T(8,128)(2,1)S(1)} %get-tuple-element.68), channel_id=1, source_target_pairs={{0,16},{8,24},{16,0},{24,8},{32,48},{40,56},{48,32},{56,40},{64,80... | collective-permute-start | bytes 393224 | tf_op jit(solution)/shard_map/ppermute | solution.py:453
  163.1 1.8 %collective-permute-done.37 = bf16[256,256]{1,0:T(8,128)(2,1)S(1)} collective-permute-done((bf16[256,256]{1,0:T(8,128)(2,1)S(1)}, bf16[256,256]{1,0:T(8,128)(2,1)S(1)}, u32[]{:S(2)}, u32[]{:S(2)}) %collective-permute-start.37) | collective-permute-done | bytes 131104 | tf_op jit(solution)/shard_map/ppermute | solution.py:453
  (103 shorter events, 16.5 us)
Async XLA Ops:
  2.1 7.7 %copy-start = (bf16[512,512]{1,0:T(8,128)(2,1)}, bf16[512,512]{1,0:T(8,128)(2,1)S(1)}, u32[]{:S(2)}) copy-start(bf16[512,512]{1,0:T(8,128)(2,1)S(1)} %pad_maximum_fusion.rest_0_) | copy-start | bytes 1572868
  2.1 16.1 %collective-permute-start.2 = (bf16[512,512]{1,0:T(8,128)(2,1)S(1)}, bf16[512,512]{1,0:T(8,128)(2,1)S(1)}, u32[]{:S(2)}, u32[]{:S(2)}) collective-permute-start(bf16[512,512]{1,0:T(8,128)(2,1)S(1)} %pad_maximum_fusion.rest_0_), channel_id=1, source_target_pairs={{0,32},{8,40},{16,48},{24,56},{32,64},{40,72},{48,80},{56,88},{64,... | collective-permute-start | bytes 1572872 | tf_op jit(solution)/shard_map/ppermute | solution.py:31
  4.2 42.5 %collective-permute-start = (bf16[512,512]{1,0:T(8,128)(2,1)S(1)}, bf16[512,512]{1,0:T(8,128)(2,1)S(1)}, u32[]{:S(2)}, u32[]{:S(2)}) collective-permute-start(bf16[512,512]{1,0:T(8,128)(2,1)S(1)} %pad_maximum_fusion.rest_0_), channel_id=1, source_target_pairs={{0,96},{8,104},{16,112},{24,120},{32,0},{40,8},{48,16},{56,24},{64... | collective-permute-start | bytes 1572872 | tf_op jit(solution)/shard_map/ppermute | solution.py:31
  6.4 14.9 %copy-start.13 = (f32[512,2]{0,1:T(2,128)S(1)}, f32[512,2]{0,1:T(2,128)}, u32[]{:S(2)}) copy-start(f32[512,2]{0,1:T(2,128)} %param.9) | copy-start | bytes 12292
  6.5 41.9 %copy-start.1 = (bf16[512,512]{1,0:T(8,128)(2,1)}, bf16[512,512]{1,0:T(8,128)(2,1)S(1)}, u32[]{:S(2)}) copy-start(bf16[512,512]{1,0:T(8,128)(2,1)S(1)} %pad_maximum_fusion.1.rest_3_.rest_4_) | copy-start | bytes 1572868
  6.5 40.3 %collective-permute-start.5 = (bf16[512,512]{1,0:T(8,128)(2,1)S(1)}, bf16[512,512]{1,0:T(8,128)(2,1)S(1)}, u32[]{:S(2)}, u32[]{:S(2)}) collective-permute-start(bf16[512,512]{1,0:T(8,128)(2,1)S(1)} %pad_maximum_fusion.1.rest_3_.rest_4_), channel_id=1, source_target_pairs={{0,8},{8,16},{16,24},{24,0},{32,40},{40,48},{48,56},{56,32},{64,72... | collective-permute-start | bytes 1572872 | tf_op jit(solution)/shard_map/ppermute | solution.py:31
  8.0 40.3 %collective-permute-start.3 = (bf16[512,512]{1,0:T(8,128)(2,1)S(1)}, bf16[512,512]{1,0:T(8,128)(2,1)}, u32[]{:S(2)}, u32[]{:S(2)}) collective-permute-start(bf16[512,512]{1,0:T(8,128)(2,1)S(1)} %pad_maximum_fusion.1.rest_3_.rest_4_), channel_id=1, source_target_pairs={{0,24},{8,0},{16,8},{24,16},{32,56},{40,32},{48,40},{56,48},{64,88... | collective-permute-start | bytes 1572872 | tf_op jit(solution)/shard_map/ppermute | solution.py:31
  9.8 48.1 %collective-permute-start.1 = (bf16[512,512]{1,0:T(8,128)(2,1)S(1)}, bf16[512,512]{1,0:T(8,128)(2,1)}, u32[]{:S(2)}, u32[]{:S(2)}) collective-permute-start(bf16[512,512]{1,0:T(8,128)(2,1)S(1)} %pad_maximum_fusion.rest_0_), channel_id=1, source_target_pairs={{0,64},{8,72},{16,80},{24,88},{32,96},{40,104},{48,112},{56,120},{... | collective-permute-start | bytes 1572872 | tf_op jit(solution)/shard_map/ppermute | solution.py:31
  18.2 30.1 %copy-start.4 = (bf16[512,512]{1,0:T(8,128)(2,1)}, bf16[512,512]{1,0:T(8,128)(2,1)S(1)}, u32[]{:S(2)}) copy-start(bf16[512,512]{1,0:T(8,128)(2,1)S(1)} %collective-permute-done.2.rest_2_.rest_3_) | copy-start | bytes 1572868
  18.2 39.6 %collective-permute-start.4 = (bf16[512,512]{1,0:T(8,128)(2,1)S(1)}, bf16[512,512]{1,0:T(8,128)(2,1)}, u32[]{:S(2)}, u32[]{:S(2)}) collective-permute-start(bf16[512,512]{1,0:T(8,128)(2,1)S(1)} %pad_maximum_fusion.1.rest_3_.rest_4_), channel_id=1, source_target_pairs={{0,16},{8,24},{16,0},{24,8},{32,48},{40,56},{48,32},{56,40},{64,80... | collective-permute-start | bytes 1572872 | tf_op jit(solution)/shard_map/ppermute | solution.py:31
  57.9 15.4 %copy-start.14 = (bf16[512,512]{1,0:T(8,128)(2,1)S(1)}, bf16[512,512]{1,0:T(8,128)(2,1)}, u32[]{:S(2)}) copy-start(bf16[512,512]{1,0:T(8,128)(2,1)} %param.10) | copy-start | bytes 1572868
  65.5 6.5 %collective-permute-start.8 = (f32[4,8,512]{2,1,0:T(8,128)}, f32[4,8,512]{2,1,0:T(8,128)S(1)}, u32[]{:S(2)}, u32[]{:S(2)}) collective-permute-start(f32[4,8,512]{2,1,0:T(8,128)} %get-tuple-element.39.rest_8_), channel_id=1, source_target_pairs={{0,32},{8,40},{16,48},{24,56},{32,64},{40,72},{48,80},{56,88},{64,... | collective-permute-start | bytes 196616 | tf_op jit(solution)/shard_map/ppermute | solution.py:31
  66.1 7.2 %collective-permute-start.7 = (f32[4,8,512]{2,1,0:T(8,128)}, f32[4,8,512]{2,1,0:T(8,128)S(1)}, u32[]{:S(2)}, u32[]{:S(2)}) collective-permute-start(f32[4,8,512]{2,1,0:T(8,128)} %get-tuple-element.39.rest_8_), channel_id=1, source_target_pairs={{0,64},{8,72},{16,80},{24,88},{32,96},{40,104},{48,112},{56,120},{... | collective-permute-start | bytes 196616 | tf_op jit(solution)/shard_map/ppermute | solution.py:31
  68.1 6.0 %collective-permute-start.6 = (f32[4,8,512]{2,1,0:T(8,128)}, f32[4,8,512]{2,1,0:T(8,128)S(1)}, u32[]{:S(2)}, u32[]{:S(2)}) collective-permute-start(f32[4,8,512]{2,1,0:T(8,128)} %get-tuple-element.39.rest_8_), channel_id=1, source_target_pairs={{0,96},{8,104},{16,112},{24,120},{32,0},{40,8},{48,16},{56,24},{64... | collective-permute-start | bytes 196616 | tf_op jit(solution)/shard_map/ppermute | solution.py:31
  69.3 5.7 %collective-permute-start.11 = (f32[4,8,512]{2,1,0:T(8,128)}, f32[4,8,512]{2,1,0:T(8,128)S(1)}, u32[]{:S(2)}, u32[]{:S(2)}) collective-permute-start(f32[4,8,512]{2,1,0:T(8,128)} %get-tuple-element.40.rest_12_), channel_id=1, source_target_pairs={{0,8},{8,16},{16,24},{24,0},{32,40},{40,48},{48,56},{56,32},{64,72... | collective-permute-start | bytes 196616 | tf_op jit(solution)/shard_map/ppermute | solution.py:31
  69.9 6.0 %collective-permute-start.10 = (f32[4,8,512]{2,1,0:T(8,128)}, f32[4,8,512]{2,1,0:T(8,128)S(1)}, u32[]{:S(2)}, u32[]{:S(2)}) collective-permute-start(f32[4,8,512]{2,1,0:T(8,128)} %get-tuple-element.40.rest_12_), channel_id=1, source_target_pairs={{0,16},{8,24},{16,0},{24,8},{32,48},{40,56},{48,32},{56,40},{64,80... | collective-permute-start | bytes 196616 | tf_op jit(solution)/shard_map/ppermute | solution.py:31
  72.0 4.6 %copy-start.18 = (f32[4,8,512]{2,1,0:T(8,128)}, f32[4,8,512]{2,1,0:T(8,128)S(1)}, u32[]{:S(2)}) copy-start(f32[4,8,512]{2,1,0:T(8,128)S(1)} %collective-permute-done.8.rest_11_) | copy-start | bytes 196612
  72.0 4.6 %collective-permute-start.9 = (f32[4,8,512]{2,1,0:T(8,128)}, f32[4,8,512]{2,1,0:T(8,128)S(1)}, u32[]{:S(2)}, u32[]{:S(2)}) collective-permute-start(f32[4,8,512]{2,1,0:T(8,128)} %get-tuple-element.40.rest_12_), channel_id=1, source_target_pairs={{0,24},{8,0},{16,8},{24,16},{32,56},{40,32},{48,40},{56,48},{64,88... | collective-permute-start | bytes 196616 | tf_op jit(solution)/shard_map/ppermute | solution.py:31
  73.3 32.4 %collective-permute-start.27 = (bf16[512,512]{1,0:T(8,128)(2,1)S(1)}, bf16[512,512]{1,0:T(8,128)(2,1)S(1)}, u32[]{:S(2)}, u32[]{:S(2)}) collective-permute-start(bf16[512,512]{1,0:T(8,128)(2,1)S(1)} %copy-done.14), channel_id=1, source_target_pairs={{0,0},{1,1},{2,2},{3,3},{4,4},{5,5},{6,6},{7,7},{8,8},{9,9},{10,10... | collective-permute-start | bytes 1572872 | tf_op jit(solution)/shard_map/ppermute | solution.py:436
  97.9 9.3 %collective-permute-start.12 = (bf16[128,512]{1,0:T(8,128)(2,1)}, bf16[128,512]{1,0:T(8,128)(2,1)S(1)}, u32[]{:S(2)}, u32[]{:S(2)}) collective-permute-start(bf16[128,512]{1,0:T(8,128)(2,1)} %get-tuple-element.42), channel_id=1, source_target_pairs={{0,32},{8,40},{16,48},{24,56},{32,64},{40,72},{48,80},{56,88},{64,... | collective-permute-start | bytes 393224 | tf_op jit(solution)/shard_map/ppermute | solution.py:453
  99.9 8.9 %collective-permute-start.13 = (bf16[128,512]{1,0:T(8,128)(2,1)}, bf16[128,512]{1,0:T(8,128)(2,1)S(1)}, u32[]{:S(2)}, u32[]{:S(2)}) collective-permute-start(bf16[128,512]{1,0:T(8,128)(2,1)} %get-tuple-element.43), channel_id=1, source_target_pairs={{0,64},{8,72},{16,80},{24,88},{32,96},{40,104},{48,112},{56,120},{... | collective-permute-start | bytes 393224 | tf_op jit(solution)/shard_map/ppermute | solution.py:453
  103.5 7.8 %collective-permute-start.14 = (bf16[128,512]{1,0:T(8,128)(2,1)}, bf16[128,512]{1,0:T(8,128)(2,1)S(1)}, u32[]{:S(2)}, u32[]{:S(2)}) collective-permute-start(bf16[128,512]{1,0:T(8,128)(2,1)} %get-tuple-element.44), channel_id=1, source_target_pairs={{0,96},{8,104},{16,112},{24,120},{32,0},{40,8},{48,16},{56,24},{64... | collective-permute-start | bytes 393224 | tf_op jit(solution)/shard_map/ppermute | solution.py:453
  105.7 20.1 %collective-permute-start.28 = (bf16[512,512]{1,0:T(8,128)(2,1)S(1)}, bf16[512,512]{1,0:T(8,128)(2,1)S(1)}, u32[]{:S(2)}, u32[]{:S(2)}) collective-permute-start(bf16[512,512]{1,0:T(8,128)(2,1)S(1)} %collective-permute-done.27), channel_id=1, source_target_pairs={{0,0},{1,1},{2,34},{3,35},{4,68},{5,69},{6,102},{7,103},{8,8},{9,9... | collective-permute-start | bytes 1572872 | tf_op jit(solution)/shard_map/ppermute | solution.py:437
  106.4 9.2 %collective-permute-start.15 = (bf16[128,512]{1,0:T(8,128)(2,1)}, bf16[128,512]{1,0:T(8,128)(2,1)S(1)}, u32[]{:S(2)}, u32[]{:S(2)}) collective-permute-start(bf16[128,512]{1,0:T(8,128)(2,1)} %get-tuple-element.46), channel_id=1, source_target_pairs={{0,8},{8,16},{16,24},{24,0},{32,40},{40,48},{48,56},{56,32},{64,72... | collective-permute-start | bytes 393224 | tf_op jit(solution)/shard_map/ppermute | solution.py:453
  107.2 8.4 %collective-permute-start.16 = (bf16[128,512]{1,0:T(8,128)(2,1)}, bf16[128,512]{1,0:T(8,128)(2,1)S(1)}, u32[]{:S(2)}, u32[]{:S(2)}) collective-permute-start(bf16[128,512]{1,0:T(8,128)(2,1)} %get-tuple-element.47), channel_id=1, source_target_pairs={{0,16},{8,24},{16,0},{24,8},{32,48},{40,56},{48,32},{56,40},{64,80... | collective-permute-start | bytes 393224 | tf_op jit(solution)/shard_map/ppermute | solution.py:453
  108.8 6.8 %collective-permute-start.17 = (bf16[128,512]{1,0:T(8,128)(2,1)}, bf16[128,512]{1,0:T(8,128)(2,1)S(1)}, u32[]{:S(2)}, u32[]{:S(2)}) collective-permute-start(bf16[128,512]{1,0:T(8,128)(2,1)} %get-tuple-element.48), channel_id=1, source_target_pairs={{0,24},{8,0},{16,8},{24,16},{32,56},{40,32},{48,40},{56,48},{64,88... | collective-permute-start | bytes 393224 | tf_op jit(solution)/shard_map/ppermute | solution.py:453
  115.7 4.6 %copy-start.15 = (bf16[512,256]{1,0:T(8,128)(2,1)S(1)}, bf16[512,256]{1,0:T(8,128)(2,1)}, u32[]{:S(2)}) copy-start(bf16[512,256]{1,0:T(8,128)(2,1)} %get-tuple-element.60) | copy-start | bytes 786436
  116.6 7.6 %collective-permute-start.18 = (bf16[512,256]{1,0:T(8,128)(2,1)S(1)}, bf16[512,256]{1,0:T(8,128)(2,1)S(1)}, u32[]{:S(2)}, u32[]{:S(2)}) collective-permute-start(bf16[512,256]{1,0:T(8,128)(2,1)S(1)} %copy-done.17), channel_id=1, source_target_pairs={{0,8},{8,16},{16,24},{24,0},{32,40},{40,48},{48,56},{56,32},{64,72... | collective-permute-start | bytes 786440 | tf_op jit(solution)/shard_map/ppermute | solution.py:453
  117.8 9.7 %collective-permute-start.19 = (bf16[512,256]{1,0:T(8,128)(2,1)S(1)}, bf16[512,256]{1,0:T(8,128)(2,1)S(1)}, u32[]{:S(2)}, u32[]{:S(2)}) collective-permute-start(bf16[512,256]{1,0:T(8,128)(2,1)S(1)} %copy-done.16), channel_id=1, source_target_pairs={{0,16},{8,24},{16,0},{24,8},{32,48},{40,56},{48,32},{56,40},{64,80... | collective-permute-start | bytes 786440 | tf_op jit(solution)/shard_map/ppermute | solution.py:453
  120.3 10.0 %collective-permute-start.20 = (bf16[512,256]{1,0:T(8,128)(2,1)S(1)}, bf16[512,256]{1,0:T(8,128)(2,1)S(1)}, u32[]{:S(2)}, u32[]{:S(2)}) collective-permute-start(bf16[512,256]{1,0:T(8,128)(2,1)S(1)} %copy-done.15), channel_id=1, source_target_pairs={{0,24},{8,0},{16,8},{24,16},{32,56},{40,32},{48,40},{56,48},{64,88... | collective-permute-start | bytes 786440 | tf_op jit(solution)/shard_map/ppermute | solution.py:453
  121.0 13.1 %collective-permute-start.21 = (bf16[512,256]{1,0:T(8,128)(2,1)}, bf16[512,256]{1,0:T(8,128)(2,1)}, u32[]{:S(2)}, u32[]{:S(2)}) collective-permute-start(bf16[512,256]{1,0:T(8,128)(2,1)} %get-tuple-element.62), channel_id=1, source_target_pairs={{0,32},{8,40},{16,48},{24,56},{32,64},{40,72},{48,80},{56,88},{64,... | collective-permute-start | bytes 786440 | tf_op jit(solution)/shard_map/ppermute | solution.py:453
  124.2 6.1 %copy-start.8 = (bf16[512,256]{1,0:T(8,128)(2,1)}, bf16[512,256]{1,0:T(8,128)(2,1)S(1)}, u32[]{:S(2)}) copy-start(bf16[512,256]{1,0:T(8,128)(2,1)S(1)} %collective-permute-done.18) | copy-start | bytes 786436
  124.2 11.9 %collective-permute-start.22 = (bf16[512,256]{1,0:T(8,128)(2,1)}, bf16[512,256]{1,0:T(8,128)(2,1)}, u32[]{:S(2)}, u32[]{:S(2)}) collective-permute-start(bf16[512,256]{1,0:T(8,128)(2,1)} %get-tuple-element.63), channel_id=1, source_target_pairs={{0,64},{8,72},{16,80},{24,88},{32,96},{40,104},{48,112},{56,120},{... | collective-permute-start | bytes 786440 | tf_op jit(solution)/shard_map/ppermute | solution.py:453
  125.9 17.9 %collective-permute-start.31 = (bf16[512,512]{1,0:T(8,128)(2,1)S(1)}, bf16[512,512]{1,0:T(8,128)(2,1)S(1)}, u32[]{:S(2)}, u32[]{:S(2)}) collective-permute-start(bf16[512,512]{1,0:T(8,128)(2,1)S(1)} %collective-permute-done.28.rest_4_), channel_id=1, source_target_pairs={{0,2},{1,3},{2,4},{3,5},{4,6},{5,7},{6,0},{7,1},{8,10},{9,11},{10,... | collective-permute-start | bytes 1572872 | tf_op jit(solution)/shard_map/ppermute | solution.py:440
  127.5 16.7 %collective-permute-start.30 = (bf16[512,512]{1,0:T(8,128)(2,1)S(1)}, bf16[512,512]{1,0:T(8,128)(2,1)S(1)}, u32[]{:S(2)}, u32[]{:S(2)}) collective-permute-start(bf16[512,512]{1,0:T(8,128)(2,1)S(1)} %collective-permute-done.28.rest_4_), channel_id=1, source_target_pairs={{0,4},{1,5},{2,6},{3,7},{4,0},{5,1},{6,2},{7,3},{8,12},{9,13},{10,... | collective-permute-start | bytes 1572872 | tf_op jit(solution)/shard_map/ppermute | solution.py:440
  131.0 13.3 %collective-permute-start.29 = (bf16[512,512]{1,0:T(8,128)(2,1)S(1)}, bf16[512,512]{1,0:T(8,128)(2,1)S(1)}, u32[]{:S(2)}, u32[]{:S(2)}) collective-permute-start(bf16[512,512]{1,0:T(8,128)(2,1)S(1)} %collective-permute-done.28.rest_4_), channel_id=1, source_target_pairs={{0,6},{1,7},{2,0},{3,1},{4,2},{5,3},{6,4},{7,5},{8,14},{9,15},{10,... | collective-permute-start | bytes 1572872 | tf_op jit(solution)/shard_map/ppermute | solution.py:440
  134.1 10.7 %copy-start.2 = (f32[512,256]{1,0:T(8,128)S(1)}, f32[512,256]{1,0:T(8,128)}, u32[]{:S(2)}) copy-start(f32[512,256]{1,0:T(8,128)} %get-tuple-element.61) | copy-start | bytes 1572868
  134.1 6.6 %collective-permute-start.23 = (bf16[512,256]{1,0:T(8,128)(2,1)}, bf16[512,256]{1,0:T(8,128)(2,1)S(1)}, u32[]{:S(2)}, u32[]{:S(2)}) collective-permute-start(bf16[512,256]{1,0:T(8,128)(2,1)} %get-tuple-element.64), channel_id=1, source_target_pairs={{0,96},{8,104},{16,112},{24,120},{32,0},{40,8},{48,16},{56,24},{64... | collective-permute-start | bytes 786440 | tf_op jit(solution)/shard_map/ppermute | solution.py:453
  136.2 7.6 %collective-permute-start.26 = (bf16[256,512]{1,0:T(8,128)(2,1)S(1)}, bf16[256,512]{1,0:T(8,128)(2,1)S(1)}, u32[]{:S(2)}, u32[]{:S(2)}) collective-permute-start(bf16[256,512]{1,0:T(8,128)(2,1)S(1)} %fusion.rest_0_), channel_id=1, source_target_pairs={{0,32},{8,40},{16,48},{24,56},{32,64},{40,72},{48,80},{56,88},{64,... | collective-permute-start | bytes 786440 | tf_op jit(solution)/shard_map/ppermute | solution.py:31
  140.7 7.9 %collective-permute-start.25 = (bf16[256,512]{1,0:T(8,128)(2,1)S(1)}, bf16[256,512]{1,0:T(8,128)(2,1)S(1)}, u32[]{:S(2)}, u32[]{:S(2)}) collective-permute-start(bf16[256,512]{1,0:T(8,128)(2,1)S(1)} %fusion.rest_0_), channel_id=1, source_target_pairs={{0,64},{8,72},{16,80},{24,88},{32,96},{40,104},{48,112},{56,120},{... | collective-permute-start | bytes 786440 | tf_op jit(solution)/shard_map/ppermute | solution.py:31
  143.7 11.3 %collective-permute-start.32 = (bf16[512,512]{1,0:T(8,128)(2,1)S(1)}, bf16[512,512]{1,0:T(8,128)(2,1)S(1)}, u32[]{:S(2)}, u32[]{:S(2)}) collective-permute-start(bf16[512,512]{1,0:T(8,128)(2,1)S(1)} %collective-permute-done.28.rest_4_), channel_id=1, source_target_pairs={{0,1},{1,0},{2,3},{3,2},{4,5},{5,4},{6,7},{7,6},{8,9},{9,8},{10,11... | collective-permute-start | bytes 1572872 | tf_op jit(solution)/shard_map/ppermute | solution.py:442
  143.7 11.3 %collective-permute-start.35 = (bf16[512,512]{1,0:T(8,128)(2,1)S(1)}, bf16[512,512]{1,0:T(8,128)(2,1)S(1)}, u32[]{:S(2)}, u32[]{:S(2)}) collective-permute-start(bf16[512,512]{1,0:T(8,128)(2,1)S(1)} %collective-permute-done.31.rest_7_), channel_id=1, source_target_pairs={{0,1},{1,0},{2,3},{3,2},{4,5},{5,4},{6,7},{7,6},{8,9},{9,8},{10,11... | collective-permute-start | bytes 1572872 | tf_op jit(solution)/shard_map/ppermute | solution.py:442
  144.3 10.8 %collective-permute-start.34 = (bf16[512,512]{1,0:T(8,128)(2,1)S(1)}, bf16[512,512]{1,0:T(8,128)(2,1)S(1)}, u32[]{:S(2)}, u32[]{:S(2)}) collective-permute-start(bf16[512,512]{1,0:T(8,128)(2,1)S(1)} %collective-permute-done.30.rest_6_), channel_id=1, source_target_pairs={{0,1},{1,0},{2,3},{3,2},{4,5},{5,4},{6,7},{7,6},{8,9},{9,8},{10,11... | collective-permute-start | bytes 1572872 | tf_op jit(solution)/shard_map/ppermute | solution.py:442
  144.3 10.7 %collective-permute-start.33 = (bf16[512,512]{1,0:T(8,128)(2,1)S(1)}, bf16[512,512]{1,0:T(8,128)(2,1)S(1)}, u32[]{:S(2)}, u32[]{:S(2)}) collective-permute-start(bf16[512,512]{1,0:T(8,128)(2,1)S(1)} %collective-permute-done.29.rest_5_), channel_id=1, source_target_pairs={{0,1},{1,0},{2,3},{3,2},{4,5},{5,4},{6,7},{7,6},{8,9},{9,8},{10,11... | collective-permute-start | bytes 1572872 | tf_op jit(solution)/shard_map/ppermute | solution.py:442
  148.6 6.4 %collective-permute-start.24 = (bf16[256,512]{1,0:T(8,128)(2,1)S(1)}, bf16[256,512]{1,0:T(8,128)(2,1)S(1)}, u32[]{:S(2)}, u32[]{:S(2)}) collective-permute-start(bf16[256,512]{1,0:T(8,128)(2,1)S(1)} %fusion.rest_0_), channel_id=1, source_target_pairs={{0,96},{8,104},{16,112},{24,120},{32,0},{40,8},{48,16},{56,24},{64... | collective-permute-start | bytes 786440 | tf_op jit(solution)/shard_map/ppermute | solution.py:31
  156.9 6.2 %collective-permute-start.36 = (bf16[256,256]{1,0:T(8,128)(2,1)S(1)}, bf16[256,256]{1,0:T(8,128)(2,1)S(1)}, u32[]{:S(2)}, u32[]{:S(2)}) collective-permute-start(bf16[256,256]{1,0:T(8,128)(2,1)S(1)} %get-tuple-element.67), channel_id=1, source_target_pairs={{0,8},{8,16},{16,24},{24,0},{32,40},{40,48},{48,56},{56,32},{64,72... | collective-permute-start | bytes 393224 | tf_op jit(solution)/shard_map/ppermute | solution.py:453
  158.1 6.9 %collective-permute-start.37 = (bf16[256,256]{1,0:T(8,128)(2,1)S(1)}, bf16[256,256]{1,0:T(8,128)(2,1)S(1)}, u32[]{:S(2)}, u32[]{:S(2)}) collective-permute-start(bf16[256,256]{1,0:T(8,128)(2,1)S(1)} %get-tuple-element.68), channel_id=1, source_target_pairs={{0,16},{8,24},{16,0},{24,8},{32,48},{40,56},{48,32},{56,40},{64,80... | collective-permute-start | bytes 393224 | tf_op jit(solution)/shard_map/ppermute | solution.py:453
  160.6 5.0 %collective-permute-start.38 = (bf16[256,256]{1,0:T(8,128)(2,1)S(1)}, bf16[256,256]{1,0:T(8,128)(2,1)S(1)}, u32[]{:S(2)}, u32[]{:S(2)}) collective-permute-start(bf16[256,256]{1,0:T(8,128)(2,1)S(1)} %get-tuple-element.69), channel_id=1, source_target_pairs={{0,24},{8,0},{16,8},{24,16},{32,56},{40,32},{48,40},{56,48},{64,88... | collective-permute-start | bytes 393224 | tf_op jit(solution)/shard_map/ppermute | solution.py:453
  (15 other events, 27.3 us)

commit v3 on v2

--- a/solution.py
+++ b/solution.py
@@ -98,7 +98,7 @@
         row = bias[pl.ds(2 * span_at(h, True, r) + h, 1), :]
         for j in range(4):
             tile = jnp.broadcast_to(row[:, j * HEAD : (j + 1) * HEAD], (HEAD, HEAD))
-            bcol[r, j * HEAD : (j + 1) * HEAD, :] = tile.T
+            bcol[h, r, j * HEAD : (j + 1) * HEAD, :] = tile.T
         return 0
 
     lax.fori_loop(0, SIDE, one, 0)
@@ -166,9 +166,10 @@
             cols = slice(s * SUB, (s + 1) * SUB)
             q = qd[h, qi, cols, :HEAD]
             do = qd[h, qi, cols, HEAD:]
-            k = kv[h, ki, :, :HEAD]
-            v = kv[h, ki, :, HEAD:]
-            x = dot_nt(k, q) * (SCALE * LOG2E) - wide(bcol[ki], SUB)
+            seen = (s + 1) * SUB if diagonal else span
+            k = kv[h, ki, :seen, :HEAD]
+            v = kv[h, ki, :seen, HEAD:]
+            x = dot_nt(k, q) * (SCALE * LOG2E) - wide(bcol[h, ki, :seen], SUB)
             if diagonal:
                 x = jnp.where(visible_mask(x.shape, s * SUB), x, NEG_BIG)
             dp = dot_nt(v, do)
@@ -188,6 +189,7 @@
     stores = []
     for h in range(2):
         fill_bias(bias, bcol, h)
+    for h in range(2):
         wait_all(loads[h])
 
         def one_pair(n, _, h=h):
@@ -228,23 +230,26 @@
             cols = slice(s * SUB, (s + 1) * SUB)
             q = qd[h, qi, cols, :HEAD]
             do = qd[h, qi, cols, HEAD:]
-            k = kv[h, ki, :, :HEAD]
-            v = kv[h, ki, :, HEAD:]
-            x = dot_nt(k, q) * (SCALE * LOG2E) - wide(bcol[ki], SUB) - rows[h, qi, 0:1, cols]
+            seen = (s + 1) * SUB if diagonal else span
+            k = kv[h, ki, :seen, :HEAD]
+            v = kv[h, ki, :seen, HEAD:]
+            x = dot_nt(k, q) * (SCALE * LOG2E) - wide(bcol[h, ki, :seen], SUB)
+            x = x - rows[h, qi, 0:1, cols]
             if diagonal:
                 x = jnp.where(visible_mask(x.shape, s * SUB), x, NEG_BIG)
             p = jnp.exp2(x)
             ds = (p * (dot_nt(v, do) - rows[h, qi, 1:2, cols])).astype(jnp.bfloat16)
-            dkv[h, ki, :, HEAD:] += dot_nn(p.astype(jnp.bfloat16), do)
-            dkv[h, ki, :, :HEAD] += dot_nn(ds, q)
-            dqt[h, qi, :, cols] += dot_nn(kt[ki], ds)
-
+            dkv[h, ki, :seen, HEAD:] += dot_nn(p.astype(jnp.bfloat16), do)
+            dkv[h, ki, :seen, :HEAD] += dot_nn(ds, q)
+            dqt[h, qi, :, cols] += dot_nn(kt[ki, :, :seen], ds)
+
+    dqt[...] = jnp.zeros_like(dqt)
+    dkv[...] = jnp.zeros_like(dkv)
     bias_copy.wait()
     stores = []
     for h in range(2):
-        dqt[h] = jnp.zeros((SIDE, HEAD, span), jnp.float32)
-        dkv[h] = jnp.zeros((SIDE, span, 2 * HEAD), jnp.float32)
         fill_bias(bias, bcol, h)
+    for h in range(2):
         wait_all(loads[h])
         combine(h)
         key_outs = outs[8 + SIDE * h : 8 + SIDE * (h + 1)]
@@ -306,6 +311,25 @@
         outs[r][...] = total.astype(outs[r].dtype)
 
 
+def query_kernel(*refs):
+    parts, (low_ref, grad_ref) = refs[:8], refs[8:]
+    for h in range(2):
+        total = sum(ref[...].astype(jnp.float32) for ref in parts[SIDE * h : SIDE * (h + 1)])
+        cut = slice(h * HEAD, (h + 1) * HEAD)
+        low_ref[cut, :] = total.astype(jnp.bfloat16)
+        grad_ref[:, cut] = total.T
+
+
+def keys_kernel(*refs):
+    parts, outs = refs[:8], refs[8:]
+    for h in range(2):
+        for n, out in enumerate(outs):
+            cut = slice(n * HEAD, (n + 1) * HEAD)
+            out[:, h * HEAD : (h + 1) * HEAD] = sum(
+                ref[:, cut].astype(jnp.float32) for ref in parts[SIDE * h : SIDE * (h + 1)]
+            )
+
+
 ANY = pl.BlockSpec(memory_space=pl.ANY)
 VM = pl.BlockSpec(memory_space=pltpu.VMEM)
 
@@ -327,7 +351,7 @@
             pltpu.VMEM(bias.shape, jnp.float32),
             pltpu.VMEM((2, SIDE, span, 2 * HEAD), jnp.bfloat16),
             pltpu.VMEM((2, SIDE, span, 2 * HEAD), jnp.bfloat16),
-            pltpu.VMEM((SIDE, span, HEAD), jnp.float32),
+            pltpu.VMEM((2, SIDE, span, HEAD), jnp.float32),
             pltpu.VMEM((2, SIDE, 8, span), jnp.float32),
             pltpu.SemaphoreType.DMA((24,)),
         ],
@@ -357,7 +381,7 @@
             pltpu.VMEM(bias.shape, jnp.float32),
             pltpu.VMEM((2, SIDE, span, 2 * HEAD), jnp.bfloat16),
             pltpu.VMEM((2, SIDE, span, 2 * HEAD), jnp.bfloat16),
-            pltpu.VMEM((SIDE, span, HEAD), jnp.float32),
+            pltpu.VMEM((2, SIDE, span, HEAD), jnp.float32),
             pltpu.VMEM((2, SIDE, SIDE, 8, span), jnp.float32),
             pltpu.VMEM((2, SIDE, 8, span), jnp.float32),
             pltpu.VMEM((SIDE, HEAD, span), jnp.bfloat16),
@@ -399,6 +423,37 @@
     )(*query_grads, *inputs)
 
 
+def query_call(parts_0, parts_1):
+    rows, span = parts_0[0].shape
+    return pl.pallas_call(
+        query_kernel,
+        out_shape=[
+            jax.ShapeDtypeStruct((2 * rows, span), jnp.bfloat16),
+            jax.ShapeDtypeStruct((span, 2 * rows), jnp.float32),
+        ],
+        in_specs=[VM] * 8,
+        out_specs=[VM] * 2,
+        compiler_params=pltpu.CompilerParams(vmem_limit_bytes=16 << 20),
+        cost_estimate=pl.CostEstimate(flops=10**6, bytes_accessed=2 << 20, transcendentals=0),
+        name="query_sums",
+    )(*parts_0, *parts_1)
+
+
+def keys_call(parts_0, parts_1):
+    span, cols = parts_0[0].shape
+    block = pl.BlockSpec((span // SIDE, cols), lambda n: (n, 0))
+    return pl.pallas_call(
+        keys_kernel,
+        grid=(SIDE,),
+        out_shape=[jax.ShapeDtypeStruct((span, cols), jnp.float32)] * 2,
+        in_specs=[block] * 8,
+        out_specs=[block] * 2,
+        compiler_params=pltpu.CompilerParams(vmem_limit_bytes=16 << 20),
+        cost_estimate=pl.CostEstimate(flops=10**6, bytes_accessed=4 << 20, transcendentals=0),
+        name="key_sums",
+    )(*parts_0, *parts_1)
+
+
 def head_of(array, h):
     return array[:, h * HEAD : (h + 1) * HEAD]
 
@@ -447,21 +502,20 @@
     x_stats = fetched(stats_x, along_x)
     dq_0, dq_1, dkv_0, dkv_1 = grads_call(bias, z_parts, x_parts, z_stats, x_stats)
 
-    def summed(parts, axis_perm):
-        total = parts[0]
-        for r in range(1, SIDE):
-            total = total + lax.ppermute(parts[r], "sp", axis_perm(r)).astype(jnp.float32)
-        return total
-
-    query_t = jnp.concatenate([summed(dq_0, along_z), summed(dq_1, along_x)], axis=0)
-    low, dkv_0, dkv_1 = lax.optimization_barrier((query_t.astype(jnp.bfloat16), dkv_0, dkv_1))
+    def arrived(parts, axis_perm):
+        return [parts[0]] + [
+            lax.ppermute(parts[r], "sp", axis_perm(r)) for r in range(1, SIDE)
+        ]
+
+    dq_0, dq_1 = arrived(dq_0, along_z), arrived(dq_1, along_x)
+    low, query_grad = query_call(dq_0, dq_1)
+    low, dkv_0, dkv_1 = lax.optimization_barrier((low, dkv_0, dkv_1))
     low_parts = fetched(low, along_z)
     terms = weight_call(low_parts, inputs)
-    weight_grad = summed(terms, along_x).T
-    sum_0, sum_1 = summed(dkv_0, along_x), summed(dkv_1, along_z)
-    query_grad = query_t.T
-    key_grad = jnp.concatenate([head_of(sum_0, 0), head_of(sum_1, 0)], axis=1)
-    value_grad = jnp.concatenate([head_of(sum_0, 1), head_of(sum_1, 1)], axis=1)
+    terms = arrived(terms, along_x)
+    weight_grad = sum(part.astype(jnp.float32) for part in terms).T
+    dkv_0, dkv_1 = arrived(dkv_0, along_x), arrived(dkv_1, along_z)
+    key_grad, value_grad = keys_call(dkv_0, dkv_1)
     return (query_grad, key_grad, value_grad, weight_grad)
 
 

time: 169 us -> 165 us (0.976); the launches traced: 166 us -> 164 us
  waiting for transfers between devices: 27.5 us -> 39.3 us
  blocking collectives: 22.5 us -> 14.6 us
  other arithmetic: 5.37 us -> 0.18 us
    all_to_all x1, blocking collectives: 22.5 us -> 14.6 us  [local(): lax.all_to_all(jnp.tile(forget_logits.T, (16, 1)), 'sp', 0, 0, tiled=True)]
    ppermute x15, waiting for transfers between devices: 17.1 us -> 25 us  [fetched(): parts.append(lax.ppermute(array, 'sp', axis_perm(-r)))]
    ppermute x1, starting transfers between devices: 0.87 us -> 5.35 us  [local(): lax.ppermute(layer_input, everywhere, over_zy(lambda a, b: (a, a + b)))]
    ppermute x15, waiting for transfers between devices: 10.3 us -> 14.3 us  [arrived(): lax.ppermute(parts[r], 'sp', axis_perm(r))]
    add x4 -> x0, other arithmetic: 3.47 us -> none  [summed(): total + lax.ppermute(parts[r], 'sp', axis_perm(r)).astype(jnp.float32)]
    ppermute x3, starting transfers between devices: 6.44 us -> 3.12 us  [local(): lax.ppermute(moved, 'tp', [(p, (p - 2 * r) % 8) for p in range(8)])]
    ppermute x15, starting transfers between devices: 26.4 us -> 23.3 us  [arrived(): lax.ppermute(parts[r], 'sp', axis_perm(r))]
    pallas_call x0 -> x2, Pallas kernels: none -> 2.6 us  [the longest x1 1.6 us: keys_call(): pl.pallas_call(keys_kernel, grid=(SIDE,), out_shape=[jax.ShapeDtypeStruct...]
  transfers between devices with their start and end apart: 39 -> 39, of which waited for: 14 -> 14; matrix products, arithmetic and copies ran while one was open for 4% -> 0% of each run, Pallas kernels for 19% -> 27%
where the time goes in v3:
time: 165 us; the launch traced here: 164 us
  starting transfers between devices  58.9 us (36%)
  Pallas kernels  43.5 us (26%)
  waiting for transfers between devices  39.3 us (24%)
  blocking collectives  14.6 us (9%)
  local copies, waits for them, and re-layouts  7.04 us (4%)
    ppermute x15, waiting for transfers between devices, fetched(): parts.append(lax.ppermute(array, 'sp', axis_perm(-r)))  25 us
    ppermute x15, starting transfers between devices, fetched(): parts.append(lax.ppermute(array, 'sp', axis_perm(-r)))  24.4 us
    ppermute x15, starting transfers between devices, arrived(): lax.ppermute(parts[r], 'sp', axis_perm(r))  23.3 us
    pallas_call x1, Pallas kernels, grads_call(): pl.pallas_call(grads_kernel, out_shape=shapes(HEAD, span) + shapes(span,...  20.1 us
    pallas_call x2, Pallas kernels, stats_call(): pl.pallas_call(functools.partial(stats_kernel, slots, pair_count, pair_of...  16.8 us
    all_to_all x1, blocking collectives, local(): lax.all_to_all(jnp.tile(forget_logits.T, (16, 1)), 'sp', 0, 0, tiled=True)  14.6 us
    ppermute x15, waiting for transfers between devices, arrived(): lax.ppermute(parts[r], 'sp', axis_perm(r))  14.3 us
    ppermute x1, starting transfers between devices, local(): lax.ppermute(layer_input, everywhere, over_zy(lambda a, b: (a, a + b)))  5.35 us
  transfers between devices with their start and end apart: 39, of which 14 were waited for; matrix products, arithmetic and copies ran while one was open for 0% of the time, Pallas kernels for 27%

profile of v3, /device:TPU:0, one launch (start us, length us, event | category | flops | bytes accessed | tf_op | source)
XLA Modules:
  0.0 164.3 jit_solution(22748397729669765)
XLA Ops:
  0.7 1.2 fusion.2
  2.1 2.1 %collective-permute-start.2 = (bf16[512,512]{1,0:T(8,128)(2,1)S(1)}, bf16[512,512]{1,0:T(8,128)(2,1)S(1)}, u32[]{:S(2)}, u32[]{:S(2)}) collective-permute-start(bf16[512,512]{1,0:T(8,128)(2,1)S(1)} %pad_maximum_fusion.rest_0_), channel_id=1, source_target_pairs={{0,32},{8,40},{16,48},{24,56},{32,64},{40,72},{48,80},{56,88},{64,... | collective-permute-start | bytes 1572872 | tf_op jit(solution)/shard_map/ppermute | solution.py:31
  4.2 2.2 %collective-permute-start = (bf16[512,512]{1,0:T(8,128)(2,1)S(1)}, bf16[512,512]{1,0:T(8,128)(2,1)S(1)}, u32[]{:S(2)}, u32[]{:S(2)}) collective-permute-start(bf16[512,512]{1,0:T(8,128)(2,1)S(1)} %pad_maximum_fusion.rest_0_), channel_id=1, source_target_pairs={{0,96},{8,104},{16,112},{24,120},{32,0},{40,8},{48,16},{56,24},{64... | collective-permute-start | bytes 1572872 | tf_op jit(solution)/shard_map/ppermute | solution.py:31
  6.5 1.6 collective-permute-start.5
  8.0 1.7 %collective-permute-start.3 = (bf16[512,512]{1,0:T(8,128)(2,1)S(1)}, bf16[512,512]{1,0:T(8,128)(2,1)}, u32[]{:S(2)}, u32[]{:S(2)}) collective-permute-start(bf16[512,512]{1,0:T(8,128)(2,1)S(1)} %pad_maximum_fusion.1.rest_3_.rest_4_), channel_id=1, source_target_pairs={{0,24},{8,0},{16,8},{24,16},{32,56},{40,32},{48,40},{56,48},{64,88... | collective-permute-start | bytes 1572872 | tf_op jit(solution)/shard_map/ppermute | solution.py:31
  9.8 1.8 %collective-permute-start.1 = (bf16[512,512]{1,0:T(8,128)(2,1)S(1)}, bf16[512,512]{1,0:T(8,128)(2,1)}, u32[]{:S(2)}, u32[]{:S(2)}) collective-permute-start(bf16[512,512]{1,0:T(8,128)(2,1)S(1)} %pad_maximum_fusion.rest_0_), channel_id=1, source_target_pairs={{0,64},{8,72},{16,80},{24,88},{32,96},{40,104},{48,112},{56,120},{... | collective-permute-start | bytes 1572872 | tf_op jit(solution)/shard_map/ppermute | solution.py:31
  11.6 6.7 %collective-permute-done.2.rest_2_.rest_3_ = bf16[512,512]{1,0:T(8,128)(2,1)S(1)} collective-permute-done((bf16[512,512]{1,0:T(8,128)(2,1)S(1)}, bf16[512,512]{1,0:T(8,128)(2,1)S(1)}, u32[]{:S(2)}, u32[]{:S(2)}) %collective-permute-start.2) | collective-permute-done | bytes 524320 | tf_op jit(solution)/shard_map/ppermute | solution.py:31
  18.2 3.0 %collective-permute-start.4 = (bf16[512,512]{1,0:T(8,128)(2,1)S(1)}, bf16[512,512]{1,0:T(8,128)(2,1)}, u32[]{:S(2)}, u32[]{:S(2)}) collective-permute-start(bf16[512,512]{1,0:T(8,128)(2,1)S(1)} %pad_maximum_fusion.1.rest_3_.rest_4_), channel_id=1, source_target_pairs={{0,16},{8,24},{16,0},{24,8},{32,48},{40,56},{48,32},{56,40},{64,80... | collective-permute-start | bytes 1572872 | tf_op jit(solution)/shard_map/ppermute | solution.py:31
  21.3 7.6 %collective-permute-done.rest_1_ = bf16[512,512]{1,0:T(8,128)(2,1)S(1)} collective-permute-done((bf16[512,512]{1,0:T(8,128)(2,1)S(1)}, bf16[512,512]{1,0:T(8,128)(2,1)S(1)}, u32[]{:S(2)}, u32[]{:S(2)}) %collective-permute-start) | collective-permute-done | bytes 524320 | tf_op jit(solution)/shard_map/ppermute | solution.py:31
  29.6 5.3 %collective-permute-start.27 = (bf16[512,512]{1,0:T(8,128)(2,1)}, bf16[512,512]{1,0:T(8,128)(2,1)}, u32[]{:S(2)}, u32[]{:S(2)}) collective-permute-start(bf16[512,512]{1,0:T(8,128)(2,1)} %param.10), channel_id=1, source_target_pairs={{0,0},{1,1},{2,2},{3,3},{4,4},{5,5},{6,6},{7,7},{8,8},{9,9},{10,10... | collective-permute-start | bytes 1572872 | tf_op jit(solution)/shard_map/ppermute | solution.py:491
  35.0 14.6 %all_to_all.8 = f32[16,2,512]{2,1,0:T(2,128)S(1)} all-to-all(f32[16,2,512]{2,1,0:T(2,128)S(1)} %tile.2), channel_id=1, replica_groups=mesh['sp'=16,'tp'=8] {'sp'}, dimensions={0} | all-to-all | bytes 131072 | tf_op jit(solution)/shard_map/all_to_all | solution.py:462
  50.2 2.2 %gate_sums.1.bias_ref = f32[32,512]{1,0:T(8,128)} custom-call(f32[32,512]{1,0:T(8,128)} %all_to_all.6.logits_ref), custom_call_target="tpu_custom_call" | custom-call | flops 1000000 | bytes 131072 | tf_op jit(solution)/shard_map/gate_sums/pallas_call | solution.py:473
  53.3 9.3 %stats.2 = (f32[4,8,512]{2,1,0:T(8,128)}, f32[4,8,512]{2,1,0:T(8,128)}) custom-call(f32[32,512]{1,0:T(8,128)} %gate_sums.1.bias_ref, bf16[512,512]{1,0:T(8,128)(2,1)} %copy-done.4, bf16[512,512]{1,0:T(8,128)(2,1)} %copy-done.7, bf16[512,512]{1,0:T(8,128)(2,1)} %copy-done.6, bf16[512,512]{1,0:T(8,128)(2,1)} %copy-done.5, ...), custom_call_target="tpu_custom_call" | custom-call | flops 1207959552 | bytes 4194304 | tf_op jit(solution)/shard_map/stats/pallas_call | solution.py:345
  62.7 7.5 %stats.3 = (f32[4,8,512]{2,1,0:T(8,128)}, f32[4,8,512]{2,1,0:T(8,128)}) custom-call(f32[32,512]{1,0:T(8,128)} %gate_sums.1.bias_ref, bf16[512,512]{1,0:T(8,128)(2,1)} %copy-done.4, bf16[512,512]{1,0:T(8,128)(2,1)} %copy-done.7, bf16[512,512]{1,0:T(8,128)(2,1)} %collective-permute-done.1.rest_2_, bf16[512,512]{1,0:T(8,128)(2,1)} %copy-done.6, ...), custom_call_target="tpu_custom_call" | custom-call | flops 939524096 | bytes 4194304 | tf_op jit(solution)/shard_map/stats/pallas_call | solution.py:345
  70.7 2.1 %collective-permute-start.7 = (f32[4,8,512]{2,1,0:T(8,128)}, f32[4,8,512]{2,1,0:T(8,128)S(1)}, u32[]{:S(2)}, u32[]{:S(2)}) collective-permute-start(f32[4,8,512]{2,1,0:T(8,128)} %get-tuple-element.43.rest_8_), channel_id=1, source_target_pairs={{0,64},{8,72},{16,80},{24,88},{32,96},{40,104},{48,112},{56,120},{... | collective-permute-start | bytes 196616 | tf_op jit(solution)/shard_map/ppermute | solution.py:31
  72.8 1.2 collective-permute-start.6
  74.6 2.1 %collective-permute-start.10 = (f32[4,8,512]{2,1,0:T(8,128)}, f32[4,8,512]{2,1,0:T(8,128)S(1)}, u32[]{:S(2)}, u32[]{:S(2)}) collective-permute-start(f32[4,8,512]{2,1,0:T(8,128)} %get-tuple-element.44.rest_12_), channel_id=1, source_target_pairs={{0,16},{8,24},{16,0},{24,8},{32,48},{40,56},{48,32},{56,40},{64,80... | collective-permute-start | bytes 196616 | tf_op jit(solution)/shard_map/ppermute | solution.py:31
  76.7 1.3 collective-permute-start.9
  78.0 1.7 %collective-permute-start.28 = (bf16[512,512]{1,0:T(8,128)(2,1)}, bf16[512,512]{1,0:T(8,128)(2,1)S(1)}, u32[]{:S(2)}, u32[]{:S(2)}) collective-permute-start(bf16[512,512]{1,0:T(8,128)(2,1)} %collective-permute-done.27), channel_id=1, source_target_pairs={{0,0},{1,1},{2,34},{3,35},{4,68},{5,69},{6,102},{7,103},{8,8},{9,9... | collective-permute-start | bytes 1572872 | tf_op jit(solution)/shard_map/ppermute | solution.py:492
  81.9 20.1 %grads.1 = (f32[128,512]{1,0:T(8,128)}, bf16[128,512]{1,0:T(8,128)(2,1)}, bf16[128,512]{1,0:T(8,128)(2,1)}, bf16[128,512]{1,0:T(8,128)(2,1)}, f32[128,512]{1,0:T...) custom-call(f32[32,512]{1,0:T(8,128)} %gate_sums.1.bias_ref, ...), custom_call_target="tpu_custom_call" | custom-call | flops 5704253440 | bytes 8388608 | tf_op jit(solution)/shard_map/grads/pallas_call | solution.py:375
  102.0 1.9 %collective-permute-start.12 = (bf16[128,512]{1,0:T(8,128)(2,1)}, bf16[128,512]{1,0:T(8,128)(2,1)S(1)}, u32[]{:S(2)}, u32[]{:S(2)}) collective-permute-start(bf16[128,512]{1,0:T(8,128)(2,1)} %get-tuple-element.46), channel_id=1, source_target_pairs={{0,32},{8,40},{16,48},{24,56},{32,64},{40,72},{48,80},{56,88},{64,... | collective-permute-start | bytes 393224 | tf_op jit(solution)/shard_map/ppermute | solution.py:507
  103.9 2.7 %collective-permute-start.13 = (bf16[128,512]{1,0:T(8,128)(2,1)}, bf16[128,512]{1,0:T(8,128)(2,1)S(1)}, u32[]{:S(2)}, u32[]{:S(2)}) collective-permute-start(bf16[128,512]{1,0:T(8,128)(2,1)} %get-tuple-element.47), channel_id=1, source_target_pairs={{0,64},{8,72},{16,80},{24,88},{32,96},{40,104},{48,112},{56,120},{... | collective-permute-start | bytes 393224 | tf_op jit(solution)/shard_map/ppermute | solution.py:507
  107.1 1.3 collective-permute-start.15
  109.4 2.4 %collective-permute-start.16 = (bf16[128,512]{1,0:T(8,128)(2,1)}, bf16[128,512]{1,0:T(8,128)(2,1)S(1)}, u32[]{:S(2)}, u32[]{:S(2)}) collective-permute-start(bf16[128,512]{1,0:T(8,128)(2,1)} %get-tuple-element.51), channel_id=1, source_target_pairs={{0,16},{8,24},{16,0},{24,8},{32,48},{40,56},{48,32},{56,40},{64,80... | collective-permute-start | bytes 393224 | tf_op jit(solution)/shard_map/ppermute | solution.py:507
  112.3 2.3 %collective-permute-start.17 = (bf16[128,512]{1,0:T(8,128)(2,1)}, bf16[128,512]{1,0:T(8,128)(2,1)S(1)}, u32[]{:S(2)}, u32[]{:S(2)}) collective-permute-start(bf16[128,512]{1,0:T(8,128)(2,1)} %get-tuple-element.52), channel_id=1, source_target_pairs={{0,24},{8,0},{16,8},{24,16},{32,56},{40,32},{48,40},{56,48},{64,88... | collective-permute-start | bytes 393224 | tf_op jit(solution)/shard_map/ppermute | solution.py:507
  114.6 0.9 collective-permute-start.30
  115.5 1.6 %collective-permute-start.29 = (bf16[512,512]{1,0:T(8,128)(2,1)S(1)}, bf16[512,512]{1,0:T(8,128)(2,1)S(1)}, u32[]{:S(2)}, u32[]{:S(2)}) collective-permute-start(bf16[512,512]{1,0:T(8,128)(2,1)S(1)} %collective-permute-done.28.rest_4_), channel_id=1, source_target_pairs={{0,6},{1,7},{2,0},{3,1},{4,2},{5,3},{6,4},{7,5},{8,14},{9,15},{10,... | collective-permute-start | bytes 1572872 | tf_op jit(solution)/shard_map/ppermute | solution.py:495
  117.5 0.9 copy-done.2
  118.4 0.9 copy-done.3
  119.4 1.0 query_sums.1
  120.4 1.8 %collective-permute-start.18 = (bf16[512,256]{1,0:T(8,128)(2,1)}, bf16[512,256]{1,0:T(8,128)(2,1)S(1)}, u32[]{:S(2)}, u32[]{:S(2)}) collective-permute-start(bf16[512,256]{1,0:T(8,128)(2,1)} %get-tuple-element.64), channel_id=1, source_target_pairs={{0,8},{8,16},{16,24},{24,0},{32,40},{40,48},{48,56},{56,32},{64,72... | collective-permute-start | bytes 786440 | tf_op jit(solution)/shard_map/ppermute | solution.py:507
  122.2 6.2 %collective-permute-done.18.refs_1_ = bf16[512,256]{1,0:T(8,128)(2,1)S(1)} collective-permute-done((bf16[512,256]{1,0:T(8,128)(2,1)}, bf16[512,256]{1,0:T(8,128)(2,1)S(1)}, u32[]{:S(2)}, u32[]{:S(2)}) %collective-permute-start.18) | collective-permute-done | bytes 262176 | tf_op jit(solution)/shard_map/ppermute | solution.py:507
  128.5 1.8 %collective-permute-start.25 = (bf16[256,512]{1,0:T(8,128)(2,1)S(1)}, bf16[256,512]{1,0:T(8,128)(2,1)S(1)}, u32[]{:S(2)}, u32[]{:S(2)}) collective-permute-start(bf16[256,512]{1,0:T(8,128)(2,1)S(1)} %get-tuple-element.73.rest_0_), channel_id=1, source_target_pairs={{0,64},{8,72},{16,80},{24,88},{32,96},{40,104},{48,112},{56,120},{... | collective-permute-start | bytes 786440 | tf_op jit(solution)/shard_map/ppermute | solution.py:31
  131.3 5.0 %collective-permute-done.25.rest_2_ = bf16[256,512]{1,0:T(8,128)(2,1)S(1)} collective-permute-done((bf16[256,512]{1,0:T(8,128)(2,1)S(1)}, bf16[256,512]{1,0:T(8,128)(2,1)S(1)}, u32[]{:S(2)}, u32[]{:S(2)}) %collective-permute-start.25) | collective-permute-done | bytes 262176 | tf_op jit(solution)/shard_map/ppermute | solution.py:31
  136.3 2.2 %collective-permute-start.24 = (bf16[256,512]{1,0:T(8,128)(2,1)S(1)}, bf16[256,512]{1,0:T(8,128)(2,1)S(1)}, u32[]{:S(2)}, u32[]{:S(2)}) collective-permute-start(bf16[256,512]{1,0:T(8,128)(2,1)S(1)} %get-tuple-element.73.rest_0_), channel_id=1, source_target_pairs={{0,96},{8,104},{16,112},{24,120},{32,0},{40,8},{48,16},{56,24},{64... | collective-permute-start | bytes 786440 | tf_op jit(solution)/shard_map/ppermute | solution.py:31
  138.6 4.2 %collective-permute-done.24.rest_1_ = bf16[256,512]{1,0:T(8,128)(2,1)S(1)} collective-permute-done((bf16[256,512]{1,0:T(8,128)(2,1)S(1)}, bf16[256,512]{1,0:T(8,128)(2,1)S(1)}, u32[]{:S(2)}, u32[]{:S(2)}) %collective-permute-start.24) | collective-permute-done | bytes 262176 | tf_op jit(solution)/shard_map/ppermute | solution.py:31
  142.7 1.9 %collective-permute-start.19 = (bf16[512,256]{1,0:T(8,128)(2,1)S(1)}, bf16[512,256]{1,0:T(8,128)(2,1)S(1)}, u32[]{:S(2)}, u32[]{:S(2)}) collective-permute-start(bf16[512,256]{1,0:T(8,128)(2,1)S(1)} %copy-done.16), channel_id=1, source_target_pairs={{0,16},{8,24},{16,0},{24,8},{32,48},{40,56},{48,32},{56,40},{64,80... | collective-permute-start | bytes 786440 | tf_op jit(solution)/shard_map/ppermute | solution.py:507
  144.6 1.1 collective-permute-start.20
  145.8 0.9 collective-permute-start.21
  146.6 2.5 %collective-permute-start.22 = (bf16[512,256]{1,0:T(8,128)(2,1)S(1)}, bf16[512,256]{1,0:T(8,128)(2,1)S(1)}, u32[]{:S(2)}, u32[]{:S(2)}) collective-permute-start(bf16[512,256]{1,0:T(8,128)(2,1)S(1)} %copy-done.13), channel_id=1, source_target_pairs={{0,64},{8,72},{16,80},{24,88},{32,96},{40,104},{48,112},{56,120},{... | collective-permute-start | bytes 786440 | tf_op jit(solution)/shard_map/ppermute | solution.py:507
  149.5 1.8 %weight.1 = (f32[256,256]{1,0:T(8,128)S(1)}, bf16[256,256]{1,0:T(8,128)(2,1)S(1)}, bf16[256,256]{1,0:T(8,128)(2,1)S(1)}, bf16[256,256]{1,0:T(8,128)(2,1)S(1)}) custom-call(bf16[256,512]{1,0:T(8,128)(2,1)S(1)} %get-tuple-element.73.rest_0_, bf16[256,512]{1,0:T(8,128)(2,1)S(1)} %collective-permute-done.24.rest_1_, ...), custom_call_target="tpu_custom_call" | custom-call | flops 1073741824 | bytes 6291456 | tf_op jit(solution)/shard_map/weight/pallas_call | solution.py:408
  151.3 1.3 collective-permute-done.19.refs_2_
  152.6 3.0 %collective-permute-done.20.refs_3_ = bf16[512,256]{1,0:T(8,128)(2,1)S(1)} collective-permute-done((bf16[512,256]{1,0:T(8,128)(2,1)S(1)}, bf16[512,256]{1,0:T(8,128)(2,1)S(1)}, u32[]{:S(2)}, u32[]{:S(2)}) %collective-permute-start.20) | collective-permute-done | bytes 262176 | tf_op jit(solution)/shard_map/ppermute | solution.py:507
  155.6 1.3 collective-permute-start.37
  156.9 2.4 %collective-permute-start.38 = (bf16[256,256]{1,0:T(8,128)(2,1)S(1)}, bf16[256,256]{1,0:T(8,128)(2,1)S(1)}, u32[]{:S(2)}, u32[]{:S(2)}) collective-permute-start(bf16[256,256]{1,0:T(8,128)(2,1)S(1)} %get-tuple-element.77), channel_id=1, source_target_pairs={{0,24},{8,0},{16,8},{24,16},{32,56},{40,32},{48,40},{56,48},{64,88... | collective-permute-start | bytes 393224 | tf_op jit(solution)/shard_map/ppermute | solution.py:507
  159.3 1.6 key_sums.1
  160.9 1.2 collective-permute-done.37
  162.1 1.4 collective-permute-done.38
  (92 shorter events, 10.6 us)
Async XLA Ops:
  2.1 16.1 %collective-permute-start.2 = (bf16[512,512]{1,0:T(8,128)(2,1)S(1)}, bf16[512,512]{1,0:T(8,128)(2,1)S(1)}, u32[]{:S(2)}, u32[]{:S(2)}) collective-permute-start(bf16[512,512]{1,0:T(8,128)(2,1)S(1)} %pad_maximum_fusion.rest_0_), channel_id=1, source_target_pairs={{0,32},{8,40},{16,48},{24,56},{32,64},{40,72},{48,80},{56,88},{64,... | collective-permute-start | bytes 1572872 | tf_op jit(solution)/shard_map/ppermute | solution.py:31
  4.2 24.7 %collective-permute-start = (bf16[512,512]{1,0:T(8,128)(2,1)S(1)}, bf16[512,512]{1,0:T(8,128)(2,1)S(1)}, u32[]{:S(2)}, u32[]{:S(2)}) collective-permute-start(bf16[512,512]{1,0:T(8,128)(2,1)S(1)} %pad_maximum_fusion.rest_0_), channel_id=1, source_target_pairs={{0,96},{8,104},{16,112},{24,120},{32,0},{40,8},{48,16},{56,24},{64... | collective-permute-start | bytes 1572872 | tf_op jit(solution)/shard_map/ppermute | solution.py:31
  6.4 28.6 %copy-start.11 = (f32[512,2]{0,1:T(2,128)S(1)}, f32[512,2]{0,1:T(2,128)}, u32[]{:S(2)}) copy-start(f32[512,2]{0,1:T(2,128)} %param.9) | copy-start | bytes 12292
  6.5 46.8 %copy-start.5 = (bf16[512,512]{1,0:T(8,128)(2,1)}, bf16[512,512]{1,0:T(8,128)(2,1)S(1)}, u32[]{:S(2)}) copy-start(bf16[512,512]{1,0:T(8,128)(2,1)S(1)} %pad_maximum_fusion.1.rest_3_.rest_4_) | copy-start | bytes 1572868
  6.5 46.0 %collective-permute-start.5 = (bf16[512,512]{1,0:T(8,128)(2,1)S(1)}, bf16[512,512]{1,0:T(8,128)(2,1)S(1)}, u32[]{:S(2)}, u32[]{:S(2)}) collective-permute-start(bf16[512,512]{1,0:T(8,128)(2,1)S(1)} %pad_maximum_fusion.1.rest_3_.rest_4_), channel_id=1, source_target_pairs={{0,8},{8,16},{16,24},{24,0},{32,40},{40,48},{48,56},{56,32},{64,72... | collective-permute-start | bytes 1572872 | tf_op jit(solution)/shard_map/ppermute | solution.py:31
  8.0 45.3 %collective-permute-start.3 = (bf16[512,512]{1,0:T(8,128)(2,1)S(1)}, bf16[512,512]{1,0:T(8,128)(2,1)}, u32[]{:S(2)}, u32[]{:S(2)}) collective-permute-start(bf16[512,512]{1,0:T(8,128)(2,1)S(1)} %pad_maximum_fusion.1.rest_3_.rest_4_), channel_id=1, source_target_pairs={{0,24},{8,0},{16,8},{24,16},{32,56},{40,32},{48,40},{56,48},{64,88... | collective-permute-start | bytes 1572872 | tf_op jit(solution)/shard_map/ppermute | solution.py:31
  9.8 52.9 %collective-permute-start.1 = (bf16[512,512]{1,0:T(8,128)(2,1)S(1)}, bf16[512,512]{1,0:T(8,128)(2,1)}, u32[]{:S(2)}, u32[]{:S(2)}) collective-permute-start(bf16[512,512]{1,0:T(8,128)(2,1)S(1)} %pad_maximum_fusion.rest_0_), channel_id=1, source_target_pairs={{0,64},{8,72},{16,80},{24,88},{32,96},{40,104},{48,112},{56,120},{... | collective-permute-start | bytes 1572872 | tf_op jit(solution)/shard_map/ppermute | solution.py:31
  18.2 35.1 %copy-start.6 = (bf16[512,512]{1,0:T(8,128)(2,1)}, bf16[512,512]{1,0:T(8,128)(2,1)S(1)}, u32[]{:S(2)}) copy-start(bf16[512,512]{1,0:T(8,128)(2,1)S(1)} %collective-permute-done.2.rest_2_.rest_3_) | copy-start | bytes 1572868
  18.2 44.4 %collective-permute-start.4 = (bf16[512,512]{1,0:T(8,128)(2,1)S(1)}, bf16[512,512]{1,0:T(8,128)(2,1)}, u32[]{:S(2)}, u32[]{:S(2)}) collective-permute-start(bf16[512,512]{1,0:T(8,128)(2,1)S(1)} %pad_maximum_fusion.1.rest_3_.rest_4_), channel_id=1, source_target_pairs={{0,16},{8,24},{16,0},{24,8},{32,48},{40,56},{48,32},{56,40},{64,80... | collective-permute-start | bytes 1572872 | tf_op jit(solution)/shard_map/ppermute | solution.py:31
  29.6 44.9 %collective-permute-start.27 = (bf16[512,512]{1,0:T(8,128)(2,1)}, bf16[512,512]{1,0:T(8,128)(2,1)}, u32[]{:S(2)}, u32[]{:S(2)}) collective-permute-start(bf16[512,512]{1,0:T(8,128)(2,1)} %param.10), channel_id=1, source_target_pairs={{0,0},{1,1},{2,2},{3,3},{4,4},{5,5},{6,6},{7,7},{8,8},{9,9},{10,10... | collective-permute-start | bytes 1572872 | tf_op jit(solution)/shard_map/ppermute | solution.py:491
  70.1 6.6 %collective-permute-start.8 = (f32[4,8,512]{2,1,0:T(8,128)}, f32[4,8,512]{2,1,0:T(8,128)S(1)}, u32[]{:S(2)}, u32[]{:S(2)}) collective-permute-start(f32[4,8,512]{2,1,0:T(8,128)} %get-tuple-element.43.rest_8_), channel_id=1, source_target_pairs={{0,32},{8,40},{16,48},{24,56},{32,64},{40,72},{48,80},{56,88},{64,... | collective-permute-start | bytes 196616 | tf_op jit(solution)/shard_map/ppermute | solution.py:31
  70.7 7.3 %collective-permute-start.7 = (f32[4,8,512]{2,1,0:T(8,128)}, f32[4,8,512]{2,1,0:T(8,128)S(1)}, u32[]{:S(2)}, u32[]{:S(2)}) collective-permute-start(f32[4,8,512]{2,1,0:T(8,128)} %get-tuple-element.43.rest_8_), channel_id=1, source_target_pairs={{0,64},{8,72},{16,80},{24,88},{32,96},{40,104},{48,112},{56,120},{... | collective-permute-start | bytes 196616 | tf_op jit(solution)/shard_map/ppermute | solution.py:31
  72.8 6.9 %collective-permute-start.6 = (f32[4,8,512]{2,1,0:T(8,128)}, f32[4,8,512]{2,1,0:T(8,128)S(1)}, u32[]{:S(2)}, u32[]{:S(2)}) collective-permute-start(f32[4,8,512]{2,1,0:T(8,128)} %get-tuple-element.43.rest_8_), channel_id=1, source_target_pairs={{0,96},{8,104},{16,112},{24,120},{32,0},{40,8},{48,16},{56,24},{64... | collective-permute-start | bytes 196616 | tf_op jit(solution)/shard_map/ppermute | solution.py:31
  74.0 5.7 %collective-permute-start.11 = (f32[4,8,512]{2,1,0:T(8,128)}, f32[4,8,512]{2,1,0:T(8,128)S(1)}, u32[]{:S(2)}, u32[]{:S(2)}) collective-permute-start(f32[4,8,512]{2,1,0:T(8,128)} %get-tuple-element.44.rest_12_), channel_id=1, source_target_pairs={{0,8},{8,16},{16,24},{24,0},{32,40},{40,48},{48,56},{56,32},{64,72... | collective-permute-start | bytes 196616 | tf_op jit(solution)/shard_map/ppermute | solution.py:31
  74.6 6.0 %collective-permute-start.10 = (f32[4,8,512]{2,1,0:T(8,128)}, f32[4,8,512]{2,1,0:T(8,128)S(1)}, u32[]{:S(2)}, u32[]{:S(2)}) collective-permute-start(f32[4,8,512]{2,1,0:T(8,128)} %get-tuple-element.44.rest_12_), channel_id=1, source_target_pairs={{0,16},{8,24},{16,0},{24,8},{32,48},{40,56},{48,32},{56,40},{64,80... | collective-permute-start | bytes 196616 | tf_op jit(solution)/shard_map/ppermute | solution.py:31
  76.7 4.5 %collective-permute-start.9 = (f32[4,8,512]{2,1,0:T(8,128)}, f32[4,8,512]{2,1,0:T(8,128)S(1)}, u32[]{:S(2)}, u32[]{:S(2)}) collective-permute-start(f32[4,8,512]{2,1,0:T(8,128)} %get-tuple-element.44.rest_12_), channel_id=1, source_target_pairs={{0,24},{8,0},{16,8},{24,16},{32,56},{40,32},{48,40},{56,48},{64,88... | collective-permute-start | bytes 196616 | tf_op jit(solution)/shard_map/ppermute | solution.py:31
  78.0 30.4 %collective-permute-start.28 = (bf16[512,512]{1,0:T(8,128)(2,1)}, bf16[512,512]{1,0:T(8,128)(2,1)S(1)}, u32[]{:S(2)}, u32[]{:S(2)}) collective-permute-start(bf16[512,512]{1,0:T(8,128)(2,1)} %collective-permute-done.27), channel_id=1, source_target_pairs={{0,0},{1,1},{2,34},{3,35},{4,68},{5,69},{6,102},{7,103},{8,8},{9,9... | collective-permute-start | bytes 1572872 | tf_op jit(solution)/shard_map/ppermute | solution.py:492
  102.0 7.3 %collective-permute-start.12 = (bf16[128,512]{1,0:T(8,128)(2,1)}, bf16[128,512]{1,0:T(8,128)(2,1)S(1)}, u32[]{:S(2)}, u32[]{:S(2)}) collective-permute-start(bf16[128,512]{1,0:T(8,128)(2,1)} %get-tuple-element.46), channel_id=1, source_target_pairs={{0,32},{8,40},{16,48},{24,56},{32,64},{40,72},{48,80},{56,88},{64,... | collective-permute-start | bytes 393224 | tf_op jit(solution)/shard_map/ppermute | solution.py:507
  103.9 8.4 %collective-permute-start.13 = (bf16[128,512]{1,0:T(8,128)(2,1)}, bf16[128,512]{1,0:T(8,128)(2,1)S(1)}, u32[]{:S(2)}, u32[]{:S(2)}) collective-permute-start(bf16[128,512]{1,0:T(8,128)(2,1)} %get-tuple-element.47), channel_id=1, source_target_pairs={{0,64},{8,72},{16,80},{24,88},{32,96},{40,104},{48,112},{56,120},{... | collective-permute-start | bytes 393224 | tf_op jit(solution)/shard_map/ppermute | solution.py:507
  106.6 8.0 %collective-permute-start.14 = (bf16[128,512]{1,0:T(8,128)(2,1)}, bf16[128,512]{1,0:T(8,128)(2,1)S(1)}, u32[]{:S(2)}, u32[]{:S(2)}) collective-permute-start(bf16[128,512]{1,0:T(8,128)(2,1)} %get-tuple-element.48), channel_id=1, source_target_pairs={{0,96},{8,104},{16,112},{24,120},{32,0},{40,8},{48,16},{56,24},{64... | collective-permute-start | bytes 393224 | tf_op jit(solution)/shard_map/ppermute | solution.py:507
  107.1 8.4 %collective-permute-start.15 = (bf16[128,512]{1,0:T(8,128)(2,1)}, bf16[128,512]{1,0:T(8,128)(2,1)S(1)}, u32[]{:S(2)}, u32[]{:S(2)}) collective-permute-start(bf16[128,512]{1,0:T(8,128)(2,1)} %get-tuple-element.50), channel_id=1, source_target_pairs={{0,8},{8,16},{16,24},{24,0},{32,40},{40,48},{48,56},{56,32},{64,72... | collective-permute-start | bytes 393224 | tf_op jit(solution)/shard_map/ppermute | solution.py:507
  108.4 21.9 %collective-permute-start.31 = (bf16[512,512]{1,0:T(8,128)(2,1)S(1)}, bf16[512,512]{1,0:T(8,128)(2,1)S(1)}, u32[]{:S(2)}, u32[]{:S(2)}) collective-permute-start(bf16[512,512]{1,0:T(8,128)(2,1)S(1)} %collective-permute-done.28.rest_4_), channel_id=1, source_target_pairs={{0,2},{1,3},{2,4},{3,5},{4,6},{5,7},{6,0},{7,1},{8,10},{9,11},{10,... | collective-permute-start | bytes 1572872 | tf_op jit(solution)/shard_map/ppermute | solution.py:495
  109.4 7.8 %collective-permute-start.16 = (bf16[128,512]{1,0:T(8,128)(2,1)}, bf16[128,512]{1,0:T(8,128)(2,1)S(1)}, u32[]{:S(2)}, u32[]{:S(2)}) collective-permute-start(bf16[128,512]{1,0:T(8,128)(2,1)} %get-tuple-element.51), channel_id=1, source_target_pairs={{0,16},{8,24},{16,0},{24,8},{32,48},{40,56},{48,32},{56,40},{64,80... | collective-permute-start | bytes 393224 | tf_op jit(solution)/shard_map/ppermute | solution.py:507
  112.3 5.2 %collective-permute-start.17 = (bf16[128,512]{1,0:T(8,128)(2,1)}, bf16[128,512]{1,0:T(8,128)(2,1)S(1)}, u32[]{:S(2)}, u32[]{:S(2)}) collective-permute-start(bf16[128,512]{1,0:T(8,128)(2,1)} %get-tuple-element.52), channel_id=1, source_target_pairs={{0,24},{8,0},{16,8},{24,16},{32,56},{40,32},{48,40},{56,48},{64,88... | collective-permute-start | bytes 393224 | tf_op jit(solution)/shard_map/ppermute | solution.py:507
  114.6 16.2 %collective-permute-start.30 = (bf16[512,512]{1,0:T(8,128)(2,1)S(1)}, bf16[512,512]{1,0:T(8,128)(2,1)S(1)}, u32[]{:S(2)}, u32[]{:S(2)}) collective-permute-start(bf16[512,512]{1,0:T(8,128)(2,1)S(1)} %collective-permute-done.28.rest_4_), channel_id=1, source_target_pairs={{0,4},{1,5},{2,6},{3,7},{4,0},{5,1},{6,2},{7,3},{8,12},{9,13},{10,... | collective-permute-start | bytes 1572872 | tf_op jit(solution)/shard_map/ppermute | solution.py:495
  115.5 15.4 %collective-permute-start.29 = (bf16[512,512]{1,0:T(8,128)(2,1)S(1)}, bf16[512,512]{1,0:T(8,128)(2,1)S(1)}, u32[]{:S(2)}, u32[]{:S(2)}) collective-permute-start(bf16[512,512]{1,0:T(8,128)(2,1)S(1)} %collective-permute-done.28.rest_4_), channel_id=1, source_target_pairs={{0,6},{1,7},{2,0},{3,1},{4,2},{5,3},{6,4},{7,5},{8,14},{9,15},{10,... | collective-permute-start | bytes 1572872 | tf_op jit(solution)/shard_map/ppermute | solution.py:495
  119.4 25.2 %copy-start.15 = (bf16[512,256]{1,0:T(8,128)(2,1)S(1)}, bf16[512,256]{1,0:T(8,128)(2,1)}, u32[]{:S(2)}) copy-start(bf16[512,256]{1,0:T(8,128)(2,1)} %get-tuple-element.66) | copy-start | bytes 786436
  119.4 26.4 %copy-start.14 = (bf16[512,256]{1,0:T(8,128)(2,1)S(1)}, bf16[512,256]{1,0:T(8,128)(2,1)}, u32[]{:S(2)}) copy-start(bf16[512,256]{1,0:T(8,128)(2,1)} %get-tuple-element.68) | copy-start | bytes 786436
  119.4 27.2 %copy-start.13 = (bf16[512,256]{1,0:T(8,128)(2,1)S(1)}, bf16[512,256]{1,0:T(8,128)(2,1)}, u32[]{:S(2)}) copy-start(bf16[512,256]{1,0:T(8,128)(2,1)} %get-tuple-element.69) | copy-start | bytes 786436
  119.4 29.8 %copy-start.12 = (bf16[512,256]{1,0:T(8,128)(2,1)S(1)}, bf16[512,256]{1,0:T(8,128)(2,1)}, u32[]{:S(2)}) copy-start(bf16[512,256]{1,0:T(8,128)(2,1)} %get-tuple-element.70) | copy-start | bytes 786436
  120.4 38.9 %copy-start = (f32[512,256]{1,0:T(8,128)S(1)}, f32[512,256]{1,0:T(8,128)}, u32[]{:S(2)}) copy-start(f32[512,256]{1,0:T(8,128)} %get-tuple-element.63.refs_0_) | copy-start | bytes 1572868
  120.4 38.9 %copy-start.1 = (f32[512,256]{1,0:T(8,128)S(1)}, f32[512,256]{1,0:T(8,128)}, u32[]{:S(2)}) copy-start(f32[512,256]{1,0:T(8,128)} %get-tuple-element.67.refs_4_) | copy-start | bytes 1572868
  120.4 8.0 %collective-permute-start.18 = (bf16[512,256]{1,0:T(8,128)(2,1)}, bf16[512,256]{1,0:T(8,128)(2,1)S(1)}, u32[]{:S(2)}, u32[]{:S(2)}) collective-permute-start(bf16[512,256]{1,0:T(8,128)(2,1)} %get-tuple-element.64), channel_id=1, source_target_pairs={{0,8},{8,16},{16,24},{24,0},{32,40},{40,48},{48,56},{56,32},{64,72... | collective-permute-start | bytes 786440 | tf_op jit(solution)/shard_map/ppermute | solution.py:507
  122.2 8.1 %collective-permute-start.26 = (bf16[256,512]{1,0:T(8,128)(2,1)S(1)}, bf16[256,512]{1,0:T(8,128)(2,1)S(1)}, u32[]{:S(2)}, u32[]{:S(2)}) collective-permute-start(bf16[256,512]{1,0:T(8,128)(2,1)S(1)} %get-tuple-element.73.rest_0_), channel_id=1, source_target_pairs={{0,32},{8,40},{16,48},{24,56},{32,64},{40,72},{48,80},{56,88},{64,... | collective-permute-start | bytes 786440 | tf_op jit(solution)/shard_map/ppermute | solution.py:31
  128.5 7.9 %collective-permute-start.25 = (bf16[256,512]{1,0:T(8,128)(2,1)S(1)}, bf16[256,512]{1,0:T(8,128)(2,1)S(1)}, u32[]{:S(2)}, u32[]{:S(2)}) collective-permute-start(bf16[256,512]{1,0:T(8,128)(2,1)S(1)} %get-tuple-element.73.rest_0_), channel_id=1, source_target_pairs={{0,64},{8,72},{16,80},{24,88},{32,96},{40,104},{48,112},{56,120},{... | collective-permute-start | bytes 786440 | tf_op jit(solution)/shard_map/ppermute | solution.py:31
  130.3 14.3 %collective-permute-start.32 = (bf16[512,512]{1,0:T(8,128)(2,1)S(1)}, bf16[512,512]{1,0:T(8,128)(2,1)S(1)}, u32[]{:S(2)}, u32[]{:S(2)}) collective-permute-start(bf16[512,512]{1,0:T(8,128)(2,1)S(1)} %collective-permute-done.28.rest_4_), channel_id=1, source_target_pairs={{0,1},{1,0},{2,3},{3,2},{4,5},{5,4},{6,7},{7,6},{8,9},{9,8},{10,11... | collective-permute-start | bytes 1572872 | tf_op jit(solution)/shard_map/ppermute | solution.py:497
  130.3 15.5 %collective-permute-start.35 = (bf16[512,512]{1,0:T(8,128)(2,1)S(1)}, bf16[512,512]{1,0:T(8,128)(2,1)S(1)}, u32[]{:S(2)}, u32[]{:S(2)}) collective-permute-start(bf16[512,512]{1,0:T(8,128)(2,1)S(1)} %collective-permute-done.31.rest_7_), channel_id=1, source_target_pairs={{0,1},{1,0},{2,3},{3,2},{4,5},{5,4},{6,7},{7,6},{8,9},{9,8},{10,11... | collective-permute-start | bytes 1572872 | tf_op jit(solution)/shard_map/ppermute | solution.py:497
  130.8 15.8 %collective-permute-start.34 = (bf16[512,512]{1,0:T(8,128)(2,1)S(1)}, bf16[512,512]{1,0:T(8,128)(2,1)S(1)}, u32[]{:S(2)}, u32[]{:S(2)}) collective-permute-start(bf16[512,512]{1,0:T(8,128)(2,1)S(1)} %collective-permute-done.30.rest_6_), channel_id=1, source_target_pairs={{0,1},{1,0},{2,3},{3,2},{4,5},{5,4},{6,7},{7,6},{8,9},{9,8},{10,11... | collective-permute-start | bytes 1572872 | tf_op jit(solution)/shard_map/ppermute | solution.py:497
  130.9 18.3 %collective-permute-start.33 = (bf16[512,512]{1,0:T(8,128)(2,1)S(1)}, bf16[512,512]{1,0:T(8,128)(2,1)S(1)}, u32[]{:S(2)}, u32[]{:S(2)}) collective-permute-start(bf16[512,512]{1,0:T(8,128)(2,1)S(1)} %collective-permute-done.29.rest_5_), channel_id=1, source_target_pairs={{0,1},{1,0},{2,3},{3,2},{4,5},{5,4},{6,7},{7,6},{8,9},{9,8},{10,11... | collective-permute-start | bytes 1572872 | tf_op jit(solution)/shard_map/ppermute | solution.py:497
  136.3 6.4 %collective-permute-start.24 = (bf16[256,512]{1,0:T(8,128)(2,1)S(1)}, bf16[256,512]{1,0:T(8,128)(2,1)S(1)}, u32[]{:S(2)}, u32[]{:S(2)}) collective-permute-start(bf16[256,512]{1,0:T(8,128)(2,1)S(1)} %get-tuple-element.73.rest_0_), channel_id=1, source_target_pairs={{0,96},{8,104},{16,112},{24,120},{32,0},{40,8},{48,16},{56,24},{64... | collective-permute-start | bytes 786440 | tf_op jit(solution)/shard_map/ppermute | solution.py:31
  142.7 9.9 %collective-permute-start.19 = (bf16[512,256]{1,0:T(8,128)(2,1)S(1)}, bf16[512,256]{1,0:T(8,128)(2,1)S(1)}, u32[]{:S(2)}, u32[]{:S(2)}) collective-permute-start(bf16[512,256]{1,0:T(8,128)(2,1)S(1)} %copy-done.16), channel_id=1, source_target_pairs={{0,16},{8,24},{16,0},{24,8},{32,48},{40,56},{48,32},{56,40},{64,80... | collective-permute-start | bytes 786440 | tf_op jit(solution)/shard_map/ppermute | solution.py:507
  144.6 11.0 %collective-permute-start.20 = (bf16[512,256]{1,0:T(8,128)(2,1)S(1)}, bf16[512,256]{1,0:T(8,128)(2,1)S(1)}, u32[]{:S(2)}, u32[]{:S(2)}) collective-permute-start(bf16[512,256]{1,0:T(8,128)(2,1)S(1)} %copy-done.15), channel_id=1, source_target_pairs={{0,24},{8,0},{16,8},{24,16},{32,56},{40,32},{48,40},{56,48},{64,88... | collective-permute-start | bytes 786440 | tf_op jit(solution)/shard_map/ppermute | solution.py:507
  145.8 11.1 %collective-permute-start.21 = (bf16[512,256]{1,0:T(8,128)(2,1)S(1)}, bf16[512,256]{1,0:T(8,128)(2,1)S(1)}, u32[]{:S(2)}, u32[]{:S(2)}) collective-permute-start(bf16[512,256]{1,0:T(8,128)(2,1)S(1)} %copy-done.14), channel_id=1, source_target_pairs={{0,32},{8,40},{16,48},{24,56},{32,64},{40,72},{48,80},{56,88},{64,... | collective-permute-start | bytes 786440 | tf_op jit(solution)/shard_map/ppermute | solution.py:507
  146.6 12.6 %collective-permute-start.22 = (bf16[512,256]{1,0:T(8,128)(2,1)S(1)}, bf16[512,256]{1,0:T(8,128)(2,1)S(1)}, u32[]{:S(2)}, u32[]{:S(2)}) collective-permute-start(bf16[512,256]{1,0:T(8,128)(2,1)S(1)} %copy-done.13), channel_id=1, source_target_pairs={{0,64},{8,72},{16,80},{24,88},{32,96},{40,104},{48,112},{56,120},{... | collective-permute-start | bytes 786440 | tf_op jit(solution)/shard_map/ppermute | solution.py:507
  149.2 10.1 %collective-permute-start.23 = (bf16[512,256]{1,0:T(8,128)(2,1)S(1)}, bf16[512,256]{1,0:T(8,128)(2,1)S(1)}, u32[]{:S(2)}, u32[]{:S(2)}) collective-permute-start(bf16[512,256]{1,0:T(8,128)(2,1)S(1)} %copy-done.12), channel_id=1, source_target_pairs={{0,96},{8,104},{16,112},{24,120},{32,0},{40,8},{48,16},{56,24},{64... | collective-permute-start | bytes 786440 | tf_op jit(solution)/shard_map/ppermute | solution.py:507
  152.6 8.3 %collective-permute-start.36 = (bf16[256,256]{1,0:T(8,128)(2,1)S(1)}, bf16[256,256]{1,0:T(8,128)(2,1)S(1)}, u32[]{:S(2)}, u32[]{:S(2)}) collective-permute-start(bf16[256,256]{1,0:T(8,128)(2,1)S(1)} %get-tuple-element.75), channel_id=1, source_target_pairs={{0,8},{8,16},{16,24},{24,0},{32,40},{40,48},{48,56},{56,32},{64,72... | collective-permute-start | bytes 393224 | tf_op jit(solution)/shard_map/ppermute | solution.py:507
  155.6 6.5 %collective-permute-start.37 = (bf16[256,256]{1,0:T(8,128)(2,1)S(1)}, bf16[256,256]{1,0:T(8,128)(2,1)S(1)}, u32[]{:S(2)}, u32[]{:S(2)}) collective-permute-start(bf16[256,256]{1,0:T(8,128)(2,1)S(1)} %get-tuple-element.76), channel_id=1, source_target_pairs={{0,16},{8,24},{16,0},{24,8},{32,48},{40,56},{48,32},{56,40},{64,80... | collective-permute-start | bytes 393224 | tf_op jit(solution)/shard_map/ppermute | solution.py:507
  156.9 6.5 %collective-permute-start.38 = (bf16[256,256]{1,0:T(8,128)(2,1)S(1)}, bf16[256,256]{1,0:T(8,128)(2,1)S(1)}, u32[]{:S(2)}, u32[]{:S(2)}) collective-permute-start(bf16[256,256]{1,0:T(8,128)(2,1)S(1)} %get-tuple-element.77), channel_id=1, source_target_pairs={{0,24},{8,0},{16,8},{24,16},{32,56},{40,32},{48,40},{56,48},{64,88... | collective-permute-start | bytes 393224 | tf_op jit(solution)/shard_map/ppermute | solution.py:507
  (14 other events, 49.2 us)

commit v4 on v3

--- a/solution.py
+++ b/solution.py
@@ -75,9 +75,12 @@
     return SIDE * z + (x + r) % SIDE
 
 
-def gates_kernel(logits_ref, out_ref):
-    sums = jax.nn.log_sigmoid(logits_ref[...])
-    rows, width = sums.shape
+def gate_sums(gates, bias):
+    spans, heads, width = gates.shape
+    for n in range(spans):
+        bias[heads * n : heads * (n + 1), :] = gates[n]
+    sums = jax.nn.log_sigmoid(bias[...])
+    rows = spans * heads
     lane = lax.broadcasted_iota(jnp.int32, sums.shape, 1)
     step = 1
     while step < width:
@@ -85,12 +88,12 @@
         step *= 2
     shape = (rows, rows)
     mine, other = (lax.broadcasted_iota(jnp.int32, shape, d) for d in (0, 1))
-    earlier = jnp.where((other < mine) & (other % 2 == mine % 2), 1.0, 0.0)
+    earlier = jnp.where((other < mine) & (other % heads == mine % heads), 1.0, 0.0)
     totals = jnp.broadcast_to(sums[:, width - 1 :], (rows, HEAD))
     before = jnp.dot(
         earlier, totals, preferred_element_type=jnp.float32, precision=lax.Precision.HIGHEST
     )
-    out_ref[...] = (sums + wide(before, width)) * LOG2E
+    bias[...] = (sums + wide(before, width)) * LOG2E
 
 
 def fill_bias(bias, bcol, h):
@@ -142,24 +145,26 @@
     return jnp.where(n < SIDE, 2, near), jnp.where(n < SIDE, n, 2)
 
 
-def stats_kernel(slots, pair_count, pair_of, bias_ref, *rest):
+def stats_kernel(slots, pair_count, pair_of, near, bias_ref, *rest):
     n_slots = len(slots)
     z_refs, x_refs = rest[:n_slots], rest[n_slots : 2 * n_slots]
     rest = rest[2 * n_slots :]
-    known, rest = rest[:-8], rest[-8:]
-    outs = rest[:2]
-    bias, qd, kv, bcol, stats, sems = rest[2:]
+    n_scratch = 7 if near else 6
+    n_outs = 3 if near else 2
+    scratch, rest = rest[-n_scratch:], rest[:-n_scratch]
+    outs, known = rest[-n_outs:], rest[:-n_outs]
+    bias, qd, kv, bcol, stats, sems = scratch[:6]
     span = qd.shape[2]
     begin = copy_list(sems)
-    bias_copy = begin(bias_ref, bias)
+    bias_copy = begin(bias_ref, scratch[6] if near else bias)
     loads = []
     for h in range(2):
         loads.append(start_loads(begin, h, z_refs, x_refs, slots, qd, kv))
-        if known:
-            loads[h].append(begin(known[h], stats.at[h]))
-        else:
+        if near:
             stats[h] = jnp.zeros((SIDE, 8, span), jnp.float32)
             stats[h, :, 0:1, :] = jnp.full((SIDE, 1, span), NEG_BIG, jnp.float32)
+        else:
+            loads[h].append(begin(known[h], stats.at[h]))
 
     def block(h, qi, ki, diagonal):
         for s in range(span // SUB):
@@ -187,6 +192,9 @@
 
     bias_copy.wait()
     stores = []
+    if near:
+        gate_sums(scratch[6], bias)
+        stores.append(begin(bias, outs[2]))
     for h in range(2):
         fill_bias(bias, bcol, h)
     for h in range(2):
@@ -312,9 +320,15 @@
 
 
 def query_kernel(*refs):
-    parts, (low_ref, grad_ref) = refs[:8], refs[8:]
-    for h in range(2):
-        total = sum(ref[...].astype(jnp.float32) for ref in parts[SIDE * h : SIDE * (h + 1)])
+    parts, (low_ref, grad_ref, own, sent, sems) = refs[:8], refs[8:]
+    begin = copy_list(sems)
+    loads = []
+    for h in range(2):
+        loads.append([begin(parts[SIDE * h], own.at[h])])
+        loads[h] += [begin(parts[SIDE * h + r], sent.at[h, r]) for r in range(1, SIDE)]
+    for h in range(2):
+        wait_all(loads[h])
+        total = own[h] + sum(sent[h, r].astype(jnp.float32) for r in range(1, SIDE))
         cut = slice(h * HEAD, (h + 1) * HEAD)
         low_ref[cut, :] = total.astype(jnp.bfloat16)
         grad_ref[:, cut] = total.T
@@ -334,27 +348,33 @@
 VM = pl.BlockSpec(memory_space=pltpu.VMEM)
 
 
-def stats_call(bias, z_parts, x_parts, known=None):
+def stats_call(bias, z_parts, x_parts, known=()):
     span = z_parts[0].shape[0]
-    if known is None:
-        slots, pair_count, pair_of, known = NEAR, 9, near_pairs, ()
+    near = not known
+    rows = 2 * SIDE * SIDE
+    out_shape = [jax.ShapeDtypeStruct((SIDE, 8, span), jnp.float32)] * 2
+    scratch = [
+        pltpu.VMEM((rows, span), jnp.float32),
+        pltpu.VMEM((2, SIDE, span, 2 * HEAD), jnp.bfloat16),
+        pltpu.VMEM((2, SIDE, span, 2 * HEAD), jnp.bfloat16),
+        pltpu.VMEM((2, SIDE, span, HEAD), jnp.float32),
+        pltpu.VMEM((2, SIDE, 8, span), jnp.float32),
+        pltpu.SemaphoreType.DMA((24,)),
+    ]
+    if near:
+        slots, pair_count, pair_of = NEAR, 9, near_pairs
         z_parts, x_parts = ([parts[r] for r in NEAR] for parts in (z_parts, x_parts))
+        out_shape.append(jax.ShapeDtypeStruct((rows, span), jnp.float32))
+        scratch.append(pltpu.VMEM(bias.shape, jnp.float32))
     else:
         slots, pair_count, pair_of = range(SIDE), 7, far_pairs
     pairs = pair_count * span * span
     return pl.pallas_call(
-        functools.partial(stats_kernel, slots, pair_count, pair_of),
-        out_shape=[jax.ShapeDtypeStruct((SIDE, 8, span), jnp.float32)] * 2,
+        functools.partial(stats_kernel, slots, pair_count, pair_of, near),
+        out_shape=out_shape,
         in_specs=[ANY] * (1 + 2 * len(slots) + len(known)),
-        out_specs=[ANY] * 2,
-        scratch_shapes=[
-            pltpu.VMEM(bias.shape, jnp.float32),
-            pltpu.VMEM((2, SIDE, span, 2 * HEAD), jnp.bfloat16),
-            pltpu.VMEM((2, SIDE, span, 2 * HEAD), jnp.bfloat16),
-            pltpu.VMEM((2, SIDE, span, HEAD), jnp.float32),
-            pltpu.VMEM((2, SIDE, 8, span), jnp.float32),
-            pltpu.SemaphoreType.DMA((24,)),
-        ],
+        out_specs=[ANY] * len(out_shape),
+        scratch_shapes=scratch,
         compiler_params=pltpu.CompilerParams(vmem_limit_bytes=62 << 20),
         cost_estimate=pl.CostEstimate(
             flops=4 * HEAD * pairs, bytes_accessed=4 << 20, transcendentals=pairs
@@ -431,8 +451,13 @@
             jax.ShapeDtypeStruct((2 * rows, span), jnp.bfloat16),
             jax.ShapeDtypeStruct((span, 2 * rows), jnp.float32),
         ],
-        in_specs=[VM] * 8,
+        in_specs=[ANY] * 8,
         out_specs=[VM] * 2,
+        scratch_shapes=[
+            pltpu.VMEM((2, rows, span), jnp.float32),
+            pltpu.VMEM((2, SIDE, rows, span), jnp.bfloat16),
+            pltpu.SemaphoreType.DMA((8,)),
+        ],
         compiler_params=pltpu.CompilerParams(vmem_limit_bytes=16 << 20),
         cost_estimate=pl.CostEstimate(flops=10**6, bytes_accessed=2 << 20, transcendentals=0),
         name="query_sums",
@@ -459,7 +484,8 @@
 
 
 def local(queries, keys, values, forget_logits, layer_input, out_grad):
-    gates = lax.all_to_all(jnp.tile(forget_logits.T, (16, 1)), "sp", 0, 0, tiled=True)
+    gates = jnp.broadcast_to(forget_logits.T, (SIDE * SIDE,) + forget_logits.shape[::-1])
+    gates = lax.all_to_all(gates, "sp", 0, 0, tiled=True)
 
     for_z = jnp.concatenate(
         [head_of(queries, 0), head_of(out_grad, 0), head_of(keys, 1), head_of(values, 1)], axis=1
@@ -470,15 +496,6 @@
     z_parts = fetched(for_z, along_z)
     x_parts = fetched(for_x, along_x)
 
-    bias = pl.pallas_call(
-        gates_kernel,
-        out_shape=jax.ShapeDtypeStruct(gates.shape, jnp.float32),
-        in_specs=[VM],
-        out_specs=VM,
-        cost_estimate=pl.CostEstimate(flops=10**6, bytes_accessed=1 << 17, transcendentals=0),
-        name="gate_sums",
-    )(gates)
-
     def over_zy(target):
         pairs = []
         for n in range(SIDE**3 * 2):
@@ -487,16 +504,14 @@
             pairs.append((n, new_z % SIDE * 32 + zxyc[1] * 8 + new_y % SIDE * 2 + zxyc[3]))
         return pairs
 
-    everywhere = ("sp", "tp")
-    moved = lax.ppermute(layer_input, everywhere, over_zy(lambda a, b: (a, a + b)))
-    moved = lax.ppermute(moved, everywhere, over_zy(lambda a, b: (b - a, b)))
+    moved = lax.ppermute(layer_input, ("sp", "tp"), over_zy(lambda a, b: (b, a + b)))
     inputs = [moved]
     for r in range(1, SIDE):
         inputs.append(lax.ppermute(moved, "tp", [(p, (p - 2 * r) % 8) for p in range(8)]))
     for part in list(inputs):
         inputs.append(lax.ppermute(part, "tp", [(p, p ^ 1) for p in range(8)]))
 
-    known = stats_call(bias, z_parts, x_parts)
+    *known, bias = stats_call(gates, z_parts, x_parts)
     stats_z, stats_x = stats_call(bias, z_parts, x_parts, known)
     z_stats = fetched(stats_z, along_z)
     x_stats = fetched(stats_x, along_x)

time: 165 us -> 168 us (1.018); the launches traced: 164 us -> 165 us
  blocking collectives: 14.6 us -> 22.6 us
  waiting for transfers between devices: 39.3 us -> 35.8 us
  starting transfers between devices: 58.9 us -> 56.1 us
    all_to_all x1, blocking collectives: 14.6 us -> 22.6 us  [local(): gates = lax.all_to_all(gates, 'sp', 0, 0, tiled=True)]
    ppermute x15, starting transfers between devices: 23.3 us -> 30.3 us  [arrived(): lax.ppermute(parts[r], 'sp', axis_perm(r))]
    ppermute x15, waiting for transfers between devices: 25 us -> 18.7 us  [fetched(): parts.append(lax.ppermute(array, 'sp', axis_perm(-r)))]
    ppermute x2 -> x1, starting transfers between devices: 7.04 us -> 0.87 us  [local(): lax.ppermute(layer_input, ('sp', 'tp'), over_zy(lambda a, b: (b, a + b)))]
    ppermute x3, starting transfers between devices: 3.12 us -> 0.01 us  [local(): lax.ppermute(moved, 'tp', [(p, (p - 2 * r) % 8) for p in range(8)])]
    ppermute x15, waiting for transfers between devices: 14.3 us -> 17.1 us  [arrived(): lax.ppermute(parts[r], 'sp', axis_perm(r))]
    pallas_call x1 -> x0, Pallas kernels: 2.25 us -> none  [local(): pl.pallas_call(gates_kernel, out_shape=jax.ShapeDtypeStruct(gates.shape,...]
    unnamed x47 -> x49, local copies, waits for them, and re-layouts: 5.07 us -> 5.06 us
  transfers between devices with their start and end apart: 39 -> 38, of which waited for: 14 -> 15; matrix products, arithmetic and copies ran while one was open for 0% -> 0% of each run, Pallas kernels for 27% -> 22%
where the time goes in v4:
time: 168 us; the launch traced here: 165 us
  starting transfers between devices  56.1 us (33%)
  Pallas kernels  43.5 us (26%)
  waiting for transfers between devices  35.8 us (21%)
  blocking collectives  22.6 us (13%)
  local copies, waits for them, and re-layouts  6.36 us (4%)
    ppermute x15, starting transfers between devices, arrived(): lax.ppermute(parts[r], 'sp', axis_perm(r))  30.3 us
    ppermute x15, starting transfers between devices, fetched(): parts.append(lax.ppermute(array, 'sp', axis_perm(-r)))  23.9 us
    all_to_all x1, blocking collectives, local(): gates = lax.all_to_all(gates, 'sp', 0, 0, tiled=True)  22.6 us
    pallas_call x1, Pallas kernels, grads_call(): pl.pallas_call(grads_kernel, out_shape=shapes(HEAD, span) + shapes(span,...  20.1 us
    ppermute x15, waiting for transfers between devices, fetched(): parts.append(lax.ppermute(array, 'sp', axis_perm(-r)))  18.7 us
    pallas_call x2, Pallas kernels, stats_call(): pl.pallas_call(functools.partial(stats_kernel, slots, pair_count, pair_of...  17.7 us
    ppermute x15, waiting for transfers between devices, arrived(): lax.ppermute(parts[r], 'sp', axis_perm(r))  17.1 us
    unnamed x49, local copies, waits for them, and re-layouts  5.06 us
  transfers between devices with their start and end apart: 38, of which 15 were waited for; matrix products, arithmetic and copies ran while one was open for 0% of the time, Pallas kernels for 22%

profile of v4, /device:TPU:0, one launch (start us, length us, event | category | flops | bytes accessed | tf_op | source)
XLA Modules:
  0.0 165.4 jit_solution(7716302480233233329)
XLA Ops:
  0.7 1.2 fusion.2
  2.1 2.1 %collective-permute-start.1 = (bf16[512,512]{1,0:T(8,128)(2,1)S(1)}, bf16[512,512]{1,0:T(8,128)(2,1)S(1)}, u32[]{:S(2)}, u32[]{:S(2)}) collective-permute-start(bf16[512,512]{1,0:T(8,128)(2,1)S(1)} %pad_maximum_fusion.rest_0_), channel_id=1, source_target_pairs={{0,32},{8,40},{16,48},{24,56},{32,64},{40,72},{48,80},{56,88},{64,... | collective-permute-start | bytes 1572872 | tf_op jit(solution)/shard_map/ppermute | solution.py:31
  4.2 2.2 %collective-permute-start = (bf16[512,512]{1,0:T(8,128)(2,1)S(1)}, bf16[512,512]{1,0:T(8,128)(2,1)S(1)}, u32[]{:S(2)}, u32[]{:S(2)}) collective-permute-start(bf16[512,512]{1,0:T(8,128)(2,1)S(1)} %pad_maximum_fusion.rest_0_), channel_id=1, source_target_pairs={{0,96},{8,104},{16,112},{24,120},{32,0},{40,8},{48,16},{56,24},{64... | collective-permute-start | bytes 1572872 | tf_op jit(solution)/shard_map/ppermute | solution.py:31
  6.5 1.6 collective-permute-start.3
  8.0 1.7 %collective-permute-start.2 = (bf16[512,512]{1,0:T(8,128)(2,1)S(1)}, bf16[512,512]{1,0:T(8,128)(2,1)}, u32[]{:S(2)}, u32[]{:S(2)}) collective-permute-start(bf16[512,512]{1,0:T(8,128)(2,1)S(1)} %pad_maximum_fusion.1.rest_3_.rest_4_), channel_id=1, source_target_pairs={{0,24},{8,0},{16,8},{24,16},{32,56},{40,32},{48,40},{56,48},{64,88... | collective-permute-start | bytes 1572872 | tf_op jit(solution)/shard_map/ppermute | solution.py:31
  9.8 1.8 %collective-permute-start.4 = (bf16[512,512]{1,0:T(8,128)(2,1)S(1)}, bf16[512,512]{1,0:T(8,128)(2,1)}, u32[]{:S(2)}, u32[]{:S(2)}) collective-permute-start(bf16[512,512]{1,0:T(8,128)(2,1)S(1)} %pad_maximum_fusion.rest_0_), channel_id=1, source_target_pairs={{0,64},{8,72},{16,80},{24,88},{32,96},{40,104},{48,112},{56,120},{... | collective-permute-start | bytes 1572872 | tf_op jit(solution)/shard_map/ppermute | solution.py:31
  11.6 6.7 %collective-permute-done.1.rest_2_.rest_3_ = bf16[512,512]{1,0:T(8,128)(2,1)S(1)} collective-permute-done((bf16[512,512]{1,0:T(8,128)(2,1)S(1)}, bf16[512,512]{1,0:T(8,128)(2,1)S(1)}, u32[]{:S(2)}, u32[]{:S(2)}) %collective-permute-start.1) | collective-permute-done | bytes 524320 | tf_op jit(solution)/shard_map/ppermute | solution.py:31
  18.2 3.0 %collective-permute-start.5 = (bf16[512,512]{1,0:T(8,128)(2,1)S(1)}, bf16[512,512]{1,0:T(8,128)(2,1)}, u32[]{:S(2)}, u32[]{:S(2)}) collective-permute-start(bf16[512,512]{1,0:T(8,128)(2,1)S(1)} %pad_maximum_fusion.1.rest_3_.rest_4_), channel_id=1, source_target_pairs={{0,16},{8,24},{16,0},{24,8},{32,48},{40,56},{48,32},{56,40},{64,80... | collective-permute-start | bytes 1572872 | tf_op jit(solution)/shard_map/ppermute | solution.py:31
  21.3 22.6 %all_to_all.5.bias_ref = f32[16,2,512]{2,1,0:T(2,128)} all-to-all(f32[16,2,512]{2,1,0:T(2,128)S(1)} %broadcast_in_dim.3), channel_id=1, replica_groups=mesh['sp'=16,'tp'=8] {'sp'}, dimensions={0} | all-to-all | bytes 131072 | tf_op jit(solution)/shard_map/all_to_all | solution.py:488
  43.9 0.8 copy-done.7
  44.7 0.8 copy-done.8
  45.5 10.2 %stats.2 = (f32[4,8,512]{2,1,0:T(8,128)}, f32[4,8,512]{2,1,0:T(8,128)}, f32[32,512]{1,0:T(8,128)}) custom-call(f32[16,2,512]{2,1,0:T(2,128)} %all_to_all.5.bias_ref, bf16[512,512]{1,0:T(8,128)(2,1)} %copy-done.4, bf16[512,512]{1,0:T(8,128)(2,1)} %copy-done.7, bf16[512,512]{1,0:T(8,128)(2,1)} %copy-done.6, bf16[512,512]{1,0:T(8,128)(2,1)} %copy-done.5, ...), custom_call_target="tpu_custom_call" | custom-call | flops 1207959552 | bytes 4194304 | tf_op jit(solution)/shard_map/stats/pallas_call | solution.py:372
  55.7 7.5 %stats.3 = (f32[4,8,512]{2,1,0:T(8,128)}, f32[4,8,512]{2,1,0:T(8,128)}) custom-call(f32[32,512]{1,0:T(8,128)} %get-tuple-element.42.bias_ref, bf16[512,512]{1,0:T(8,128)(2,1)} %copy-done.4, bf16[512,512]{1,0:T(8,128)(2,1)} %copy-done.7, bf16[512,512]{1,0:T(8,128)(2,1)} %collective-permute-done.4.rest_2_, bf16[512,512]{1,0:T(8,128)(2,1)} %copy-done.6, ...), custom_call_target="tpu_custom_call" | custom-call | flops 939524096 | bytes 4194304 | tf_op jit(solution)/shard_map/stats/pallas_call | solution.py:372
  63.9 2.1 %collective-permute-start.7 = (f32[4,8,512]{2,1,0:T(8,128)}, f32[4,8,512]{2,1,0:T(8,128)S(1)}, u32[]{:S(2)}, u32[]{:S(2)}) collective-permute-start(f32[4,8,512]{2,1,0:T(8,128)} %get-tuple-element.45.rest_8_), channel_id=1, source_target_pairs={{0,64},{8,72},{16,80},{24,88},{32,96},{40,104},{48,112},{56,120},{... | collective-permute-start | bytes 196616 | tf_op jit(solution)/shard_map/ppermute | solution.py:31
  65.9 1.2 collective-permute-start.6
  67.7 2.1 %collective-permute-start.10 = (f32[4,8,512]{2,1,0:T(8,128)}, f32[4,8,512]{2,1,0:T(8,128)S(1)}, u32[]{:S(2)}, u32[]{:S(2)}) collective-permute-start(f32[4,8,512]{2,1,0:T(8,128)} %get-tuple-element.46.rest_12_), channel_id=1, source_target_pairs={{0,16},{8,24},{16,0},{24,8},{32,48},{40,56},{48,32},{56,40},{64,80... | collective-permute-start | bytes 196616 | tf_op jit(solution)/shard_map/ppermute | solution.py:31
  69.8 1.3 collective-permute-start.9
  71.1 0.9 collective-permute-start.27
  72.0 1.5 collective-permute-done.6.rest_9_
  73.7 0.7 collective-permute-done.9.rest_13_
  75.0 20.1 %grads.1 = (f32[128,512]{1,0:T(8,128)}, bf16[128,512]{1,0:T(8,128)(2,1)}, bf16[128,512]{1,0:T(8,128)(2,1)}, bf16[128,512]{1,0:T(8,128)(2,1)}, f32[128,512]{1,0:T...) custom-call(f32[32,512]{1,0:T(8,128)} %get-tuple-element.42.bias_ref, ...), custom_call_target="tpu_custom_call" | custom-call | flops 5704253440 | bytes 8388608 | tf_op jit(solution)/shard_map/grads/pallas_call | solution.py:395
  95.2 5.6 %collective-permute-start.12 = (bf16[128,512]{1,0:T(8,128)(2,1)}, bf16[128,512]{1,0:T(8,128)(2,1)S(1)}, u32[]{:S(2)}, u32[]{:S(2)}) collective-permute-start(bf16[128,512]{1,0:T(8,128)(2,1)} %get-tuple-element.48), channel_id=1, source_target_pairs={{0,32},{8,40},{16,48},{24,56},{32,64},{40,72},{48,80},{56,88},{64,... | collective-permute-start | bytes 393224 | tf_op jit(solution)/shard_map/ppermute | solution.py:522
  100.8 5.6 %collective-permute-start.13 = (bf16[128,512]{1,0:T(8,128)(2,1)}, bf16[128,512]{1,0:T(8,128)(2,1)S(1)}, u32[]{:S(2)}, u32[]{:S(2)}) collective-permute-start(bf16[128,512]{1,0:T(8,128)(2,1)} %get-tuple-element.49), channel_id=1, source_target_pairs={{0,64},{8,72},{16,80},{24,88},{32,96},{40,104},{48,112},{56,120},{... | collective-permute-start | bytes 393224 | tf_op jit(solution)/shard_map/ppermute | solution.py:522
  106.4 2.3 %collective-permute-start.14 = (bf16[128,512]{1,0:T(8,128)(2,1)}, bf16[128,512]{1,0:T(8,128)(2,1)S(1)}, u32[]{:S(2)}, u32[]{:S(2)}) collective-permute-start(bf16[128,512]{1,0:T(8,128)(2,1)} %get-tuple-element.50), channel_id=1, source_target_pairs={{0,96},{8,104},{16,112},{24,120},{32,0},{40,8},{48,16},{56,24},{64... | collective-permute-start | bytes 393224 | tf_op jit(solution)/shard_map/ppermute | solution.py:522
  108.8 2.4 %collective-permute-start.16 = (bf16[128,512]{1,0:T(8,128)(2,1)}, bf16[128,512]{1,0:T(8,128)(2,1)S(1)}, u32[]{:S(2)}, u32[]{:S(2)}) collective-permute-start(bf16[128,512]{1,0:T(8,128)(2,1)} %get-tuple-element.53), channel_id=1, source_target_pairs={{0,16},{8,24},{16,0},{24,8},{32,48},{40,56},{48,32},{56,40},{64,80... | collective-permute-start | bytes 393224 | tf_op jit(solution)/shard_map/ppermute | solution.py:522
  111.1 1.7 %collective-permute-done.13.refs_2_ = bf16[128,512]{1,0:T(8,128)(2,1)S(1)} collective-permute-done((bf16[128,512]{1,0:T(8,128)(2,1)}, bf16[128,512]{1,0:T(8,128)(2,1)S(1)}, u32[]{:S(2)}, u32[]{:S(2)}) %collective-permute-start.13) | collective-permute-done | bytes 131104 | tf_op jit(solution)/shard_map/ppermute | solution.py:522
  112.9 1.4 collective-permute-start.17
  114.4 2.1 %collective-permute-done.15.refs_5_ = bf16[128,512]{1,0:T(8,128)(2,1)S(1)} collective-permute-done((bf16[128,512]{1,0:T(8,128)(2,1)}, bf16[128,512]{1,0:T(8,128)(2,1)S(1)}, u32[]{:S(2)}, u32[]{:S(2)}) %collective-permute-start.15) | collective-permute-done | bytes 131104 | tf_op jit(solution)/shard_map/ppermute | solution.py:522
  116.6 1.5 collective-permute-done.17.refs_7_
  118.1 0.9 copy-done.2
  119.0 0.9 copy-done.3
  120.0 2.2 %query_sums.1 = (bf16[256,512]{1,0:T(8,128)(2,1)S(1)}, f32[512,256]{1,0:T(8,128)}) custom-call(f32[128,512]{1,0:T(8,128)S(1)} %copy-done.2, bf16[128,512]{1,0:T(8,128)(2,1)S(1)} %collective-permute-done.12.refs_1_, bf16[128,512]{1,0:T(8,128)(2,1)S(1)} %collective-permute-done.13.refs_2_, bf16[128,512]{1,0:T(8,128)(2,1)S(1)} %collective-permute-done.14.refs_3_, ...), custom_call_target="tpu_custom_call" | custom-call | flops 1000000 | bytes 2097152 | tf_op jit(solution)/shard_map/query_sums/pallas_call | solution.py:448
  122.2 1.3 collective-permute-start.18
  123.5 6.6 %collective-permute-done.18.refs_1_ = bf16[512,256]{1,0:T(8,128)(2,1)S(1)} collective-permute-done((bf16[512,256]{1,0:T(8,128)(2,1)}, bf16[512,256]{1,0:T(8,128)(2,1)S(1)}, u32[]{:S(2)}, u32[]{:S(2)}) %collective-permute-start.18) | collective-permute-done | bytes 262176 | tf_op jit(solution)/shard_map/ppermute | solution.py:522
  130.1 2.5 %collective-permute-start.25 = (bf16[256,512]{1,0:T(8,128)(2,1)S(1)}, bf16[256,512]{1,0:T(8,128)(2,1)S(1)}, u32[]{:S(2)}, u32[]{:S(2)}) collective-permute-start(bf16[256,512]{1,0:T(8,128)(2,1)S(1)} %get-tuple-element.75.rest_0_), channel_id=1, source_target_pairs={{0,64},{8,72},{16,80},{24,88},{32,96},{40,104},{48,112},{56,120},{... | collective-permute-start | bytes 786440 | tf_op jit(solution)/shard_map/ppermute | solution.py:31
  133.7 4.3 %collective-permute-done.25.rest_2_ = bf16[256,512]{1,0:T(8,128)(2,1)S(1)} collective-permute-done((bf16[256,512]{1,0:T(8,128)(2,1)S(1)}, bf16[256,512]{1,0:T(8,128)(2,1)S(1)}, u32[]{:S(2)}, u32[]{:S(2)}) %collective-permute-start.25) | collective-permute-done | bytes 262176 | tf_op jit(solution)/shard_map/ppermute | solution.py:31
  138.0 1.1 collective-permute-start.24
  139.0 5.3 %collective-permute-done.24.rest_1_ = bf16[256,512]{1,0:T(8,128)(2,1)S(1)} collective-permute-done((bf16[256,512]{1,0:T(8,128)(2,1)S(1)}, bf16[256,512]{1,0:T(8,128)(2,1)S(1)}, u32[]{:S(2)}, u32[]{:S(2)}) %collective-permute-start.24) | collective-permute-done | bytes 262176 | tf_op jit(solution)/shard_map/ppermute | solution.py:31
  144.3 1.3 collective-permute-start.19
  145.6 1.4 collective-permute-start.20
  147.5 3.9 %collective-permute-start.22 = (bf16[512,256]{1,0:T(8,128)(2,1)S(1)}, bf16[512,256]{1,0:T(8,128)(2,1)S(1)}, u32[]{:S(2)}, u32[]{:S(2)}) collective-permute-start(bf16[512,256]{1,0:T(8,128)(2,1)S(1)} %copy-done.14), channel_id=1, source_target_pairs={{0,64},{8,72},{16,80},{24,88},{32,96},{40,104},{48,112},{56,120},{... | collective-permute-start | bytes 786440 | tf_op jit(solution)/shard_map/ppermute | solution.py:522
  151.4 1.8 %weight.1 = (f32[256,256]{1,0:T(8,128)S(1)}, bf16[256,256]{1,0:T(8,128)(2,1)S(1)}, bf16[256,256]{1,0:T(8,128)(2,1)S(1)}, bf16[256,256]{1,0:T(8,128)(2,1)S(1)}) custom-call(bf16[256,512]{1,0:T(8,128)(2,1)S(1)} %get-tuple-element.75.rest_0_, bf16[256,512]{1,0:T(8,128)(2,1)S(1)} %collective-permute-done.24.rest_1_, ...), custom_call_target="tpu_custom_call" | custom-call | flops 1073741824 | bytes 6291456 | tf_op jit(solution)/shard_map/weight/pallas_call | solution.py:428
  154.3 2.1 %collective-permute-done.20.refs_3_ = bf16[512,256]{1,0:T(8,128)(2,1)S(1)} collective-permute-done((bf16[512,256]{1,0:T(8,128)(2,1)S(1)}, bf16[512,256]{1,0:T(8,128)(2,1)S(1)}, u32[]{:S(2)}, u32[]{:S(2)}) %collective-permute-start.20) | collective-permute-done | bytes 262176 | tf_op jit(solution)/shard_map/ppermute | solution.py:522
  156.4 1.6 collective-permute-start.36
  158.0 2.5 %collective-permute-start.37 = (bf16[256,256]{1,0:T(8,128)(2,1)S(1)}, bf16[256,256]{1,0:T(8,128)(2,1)S(1)}, u32[]{:S(2)}, u32[]{:S(2)}) collective-permute-start(bf16[256,256]{1,0:T(8,128)(2,1)S(1)} %get-tuple-element.79), channel_id=1, source_target_pairs={{0,24},{8,0},{16,8},{24,16},{32,56},{40,32},{48,40},{56,48},{64,88... | collective-permute-start | bytes 393224 | tf_op jit(solution)/shard_map/ppermute | solution.py:522
  160.5 1.6 key_sums.1
  162.8 1.6 collective-permute-done.37
  164.5 0.8 copy.10
  (90 shorter events, 5.7 us)
Async XLA Ops:
  2.1 16.1 %collective-permute-start.1 = (bf16[512,512]{1,0:T(8,128)(2,1)S(1)}, bf16[512,512]{1,0:T(8,128)(2,1)S(1)}, u32[]{:S(2)}, u32[]{:S(2)}) collective-permute-start(bf16[512,512]{1,0:T(8,128)(2,1)S(1)} %pad_maximum_fusion.rest_0_), channel_id=1, source_target_pairs={{0,32},{8,40},{16,48},{24,56},{32,64},{40,72},{48,80},{56,88},{64,... | collective-permute-start | bytes 1572872 | tf_op jit(solution)/shard_map/ppermute | solution.py:31
  4.2 39.7 %collective-permute-start = (bf16[512,512]{1,0:T(8,128)(2,1)S(1)}, bf16[512,512]{1,0:T(8,128)(2,1)S(1)}, u32[]{:S(2)}, u32[]{:S(2)}) collective-permute-start(bf16[512,512]{1,0:T(8,128)(2,1)S(1)} %pad_maximum_fusion.rest_0_), channel_id=1, source_target_pairs={{0,96},{8,104},{16,112},{24,120},{32,0},{40,8},{48,16},{56,24},{64... | collective-permute-start | bytes 1572872 | tf_op jit(solution)/shard_map/ppermute | solution.py:31
  6.5 39.0 %copy-start.5 = (bf16[512,512]{1,0:T(8,128)(2,1)}, bf16[512,512]{1,0:T(8,128)(2,1)S(1)}, u32[]{:S(2)}) copy-start(bf16[512,512]{1,0:T(8,128)(2,1)S(1)} %pad_maximum_fusion.1.rest_3_.rest_4_) | copy-start | bytes 1572868
  6.5 37.4 %collective-permute-start.3 = (bf16[512,512]{1,0:T(8,128)(2,1)S(1)}, bf16[512,512]{1,0:T(8,128)(2,1)S(1)}, u32[]{:S(2)}, u32[]{:S(2)}) collective-permute-start(bf16[512,512]{1,0:T(8,128)(2,1)S(1)} %pad_maximum_fusion.1.rest_3_.rest_4_), channel_id=1, source_target_pairs={{0,8},{8,16},{16,24},{24,0},{32,40},{40,48},{48,56},{56,32},{64,72... | collective-permute-start | bytes 1572872 | tf_op jit(solution)/shard_map/ppermute | solution.py:31
  8.0 37.5 %collective-permute-start.2 = (bf16[512,512]{1,0:T(8,128)(2,1)S(1)}, bf16[512,512]{1,0:T(8,128)(2,1)}, u32[]{:S(2)}, u32[]{:S(2)}) collective-permute-start(bf16[512,512]{1,0:T(8,128)(2,1)S(1)} %pad_maximum_fusion.1.rest_3_.rest_4_), channel_id=1, source_target_pairs={{0,24},{8,0},{16,8},{24,16},{32,56},{40,32},{48,40},{56,48},{64,88... | collective-permute-start | bytes 1572872 | tf_op jit(solution)/shard_map/ppermute | solution.py:31
  9.8 45.9 %collective-permute-start.4 = (bf16[512,512]{1,0:T(8,128)(2,1)S(1)}, bf16[512,512]{1,0:T(8,128)(2,1)}, u32[]{:S(2)}, u32[]{:S(2)}) collective-permute-start(bf16[512,512]{1,0:T(8,128)(2,1)S(1)} %pad_maximum_fusion.rest_0_), channel_id=1, source_target_pairs={{0,64},{8,72},{16,80},{24,88},{32,96},{40,104},{48,112},{56,120},{... | collective-permute-start | bytes 1572872 | tf_op jit(solution)/shard_map/ppermute | solution.py:31
  18.2 27.3 %copy-start.6 = (bf16[512,512]{1,0:T(8,128)(2,1)}, bf16[512,512]{1,0:T(8,128)(2,1)S(1)}, u32[]{:S(2)}) copy-start(bf16[512,512]{1,0:T(8,128)(2,1)S(1)} %collective-permute-done.1.rest_2_.rest_3_) | copy-start | bytes 1572868
  18.2 37.5 %collective-permute-start.5 = (bf16[512,512]{1,0:T(8,128)(2,1)S(1)}, bf16[512,512]{1,0:T(8,128)(2,1)}, u32[]{:S(2)}, u32[]{:S(2)}) collective-permute-start(bf16[512,512]{1,0:T(8,128)(2,1)S(1)} %pad_maximum_fusion.1.rest_3_.rest_4_), channel_id=1, source_target_pairs={{0,16},{8,24},{16,0},{24,8},{32,48},{40,56},{48,32},{56,40},{64,80... | collective-permute-start | bytes 1572872 | tf_op jit(solution)/shard_map/ppermute | solution.py:31
  55.7 15.4 %copy-start.12 = (bf16[512,512]{1,0:T(8,128)(2,1)S(1)}, bf16[512,512]{1,0:T(8,128)(2,1)}, u32[]{:S(2)}) copy-start(bf16[512,512]{1,0:T(8,128)(2,1)} %param.10) | copy-start | bytes 1572868
  63.3 6.5 %collective-permute-start.8 = (f32[4,8,512]{2,1,0:T(8,128)}, f32[4,8,512]{2,1,0:T(8,128)S(1)}, u32[]{:S(2)}, u32[]{:S(2)}) collective-permute-start(f32[4,8,512]{2,1,0:T(8,128)} %get-tuple-element.45.rest_8_), channel_id=1, source_target_pairs={{0,32},{8,40},{16,48},{24,56},{32,64},{40,72},{48,80},{56,88},{64,... | collective-permute-start | bytes 196616 | tf_op jit(solution)/shard_map/ppermute | solution.py:31
  63.9 7.3 %collective-permute-start.7 = (f32[4,8,512]{2,1,0:T(8,128)}, f32[4,8,512]{2,1,0:T(8,128)S(1)}, u32[]{:S(2)}, u32[]{:S(2)}) collective-permute-start(f32[4,8,512]{2,1,0:T(8,128)} %get-tuple-element.45.rest_8_), channel_id=1, source_target_pairs={{0,64},{8,72},{16,80},{24,88},{32,96},{40,104},{48,112},{56,120},{... | collective-permute-start | bytes 196616 | tf_op jit(solution)/shard_map/ppermute | solution.py:31
  65.9 7.6 %collective-permute-start.6 = (f32[4,8,512]{2,1,0:T(8,128)}, f32[4,8,512]{2,1,0:T(8,128)S(1)}, u32[]{:S(2)}, u32[]{:S(2)}) collective-permute-start(f32[4,8,512]{2,1,0:T(8,128)} %get-tuple-element.45.rest_8_), channel_id=1, source_target_pairs={{0,96},{8,104},{16,112},{24,120},{32,0},{40,8},{48,16},{56,24},{64... | collective-permute-start | bytes 196616 | tf_op jit(solution)/shard_map/ppermute | solution.py:31
  67.1 6.4 %collective-permute-start.11 = (f32[4,8,512]{2,1,0:T(8,128)}, f32[4,8,512]{2,1,0:T(8,128)S(1)}, u32[]{:S(2)}, u32[]{:S(2)}) collective-permute-start(f32[4,8,512]{2,1,0:T(8,128)} %get-tuple-element.46.rest_12_), channel_id=1, source_target_pairs={{0,8},{8,16},{16,24},{24,0},{32,40},{40,48},{48,56},{56,32},{64,72... | collective-permute-start | bytes 196616 | tf_op jit(solution)/shard_map/ppermute | solution.py:31
  67.7 6.0 %collective-permute-start.10 = (f32[4,8,512]{2,1,0:T(8,128)}, f32[4,8,512]{2,1,0:T(8,128)S(1)}, u32[]{:S(2)}, u32[]{:S(2)}) collective-permute-start(f32[4,8,512]{2,1,0:T(8,128)} %get-tuple-element.46.rest_12_), channel_id=1, source_target_pairs={{0,16},{8,24},{16,0},{24,8},{32,48},{40,56},{48,32},{56,40},{64,80... | collective-permute-start | bytes 196616 | tf_op jit(solution)/shard_map/ppermute | solution.py:31
  69.8 4.6 %collective-permute-start.9 = (f32[4,8,512]{2,1,0:T(8,128)}, f32[4,8,512]{2,1,0:T(8,128)S(1)}, u32[]{:S(2)}, u32[]{:S(2)}) collective-permute-start(f32[4,8,512]{2,1,0:T(8,128)} %get-tuple-element.46.rest_12_), channel_id=1, source_target_pairs={{0,24},{8,0},{16,8},{24,16},{32,56},{40,32},{48,40},{56,48},{64,88... | collective-permute-start | bytes 196616 | tf_op jit(solution)/shard_map/ppermute | solution.py:31
  71.1 37.6 %collective-permute-start.27 = (bf16[512,512]{1,0:T(8,128)(2,1)S(1)}, bf16[512,512]{1,0:T(8,128)(2,1)S(1)}, u32[]{:S(2)}, u32[]{:S(2)}) collective-permute-start(bf16[512,512]{1,0:T(8,128)(2,1)S(1)} %copy-done.12), channel_id=1, source_target_pairs={{0,0},{1,1},{2,34},{3,35},{4,68},{5,69},{6,102},{7,103},{8,8},{9,9... | collective-permute-start | bytes 1572872 | tf_op jit(solution)/shard_map/ppermute | solution.py:507
  95.2 13.6 %collective-permute-start.12 = (bf16[128,512]{1,0:T(8,128)(2,1)}, bf16[128,512]{1,0:T(8,128)(2,1)S(1)}, u32[]{:S(2)}, u32[]{:S(2)}) collective-permute-start(bf16[128,512]{1,0:T(8,128)(2,1)} %get-tuple-element.48), channel_id=1, source_target_pairs={{0,32},{8,40},{16,48},{24,56},{32,64},{40,72},{48,80},{56,88},{64,... | collective-permute-start | bytes 393224 | tf_op jit(solution)/shard_map/ppermute | solution.py:522
  100.8 12.1 %collective-permute-start.13 = (bf16[128,512]{1,0:T(8,128)(2,1)}, bf16[128,512]{1,0:T(8,128)(2,1)S(1)}, u32[]{:S(2)}, u32[]{:S(2)}) collective-permute-start(bf16[128,512]{1,0:T(8,128)(2,1)} %get-tuple-element.49), channel_id=1, source_target_pairs={{0,64},{8,72},{16,80},{24,88},{32,96},{40,104},{48,112},{56,120},{... | collective-permute-start | bytes 393224 | tf_op jit(solution)/shard_map/ppermute | solution.py:522
  106.4 8.0 %collective-permute-start.14 = (bf16[128,512]{1,0:T(8,128)(2,1)}, bf16[128,512]{1,0:T(8,128)(2,1)S(1)}, u32[]{:S(2)}, u32[]{:S(2)}) collective-permute-start(bf16[128,512]{1,0:T(8,128)(2,1)} %get-tuple-element.50), channel_id=1, source_target_pairs={{0,96},{8,104},{16,112},{24,120},{32,0},{40,8},{48,16},{56,24},{64... | collective-permute-start | bytes 393224 | tf_op jit(solution)/shard_map/ppermute | solution.py:522
  108.8 7.8 %collective-permute-start.15 = (bf16[128,512]{1,0:T(8,128)(2,1)}, bf16[128,512]{1,0:T(8,128)(2,1)S(1)}, u32[]{:S(2)}, u32[]{:S(2)}) collective-permute-start(bf16[128,512]{1,0:T(8,128)(2,1)} %get-tuple-element.52), channel_id=1, source_target_pairs={{0,8},{8,16},{16,24},{24,0},{32,40},{40,48},{48,56},{56,32},{64,72... | collective-permute-start | bytes 393224 | tf_op jit(solution)/shard_map/ppermute | solution.py:522
  108.8 23.9 %collective-permute-start.30 = (bf16[512,512]{1,0:T(8,128)(2,1)S(1)}, bf16[512,512]{1,0:T(8,128)(2,1)S(1)}, u32[]{:S(2)}, u32[]{:S(2)}) collective-permute-start(bf16[512,512]{1,0:T(8,128)(2,1)S(1)} %collective-permute-done.27.rest_4_), channel_id=1, source_target_pairs={{0,2},{1,3},{2,4},{3,5},{4,6},{5,7},{6,0},{7,1},{8,10},{9,11},{10,... | collective-permute-start | bytes 1572872 | tf_op jit(solution)/shard_map/ppermute | solution.py:510
  108.8 7.8 %collective-permute-start.16 = (bf16[128,512]{1,0:T(8,128)(2,1)}, bf16[128,512]{1,0:T(8,128)(2,1)S(1)}, u32[]{:S(2)}, u32[]{:S(2)}) collective-permute-start(bf16[128,512]{1,0:T(8,128)(2,1)} %get-tuple-element.53), channel_id=1, source_target_pairs={{0,16},{8,24},{16,0},{24,8},{32,48},{40,56},{48,32},{56,40},{64,80... | collective-permute-start | bytes 393224 | tf_op jit(solution)/shard_map/ppermute | solution.py:522
  112.9 5.2 %collective-permute-start.17 = (bf16[128,512]{1,0:T(8,128)(2,1)}, bf16[128,512]{1,0:T(8,128)(2,1)S(1)}, u32[]{:S(2)}, u32[]{:S(2)}) collective-permute-start(bf16[128,512]{1,0:T(8,128)(2,1)} %get-tuple-element.54), channel_id=1, source_target_pairs={{0,24},{8,0},{16,8},{24,16},{32,56},{40,32},{48,40},{56,48},{64,88... | collective-permute-start | bytes 393224 | tf_op jit(solution)/shard_map/ppermute | solution.py:522
  114.4 18.7 %collective-permute-start.29 = (bf16[512,512]{1,0:T(8,128)(2,1)S(1)}, bf16[512,512]{1,0:T(8,128)(2,1)S(1)}, u32[]{:S(2)}, u32[]{:S(2)}) collective-permute-start(bf16[512,512]{1,0:T(8,128)(2,1)S(1)} %collective-permute-done.27.rest_4_), channel_id=1, source_target_pairs={{0,4},{1,5},{2,6},{3,7},{4,0},{5,1},{6,2},{7,3},{8,12},{9,13},{10,... | collective-permute-start | bytes 1572872 | tf_op jit(solution)/shard_map/ppermute | solution.py:510
  116.5 16.7 %collective-permute-start.28 = (bf16[512,512]{1,0:T(8,128)(2,1)S(1)}, bf16[512,512]{1,0:T(8,128)(2,1)S(1)}, u32[]{:S(2)}, u32[]{:S(2)}) collective-permute-start(bf16[512,512]{1,0:T(8,128)(2,1)S(1)} %collective-permute-done.27.rest_4_), channel_id=1, source_target_pairs={{0,6},{1,7},{2,0},{3,1},{4,2},{5,3},{6,4},{7,5},{8,14},{9,15},{10,... | collective-permute-start | bytes 1572872 | tf_op jit(solution)/shard_map/ppermute | solution.py:510
  120.0 24.4 %copy-start.17 = (bf16[512,256]{1,0:T(8,128)(2,1)S(1)}, bf16[512,256]{1,0:T(8,128)(2,1)}, u32[]{:S(2)}) copy-start(bf16[512,256]{1,0:T(8,128)(2,1)} %get-tuple-element.67) | copy-start | bytes 786436
  120.0 25.7 %copy-start.16 = (bf16[512,256]{1,0:T(8,128)(2,1)S(1)}, bf16[512,256]{1,0:T(8,128)(2,1)}, u32[]{:S(2)}) copy-start(bf16[512,256]{1,0:T(8,128)(2,1)} %get-tuple-element.68) | copy-start | bytes 786436
  120.0 27.1 %copy-start.15 = (bf16[512,256]{1,0:T(8,128)(2,1)S(1)}, bf16[512,256]{1,0:T(8,128)(2,1)}, u32[]{:S(2)}) copy-start(bf16[512,256]{1,0:T(8,128)(2,1)} %get-tuple-element.70) | copy-start | bytes 786436
  120.0 27.5 %copy-start.14 = (bf16[512,256]{1,0:T(8,128)(2,1)S(1)}, bf16[512,256]{1,0:T(8,128)(2,1)}, u32[]{:S(2)}) copy-start(bf16[512,256]{1,0:T(8,128)(2,1)} %get-tuple-element.71) | copy-start | bytes 786436
  120.0 31.4 %copy-start.13 = (bf16[512,256]{1,0:T(8,128)(2,1)S(1)}, bf16[512,256]{1,0:T(8,128)(2,1)}, u32[]{:S(2)}) copy-start(bf16[512,256]{1,0:T(8,128)(2,1)} %get-tuple-element.72) | copy-start | bytes 786436
  122.2 38.3 %copy-start = (f32[512,256]{1,0:T(8,128)S(1)}, f32[512,256]{1,0:T(8,128)}, u32[]{:S(2)}) copy-start(f32[512,256]{1,0:T(8,128)} %get-tuple-element.65.refs_0_) | copy-start | bytes 1572868
  122.2 38.3 %copy-start.1 = (f32[512,256]{1,0:T(8,128)S(1)}, f32[512,256]{1,0:T(8,128)}, u32[]{:S(2)}) copy-start(f32[512,256]{1,0:T(8,128)} %get-tuple-element.69.refs_4_) | copy-start | bytes 1572868
  122.2 7.9 %collective-permute-start.18 = (bf16[512,256]{1,0:T(8,128)(2,1)}, bf16[512,256]{1,0:T(8,128)(2,1)S(1)}, u32[]{:S(2)}, u32[]{:S(2)}) collective-permute-start(bf16[512,256]{1,0:T(8,128)(2,1)} %get-tuple-element.66), channel_id=1, source_target_pairs={{0,8},{8,16},{16,24},{24,0},{32,40},{40,48},{48,56},{56,32},{64,72... | collective-permute-start | bytes 786440 | tf_op jit(solution)/shard_map/ppermute | solution.py:522
  123.5 9.1 %collective-permute-start.26 = (bf16[256,512]{1,0:T(8,128)(2,1)S(1)}, bf16[256,512]{1,0:T(8,128)(2,1)S(1)}, u32[]{:S(2)}, u32[]{:S(2)}) collective-permute-start(bf16[256,512]{1,0:T(8,128)(2,1)S(1)} %get-tuple-element.75.rest_0_), channel_id=1, source_target_pairs={{0,32},{8,40},{16,48},{24,56},{32,64},{40,72},{48,80},{56,88},{64,... | collective-permute-start | bytes 786440 | tf_op jit(solution)/shard_map/ppermute | solution.py:31
  130.1 7.9 %collective-permute-start.25 = (bf16[256,512]{1,0:T(8,128)(2,1)S(1)}, bf16[256,512]{1,0:T(8,128)(2,1)S(1)}, u32[]{:S(2)}, u32[]{:S(2)}) collective-permute-start(bf16[256,512]{1,0:T(8,128)(2,1)S(1)} %get-tuple-element.75.rest_0_), channel_id=1, source_target_pairs={{0,64},{8,72},{16,80},{24,88},{32,96},{40,104},{48,112},{56,120},{... | collective-permute-start | bytes 786440 | tf_op jit(solution)/shard_map/ppermute | solution.py:31
  132.6 13.0 %collective-permute-start.31 = (bf16[512,512]{1,0:T(8,128)(2,1)S(1)}, bf16[512,512]{1,0:T(8,128)(2,1)S(1)}, u32[]{:S(2)}, u32[]{:S(2)}) collective-permute-start(bf16[512,512]{1,0:T(8,128)(2,1)S(1)} %collective-permute-done.27.rest_4_), channel_id=1, source_target_pairs={{0,1},{1,0},{2,3},{3,2},{4,5},{5,4},{6,7},{7,6},{8,9},{9,8},{10,11... | collective-permute-start | bytes 1572872 | tf_op jit(solution)/shard_map/ppermute | solution.py:512
  132.6 14.4 %collective-permute-start.34 = (bf16[512,512]{1,0:T(8,128)(2,1)S(1)}, bf16[512,512]{1,0:T(8,128)(2,1)S(1)}, u32[]{:S(2)}, u32[]{:S(2)}) collective-permute-start(bf16[512,512]{1,0:T(8,128)(2,1)S(1)} %collective-permute-done.30.rest_7_), channel_id=1, source_target_pairs={{0,1},{1,0},{2,3},{3,2},{4,5},{5,4},{6,7},{7,6},{8,9},{9,8},{10,11... | collective-permute-start | bytes 1572872 | tf_op jit(solution)/shard_map/ppermute | solution.py:512
  133.1 14.3 %collective-permute-start.33 = (bf16[512,512]{1,0:T(8,128)(2,1)S(1)}, bf16[512,512]{1,0:T(8,128)(2,1)S(1)}, u32[]{:S(2)}, u32[]{:S(2)}) collective-permute-start(bf16[512,512]{1,0:T(8,128)(2,1)S(1)} %collective-permute-done.29.rest_6_), channel_id=1, source_target_pairs={{0,1},{1,0},{2,3},{3,2},{4,5},{5,4},{6,7},{7,6},{8,9},{9,8},{10,11... | collective-permute-start | bytes 1572872 | tf_op jit(solution)/shard_map/ppermute | solution.py:512
  133.2 18.1 %collective-permute-start.32 = (bf16[512,512]{1,0:T(8,128)(2,1)S(1)}, bf16[512,512]{1,0:T(8,128)(2,1)S(1)}, u32[]{:S(2)}, u32[]{:S(2)}) collective-permute-start(bf16[512,512]{1,0:T(8,128)(2,1)S(1)} %collective-permute-done.28.rest_5_), channel_id=1, source_target_pairs={{0,1},{1,0},{2,3},{3,2},{4,5},{5,4},{6,7},{7,6},{8,9},{9,8},{10,11... | collective-permute-start | bytes 1572872 | tf_op jit(solution)/shard_map/ppermute | solution.py:512
  138.0 6.4 %collective-permute-start.24 = (bf16[256,512]{1,0:T(8,128)(2,1)S(1)}, bf16[256,512]{1,0:T(8,128)(2,1)S(1)}, u32[]{:S(2)}, u32[]{:S(2)}) collective-permute-start(bf16[256,512]{1,0:T(8,128)(2,1)S(1)} %get-tuple-element.75.rest_0_), channel_id=1, source_target_pairs={{0,96},{8,104},{16,112},{24,120},{32,0},{40,8},{48,16},{56,24},{64... | collective-permute-start | bytes 786440 | tf_op jit(solution)/shard_map/ppermute | solution.py:31
  144.3 9.5 %collective-permute-start.19 = (bf16[512,256]{1,0:T(8,128)(2,1)S(1)}, bf16[512,256]{1,0:T(8,128)(2,1)S(1)}, u32[]{:S(2)}, u32[]{:S(2)}) collective-permute-start(bf16[512,256]{1,0:T(8,128)(2,1)S(1)} %copy-done.17), channel_id=1, source_target_pairs={{0,16},{8,24},{16,0},{24,8},{32,48},{40,56},{48,32},{56,40},{64,80... | collective-permute-start | bytes 786440 | tf_op jit(solution)/shard_map/ppermute | solution.py:522
  145.6 10.7 %collective-permute-start.20 = (bf16[512,256]{1,0:T(8,128)(2,1)S(1)}, bf16[512,256]{1,0:T(8,128)(2,1)S(1)}, u32[]{:S(2)}, u32[]{:S(2)}) collective-permute-start(bf16[512,256]{1,0:T(8,128)(2,1)S(1)} %copy-done.16), channel_id=1, source_target_pairs={{0,24},{8,0},{16,8},{24,16},{32,56},{40,32},{48,40},{56,48},{64,88... | collective-permute-start | bytes 786440 | tf_op jit(solution)/shard_map/ppermute | solution.py:522
  147.0 10.9 %collective-permute-start.21 = (bf16[512,256]{1,0:T(8,128)(2,1)S(1)}, bf16[512,256]{1,0:T(8,128)(2,1)S(1)}, u32[]{:S(2)}, u32[]{:S(2)}) collective-permute-start(bf16[512,256]{1,0:T(8,128)(2,1)S(1)} %copy-done.15), channel_id=1, source_target_pairs={{0,32},{8,40},{16,48},{24,56},{32,64},{40,72},{48,80},{56,88},{64,... | collective-permute-start | bytes 786440 | tf_op jit(solution)/shard_map/ppermute | solution.py:522
  147.5 13.1 %collective-permute-start.22 = (bf16[512,256]{1,0:T(8,128)(2,1)S(1)}, bf16[512,256]{1,0:T(8,128)(2,1)S(1)}, u32[]{:S(2)}, u32[]{:S(2)}) collective-permute-start(bf16[512,256]{1,0:T(8,128)(2,1)S(1)} %copy-done.14), channel_id=1, source_target_pairs={{0,64},{8,72},{16,80},{24,88},{32,96},{40,104},{48,112},{56,120},{... | collective-permute-start | bytes 786440 | tf_op jit(solution)/shard_map/ppermute | solution.py:522
  151.4 9.1 %collective-permute-start.23 = (bf16[512,256]{1,0:T(8,128)(2,1)S(1)}, bf16[512,256]{1,0:T(8,128)(2,1)S(1)}, u32[]{:S(2)}, u32[]{:S(2)}) collective-permute-start(bf16[512,256]{1,0:T(8,128)(2,1)S(1)} %copy-done.13), channel_id=1, source_target_pairs={{0,96},{8,104},{16,112},{24,120},{32,0},{40,8},{48,16},{56,24},{64... | collective-permute-start | bytes 786440 | tf_op jit(solution)/shard_map/ppermute | solution.py:522
  153.8 8.3 %collective-permute-start.35 = (bf16[256,256]{1,0:T(8,128)(2,1)S(1)}, bf16[256,256]{1,0:T(8,128)(2,1)S(1)}, u32[]{:S(2)}, u32[]{:S(2)}) collective-permute-start(bf16[256,256]{1,0:T(8,128)(2,1)S(1)} %get-tuple-element.77), channel_id=1, source_target_pairs={{0,8},{8,16},{16,24},{24,0},{32,40},{40,48},{48,56},{56,32},{64,72... | collective-permute-start | bytes 393224 | tf_op jit(solution)/shard_map/ppermute | solution.py:522
  156.4 6.5 %collective-permute-start.36 = (bf16[256,256]{1,0:T(8,128)(2,1)S(1)}, bf16[256,256]{1,0:T(8,128)(2,1)S(1)}, u32[]{:S(2)}, u32[]{:S(2)}) collective-permute-start(bf16[256,256]{1,0:T(8,128)(2,1)S(1)} %get-tuple-element.78), channel_id=1, source_target_pairs={{0,16},{8,24},{16,0},{24,8},{32,48},{40,56},{48,32},{56,40},{64,80... | collective-permute-start | bytes 393224 | tf_op jit(solution)/shard_map/ppermute | solution.py:522
  158.0 6.5 %collective-permute-start.37 = (bf16[256,256]{1,0:T(8,128)(2,1)S(1)}, bf16[256,256]{1,0:T(8,128)(2,1)S(1)}, u32[]{:S(2)}, u32[]{:S(2)}) collective-permute-start(bf16[256,256]{1,0:T(8,128)(2,1)S(1)} %get-tuple-element.79), channel_id=1, source_target_pairs={{0,24},{8,0},{16,8},{24,16},{32,56},{40,32},{48,40},{56,48},{64,88... | collective-permute-start | bytes 393224 | tf_op jit(solution)/shard_map/ppermute | solution.py:522
  (14 other events, 39.6 us)

commit v5 on v4

--- a/solution.py
+++ b/solution.py
@@ -458,7 +458,7 @@
             pltpu.VMEM((2, SIDE, rows, span), jnp.bfloat16),
             pltpu.SemaphoreType.DMA((8,)),
         ],
-        compiler_params=pltpu.CompilerParams(vmem_limit_bytes=16 << 20),
+        compiler_params=pltpu.CompilerParams(vmem_limit_bytes=62 << 20),
         cost_estimate=pl.CostEstimate(flops=10**6, bytes_accessed=2 << 20, transcendentals=0),
         name="query_sums",
     )(*parts_0, *parts_1)
@@ -504,7 +504,9 @@
             pairs.append((n, new_z % SIDE * 32 + zxyc[1] * 8 + new_y % SIDE * 2 + zxyc[3]))
         return pairs
 
-    moved = lax.ppermute(layer_input, ("sp", "tp"), over_zy(lambda a, b: (b, a + b)))
+    everywhere = ("sp", "tp")
+    moved = lax.ppermute(layer_input, everywhere, over_zy(lambda a, b: (a, a + b)))
+    moved = lax.ppermute(moved, everywhere, over_zy(lambda a, b: (b - a, b)))
     inputs = [moved]
     for r in range(1, SIDE):
         inputs.append(lax.ppermute(moved, "tp", [(p, (p - 2 * r) % 8) for p in range(8)]))

time: 168 us -> 164 us (0.976)
  blocking collectives: 22.6 us -> 14.6 us
  starting transfers between devices: 56.1 us -> 61.8 us
  local copies, waits for them, and re-layouts: 6.36 us -> 4.65 us
    all_to_all x1, blocking collectives: 22.6 us -> 14.6 us  [local(): gates = lax.all_to_all(gates, 'sp', 0, 0, tiled=True)]
    ppermute x15, waiting for transfers between devices: 17.1 us -> 9.2 us  [arrived(): lax.ppermute(parts[r], 'sp', axis_perm(r))]
    ppermute x15, waiting for transfers between devices: 18.7 us -> 25.7 us  [fetched(): parts.append(lax.ppermute(array, 'sp', axis_perm(-r)))]
    ppermute x1 -> x2, starting transfers between devices: 0.87 us -> 7.06 us  [the longest x1 5.37 us: local(): lax.ppermute(layer_input, everywhere, over_zy(lambda a, b: (a, a + b)))]
    ppermute x15, starting transfers between devices: 30.3 us -> 25.4 us  [arrived(): lax.ppermute(parts[r], 'sp', axis_perm(r))]
    ppermute x3, starting transfers between devices: 0.01 us -> 4.22 us  [local(): lax.ppermute(moved, 'tp', [(p, (p - 2 * r) % 8) for p in range(8)])]
    unnamed x49 -> x41, local copies, waits for them, and re-layouts: 5.06 us -> 3.36 us
  transfers between devices with their start and end apart: 38 -> 39, of which waited for: 15 -> 13; matrix products, arithmetic and copies ran while one was open for 0% -> 0% of each run, Pallas kernels for 22% -> 27%
where the time goes in v5:
time: 164 us; the launch traced here: 161 us
  starting transfers between devices  61.8 us (38%)
  Pallas kernels  44.2 us (27%)
  waiting for transfers between devices  34.9 us (21%)
  blocking collectives  14.6 us (9%)
  local copies, waits for them, and re-layouts  4.65 us (3%)
    ppermute x15, waiting for transfers between devices, fetched(): parts.append(lax.ppermute(array, 'sp', axis_perm(-r)))  25.7 us
    ppermute x15, starting transfers between devices, arrived(): lax.ppermute(parts[r], 'sp', axis_perm(r))  25.4 us
    ppermute x15, starting transfers between devices, fetched(): parts.append(lax.ppermute(array, 'sp', axis_perm(-r)))  24.1 us
    pallas_call x1, Pallas kernels, grads_call(): pl.pallas_call(grads_kernel, out_shape=shapes(HEAD, span) + shapes(span,...  20.1 us
    pallas_call x2, Pallas kernels, stats_call(): pl.pallas_call(functools.partial(stats_kernel, slots, pair_count, pair_of...  17.7 us
    all_to_all x1, blocking collectives, local(): gates = lax.all_to_all(gates, 'sp', 0, 0, tiled=True)  14.6 us
    ppermute x15, waiting for transfers between devices, arrived(): lax.ppermute(parts[r], 'sp', axis_perm(r))  9.2 us
    ppermute x1, starting transfers between devices, local(): lax.ppermute(layer_input, everywhere, over_zy(lambda a, b: (a, a + b)))  5.37 us
  transfers between devices with their start and end apart: 39, of which 13 were waited for; matrix products, arithmetic and copies ran while one was open for 0% of the time, Pallas kernels for 27%

profile of v5, /device:TPU:0, one launch (start us, length us, event | category | flops | bytes accessed | tf_op | source)
XLA Modules:
  0.0 161.3 jit_solution(12607592241236389387)
XLA Ops:
  0.7 1.2 fusion.2
  2.1 2.1 %collective-permute-start.1 = (bf16[512,512]{1,0:T(8,128)(2,1)S(1)}, bf16[512,512]{1,0:T(8,128)(2,1)S(1)}, u32[]{:S(2)}, u32[]{:S(2)}) collective-permute-start(bf16[512,512]{1,0:T(8,128)(2,1)S(1)} %pad_maximum_fusion.rest_0_), channel_id=1, source_target_pairs={{0,32},{8,40},{16,48},{24,56},{32,64},{40,72},{48,80},{56,88},{64,... | collective-permute-start | bytes 1572872 | tf_op jit(solution)/shard_map/ppermute | solution.py:31
  4.2 2.2 %collective-permute-start = (bf16[512,512]{1,0:T(8,128)(2,1)S(1)}, bf16[512,512]{1,0:T(8,128)(2,1)S(1)}, u32[]{:S(2)}, u32[]{:S(2)}) collective-permute-start(bf16[512,512]{1,0:T(8,128)(2,1)S(1)} %pad_maximum_fusion.rest_0_), channel_id=1, source_target_pairs={{0,96},{8,104},{16,112},{24,120},{32,0},{40,8},{48,16},{56,24},{64... | collective-permute-start | bytes 1572872 | tf_op jit(solution)/shard_map/ppermute | solution.py:31
  6.5 1.6 collective-permute-start.3
  8.0 1.7 %collective-permute-start.2 = (bf16[512,512]{1,0:T(8,128)(2,1)S(1)}, bf16[512,512]{1,0:T(8,128)(2,1)}, u32[]{:S(2)}, u32[]{:S(2)}) collective-permute-start(bf16[512,512]{1,0:T(8,128)(2,1)S(1)} %pad_maximum_fusion.1.rest_3_.rest_4_), channel_id=1, source_target_pairs={{0,24},{8,0},{16,8},{24,16},{32,56},{40,32},{48,40},{56,48},{64,88... | collective-permute-start | bytes 1572872 | tf_op jit(solution)/shard_map/ppermute | solution.py:31
  9.8 1.8 %collective-permute-start.4 = (bf16[512,512]{1,0:T(8,128)(2,1)S(1)}, bf16[512,512]{1,0:T(8,128)(2,1)}, u32[]{:S(2)}, u32[]{:S(2)}) collective-permute-start(bf16[512,512]{1,0:T(8,128)(2,1)S(1)} %pad_maximum_fusion.rest_0_), channel_id=1, source_target_pairs={{0,64},{8,72},{16,80},{24,88},{32,96},{40,104},{48,112},{56,120},{... | collective-permute-start | bytes 1572872 | tf_op jit(solution)/shard_map/ppermute | solution.py:31
  11.6 6.7 %collective-permute-done.1.rest_2_.rest_3_ = bf16[512,512]{1,0:T(8,128)(2,1)S(1)} collective-permute-done((bf16[512,512]{1,0:T(8,128)(2,1)S(1)}, bf16[512,512]{1,0:T(8,128)(2,1)S(1)}, u32[]{:S(2)}, u32[]{:S(2)}) %collective-permute-start.1) | collective-permute-done | bytes 524320 | tf_op jit(solution)/shard_map/ppermute | solution.py:31
  18.2 3.0 %collective-permute-start.5 = (bf16[512,512]{1,0:T(8,128)(2,1)S(1)}, bf16[512,512]{1,0:T(8,128)(2,1)}, u32[]{:S(2)}, u32[]{:S(2)}) collective-permute-start(bf16[512,512]{1,0:T(8,128)(2,1)S(1)} %pad_maximum_fusion.1.rest_3_.rest_4_), channel_id=1, source_target_pairs={{0,16},{8,24},{16,0},{24,8},{32,48},{40,56},{48,32},{56,40},{64,80... | collective-permute-start | bytes 1572872 | tf_op jit(solution)/shard_map/ppermute | solution.py:31
  21.3 7.6 %collective-permute-done.rest_1_ = bf16[512,512]{1,0:T(8,128)(2,1)S(1)} collective-permute-done((bf16[512,512]{1,0:T(8,128)(2,1)S(1)}, bf16[512,512]{1,0:T(8,128)(2,1)S(1)}, u32[]{:S(2)}, u32[]{:S(2)}) %collective-permute-start) | collective-permute-done | bytes 524320 | tf_op jit(solution)/shard_map/ppermute | solution.py:31
  28.8 5.4 %collective-permute-start.27 = (bf16[512,512]{1,0:T(8,128)(2,1)}, bf16[512,512]{1,0:T(8,128)(2,1)}, u32[]{:S(2)}, u32[]{:S(2)}) collective-permute-start(bf16[512,512]{1,0:T(8,128)(2,1)} %param.10), channel_id=1, source_target_pairs={{0,0},{1,1},{2,2},{3,3},{4,4},{5,5},{6,6},{7,7},{8,8},{9,9},{10,10... | collective-permute-start | bytes 1572872 | tf_op jit(solution)/shard_map/ppermute | solution.py:508
  34.2 14.6 %all_to_all.5.bias_ref = f32[16,2,512]{2,1,0:T(2,128)} all-to-all(f32[16,2,512]{2,1,0:T(2,128)S(1)} %broadcast_in_dim.3), channel_id=1, replica_groups=mesh['sp'=16,'tp'=8] {'sp'}, dimensions={0} | all-to-all | bytes 131072 | tf_op jit(solution)/shard_map/all_to_all | solution.py:488
  48.9 0.8 copy-done.7
  49.7 10.2 %stats.2 = (f32[4,8,512]{2,1,0:T(8,128)}, f32[4,8,512]{2,1,0:T(8,128)}, f32[32,512]{1,0:T(8,128)}) custom-call(f32[16,2,512]{2,1,0:T(2,128)} %all_to_all.5.bias_ref, bf16[512,512]{1,0:T(8,128)(2,1)} %copy-done.3, bf16[512,512]{1,0:T(8,128)(2,1)} %copy-done.6, bf16[512,512]{1,0:T(8,128)(2,1)} %copy-done.5, bf16[512,512]{1,0:T(8,128)(2,1)} %copy-done.4, ...), custom_call_target="tpu_custom_call" | custom-call | flops 1207959552 | bytes 4194304 | tf_op jit(solution)/shard_map/stats/pallas_call | solution.py:372
  60.0 7.5 %stats.3 = (f32[4,8,512]{2,1,0:T(8,128)}, f32[4,8,512]{2,1,0:T(8,128)}) custom-call(f32[32,512]{1,0:T(8,128)} %get-tuple-element.42.bias_ref, bf16[512,512]{1,0:T(8,128)(2,1)} %copy-done.3, bf16[512,512]{1,0:T(8,128)(2,1)} %copy-done.6, bf16[512,512]{1,0:T(8,128)(2,1)} %collective-permute-done.4.rest_2_, bf16[512,512]{1,0:T(8,128)(2,1)} %copy-done.5, ...), custom_call_target="tpu_custom_call" | custom-call | flops 939524096 | bytes 4194304 | tf_op jit(solution)/shard_map/stats/pallas_call | solution.py:372
  68.0 2.1 %collective-permute-start.7 = (f32[4,8,512]{2,1,0:T(8,128)}, f32[4,8,512]{2,1,0:T(8,128)S(1)}, u32[]{:S(2)}, u32[]{:S(2)}) collective-permute-start(f32[4,8,512]{2,1,0:T(8,128)} %get-tuple-element.45.rest_8_), channel_id=1, source_target_pairs={{0,64},{8,72},{16,80},{24,88},{32,96},{40,104},{48,112},{56,120},{... | collective-permute-start | bytes 196616 | tf_op jit(solution)/shard_map/ppermute | solution.py:31
  70.1 1.2 collective-permute-start.6
  71.9 2.1 %collective-permute-start.10 = (f32[4,8,512]{2,1,0:T(8,128)}, f32[4,8,512]{2,1,0:T(8,128)S(1)}, u32[]{:S(2)}, u32[]{:S(2)}) collective-permute-start(f32[4,8,512]{2,1,0:T(8,128)} %get-tuple-element.46.rest_12_), channel_id=1, source_target_pairs={{0,16},{8,24},{16,0},{24,8},{32,48},{40,56},{48,32},{56,40},{64,80... | collective-permute-start | bytes 196616 | tf_op jit(solution)/shard_map/ppermute | solution.py:31
  74.0 1.3 collective-permute-start.9
  75.3 1.7 %collective-permute-start.28 = (bf16[512,512]{1,0:T(8,128)(2,1)}, bf16[512,512]{1,0:T(8,128)(2,1)S(1)}, u32[]{:S(2)}, u32[]{:S(2)}) collective-permute-start(bf16[512,512]{1,0:T(8,128)(2,1)} %collective-permute-done.27), channel_id=1, source_target_pairs={{0,0},{1,1},{2,34},{3,35},{4,68},{5,69},{6,102},{7,103},{8,8},{9,9... | collective-permute-start | bytes 1572872 | tf_op jit(solution)/shard_map/ppermute | solution.py:509
  77.0 0.8 collective-permute-done.10.rest_14_
  77.9 0.7 collective-permute-done.9.rest_13_
  79.2 20.1 %grads.1 = (f32[128,512]{1,0:T(8,128)}, bf16[128,512]{1,0:T(8,128)(2,1)}, bf16[128,512]{1,0:T(8,128)(2,1)}, bf16[128,512]{1,0:T(8,128)(2,1)}, f32[128,512]{1,0:T...) custom-call(f32[32,512]{1,0:T(8,128)} %get-tuple-element.42.bias_ref, ...), custom_call_target="tpu_custom_call" | custom-call | flops 5704253440 | bytes 8388608 | tf_op jit(solution)/shard_map/grads/pallas_call | solution.py:395
  99.3 1.9 %collective-permute-start.12 = (bf16[128,512]{1,0:T(8,128)(2,1)}, bf16[128,512]{1,0:T(8,128)(2,1)S(1)}, u32[]{:S(2)}, u32[]{:S(2)}) collective-permute-start(bf16[128,512]{1,0:T(8,128)(2,1)} %get-tuple-element.48), channel_id=1, source_target_pairs={{0,32},{8,40},{16,48},{24,56},{32,64},{40,72},{48,80},{56,88},{64,... | collective-permute-start | bytes 393224 | tf_op jit(solution)/shard_map/ppermute | solution.py:524
  101.2 2.7 %collective-permute-start.13 = (bf16[128,512]{1,0:T(8,128)(2,1)}, bf16[128,512]{1,0:T(8,128)(2,1)S(1)}, u32[]{:S(2)}, u32[]{:S(2)}) collective-permute-start(bf16[128,512]{1,0:T(8,128)(2,1)} %get-tuple-element.49), channel_id=1, source_target_pairs={{0,64},{8,72},{16,80},{24,88},{32,96},{40,104},{48,112},{56,120},{... | collective-permute-start | bytes 393224 | tf_op jit(solution)/shard_map/ppermute | solution.py:524
  104.4 1.3 collective-permute-start.15
  106.4 2.7 %collective-permute-start.16 = (bf16[128,512]{1,0:T(8,128)(2,1)}, bf16[128,512]{1,0:T(8,128)(2,1)}, u32[]{:S(2)}, u32[]{:S(2)}) collective-permute-start(bf16[128,512]{1,0:T(8,128)(2,1)} %get-tuple-element.53), channel_id=1, source_target_pairs={{0,16},{8,24},{16,0},{24,8},{32,48},{40,56},{48,32},{56,40},{64,80... | collective-permute-start | bytes 393224 | tf_op jit(solution)/shard_map/ppermute | solution.py:524
  109.5 2.1 %collective-permute-start.17 = (bf16[128,512]{1,0:T(8,128)(2,1)}, bf16[128,512]{1,0:T(8,128)(2,1)}, u32[]{:S(2)}, u32[]{:S(2)}) collective-permute-start(bf16[128,512]{1,0:T(8,128)(2,1)} %get-tuple-element.54), channel_id=1, source_target_pairs={{0,24},{8,0},{16,8},{24,16},{32,56},{40,32},{48,40},{56,48},{64,88... | collective-permute-start | bytes 393224 | tf_op jit(solution)/shard_map/ppermute | solution.py:524
  111.6 1.8 %collective-permute-start.30 = (bf16[512,512]{1,0:T(8,128)(2,1)S(1)}, bf16[512,512]{1,0:T(8,128)(2,1)S(1)}, u32[]{:S(2)}, u32[]{:S(2)}) collective-permute-start(bf16[512,512]{1,0:T(8,128)(2,1)S(1)} %collective-permute-done.28.rest_4_), channel_id=1, source_target_pairs={{0,4},{1,5},{2,6},{3,7},{4,0},{5,1},{6,2},{7,3},{8,12},{9,13},{10,... | collective-permute-start | bytes 1572872 | tf_op jit(solution)/shard_map/ppermute | solution.py:512
  113.4 1.8 %collective-permute-start.29 = (bf16[512,512]{1,0:T(8,128)(2,1)S(1)}, bf16[512,512]{1,0:T(8,128)(2,1)}, u32[]{:S(2)}, u32[]{:S(2)}) collective-permute-start(bf16[512,512]{1,0:T(8,128)(2,1)S(1)} %collective-permute-done.28.rest_4_), channel_id=1, source_target_pairs={{0,6},{1,7},{2,0},{3,1},{4,2},{5,3},{6,4},{7,5},{8,14},{9,15},{10,... | collective-permute-start | bytes 1572872 | tf_op jit(solution)/shard_map/ppermute | solution.py:512
  115.3 2.3 %query_sums.1 = (bf16[256,512]{1,0:T(8,128)(2,1)}, f32[512,256]{1,0:T(8,128)}) custom-call(f32[128,512]{1,0:T(8,128)} %get-tuple-element.47.refs_0_, bf16[128,512]{1,0:T(8,128)(2,1)} %copy-done.10, bf16[128,512]{1,0:T(8,128)(2,1)} %copy-done.11, bf16[128,512]{1,0:T(8,128)(2,1)} %copy-done.12, f32[128,512]{1,0:T(8,128)} %get-tuple-element.51.refs_4_, ...), custom_call_target="tpu_custom_call" | custom-call | flops 1000000 | bytes 2097152 | tf_op jit(solution)/shard_map/query_sums/pallas_call | solution.py:448
  117.7 1.5 collective-permute-start.18
  119.2 6.4 %collective-permute-done.18.refs_1_ = bf16[512,256]{1,0:T(8,128)(2,1)S(1)} collective-permute-done((bf16[512,256]{1,0:T(8,128)(2,1)}, bf16[512,256]{1,0:T(8,128)(2,1)S(1)}, u32[]{:S(2)}, u32[]{:S(2)}) %collective-permute-start.18) | collective-permute-done | bytes 262176 | tf_op jit(solution)/shard_map/ppermute | solution.py:524
  125.5 1.7 %collective-permute-start.25 = (bf16[256,512]{1,0:T(8,128)(2,1)}, bf16[256,512]{1,0:T(8,128)(2,1)S(1)}, u32[]{:S(2)}, u32[]{:S(2)}) collective-permute-start(bf16[256,512]{1,0:T(8,128)(2,1)} %get-tuple-element.75.rest_0_), channel_id=1, source_target_pairs={{0,64},{8,72},{16,80},{24,88},{32,96},{40,104},{48,112},{56,120},{... | collective-permute-start | bytes 786440 | tf_op jit(solution)/shard_map/ppermute | solution.py:31
  128.3 5.4 %collective-permute-done.25.rest_2_ = bf16[256,512]{1,0:T(8,128)(2,1)S(1)} collective-permute-done((bf16[256,512]{1,0:T(8,128)(2,1)}, bf16[256,512]{1,0:T(8,128)(2,1)S(1)}, u32[]{:S(2)}, u32[]{:S(2)}) %collective-permute-start.25) | collective-permute-done | bytes 262176 | tf_op jit(solution)/shard_map/ppermute | solution.py:31
  133.6 2.1 %collective-permute-start.24 = (bf16[256,512]{1,0:T(8,128)(2,1)}, bf16[256,512]{1,0:T(8,128)(2,1)S(1)}, u32[]{:S(2)}, u32[]{:S(2)}) collective-permute-start(bf16[256,512]{1,0:T(8,128)(2,1)} %get-tuple-element.75.rest_0_), channel_id=1, source_target_pairs={{0,96},{8,104},{16,112},{24,120},{32,0},{40,8},{48,16},{56,24},{64... | collective-permute-start | bytes 786440 | tf_op jit(solution)/shard_map/ppermute | solution.py:31
  135.7 4.5 %collective-permute-done.24.rest_1_ = bf16[256,512]{1,0:T(8,128)(2,1)S(1)} collective-permute-done((bf16[256,512]{1,0:T(8,128)(2,1)}, bf16[256,512]{1,0:T(8,128)(2,1)S(1)}, u32[]{:S(2)}, u32[]{:S(2)}) %collective-permute-start.24) | collective-permute-done | bytes 262176 | tf_op jit(solution)/shard_map/ppermute | solution.py:31
  140.2 1.4 collective-permute-start.19
  141.6 1.5 collective-permute-start.20
  143.1 1.0 collective-permute-start.21
  144.0 2.4 %collective-permute-start.22 = (bf16[512,256]{1,0:T(8,128)(2,1)}, bf16[512,256]{1,0:T(8,128)(2,1)S(1)}, u32[]{:S(2)}, u32[]{:S(2)}) collective-permute-start(bf16[512,256]{1,0:T(8,128)(2,1)} %get-tuple-element.71), channel_id=1, source_target_pairs={{0,64},{8,72},{16,80},{24,88},{32,96},{40,104},{48,112},{56,120},{... | collective-permute-start | bytes 786440 | tf_op jit(solution)/shard_map/ppermute | solution.py:524
  146.9 0.9 copy-done.2
  147.8 2.5 %weight.1 = (f32[256,256]{1,0:T(8,128)S(1)}, bf16[256,256]{1,0:T(8,128)(2,1)S(1)}, bf16[256,256]{1,0:T(8,128)(2,1)S(1)}, bf16[256,256]{1,0:T(8,128)(2,1)S(1)}) custom-call(bf16[256,512]{1,0:T(8,128)(2,1)S(1)} %copy-done.2, bf16[256,512]{1,0:T(8,128)(2,1)S(1)} %collective-permute-done.24.rest_1_, bf16[256,512]{1,0:T(8,128)(2,1)S(1)} %collective-permute-done.25.rest_2_, ...), custom_call_target="tpu_custom_call" | custom-call | flops 1073741824 | bytes 6291456 | tf_op jit(solution)/shard_map/weight/pallas_call | solution.py:428
  150.4 0.9 collective-permute-start.36
  151.5 2.6 %collective-permute-start.37 = (bf16[256,256]{1,0:T(8,128)(2,1)S(1)}, bf16[256,256]{1,0:T(8,128)(2,1)S(1)}, u32[]{:S(2)}, u32[]{:S(2)}) collective-permute-start(bf16[256,256]{1,0:T(8,128)(2,1)S(1)} %get-tuple-element.78), channel_id=1, source_target_pairs={{0,16},{8,24},{16,0},{24,8},{32,48},{40,56},{48,32},{56,40},{64,80... | collective-permute-start | bytes 393224 | tf_op jit(solution)/shard_map/ppermute | solution.py:524
  154.1 2.5 %collective-permute-start.38 = (bf16[256,256]{1,0:T(8,128)(2,1)S(1)}, bf16[256,256]{1,0:T(8,128)(2,1)S(1)}, u32[]{:S(2)}, u32[]{:S(2)}) collective-permute-start(bf16[256,256]{1,0:T(8,128)(2,1)S(1)} %get-tuple-element.79), channel_id=1, source_target_pairs={{0,24},{8,0},{16,8},{24,16},{32,56},{40,32},{48,40},{56,48},{64,88... | collective-permute-start | bytes 393224 | tf_op jit(solution)/shard_map/ppermute | solution.py:524
  156.7 1.6 key_sums.1
  158.4 1.9 %collective-permute-done.38 = bf16[256,256]{1,0:T(8,128)(2,1)S(1)} collective-permute-done((bf16[256,256]{1,0:T(8,128)(2,1)S(1)}, bf16[256,256]{1,0:T(8,128)(2,1)S(1)}, u32[]{:S(2)}, u32[]{:S(2)}) %collective-permute-start.38) | collective-permute-done | bytes 131104 | tf_op jit(solution)/shard_map/ppermute | solution.py:524
  160.4 0.8 copy.10
  (84 shorter events, 5.6 us)
Async XLA Ops:
  2.1 7.7 %copy-start.3 = (bf16[512,512]{1,0:T(8,128)(2,1)}, bf16[512,512]{1,0:T(8,128)(2,1)S(1)}, u32[]{:S(2)}) copy-start(bf16[512,512]{1,0:T(8,128)(2,1)S(1)} %pad_maximum_fusion.rest_0_) | copy-start | bytes 1572868
  2.1 16.1 %collective-permute-start.1 = (bf16[512,512]{1,0:T(8,128)(2,1)S(1)}, bf16[512,512]{1,0:T(8,128)(2,1)S(1)}, u32[]{:S(2)}, u32[]{:S(2)}) collective-permute-start(bf16[512,512]{1,0:T(8,128)(2,1)S(1)} %pad_maximum_fusion.rest_0_), channel_id=1, source_target_pairs={{0,32},{8,40},{16,48},{24,56},{32,64},{40,72},{48,80},{56,88},{64,... | collective-permute-start | bytes 1572872 | tf_op jit(solution)/shard_map/ppermute | solution.py:31
  4.2 24.7 %collective-permute-start = (bf16[512,512]{1,0:T(8,128)(2,1)S(1)}, bf16[512,512]{1,0:T(8,128)(2,1)S(1)}, u32[]{:S(2)}, u32[]{:S(2)}) collective-permute-start(bf16[512,512]{1,0:T(8,128)(2,1)S(1)} %pad_maximum_fusion.rest_0_), channel_id=1, source_target_pairs={{0,96},{8,104},{16,112},{24,120},{32,0},{40,8},{48,16},{56,24},{64... | collective-permute-start | bytes 1572872 | tf_op jit(solution)/shard_map/ppermute | solution.py:31
  6.4 27.8 %copy-start.13 = (f32[512,2]{0,1:T(2,128)S(1)}, f32[512,2]{0,1:T(2,128)}, u32[]{:S(2)}) copy-start(f32[512,2]{0,1:T(2,128)} %param.9) | copy-start | bytes 12292
  6.5 43.3 %copy-start.4 = (bf16[512,512]{1,0:T(8,128)(2,1)}, bf16[512,512]{1,0:T(8,128)(2,1)S(1)}, u32[]{:S(2)}) copy-start(bf16[512,512]{1,0:T(8,128)(2,1)S(1)} %pad_maximum_fusion.1.rest_3_.rest_4_) | copy-start | bytes 1572868
  6.5 42.4 %collective-permute-start.3 = (bf16[512,512]{1,0:T(8,128)(2,1)S(1)}, bf16[512,512]{1,0:T(8,128)(2,1)S(1)}, u32[]{:S(2)}, u32[]{:S(2)}) collective-permute-start(bf16[512,512]{1,0:T(8,128)(2,1)S(1)} %pad_maximum_fusion.1.rest_3_.rest_4_), channel_id=1, source_target_pairs={{0,8},{8,16},{16,24},{24,0},{32,40},{40,48},{48,56},{56,32},{64,72... | collective-permute-start | bytes 1572872 | tf_op jit(solution)/shard_map/ppermute | solution.py:31
  8.0 41.7 %collective-permute-start.2 = (bf16[512,512]{1,0:T(8,128)(2,1)S(1)}, bf16[512,512]{1,0:T(8,128)(2,1)}, u32[]{:S(2)}, u32[]{:S(2)}) collective-permute-start(bf16[512,512]{1,0:T(8,128)(2,1)S(1)} %pad_maximum_fusion.1.rest_3_.rest_4_), channel_id=1, source_target_pairs={{0,24},{8,0},{16,8},{24,16},{32,56},{40,32},{48,40},{56,48},{64,88... | collective-permute-start | bytes 1572872 | tf_op jit(solution)/shard_map/ppermute | solution.py:31
  9.8 50.2 %collective-permute-start.4 = (bf16[512,512]{1,0:T(8,128)(2,1)S(1)}, bf16[512,512]{1,0:T(8,128)(2,1)}, u32[]{:S(2)}, u32[]{:S(2)}) collective-permute-start(bf16[512,512]{1,0:T(8,128)(2,1)S(1)} %pad_maximum_fusion.rest_0_), channel_id=1, source_target_pairs={{0,64},{8,72},{16,80},{24,88},{32,96},{40,104},{48,112},{56,120},{... | collective-permute-start | bytes 1572872 | tf_op jit(solution)/shard_map/ppermute | solution.py:31
  18.2 31.5 %copy-start.5 = (bf16[512,512]{1,0:T(8,128)(2,1)}, bf16[512,512]{1,0:T(8,128)(2,1)S(1)}, u32[]{:S(2)}) copy-start(bf16[512,512]{1,0:T(8,128)(2,1)S(1)} %collective-permute-done.1.rest_2_.rest_3_) | copy-start | bytes 1572868
  18.2 41.7 %collective-permute-start.5 = (bf16[512,512]{1,0:T(8,128)(2,1)S(1)}, bf16[512,512]{1,0:T(8,128)(2,1)}, u32[]{:S(2)}, u32[]{:S(2)}) collective-permute-start(bf16[512,512]{1,0:T(8,128)(2,1)S(1)} %pad_maximum_fusion.1.rest_3_.rest_4_), channel_id=1, source_target_pairs={{0,16},{8,24},{16,0},{24,8},{32,48},{40,56},{48,32},{56,40},{64,80... | collective-permute-start | bytes 1572872 | tf_op jit(solution)/shard_map/ppermute | solution.py:31
  28.8 20.0 %copy-start.6 = (bf16[512,512]{1,0:T(8,128)(2,1)}, bf16[512,512]{1,0:T(8,128)(2,1)S(1)}, u32[]{:S(2)}) copy-start(bf16[512,512]{1,0:T(8,128)(2,1)S(1)} %collective-permute-done.rest_1_) | copy-start | bytes 1572868
  28.8 43.0 %collective-permute-start.27 = (bf16[512,512]{1,0:T(8,128)(2,1)}, bf16[512,512]{1,0:T(8,128)(2,1)}, u32[]{:S(2)}, u32[]{:S(2)}) collective-permute-start(bf16[512,512]{1,0:T(8,128)(2,1)} %param.10), channel_id=1, source_target_pairs={{0,0},{1,1},{2,2},{3,3},{4,4},{5,5},{6,6},{7,7},{8,8},{9,9},{10,10... | collective-permute-start | bytes 1572872 | tf_op jit(solution)/shard_map/ppermute | solution.py:508
  67.4 6.6 %collective-permute-start.8 = (f32[4,8,512]{2,1,0:T(8,128)}, f32[4,8,512]{2,1,0:T(8,128)S(1)}, u32[]{:S(2)}, u32[]{:S(2)}) collective-permute-start(f32[4,8,512]{2,1,0:T(8,128)} %get-tuple-element.45.rest_8_), channel_id=1, source_target_pairs={{0,32},{8,40},{16,48},{24,56},{32,64},{40,72},{48,80},{56,88},{64,... | collective-permute-start | bytes 196616 | tf_op jit(solution)/shard_map/ppermute | solution.py:31
  68.0 7.3 %collective-permute-start.7 = (f32[4,8,512]{2,1,0:T(8,128)}, f32[4,8,512]{2,1,0:T(8,128)S(1)}, u32[]{:S(2)}, u32[]{:S(2)}) collective-permute-start(f32[4,8,512]{2,1,0:T(8,128)} %get-tuple-element.45.rest_8_), channel_id=1, source_target_pairs={{0,64},{8,72},{16,80},{24,88},{32,96},{40,104},{48,112},{56,120},{... | collective-permute-start | bytes 196616 | tf_op jit(solution)/shard_map/ppermute | solution.py:31
  70.1 6.9 %collective-permute-start.6 = (f32[4,8,512]{2,1,0:T(8,128)}, f32[4,8,512]{2,1,0:T(8,128)S(1)}, u32[]{:S(2)}, u32[]{:S(2)}) collective-permute-start(f32[4,8,512]{2,1,0:T(8,128)} %get-tuple-element.45.rest_8_), channel_id=1, source_target_pairs={{0,96},{8,104},{16,112},{24,120},{32,0},{40,8},{48,16},{56,24},{64... | collective-permute-start | bytes 196616 | tf_op jit(solution)/shard_map/ppermute | solution.py:31
  71.3 5.7 %collective-permute-start.11 = (f32[4,8,512]{2,1,0:T(8,128)}, f32[4,8,512]{2,1,0:T(8,128)S(1)}, u32[]{:S(2)}, u32[]{:S(2)}) collective-permute-start(f32[4,8,512]{2,1,0:T(8,128)} %get-tuple-element.46.rest_12_), channel_id=1, source_target_pairs={{0,8},{8,16},{16,24},{24,0},{32,40},{40,48},{48,56},{56,32},{64,72... | collective-permute-start | bytes 196616 | tf_op jit(solution)/shard_map/ppermute | solution.py:31
  71.9 6.0 %collective-permute-start.10 = (f32[4,8,512]{2,1,0:T(8,128)}, f32[4,8,512]{2,1,0:T(8,128)S(1)}, u32[]{:S(2)}, u32[]{:S(2)}) collective-permute-start(f32[4,8,512]{2,1,0:T(8,128)} %get-tuple-element.46.rest_12_), channel_id=1, source_target_pairs={{0,16},{8,24},{16,0},{24,8},{32,48},{40,56},{48,32},{56,40},{64,80... | collective-permute-start | bytes 196616 | tf_op jit(solution)/shard_map/ppermute | solution.py:31
  74.0 4.5 %collective-permute-start.9 = (f32[4,8,512]{2,1,0:T(8,128)}, f32[4,8,512]{2,1,0:T(8,128)S(1)}, u32[]{:S(2)}, u32[]{:S(2)}) collective-permute-start(f32[4,8,512]{2,1,0:T(8,128)} %get-tuple-element.46.rest_12_), channel_id=1, source_target_pairs={{0,24},{8,0},{16,8},{24,16},{32,56},{40,32},{48,40},{56,48},{64,88... | collective-permute-start | bytes 196616 | tf_op jit(solution)/shard_map/ppermute | solution.py:31
  75.3 30.4 %collective-permute-start.28 = (bf16[512,512]{1,0:T(8,128)(2,1)}, bf16[512,512]{1,0:T(8,128)(2,1)S(1)}, u32[]{:S(2)}, u32[]{:S(2)}) collective-permute-start(bf16[512,512]{1,0:T(8,128)(2,1)} %collective-permute-done.27), channel_id=1, source_target_pairs={{0,0},{1,1},{2,34},{3,35},{4,68},{5,69},{6,102},{7,103},{8,8},{9,9... | collective-permute-start | bytes 1572872 | tf_op jit(solution)/shard_map/ppermute | solution.py:509
  99.3 7.0 %collective-permute-start.12 = (bf16[128,512]{1,0:T(8,128)(2,1)}, bf16[128,512]{1,0:T(8,128)(2,1)S(1)}, u32[]{:S(2)}, u32[]{:S(2)}) collective-permute-start(bf16[128,512]{1,0:T(8,128)(2,1)} %get-tuple-element.48), channel_id=1, source_target_pairs={{0,32},{8,40},{16,48},{24,56},{32,64},{40,72},{48,80},{56,88},{64,... | collective-permute-start | bytes 393224 | tf_op jit(solution)/shard_map/ppermute | solution.py:524
  101.2 8.2 %collective-permute-start.13 = (bf16[128,512]{1,0:T(8,128)(2,1)}, bf16[128,512]{1,0:T(8,128)(2,1)S(1)}, u32[]{:S(2)}, u32[]{:S(2)}) collective-permute-start(bf16[128,512]{1,0:T(8,128)(2,1)} %get-tuple-element.49), channel_id=1, source_target_pairs={{0,64},{8,72},{16,80},{24,88},{32,96},{40,104},{48,112},{56,120},{... | collective-permute-start | bytes 393224 | tf_op jit(solution)/shard_map/ppermute | solution.py:524
  103.9 7.7 %collective-permute-start.14 = (bf16[128,512]{1,0:T(8,128)(2,1)}, bf16[128,512]{1,0:T(8,128)(2,1)S(1)}, u32[]{:S(2)}, u32[]{:S(2)}) collective-permute-start(bf16[128,512]{1,0:T(8,128)(2,1)} %get-tuple-element.50), channel_id=1, source_target_pairs={{0,96},{8,104},{16,112},{24,120},{32,0},{40,8},{48,16},{56,24},{64... | collective-permute-start | bytes 393224 | tf_op jit(solution)/shard_map/ppermute | solution.py:524
  104.4 9.0 %collective-permute-start.15 = (bf16[128,512]{1,0:T(8,128)(2,1)}, bf16[128,512]{1,0:T(8,128)(2,1)}, u32[]{:S(2)}, u32[]{:S(2)}) collective-permute-start(bf16[128,512]{1,0:T(8,128)(2,1)} %get-tuple-element.52), channel_id=1, source_target_pairs={{0,8},{8,16},{16,24},{24,0},{32,40},{40,48},{48,56},{56,32},{64,72... | collective-permute-start | bytes 393224 | tf_op jit(solution)/shard_map/ppermute | solution.py:524
  105.7 21.5 %collective-permute-start.31 = (bf16[512,512]{1,0:T(8,128)(2,1)S(1)}, bf16[512,512]{1,0:T(8,128)(2,1)S(1)}, u32[]{:S(2)}, u32[]{:S(2)}) collective-permute-start(bf16[512,512]{1,0:T(8,128)(2,1)S(1)} %collective-permute-done.28.rest_4_), channel_id=1, source_target_pairs={{0,2},{1,3},{2,4},{3,5},{4,6},{5,7},{6,0},{7,1},{8,10},{9,11},{10,... | collective-permute-start | bytes 1572872 | tf_op jit(solution)/shard_map/ppermute | solution.py:512
  106.3 9.0 %copy-start.10 = (bf16[128,512]{1,0:T(8,128)(2,1)}, bf16[128,512]{1,0:T(8,128)(2,1)S(1)}, u32[]{:S(2)}) copy-start(bf16[128,512]{1,0:T(8,128)(2,1)S(1)} %collective-permute-done.12.refs_1_) | copy-start | bytes 393220
  106.4 8.9 %collective-permute-start.16 = (bf16[128,512]{1,0:T(8,128)(2,1)}, bf16[128,512]{1,0:T(8,128)(2,1)}, u32[]{:S(2)}, u32[]{:S(2)}) collective-permute-start(bf16[128,512]{1,0:T(8,128)(2,1)} %get-tuple-element.53), channel_id=1, source_target_pairs={{0,16},{8,24},{16,0},{24,8},{32,48},{40,56},{48,32},{56,40},{64,80... | collective-permute-start | bytes 393224 | tf_op jit(solution)/shard_map/ppermute | solution.py:524
  109.5 5.9 %copy-start.11 = (bf16[128,512]{1,0:T(8,128)(2,1)}, bf16[128,512]{1,0:T(8,128)(2,1)S(1)}, u32[]{:S(2)}) copy-start(bf16[128,512]{1,0:T(8,128)(2,1)S(1)} %collective-permute-done.13.refs_2_) | copy-start | bytes 393220
  109.5 5.8 %collective-permute-start.17 = (bf16[128,512]{1,0:T(8,128)(2,1)}, bf16[128,512]{1,0:T(8,128)(2,1)}, u32[]{:S(2)}, u32[]{:S(2)}) collective-permute-start(bf16[128,512]{1,0:T(8,128)(2,1)} %get-tuple-element.54), channel_id=1, source_target_pairs={{0,24},{8,0},{16,8},{24,16},{32,56},{40,32},{48,40},{56,48},{64,88... | collective-permute-start | bytes 393224 | tf_op jit(solution)/shard_map/ppermute | solution.py:524
  111.6 16.1 %collective-permute-start.30 = (bf16[512,512]{1,0:T(8,128)(2,1)S(1)}, bf16[512,512]{1,0:T(8,128)(2,1)S(1)}, u32[]{:S(2)}, u32[]{:S(2)}) collective-permute-start(bf16[512,512]{1,0:T(8,128)(2,1)S(1)} %collective-permute-done.28.rest_4_), channel_id=1, source_target_pairs={{0,4},{1,5},{2,6},{3,7},{4,0},{5,1},{6,2},{7,3},{8,12},{9,13},{10,... | collective-permute-start | bytes 1572872 | tf_op jit(solution)/shard_map/ppermute | solution.py:512
  113.4 14.4 %collective-permute-start.29 = (bf16[512,512]{1,0:T(8,128)(2,1)S(1)}, bf16[512,512]{1,0:T(8,128)(2,1)}, u32[]{:S(2)}, u32[]{:S(2)}) collective-permute-start(bf16[512,512]{1,0:T(8,128)(2,1)S(1)} %collective-permute-done.28.rest_4_), channel_id=1, source_target_pairs={{0,6},{1,7},{2,0},{3,1},{4,2},{5,3},{6,4},{7,5},{8,14},{9,15},{10,... | collective-permute-start | bytes 1572872 | tf_op jit(solution)/shard_map/ppermute | solution.py:512
  117.7 39.0 %copy-start = (f32[512,256]{1,0:T(8,128)S(1)}, f32[512,256]{1,0:T(8,128)}, u32[]{:S(2)}) copy-start(f32[512,256]{1,0:T(8,128)} %get-tuple-element.65.refs_0_) | copy-start | bytes 1572868
  117.7 39.0 %copy-start.1 = (f32[512,256]{1,0:T(8,128)S(1)}, f32[512,256]{1,0:T(8,128)}, u32[]{:S(2)}) copy-start(f32[512,256]{1,0:T(8,128)} %get-tuple-element.69.refs_4_) | copy-start | bytes 1572868
  117.7 7.9 %collective-permute-start.18 = (bf16[512,256]{1,0:T(8,128)(2,1)}, bf16[512,256]{1,0:T(8,128)(2,1)S(1)}, u32[]{:S(2)}, u32[]{:S(2)}) collective-permute-start(bf16[512,256]{1,0:T(8,128)(2,1)} %get-tuple-element.66), channel_id=1, source_target_pairs={{0,8},{8,16},{16,24},{24,0},{32,40},{40,48},{48,56},{56,32},{64,72... | collective-permute-start | bytes 786440 | tf_op jit(solution)/shard_map/ppermute | solution.py:524
  119.1 8.1 %collective-permute-start.26 = (bf16[256,512]{1,0:T(8,128)(2,1)}, bf16[256,512]{1,0:T(8,128)(2,1)S(1)}, u32[]{:S(2)}, u32[]{:S(2)}) collective-permute-start(bf16[256,512]{1,0:T(8,128)(2,1)} %get-tuple-element.75.rest_0_), channel_id=1, source_target_pairs={{0,32},{8,40},{16,48},{24,56},{32,64},{40,72},{48,80},{56,88},{64,... | collective-permute-start | bytes 786440 | tf_op jit(solution)/shard_map/ppermute | solution.py:31
  125.5 8.1 %collective-permute-start.25 = (bf16[256,512]{1,0:T(8,128)(2,1)}, bf16[256,512]{1,0:T(8,128)(2,1)S(1)}, u32[]{:S(2)}, u32[]{:S(2)}) collective-permute-start(bf16[256,512]{1,0:T(8,128)(2,1)} %get-tuple-element.75.rest_0_), channel_id=1, source_target_pairs={{0,64},{8,72},{16,80},{24,88},{32,96},{40,104},{48,112},{56,120},{... | collective-permute-start | bytes 786440 | tf_op jit(solution)/shard_map/ppermute | solution.py:31
  127.2 14.4 %collective-permute-start.32 = (bf16[512,512]{1,0:T(8,128)(2,1)S(1)}, bf16[512,512]{1,0:T(8,128)(2,1)S(1)}, u32[]{:S(2)}, u32[]{:S(2)}) collective-permute-start(bf16[512,512]{1,0:T(8,128)(2,1)S(1)} %collective-permute-done.28.rest_4_), channel_id=1, source_target_pairs={{0,1},{1,0},{2,3},{3,2},{4,5},{5,4},{6,7},{7,6},{8,9},{9,8},{10,11... | collective-permute-start | bytes 1572872 | tf_op jit(solution)/shard_map/ppermute | solution.py:514
  127.2 15.8 %collective-permute-start.35 = (bf16[512,512]{1,0:T(8,128)(2,1)S(1)}, bf16[512,512]{1,0:T(8,128)(2,1)S(1)}, u32[]{:S(2)}, u32[]{:S(2)}) collective-permute-start(bf16[512,512]{1,0:T(8,128)(2,1)S(1)} %collective-permute-done.31.rest_7_), channel_id=1, source_target_pairs={{0,1},{1,0},{2,3},{3,2},{4,5},{5,4},{6,7},{7,6},{8,9},{9,8},{10,11... | collective-permute-start | bytes 1572872 | tf_op jit(solution)/shard_map/ppermute | solution.py:514
  127.7 16.3 %collective-permute-start.34 = (bf16[512,512]{1,0:T(8,128)(2,1)S(1)}, bf16[512,512]{1,0:T(8,128)(2,1)S(1)}, u32[]{:S(2)}, u32[]{:S(2)}) collective-permute-start(bf16[512,512]{1,0:T(8,128)(2,1)S(1)} %collective-permute-done.30.rest_6_), channel_id=1, source_target_pairs={{0,1},{1,0},{2,3},{3,2},{4,5},{5,4},{6,7},{7,6},{8,9},{9,8},{10,11... | collective-permute-start | bytes 1572872 | tf_op jit(solution)/shard_map/ppermute | solution.py:514
  127.8 18.7 %collective-permute-start.33 = (bf16[512,512]{1,0:T(8,128)(2,1)}, bf16[512,512]{1,0:T(8,128)(2,1)S(1)}, u32[]{:S(2)}, u32[]{:S(2)}) collective-permute-start(bf16[512,512]{1,0:T(8,128)(2,1)} %collective-permute-done.29.rest_5_), channel_id=1, source_target_pairs={{0,1},{1,0},{2,3},{3,2},{4,5},{5,4},{6,7},{7,6},{8,9},{9,8},{10,11... | collective-permute-start | bytes 1572872 | tf_op jit(solution)/shard_map/ppermute | solution.py:514
  133.6 6.6 %collective-permute-start.24 = (bf16[256,512]{1,0:T(8,128)(2,1)}, bf16[256,512]{1,0:T(8,128)(2,1)S(1)}, u32[]{:S(2)}, u32[]{:S(2)}) collective-permute-start(bf16[256,512]{1,0:T(8,128)(2,1)} %get-tuple-element.75.rest_0_), channel_id=1, source_target_pairs={{0,96},{8,104},{16,112},{24,120},{32,0},{40,8},{48,16},{56,24},{64... | collective-permute-start | bytes 786440 | tf_op jit(solution)/shard_map/ppermute | solution.py:31
  140.2 10.1 %collective-permute-start.19 = (bf16[512,256]{1,0:T(8,128)(2,1)}, bf16[512,256]{1,0:T(8,128)(2,1)S(1)}, u32[]{:S(2)}, u32[]{:S(2)}) collective-permute-start(bf16[512,256]{1,0:T(8,128)(2,1)} %get-tuple-element.67), channel_id=1, source_target_pairs={{0,16},{8,24},{16,0},{24,8},{32,48},{40,56},{48,32},{56,40},{64,80... | collective-permute-start | bytes 786440 | tf_op jit(solution)/shard_map/ppermute | solution.py:524
  141.6 9.9 %collective-permute-start.20 = (bf16[512,256]{1,0:T(8,128)(2,1)}, bf16[512,256]{1,0:T(8,128)(2,1)S(1)}, u32[]{:S(2)}, u32[]{:S(2)}) collective-permute-start(bf16[512,256]{1,0:T(8,128)(2,1)} %get-tuple-element.68), channel_id=1, source_target_pairs={{0,24},{8,0},{16,8},{24,16},{32,56},{40,32},{48,40},{56,48},{64,88... | collective-permute-start | bytes 786440 | tf_op jit(solution)/shard_map/ppermute | solution.py:524
  143.1 11.0 %collective-permute-start.21 = (bf16[512,256]{1,0:T(8,128)(2,1)}, bf16[512,256]{1,0:T(8,128)(2,1)S(1)}, u32[]{:S(2)}, u32[]{:S(2)}) collective-permute-start(bf16[512,256]{1,0:T(8,128)(2,1)} %get-tuple-element.70), channel_id=1, source_target_pairs={{0,32},{8,40},{16,48},{24,56},{32,64},{40,72},{48,80},{56,88},{64,... | collective-permute-start | bytes 786440 | tf_op jit(solution)/shard_map/ppermute | solution.py:524
  144.0 12.6 %collective-permute-start.22 = (bf16[512,256]{1,0:T(8,128)(2,1)}, bf16[512,256]{1,0:T(8,128)(2,1)S(1)}, u32[]{:S(2)}, u32[]{:S(2)}) collective-permute-start(bf16[512,256]{1,0:T(8,128)(2,1)} %get-tuple-element.71), channel_id=1, source_target_pairs={{0,64},{8,72},{16,80},{24,88},{32,96},{40,104},{48,112},{56,120},{... | collective-permute-start | bytes 786440 | tf_op jit(solution)/shard_map/ppermute | solution.py:524
  146.5 10.2 %collective-permute-start.23 = (bf16[512,256]{1,0:T(8,128)(2,1)}, bf16[512,256]{1,0:T(8,128)(2,1)S(1)}, u32[]{:S(2)}, u32[]{:S(2)}) collective-permute-start(bf16[512,256]{1,0:T(8,128)(2,1)} %get-tuple-element.72), channel_id=1, source_target_pairs={{0,96},{8,104},{16,112},{24,120},{32,0},{40,8},{48,16},{56,24},{64... | collective-permute-start | bytes 786440 | tf_op jit(solution)/shard_map/ppermute | solution.py:524
  150.4 7.9 %collective-permute-start.36 = (bf16[256,256]{1,0:T(8,128)(2,1)S(1)}, bf16[256,256]{1,0:T(8,128)(2,1)S(1)}, u32[]{:S(2)}, u32[]{:S(2)}) collective-permute-start(bf16[256,256]{1,0:T(8,128)(2,1)S(1)} %get-tuple-element.77), channel_id=1, source_target_pairs={{0,8},{8,16},{16,24},{24,0},{32,40},{40,48},{48,56},{56,32},{64,72... | collective-permute-start | bytes 393224 | tf_op jit(solution)/shard_map/ppermute | solution.py:524
  151.5 7.0 %collective-permute-start.37 = (bf16[256,256]{1,0:T(8,128)(2,1)S(1)}, bf16[256,256]{1,0:T(8,128)(2,1)S(1)}, u32[]{:S(2)}, u32[]{:S(2)}) collective-permute-start(bf16[256,256]{1,0:T(8,128)(2,1)S(1)} %get-tuple-element.78), channel_id=1, source_target_pairs={{0,16},{8,24},{16,0},{24,8},{32,48},{40,56},{48,32},{56,40},{64,80... | collective-permute-start | bytes 393224 | tf_op jit(solution)/shard_map/ppermute | solution.py:524
  154.1 6.3 %collective-permute-start.38 = (bf16[256,256]{1,0:T(8,128)(2,1)S(1)}, bf16[256,256]{1,0:T(8,128)(2,1)S(1)}, u32[]{:S(2)}, u32[]{:S(2)}) collective-permute-start(bf16[256,256]{1,0:T(8,128)(2,1)S(1)} %get-tuple-element.79), channel_id=1, source_target_pairs={{0,24},{8,0},{16,8},{24,16},{32,56},{40,32},{48,40},{56,48},{64,88... | collective-permute-start | bytes 393224 | tf_op jit(solution)/shard_map/ppermute | solution.py:524
  (11 other events, 20.2 us)

commit v6 on v5

--- a/solution.py
+++ b/solution.py
@@ -25,11 +25,10 @@
     return [(4 * z + x, 4 * z + (x + r) % SIDE) for z in range(SIDE) for x in range(SIDE)]
 
 
-def fetched(array, axis_perm):
-    parts = [array]
-    for r in range(1, SIDE):
-        parts.append(lax.ppermute(array, "sp", axis_perm(-r)))
-    return parts
+def fetched(array, axis_perm, axis="sp"):
+    after, before = (lax.ppermute(array, axis, axis_perm(-r)) for r in (1, SIDE - 1))
+    across = lax.ppermute(after, axis, axis_perm(-1))
+    return [array, after, across, before]
 
 
 def dot_nt(a, b):
@@ -320,15 +319,9 @@
 
 
 def query_kernel(*refs):
-    parts, (low_ref, grad_ref, own, sent, sems) = refs[:8], refs[8:]
-    begin = copy_list(sems)
-    loads = []
-    for h in range(2):
-        loads.append([begin(parts[SIDE * h], own.at[h])])
-        loads[h] += [begin(parts[SIDE * h + r], sent.at[h, r]) for r in range(1, SIDE)]
-    for h in range(2):
-        wait_all(loads[h])
-        total = own[h] + sum(sent[h, r].astype(jnp.float32) for r in range(1, SIDE))
+    parts, (low_ref, grad_ref) = refs[:8], refs[8:]
+    for h in range(2):
+        total = sum(ref[...].astype(jnp.float32) for ref in parts[SIDE * h : SIDE * (h + 1)])
         cut = slice(h * HEAD, (h + 1) * HEAD)
         low_ref[cut, :] = total.astype(jnp.bfloat16)
         grad_ref[:, cut] = total.T
@@ -451,14 +444,9 @@
             jax.ShapeDtypeStruct((2 * rows, span), jnp.bfloat16),
             jax.ShapeDtypeStruct((span, 2 * rows), jnp.float32),
         ],
-        in_specs=[ANY] * 8,
+        in_specs=[VM] * 8,
         out_specs=[VM] * 2,
-        scratch_shapes=[
-            pltpu.VMEM((2, rows, span), jnp.float32),
-            pltpu.VMEM((2, SIDE, rows, span), jnp.bfloat16),
-            pltpu.SemaphoreType.DMA((8,)),
-        ],
-        compiler_params=pltpu.CompilerParams(vmem_limit_bytes=62 << 20),
+        compiler_params=pltpu.CompilerParams(vmem_limit_bytes=16 << 20),
         cost_estimate=pl.CostEstimate(flops=10**6, bytes_accessed=2 << 20, transcendentals=0),
         name="query_sums",
     )(*parts_0, *parts_1)
@@ -507,9 +495,7 @@
     everywhere = ("sp", "tp")
     moved = lax.ppermute(layer_input, everywhere, over_zy(lambda a, b: (a, a + b)))
     moved = lax.ppermute(moved, everywhere, over_zy(lambda a, b: (b - a, b)))
-    inputs = [moved]
-    for r in range(1, SIDE):
-        inputs.append(lax.ppermute(moved, "tp", [(p, (p - 2 * r) % 8) for p in range(8)]))
+    inputs = fetched(moved, lambda r: [(p, (p + 2 * r) % 8) for p in range(8)], "tp")
     for part in list(inputs):
         inputs.append(lax.ppermute(part, "tp", [(p, p ^ 1) for p in range(8)]))
 
@@ -531,7 +517,8 @@
     terms = weight_call(low_parts, inputs)
     terms = arrived(terms, along_x)
     weight_grad = sum(part.astype(jnp.float32) for part in terms).T
-    dkv_0, dkv_1 = arrived(dkv_0, along_x), arrived(dkv_1, along_z)
+    dkv_0 = arrived(dkv_0, along_x)
+    dkv_1 = arrived(dkv_1, along_z)
     key_grad, value_grad = keys_call(dkv_0, dkv_1)
     return (query_grad, key_grad, value_grad, weight_grad)
 

time: 164 us -> 161 us (0.982); the launches traced: 161 us -> 160 us
  starting transfers between devices: 61.8 us -> 55.1 us
  blocking collectives: 14.6 us -> 18.1 us
  waiting for transfers between devices: 34.9 us -> 37.6 us
  Pallas kernels: 44.2 us -> 42.2 us
    ppermute x15, waiting for transfers between devices: 9.2 us -> 25.7 us  [arrived(): lax.ppermute(parts[r], 'sp', axis_perm(r))]
    ppermute x18, waiting for transfers between devices: 25.7 us -> 11.9 us  [the longest x12 11.1 us: fetched(): lax.ppermute(array, axis, axis_perm(-r))]
    ppermute x15, starting transfers between devices: 25.4 us -> 13.9 us  [arrived(): lax.ppermute(parts[r], 'sp', axis_perm(r))]
    ppermute x18, starting transfers between devices: 28.3 us -> 37.5 us  [the longest x12 21.2 us: fetched(): lax.ppermute(array, axis, axis_perm(-r))]
    ppermute x1, starting transfers between devices: 5.37 us -> 1.44 us  [local(): lax.ppermute(layer_input, everywhere, over_zy(lambda a, b: (a, a + b)))]
    all_to_all x1, blocking collectives: 14.6 us -> 18.1 us  [local(): gates = lax.all_to_all(gates, 'sp', 0, 0, tiled=True)]
    unnamed x41 -> x45, local copies, waits for them, and re-layouts: 3.36 us -> 4.87 us
  transfers between devices with their start and end apart: 39 -> 39, of which waited for: 13 -> 12; matrix products, arithmetic and copies ran while one was open for 0% -> 0% of each run, Pallas kernels for 27% -> 26%
where the time goes in v6:
time: 161 us; the launch traced here: 160 us
  starting transfers between devices  55.1 us (34%)
  Pallas kernels  42.2 us (26%)
  waiting for transfers between devices  37.6 us (23%)
  blocking collectives  18.1 us (11%)
  local copies, waits for them, and re-layouts  6.17 us (4%)
    ppermute x15, waiting for transfers between devices, arrived(): lax.ppermute(parts[r], 'sp', axis_perm(r))  25.7 us
    ppermute x12, starting transfers between devices, fetched(): lax.ppermute(array, axis, axis_perm(-r))  21.2 us
    pallas_call x1, Pallas kernels, grads_call(): pl.pallas_call(grads_kernel, out_shape=shapes(HEAD, span) + shapes(span,...  20.1 us
    all_to_all x1, blocking collectives, local(): gates = lax.all_to_all(gates, 'sp', 0, 0, tiled=True)  18.1 us
    pallas_call x2, Pallas kernels, stats_call(): pl.pallas_call(functools.partial(stats_kernel, slots, pair_count, pair_of...  17.7 us
    ppermute x6, starting transfers between devices, fetched(): across = lax.ppermute(after, axis, axis_perm(-1))  16.3 us
    ppermute x15, starting transfers between devices, arrived(): lax.ppermute(parts[r], 'sp', axis_perm(r))  13.9 us
    ppermute x12, waiting for transfers between devices, fetched(): lax.ppermute(array, axis, axis_perm(-r))  11.1 us
  transfers between devices with their start and end apart: 39, of which 12 were waited for; matrix products, arithmetic and copies ran while one was open for 0% of the time, Pallas kernels for 26%

profile of v6, /device:TPU:0, one launch (start us, length us, event | category | flops | bytes accessed | tf_op | source)
XLA Modules:
  0.0 160.3 jit_solution(3004582786368934427)
XLA Ops:
  0.7 1.2 fusion.2
  2.1 4.2 %collective-permute-start = (bf16[512,512]{1,0:T(8,128)(2,1)S(1)}, bf16[512,512]{1,0:T(8,128)(2,1)}, u32[]{:S(2)}, u32[]{:S(2)}) collective-permute-start(bf16[512,512]{1,0:T(8,128)(2,1)S(1)} %pad_maximum_fusion.rest_0_), channel_id=1, source_target_pairs={{0,96},{8,104},{16,112},{24,120},{32,0},{40,8},{48,16},{56,24},{64... | collective-permute-start | bytes 1572872 | tf_op jit(solution)/shard_map/ppermute | solution.py:29
  6.4 2.8 %collective-permute-start.2 = (bf16[512,512]{1,0:T(8,128)(2,1)S(1)}, bf16[512,512]{1,0:T(8,128)(2,1)}, u32[]{:S(2)}, u32[]{:S(2)}) collective-permute-start(bf16[512,512]{1,0:T(8,128)(2,1)S(1)} %pad_maximum_fusion.1.rest_3_.rest_4_), channel_id=1, source_target_pairs={{0,24},{8,0},{16,8},{24,16},{32,56},{40,32},{48,40},{56,48},{64,88... | collective-permute-start | bytes 1572872 | tf_op jit(solution)/shard_map/ppermute | solution.py:29
  9.2 1.4 collective-permute-start.27
  10.8 6.7 %collective-permute-done.rest_1_ = bf16[512,512]{1,0:T(8,128)(2,1)} collective-permute-done((bf16[512,512]{1,0:T(8,128)(2,1)S(1)}, bf16[512,512]{1,0:T(8,128)(2,1)}, u32[]{:S(2)}, u32[]{:S(2)}) %collective-permute-start) | collective-permute-done | bytes 524320 | tf_op jit(solution)/shard_map/ppermute | solution.py:29
  17.5 3.8 %collective-permute-start.4 = (bf16[512,512]{1,0:T(8,128)(2,1)}, bf16[512,512]{1,0:T(8,128)(2,1)}, u32[]{:S(2)}, u32[]{:S(2)}) collective-permute-start(bf16[512,512]{1,0:T(8,128)(2,1)} %collective-permute-done.rest_1_), channel_id=1, source_target_pairs={{0,96},{8,104},{16,112},{24,120},{32,0},{40,8},{48,16},{56,24},{64... | collective-permute-start | bytes 1572872 | tf_op jit(solution)/shard_map/ppermute | solution.py:30
  21.3 2.8 %collective-permute-start.5 = (bf16[512,512]{1,0:T(8,128)(2,1)}, bf16[512,512]{1,0:T(8,128)(2,1)}, u32[]{:S(2)}, u32[]{:S(2)}) collective-permute-start(bf16[512,512]{1,0:T(8,128)(2,1)} %collective-permute-done.2.rest_4_.rest_5_), channel_id=1, source_target_pairs={{0,24},{8,0},{16,8},{24,16},{32,56},{40,32},{48,40},{56,48},{64,88... | collective-permute-start | bytes 1572872 | tf_op jit(solution)/shard_map/ppermute | solution.py:30
  24.1 1.7 %collective-permute-start.28 = (bf16[512,512]{1,0:T(8,128)(2,1)}, bf16[512,512]{1,0:T(8,128)(2,1)S(1)}, u32[]{:S(2)}, u32[]{:S(2)}) collective-permute-start(bf16[512,512]{1,0:T(8,128)(2,1)} %collective-permute-done.27), channel_id=1, source_target_pairs={{0,0},{1,1},{2,34},{3,35},{4,68},{5,69},{6,102},{7,103},{8,8},{9,9... | collective-permute-start | bytes 1572872 | tf_op jit(solution)/shard_map/ppermute | solution.py:497
  25.8 18.1 %all_to_all.5.bias_ref = f32[16,2,512]{2,1,0:T(2,128)} all-to-all(f32[16,2,512]{2,1,0:T(2,128)S(1)} %broadcast_in_dim.3), channel_id=1, replica_groups=mesh['sp'=16,'tp'=8] {'sp'}, dimensions={0} | all-to-all | bytes 131072 | tf_op jit(solution)/shard_map/all_to_all | solution.py:476
  43.8 0.8 copy-done.6
  44.6 10.2 %stats.2 = (f32[4,8,512]{2,1,0:T(8,128)}, f32[4,8,512]{2,1,0:T(8,128)}, f32[32,512]{1,0:T(8,128)}) custom-call(f32[16,2,512]{2,1,0:T(2,128)} %all_to_all.5.bias_ref, bf16[512,512]{1,0:T(8,128)(2,1)} %copy-done.4, bf16[512,512]{1,0:T(8,128)(2,1)} %collective-permute-done.rest_1_, bf16[512,512]{1,0:T(8,128)(2,1)} %copy-done.6, bf16[512,512]{1,0:T(8,128)(2,1)} %copy-done.5, ...), custom_call_target="tpu_custom_call" | custom-call | flops 1207959552 | bytes 4194304 | tf_op jit(solution)/shard_map/stats/pallas_call | solution.py:365
  54.9 7.5 %stats.3 = (f32[4,8,512]{2,1,0:T(8,128)}, f32[4,8,512]{2,1,0:T(8,128)}) custom-call(f32[32,512]{1,0:T(8,128)} %get-tuple-element.42.bias_ref, bf16[512,512]{1,0:T(8,128)(2,1)} %copy-done.4, bf16[512,512]{1,0:T(8,128)(2,1)} %collective-permute-done.rest_1_, bf16[512,512]{1,0:T(8,128)(2,1)} %collective-permute-done.4.rest_2_, bf16[512,512]{1,0:T(8,128)(2,1)} %copy-done.6, ...), custom_call_target="tpu_custom_call" | custom-call | flops 939524096 | bytes 4194304 | tf_op jit(solution)/shard_map/stats/pallas_call | solution.py:365
  62.3 3.8 %collective-permute-start.6 = (f32[4,8,512]{2,1,0:T(8,128)}, f32[4,8,512]{2,1,0:T(8,128)S(1)}, u32[]{:S(2)}, u32[]{:S(2)}) collective-permute-start(f32[4,8,512]{2,1,0:T(8,128)} %get-tuple-element.45.rest_8_), channel_id=1, source_target_pairs={{0,96},{8,104},{16,112},{24,120},{32,0},{40,8},{48,16},{56,24},{64... | collective-permute-start | bytes 196616 | tf_op jit(solution)/shard_map/ppermute | solution.py:29
  66.1 2.8 %collective-permute-start.9 = (f32[4,8,512]{2,1,0:T(8,128)}, f32[4,8,512]{2,1,0:T(8,128)S(1)}, u32[]{:S(2)}, u32[]{:S(2)}) collective-permute-start(f32[4,8,512]{2,1,0:T(8,128)} %get-tuple-element.46.rest_12_), channel_id=1, source_target_pairs={{0,24},{8,0},{16,8},{24,16},{32,56},{40,32},{48,40},{56,48},{64,88... | collective-permute-start | bytes 196616 | tf_op jit(solution)/shard_map/ppermute | solution.py:29
  68.9 3.3 %collective-permute-start.7 = (f32[4,8,512]{2,1,0:T(8,128)S(1)}, f32[4,8,512]{2,1,0:T(8,128)S(1)}, u32[]{:S(2)}, u32[]{:S(2)}) collective-permute-start(f32[4,8,512]{2,1,0:T(8,128)S(1)} %collective-permute-done.6.rest_9_), channel_id=1, source_target_pairs={{0,96},{8,104},{16,112},{24,120},{32,0},{40,8},{48,16},{56,24},{64... | collective-permute-start | bytes 196616 | tf_op jit(solution)/shard_map/ppermute | solution.py:30
  72.2 3.2 %collective-permute-start.10 = (f32[4,8,512]{2,1,0:T(8,128)S(1)}, f32[4,8,512]{2,1,0:T(8,128)S(1)}, u32[]{:S(2)}, u32[]{:S(2)}) collective-permute-start(f32[4,8,512]{2,1,0:T(8,128)S(1)} %collective-permute-done.9.rest_13_), channel_id=1, source_target_pairs={{0,24},{8,0},{16,8},{24,16},{32,56},{40,32},{48,40},{56,48},{64,88... | collective-permute-start | bytes 196616 | tf_op jit(solution)/shard_map/ppermute | solution.py:30
  75.4 3.3 %collective-permute-start.29 = (bf16[512,512]{1,0:T(8,128)(2,1)S(1)}, bf16[512,512]{1,0:T(8,128)(2,1)S(1)}, u32[]{:S(2)}, u32[]{:S(2)}) collective-permute-start(bf16[512,512]{1,0:T(8,128)(2,1)S(1)} %collective-permute-done.28.rest_4_), channel_id=1, source_target_pairs={{0,6},{1,7},{2,0},{3,1},{4,2},{5,3},{6,4},{7,5},{8,14},{9,15},{10,... | collective-permute-start | bytes 1572872 | tf_op jit(solution)/shard_map/ppermute | solution.py:29
  78.8 0.6 copy-done.19
  79.4 0.6 copy-done.21
  80.0 20.1 %grads.1 = (f32[128,512]{1,0:T(8,128)}, bf16[128,512]{1,0:T(8,128)(2,1)}, bf16[128,512]{1,0:T(8,128)(2,1)}, bf16[128,512]{1,0:T(8,128)(2,1)}, f32[128,512]{1,0:T...) custom-call(f32[32,512]{1,0:T(8,128)} %get-tuple-element.42.bias_ref, ...), custom_call_target="tpu_custom_call" | custom-call | flops 5704253440 | bytes 8388608 | tf_op jit(solution)/shard_map/grads/pallas_call | solution.py:388
  100.2 1.5 collective-permute-start.13
  101.7 2.1 %collective-permute-start.30 = (bf16[512,512]{1,0:T(8,128)(2,1)S(1)}, bf16[512,512]{1,0:T(8,128)(2,1)S(1)}, u32[]{:S(2)}, u32[]{:S(2)}) collective-permute-start(bf16[512,512]{1,0:T(8,128)(2,1)S(1)} %collective-permute-done.29.rest_5_), channel_id=1, source_target_pairs={{0,6},{1,7},{2,0},{3,1},{4,2},{5,3},{6,4},{7,5},{8,14},{9,15},{10,... | collective-permute-start | bytes 1572872 | tf_op jit(solution)/shard_map/ppermute | solution.py:30
  103.8 4.2 %collective-permute-done.12.refs_1_ = bf16[128,512]{1,0:T(8,128)(2,1)S(1)} collective-permute-done((bf16[128,512]{1,0:T(8,128)(2,1)}, bf16[128,512]{1,0:T(8,128)(2,1)S(1)}, u32[]{:S(2)}, u32[]{:S(2)}) %collective-permute-start.12) | collective-permute-done | bytes 131104 | tf_op jit(solution)/shard_map/ppermute | solution.py:510
  108.0 5.2 %collective-permute-done.14.refs_3_ = bf16[128,512]{1,0:T(8,128)(2,1)S(1)} collective-permute-done((bf16[128,512]{1,0:T(8,128)(2,1)}, bf16[128,512]{1,0:T(8,128)(2,1)S(1)}, u32[]{:S(2)}, u32[]{:S(2)}) %collective-permute-start.14) | collective-permute-done | bytes 131104 | tf_op jit(solution)/shard_map/ppermute | solution.py:510
  113.1 2.6 %collective-permute-done.15.refs_5_ = bf16[128,512]{1,0:T(8,128)(2,1)S(1)} collective-permute-done((bf16[128,512]{1,0:T(8,128)(2,1)}, bf16[128,512]{1,0:T(8,128)(2,1)S(1)}, u32[]{:S(2)}, u32[]{:S(2)}) %collective-permute-start.15) | collective-permute-done | bytes 131104 | tf_op jit(solution)/shard_map/ppermute | solution.py:510
  115.8 4.1 %collective-permute-done.16.refs_6_ = bf16[128,512]{1,0:T(8,128)(2,1)S(1)} collective-permute-done((bf16[128,512]{1,0:T(8,128)(2,1)}, bf16[128,512]{1,0:T(8,128)(2,1)S(1)}, u32[]{:S(2)}, u32[]{:S(2)}) %collective-permute-start.16) | collective-permute-done | bytes 131104 | tf_op jit(solution)/shard_map/ppermute | solution.py:510
  119.8 1.1 collective-permute-done.17.refs_7_
  120.9 0.9 copy-done.2
  121.9 0.9 copy-done.3
  122.9 1.0 query_sums.1
  123.9 2.2 %collective-permute-start.24 = (bf16[256,512]{1,0:T(8,128)(2,1)S(1)}, bf16[256,512]{1,0:T(8,128)(2,1)S(1)}, u32[]{:S(2)}, u32[]{:S(2)}) collective-permute-start(bf16[256,512]{1,0:T(8,128)(2,1)S(1)} %get-tuple-element.75.rest_0_), channel_id=1, source_target_pairs={{0,96},{8,104},{16,112},{24,120},{32,0},{40,8},{48,16},{56,24},{64... | collective-permute-start | bytes 786440 | tf_op jit(solution)/shard_map/ppermute | solution.py:29
  126.1 0.5 collective-permute-start.33
  126.7 5.0 %collective-permute-done.18.refs_1_ = bf16[512,256]{1,0:T(8,128)(2,1)S(1)} collective-permute-done((bf16[512,256]{1,0:T(8,128)(2,1)}, bf16[512,256]{1,0:T(8,128)(2,1)S(1)}, u32[]{:S(2)}, u32[]{:S(2)}) %collective-permute-start.18) | collective-permute-done | bytes 262176 | tf_op jit(solution)/shard_map/ppermute | solution.py:510
  131.7 2.0 %collective-permute-start.26 = (bf16[256,512]{1,0:T(8,128)(2,1)S(1)}, bf16[256,512]{1,0:T(8,128)(2,1)S(1)}, u32[]{:S(2)}, u32[]{:S(2)}) collective-permute-start(bf16[256,512]{1,0:T(8,128)(2,1)S(1)} %get-tuple-element.75.rest_0_), channel_id=1, source_target_pairs={{0,32},{8,40},{16,48},{24,56},{32,64},{40,72},{48,80},{56,88},{64,... | collective-permute-start | bytes 786440 | tf_op jit(solution)/shard_map/ppermute | solution.py:29
  133.7 1.2 collective-permute-start.25
  134.9 4.3 %collective-permute-done.26.rest_3_ = bf16[256,512]{1,0:T(8,128)(2,1)S(1)} collective-permute-done((bf16[256,512]{1,0:T(8,128)(2,1)S(1)}, bf16[256,512]{1,0:T(8,128)(2,1)S(1)}, u32[]{:S(2)}, u32[]{:S(2)}) %collective-permute-start.26) | collective-permute-done | bytes 262176 | tf_op jit(solution)/shard_map/ppermute | solution.py:29
  139.2 0.8 collective-permute-done.25.rest_2_
  140.1 3.6 %collective-permute-start.20 = (bf16[512,256]{1,0:T(8,128)(2,1)S(1)}, bf16[512,256]{1,0:T(8,128)(2,1)S(1)}, u32[]{:S(2)}, u32[]{:S(2)}) collective-permute-start(bf16[512,256]{1,0:T(8,128)(2,1)S(1)} %copy-done.14), channel_id=1, source_target_pairs={{0,24},{8,0},{16,8},{24,16},{32,56},{40,32},{48,40},{56,48},{64,88... | collective-permute-start | bytes 786440 | tf_op jit(solution)/shard_map/ppermute | solution.py:510
  143.6 2.1 %collective-permute-start.21 = (bf16[512,256]{1,0:T(8,128)(2,1)S(1)}, bf16[512,256]{1,0:T(8,128)(2,1)S(1)}, u32[]{:S(2)}, u32[]{:S(2)}) collective-permute-start(bf16[512,256]{1,0:T(8,128)(2,1)S(1)} %copy-done.13), channel_id=1, source_target_pairs={{0,32},{8,40},{16,48},{24,56},{32,64},{40,72},{48,80},{56,88},{64,... | collective-permute-start | bytes 786440 | tf_op jit(solution)/shard_map/ppermute | solution.py:510
  145.7 3.2 %collective-permute-start.22 = (bf16[512,256]{1,0:T(8,128)(2,1)S(1)}, bf16[512,256]{1,0:T(8,128)(2,1)S(1)}, u32[]{:S(2)}, u32[]{:S(2)}) collective-permute-start(bf16[512,256]{1,0:T(8,128)(2,1)S(1)} %copy-done.12), channel_id=1, source_target_pairs={{0,64},{8,72},{16,80},{24,88},{32,96},{40,104},{48,112},{56,120},{... | collective-permute-start | bytes 786440 | tf_op jit(solution)/shard_map/ppermute | solution.py:510
  149.0 1.8 %weight.1 = (f32[256,256]{1,0:T(8,128)S(1)}, bf16[256,256]{1,0:T(8,128)(2,1)S(1)}, bf16[256,256]{1,0:T(8,128)(2,1)S(1)}, bf16[256,256]{1,0:T(8,128)(2,1)S(1)}) custom-call(bf16[256,512]{1,0:T(8,128)(2,1)S(1)} %get-tuple-element.75.rest_0_, bf16[256,512]{1,0:T(8,128)(2,1)S(1)} %collective-permute-done.24.rest_1_, ...), custom_call_target="tpu_custom_call" | custom-call | flops 1073741824 | bytes 6291456 | tf_op jit(solution)/shard_map/weight/pallas_call | solution.py:421
  150.9 1.5 collective-permute-start.37
  152.4 1.8 %collective-permute-start.38 = (bf16[256,256]{1,0:T(8,128)(2,1)S(1)}, bf16[256,256]{1,0:T(8,128)(2,1)S(1)}, u32[]{:S(2)}, u32[]{:S(2)}) collective-permute-start(bf16[256,256]{1,0:T(8,128)(2,1)S(1)} %get-tuple-element.79), channel_id=1, source_target_pairs={{0,24},{8,0},{16,8},{24,16},{32,56},{40,32},{48,40},{56,48},{64,88... | collective-permute-start | bytes 393224 | tf_op jit(solution)/shard_map/ppermute | solution.py:510
  154.2 1.9 %collective-permute-done.22.refs_6_ = bf16[512,256]{1,0:T(8,128)(2,1)S(1)} collective-permute-done((bf16[512,256]{1,0:T(8,128)(2,1)S(1)}, bf16[512,256]{1,0:T(8,128)(2,1)S(1)}, u32[]{:S(2)}, u32[]{:S(2)}) %collective-permute-start.22) | collective-permute-done | bytes 262176 | tf_op jit(solution)/shard_map/ppermute | solution.py:510
  156.1 1.6 key_sums.1
  157.7 0.8 collective-permute-done.36
  158.5 0.9 collective-permute-done.38
  159.4 0.8 copy.10
  (88 shorter events, 0.9 us)
Async XLA Ops:
  2.1 15.4 %collective-permute-start = (bf16[512,512]{1,0:T(8,128)(2,1)S(1)}, bf16[512,512]{1,0:T(8,128)(2,1)}, u32[]{:S(2)}, u32[]{:S(2)}) collective-permute-start(bf16[512,512]{1,0:T(8,128)(2,1)S(1)} %pad_maximum_fusion.rest_0_), channel_id=1, source_target_pairs={{0,96},{8,104},{16,112},{24,120},{32,0},{40,8},{48,16},{56,24},{64... | collective-permute-start | bytes 1572872 | tf_op jit(solution)/shard_map/ppermute | solution.py:29
  6.3 19.4 %copy-start.9 = (f32[512,2]{0,1:T(2,128)S(1)}, f32[512,2]{0,1:T(2,128)}, u32[]{:S(2)}) copy-start(f32[512,2]{0,1:T(2,128)} %param.9) | copy-start | bytes 12292
  6.4 38.3 %copy-start.5 = (bf16[512,512]{1,0:T(8,128)(2,1)}, bf16[512,512]{1,0:T(8,128)(2,1)S(1)}, u32[]{:S(2)}) copy-start(bf16[512,512]{1,0:T(8,128)(2,1)S(1)} %pad_maximum_fusion.1.rest_3_.rest_4_) | copy-start | bytes 1572868
  6.4 14.9 %collective-permute-start.2 = (bf16[512,512]{1,0:T(8,128)(2,1)S(1)}, bf16[512,512]{1,0:T(8,128)(2,1)}, u32[]{:S(2)}, u32[]{:S(2)}) collective-permute-start(bf16[512,512]{1,0:T(8,128)(2,1)S(1)} %pad_maximum_fusion.1.rest_3_.rest_4_), channel_id=1, source_target_pairs={{0,24},{8,0},{16,8},{24,16},{32,56},{40,32},{48,40},{56,48},{64,88... | collective-permute-start | bytes 1572872 | tf_op jit(solution)/shard_map/ppermute | solution.py:29
  9.2 14.8 %collective-permute-start.27 = (bf16[512,512]{1,0:T(8,128)(2,1)S(1)}, bf16[512,512]{1,0:T(8,128)(2,1)}, u32[]{:S(2)}, u32[]{:S(2)}) collective-permute-start(bf16[512,512]{1,0:T(8,128)(2,1)S(1)} %copy-done.10), channel_id=1, source_target_pairs={{0,0},{1,1},{2,2},{3,3},{4,4},{5,5},{6,6},{7,7},{8,8},{9,9},{10,10... | collective-permute-start | bytes 1572872 | tf_op jit(solution)/shard_map/ppermute | solution.py:496
  10.7 33.2 %collective-permute-start.1 = (bf16[512,512]{1,0:T(8,128)(2,1)S(1)}, bf16[512,512]{1,0:T(8,128)(2,1)S(1)}, u32[]{:S(2)}, u32[]{:S(2)}) collective-permute-start(bf16[512,512]{1,0:T(8,128)(2,1)S(1)} %pad_maximum_fusion.rest_0_), channel_id=1, source_target_pairs={{0,32},{8,40},{16,48},{24,56},{32,64},{40,72},{48,80},{56,88},{64,... | collective-permute-start | bytes 1572872 | tf_op jit(solution)/shard_map/ppermute | solution.py:29
  10.8 33.9 %collective-permute-start.3 = (bf16[512,512]{1,0:T(8,128)(2,1)S(1)}, bf16[512,512]{1,0:T(8,128)(2,1)}, u32[]{:S(2)}, u32[]{:S(2)}) collective-permute-start(bf16[512,512]{1,0:T(8,128)(2,1)S(1)} %pad_maximum_fusion.1.rest_3_.rest_4_), channel_id=1, source_target_pairs={{0,8},{8,16},{16,24},{24,0},{32,40},{40,48},{48,56},{56,32},{64,72... | collective-permute-start | bytes 1572872 | tf_op jit(solution)/shard_map/ppermute | solution.py:29
  17.5 37.4 %collective-permute-start.4 = (bf16[512,512]{1,0:T(8,128)(2,1)}, bf16[512,512]{1,0:T(8,128)(2,1)}, u32[]{:S(2)}, u32[]{:S(2)}) collective-permute-start(bf16[512,512]{1,0:T(8,128)(2,1)} %collective-permute-done.rest_1_), channel_id=1, source_target_pairs={{0,96},{8,104},{16,112},{24,120},{32,0},{40,8},{48,16},{56,24},{64... | collective-permute-start | bytes 1572872 | tf_op jit(solution)/shard_map/ppermute | solution.py:30
  21.3 33.6 %collective-permute-start.5 = (bf16[512,512]{1,0:T(8,128)(2,1)}, bf16[512,512]{1,0:T(8,128)(2,1)}, u32[]{:S(2)}, u32[]{:S(2)}) collective-permute-start(bf16[512,512]{1,0:T(8,128)(2,1)} %collective-permute-done.2.rest_4_.rest_5_), channel_id=1, source_target_pairs={{0,24},{8,0},{16,8},{24,16},{32,56},{40,32},{48,40},{56,48},{64,88... | collective-permute-start | bytes 1572872 | tf_op jit(solution)/shard_map/ppermute | solution.py:30
  24.1 51.4 %collective-permute-start.28 = (bf16[512,512]{1,0:T(8,128)(2,1)}, bf16[512,512]{1,0:T(8,128)(2,1)S(1)}, u32[]{:S(2)}, u32[]{:S(2)}) collective-permute-start(bf16[512,512]{1,0:T(8,128)(2,1)} %collective-permute-done.27), channel_id=1, source_target_pairs={{0,0},{1,1},{2,34},{3,35},{4,68},{5,69},{6,102},{7,103},{8,8},{9,9... | collective-permute-start | bytes 1572872 | tf_op jit(solution)/shard_map/ppermute | solution.py:497
  62.3 6.6 %collective-permute-start.6 = (f32[4,8,512]{2,1,0:T(8,128)}, f32[4,8,512]{2,1,0:T(8,128)S(1)}, u32[]{:S(2)}, u32[]{:S(2)}) collective-permute-start(f32[4,8,512]{2,1,0:T(8,128)} %get-tuple-element.45.rest_8_), channel_id=1, source_target_pairs={{0,96},{8,104},{16,112},{24,120},{32,0},{40,8},{48,16},{56,24},{64... | collective-permute-start | bytes 196616 | tf_op jit(solution)/shard_map/ppermute | solution.py:29
  66.1 6.1 %collective-permute-start.9 = (f32[4,8,512]{2,1,0:T(8,128)}, f32[4,8,512]{2,1,0:T(8,128)S(1)}, u32[]{:S(2)}, u32[]{:S(2)}) collective-permute-start(f32[4,8,512]{2,1,0:T(8,128)} %get-tuple-element.46.rest_12_), channel_id=1, source_target_pairs={{0,24},{8,0},{16,8},{24,16},{32,56},{40,32},{48,40},{56,48},{64,88... | collective-permute-start | bytes 196616 | tf_op jit(solution)/shard_map/ppermute | solution.py:29
  68.9 6.5 %collective-permute-start.8 = (f32[4,8,512]{2,1,0:T(8,128)}, f32[4,8,512]{2,1,0:T(8,128)S(1)}, u32[]{:S(2)}, u32[]{:S(2)}) collective-permute-start(f32[4,8,512]{2,1,0:T(8,128)} %get-tuple-element.45.rest_8_), channel_id=1, source_target_pairs={{0,32},{8,40},{16,48},{24,56},{32,64},{40,72},{48,80},{56,88},{64,... | collective-permute-start | bytes 196616 | tf_op jit(solution)/shard_map/ppermute | solution.py:29
  68.9 9.8 %collective-permute-start.11 = (f32[4,8,512]{2,1,0:T(8,128)}, f32[4,8,512]{2,1,0:T(8,128)S(1)}, u32[]{:S(2)}, u32[]{:S(2)}) collective-permute-start(f32[4,8,512]{2,1,0:T(8,128)} %get-tuple-element.46.rest_12_), channel_id=1, source_target_pairs={{0,8},{8,16},{16,24},{24,0},{32,40},{40,48},{48,56},{56,32},{64,72... | collective-permute-start | bytes 196616 | tf_op jit(solution)/shard_map/ppermute | solution.py:29
  68.9 9.8 %collective-permute-start.7 = (f32[4,8,512]{2,1,0:T(8,128)S(1)}, f32[4,8,512]{2,1,0:T(8,128)S(1)}, u32[]{:S(2)}, u32[]{:S(2)}) collective-permute-start(f32[4,8,512]{2,1,0:T(8,128)S(1)} %collective-permute-done.6.rest_9_), channel_id=1, source_target_pairs={{0,96},{8,104},{16,112},{24,120},{32,0},{40,8},{48,16},{56,24},{64... | collective-permute-start | bytes 196616 | tf_op jit(solution)/shard_map/ppermute | solution.py:30
  72.2 6.5 %collective-permute-start.10 = (f32[4,8,512]{2,1,0:T(8,128)S(1)}, f32[4,8,512]{2,1,0:T(8,128)S(1)}, u32[]{:S(2)}, u32[]{:S(2)}) collective-permute-start(f32[4,8,512]{2,1,0:T(8,128)S(1)} %collective-permute-done.9.rest_13_), channel_id=1, source_target_pairs={{0,24},{8,0},{16,8},{24,16},{32,56},{40,32},{48,40},{56,48},{64,88... | collective-permute-start | bytes 196616 | tf_op jit(solution)/shard_map/ppermute | solution.py:30
  75.4 50.7 %collective-permute-start.31 = (bf16[512,512]{1,0:T(8,128)(2,1)S(1)}, bf16[512,512]{1,0:T(8,128)(2,1)S(1)}, u32[]{:S(2)}, u32[]{:S(2)}) collective-permute-start(bf16[512,512]{1,0:T(8,128)(2,1)S(1)} %collective-permute-done.28.rest_4_), channel_id=1, source_target_pairs={{0,2},{1,3},{2,4},{3,5},{4,6},{5,7},{6,0},{7,1},{8,10},{9,11},{10,... | collective-permute-start | bytes 1572872 | tf_op jit(solution)/shard_map/ppermute | solution.py:29
  75.4 26.3 %collective-permute-start.29 = (bf16[512,512]{1,0:T(8,128)(2,1)S(1)}, bf16[512,512]{1,0:T(8,128)(2,1)S(1)}, u32[]{:S(2)}, u32[]{:S(2)}) collective-permute-start(bf16[512,512]{1,0:T(8,128)(2,1)S(1)} %collective-permute-done.28.rest_4_), channel_id=1, source_target_pairs={{0,6},{1,7},{2,0},{3,1},{4,2},{5,3},{6,4},{7,5},{8,14},{9,15},{10,... | collective-permute-start | bytes 1572872 | tf_op jit(solution)/shard_map/ppermute | solution.py:29
  100.1 7.9 %collective-permute-start.12 = (bf16[128,512]{1,0:T(8,128)(2,1)}, bf16[128,512]{1,0:T(8,128)(2,1)S(1)}, u32[]{:S(2)}, u32[]{:S(2)}) collective-permute-start(bf16[128,512]{1,0:T(8,128)(2,1)} %get-tuple-element.48), channel_id=1, source_target_pairs={{0,32},{8,40},{16,48},{24,56},{32,64},{40,72},{48,80},{56,88},{64,... | collective-permute-start | bytes 393224 | tf_op jit(solution)/shard_map/ppermute | solution.py:510
  100.2 7.8 %collective-permute-start.13 = (bf16[128,512]{1,0:T(8,128)(2,1)}, bf16[128,512]{1,0:T(8,128)(2,1)S(1)}, u32[]{:S(2)}, u32[]{:S(2)}) collective-permute-start(bf16[128,512]{1,0:T(8,128)(2,1)} %get-tuple-element.49), channel_id=1, source_target_pairs={{0,64},{8,72},{16,80},{24,88},{32,96},{40,104},{48,112},{56,120},{... | collective-permute-start | bytes 393224 | tf_op jit(solution)/shard_map/ppermute | solution.py:510
  101.7 24.4 %collective-permute-start.32 = (bf16[512,512]{1,0:T(8,128)(2,1)S(1)}, bf16[512,512]{1,0:T(8,128)(2,1)S(1)}, u32[]{:S(2)}, u32[]{:S(2)}) collective-permute-start(bf16[512,512]{1,0:T(8,128)(2,1)S(1)} %collective-permute-done.28.rest_4_), channel_id=1, source_target_pairs={{0,1},{1,0},{2,3},{3,2},{4,5},{5,4},{6,7},{7,6},{8,9},{9,8},{10,11... | collective-permute-start | bytes 1572872 | tf_op jit(solution)/shard_map/ppermute | solution.py:500
  101.7 24.9 %collective-permute-start.30 = (bf16[512,512]{1,0:T(8,128)(2,1)S(1)}, bf16[512,512]{1,0:T(8,128)(2,1)S(1)}, u32[]{:S(2)}, u32[]{:S(2)}) collective-permute-start(bf16[512,512]{1,0:T(8,128)(2,1)S(1)} %collective-permute-done.29.rest_5_), channel_id=1, source_target_pairs={{0,6},{1,7},{2,0},{3,1},{4,2},{5,3},{6,4},{7,5},{8,14},{9,15},{10,... | collective-permute-start | bytes 1572872 | tf_op jit(solution)/shard_map/ppermute | solution.py:30
  108.0 5.2 %collective-permute-start.14 = (bf16[128,512]{1,0:T(8,128)(2,1)}, bf16[128,512]{1,0:T(8,128)(2,1)S(1)}, u32[]{:S(2)}, u32[]{:S(2)}) collective-permute-start(bf16[128,512]{1,0:T(8,128)(2,1)} %get-tuple-element.50), channel_id=1, source_target_pairs={{0,96},{8,104},{16,112},{24,120},{32,0},{40,8},{48,16},{56,24},{64... | collective-permute-start | bytes 393224 | tf_op jit(solution)/shard_map/ppermute | solution.py:510
  108.0 7.8 %collective-permute-start.15 = (bf16[128,512]{1,0:T(8,128)(2,1)}, bf16[128,512]{1,0:T(8,128)(2,1)S(1)}, u32[]{:S(2)}, u32[]{:S(2)}) collective-permute-start(bf16[128,512]{1,0:T(8,128)(2,1)} %get-tuple-element.52), channel_id=1, source_target_pairs={{0,8},{8,16},{16,24},{24,0},{32,40},{40,48},{48,56},{56,32},{64,72... | collective-permute-start | bytes 393224 | tf_op jit(solution)/shard_map/ppermute | solution.py:510
  113.1 6.7 %collective-permute-start.16 = (bf16[128,512]{1,0:T(8,128)(2,1)}, bf16[128,512]{1,0:T(8,128)(2,1)S(1)}, u32[]{:S(2)}, u32[]{:S(2)}) collective-permute-start(bf16[128,512]{1,0:T(8,128)(2,1)} %get-tuple-element.53), channel_id=1, source_target_pairs={{0,16},{8,24},{16,0},{24,8},{32,48},{40,56},{48,32},{56,40},{64,80... | collective-permute-start | bytes 393224 | tf_op jit(solution)/shard_map/ppermute | solution.py:510
  115.8 5.2 %collective-permute-start.17 = (bf16[128,512]{1,0:T(8,128)(2,1)}, bf16[128,512]{1,0:T(8,128)(2,1)S(1)}, u32[]{:S(2)}, u32[]{:S(2)}) collective-permute-start(bf16[128,512]{1,0:T(8,128)(2,1)} %get-tuple-element.54), channel_id=1, source_target_pairs={{0,24},{8,0},{16,8},{24,16},{32,56},{40,32},{48,40},{56,48},{64,88... | collective-permute-start | bytes 393224 | tf_op jit(solution)/shard_map/ppermute | solution.py:510
  122.8 16.4 %copy-start.15 = (bf16[512,256]{1,0:T(8,128)(2,1)S(1)}, bf16[512,256]{1,0:T(8,128)(2,1)}, u32[]{:S(2)}) copy-start(bf16[512,256]{1,0:T(8,128)(2,1)} %get-tuple-element.67) | copy-start | bytes 786436
  122.8 17.2 %copy-start.14 = (bf16[512,256]{1,0:T(8,128)(2,1)S(1)}, bf16[512,256]{1,0:T(8,128)(2,1)}, u32[]{:S(2)}) copy-start(bf16[512,256]{1,0:T(8,128)(2,1)} %get-tuple-element.68) | copy-start | bytes 786436
  122.8 20.8 %copy-start.13 = (bf16[512,256]{1,0:T(8,128)(2,1)S(1)}, bf16[512,256]{1,0:T(8,128)(2,1)}, u32[]{:S(2)}) copy-start(bf16[512,256]{1,0:T(8,128)(2,1)} %get-tuple-element.70) | copy-start | bytes 786436
  122.8 22.9 %copy-start.12 = (bf16[512,256]{1,0:T(8,128)(2,1)S(1)}, bf16[512,256]{1,0:T(8,128)(2,1)}, u32[]{:S(2)}) copy-start(bf16[512,256]{1,0:T(8,128)(2,1)} %get-tuple-element.71) | copy-start | bytes 786436
  122.8 26.1 %copy-start.11 = (bf16[512,256]{1,0:T(8,128)(2,1)S(1)}, bf16[512,256]{1,0:T(8,128)(2,1)}, u32[]{:S(2)}) copy-start(bf16[512,256]{1,0:T(8,128)(2,1)} %get-tuple-element.72) | copy-start | bytes 786436
  123.9 32.2 %copy-start = (f32[512,256]{1,0:T(8,128)S(1)}, f32[512,256]{1,0:T(8,128)}, u32[]{:S(2)}) copy-start(f32[512,256]{1,0:T(8,128)} %get-tuple-element.65.refs_0_) | copy-start | bytes 1572868
  123.9 32.2 %copy-start.1 = (f32[512,256]{1,0:T(8,128)S(1)}, f32[512,256]{1,0:T(8,128)}, u32[]{:S(2)}) copy-start(f32[512,256]{1,0:T(8,128)} %get-tuple-element.69.refs_4_) | copy-start | bytes 1572868
  123.9 7.8 %collective-permute-start.18 = (bf16[512,256]{1,0:T(8,128)(2,1)}, bf16[512,256]{1,0:T(8,128)(2,1)S(1)}, u32[]{:S(2)}, u32[]{:S(2)}) collective-permute-start(bf16[512,256]{1,0:T(8,128)(2,1)} %get-tuple-element.66), channel_id=1, source_target_pairs={{0,8},{8,16},{16,24},{24,0},{32,40},{40,48},{48,56},{56,32},{64,72... | collective-permute-start | bytes 786440 | tf_op jit(solution)/shard_map/ppermute | solution.py:510
  123.9 9.8 %collective-permute-start.24 = (bf16[256,512]{1,0:T(8,128)(2,1)S(1)}, bf16[256,512]{1,0:T(8,128)(2,1)S(1)}, u32[]{:S(2)}, u32[]{:S(2)}) collective-permute-start(bf16[256,512]{1,0:T(8,128)(2,1)S(1)} %get-tuple-element.75.rest_0_), channel_id=1, source_target_pairs={{0,96},{8,104},{16,112},{24,120},{32,0},{40,8},{48,16},{56,24},{64... | collective-permute-start | bytes 786440 | tf_op jit(solution)/shard_map/ppermute | solution.py:29
  126.1 17.6 %collective-permute-start.35 = (bf16[512,512]{1,0:T(8,128)(2,1)S(1)}, bf16[512,512]{1,0:T(8,128)(2,1)S(1)}, u32[]{:S(2)}, u32[]{:S(2)}) collective-permute-start(bf16[512,512]{1,0:T(8,128)(2,1)S(1)} %collective-permute-done.31.rest_7_), channel_id=1, source_target_pairs={{0,1},{1,0},{2,3},{3,2},{4,5},{5,4},{6,7},{7,6},{8,9},{9,8},{10,11... | collective-permute-start | bytes 1572872 | tf_op jit(solution)/shard_map/ppermute | solution.py:500
  126.1 19.6 %collective-permute-start.33 = (bf16[512,512]{1,0:T(8,128)(2,1)S(1)}, bf16[512,512]{1,0:T(8,128)(2,1)S(1)}, u32[]{:S(2)}, u32[]{:S(2)}) collective-permute-start(bf16[512,512]{1,0:T(8,128)(2,1)S(1)} %collective-permute-done.29.rest_5_), channel_id=1, source_target_pairs={{0,1},{1,0},{2,3},{3,2},{4,5},{5,4},{6,7},{7,6},{8,9},{9,8},{10,11... | collective-permute-start | bytes 1572872 | tf_op jit(solution)/shard_map/ppermute | solution.py:500
  126.6 22.4 %collective-permute-start.34 = (bf16[512,512]{1,0:T(8,128)(2,1)S(1)}, bf16[512,512]{1,0:T(8,128)(2,1)S(1)}, u32[]{:S(2)}, u32[]{:S(2)}) collective-permute-start(bf16[512,512]{1,0:T(8,128)(2,1)S(1)} %collective-permute-done.30.rest_6_), channel_id=1, source_target_pairs={{0,1},{1,0},{2,3},{3,2},{4,5},{5,4},{6,7},{7,6},{8,9},{9,8},{10,11... | collective-permute-start | bytes 1572872 | tf_op jit(solution)/shard_map/ppermute | solution.py:500
  131.7 7.6 %collective-permute-start.26 = (bf16[256,512]{1,0:T(8,128)(2,1)S(1)}, bf16[256,512]{1,0:T(8,128)(2,1)S(1)}, u32[]{:S(2)}, u32[]{:S(2)}) collective-permute-start(bf16[256,512]{1,0:T(8,128)(2,1)S(1)} %get-tuple-element.75.rest_0_), channel_id=1, source_target_pairs={{0,32},{8,40},{16,48},{24,56},{32,64},{40,72},{48,80},{56,88},{64,... | collective-permute-start | bytes 786440 | tf_op jit(solution)/shard_map/ppermute | solution.py:29
  133.7 6.4 %collective-permute-start.25 = (bf16[256,512]{1,0:T(8,128)(2,1)S(1)}, bf16[256,512]{1,0:T(8,128)(2,1)S(1)}, u32[]{:S(2)}, u32[]{:S(2)}) collective-permute-start(bf16[256,512]{1,0:T(8,128)(2,1)S(1)} %collective-permute-done.24.rest_1_), channel_id=1, source_target_pairs={{0,96},{8,104},{16,112},{24,120},{32,0},{40,8},{48,16},{56,24},{64... | collective-permute-start | bytes 786440 | tf_op jit(solution)/shard_map/ppermute | solution.py:30
  139.2 11.6 %collective-permute-start.19 = (bf16[512,256]{1,0:T(8,128)(2,1)S(1)}, bf16[512,256]{1,0:T(8,128)(2,1)S(1)}, u32[]{:S(2)}, u32[]{:S(2)}) collective-permute-start(bf16[512,256]{1,0:T(8,128)(2,1)S(1)} %copy-done.15), channel_id=1, source_target_pairs={{0,16},{8,24},{16,0},{24,8},{32,48},{40,56},{48,32},{56,40},{64,80... | collective-permute-start | bytes 786440 | tf_op jit(solution)/shard_map/ppermute | solution.py:510
  140.1 10.8 %collective-permute-start.20 = (bf16[512,256]{1,0:T(8,128)(2,1)S(1)}, bf16[512,256]{1,0:T(8,128)(2,1)S(1)}, u32[]{:S(2)}, u32[]{:S(2)}) collective-permute-start(bf16[512,256]{1,0:T(8,128)(2,1)S(1)} %copy-done.14), channel_id=1, source_target_pairs={{0,24},{8,0},{16,8},{24,16},{32,56},{40,32},{48,40},{56,48},{64,88... | collective-permute-start | bytes 786440 | tf_op jit(solution)/shard_map/ppermute | solution.py:510
  143.6 8.8 %collective-permute-start.21 = (bf16[512,256]{1,0:T(8,128)(2,1)S(1)}, bf16[512,256]{1,0:T(8,128)(2,1)S(1)}, u32[]{:S(2)}, u32[]{:S(2)}) collective-permute-start(bf16[512,256]{1,0:T(8,128)(2,1)S(1)} %copy-done.13), channel_id=1, source_target_pairs={{0,32},{8,40},{16,48},{24,56},{32,64},{40,72},{48,80},{56,88},{64,... | collective-permute-start | bytes 786440 | tf_op jit(solution)/shard_map/ppermute | solution.py:510
  145.7 10.4 %collective-permute-start.22 = (bf16[512,256]{1,0:T(8,128)(2,1)S(1)}, bf16[512,256]{1,0:T(8,128)(2,1)S(1)}, u32[]{:S(2)}, u32[]{:S(2)}) collective-permute-start(bf16[512,256]{1,0:T(8,128)(2,1)S(1)} %copy-done.12), channel_id=1, source_target_pairs={{0,64},{8,72},{16,80},{24,88},{32,96},{40,104},{48,112},{56,120},{... | collective-permute-start | bytes 786440 | tf_op jit(solution)/shard_map/ppermute | solution.py:510
  149.0 7.1 %collective-permute-start.23 = (bf16[512,256]{1,0:T(8,128)(2,1)S(1)}, bf16[512,256]{1,0:T(8,128)(2,1)S(1)}, u32[]{:S(2)}, u32[]{:S(2)}) collective-permute-start(bf16[512,256]{1,0:T(8,128)(2,1)S(1)} %copy-done.11), channel_id=1, source_target_pairs={{0,96},{8,104},{16,112},{24,120},{32,0},{40,8},{48,16},{56,24},{64... | collective-permute-start | bytes 786440 | tf_op jit(solution)/shard_map/ppermute | solution.py:510
  150.8 7.7 %collective-permute-start.36 = (bf16[256,256]{1,0:T(8,128)(2,1)S(1)}, bf16[256,256]{1,0:T(8,128)(2,1)S(1)}, u32[]{:S(2)}, u32[]{:S(2)}) collective-permute-start(bf16[256,256]{1,0:T(8,128)(2,1)S(1)} %get-tuple-element.77), channel_id=1, source_target_pairs={{0,8},{8,16},{16,24},{24,0},{32,40},{40,48},{48,56},{56,32},{64,72... | collective-permute-start | bytes 393224 | tf_op jit(solution)/shard_map/ppermute | solution.py:510
  150.9 7.6 %collective-permute-start.37 = (bf16[256,256]{1,0:T(8,128)(2,1)S(1)}, bf16[256,256]{1,0:T(8,128)(2,1)S(1)}, u32[]{:S(2)}, u32[]{:S(2)}) collective-permute-start(bf16[256,256]{1,0:T(8,128)(2,1)S(1)} %get-tuple-element.78), channel_id=1, source_target_pairs={{0,16},{8,24},{16,0},{24,8},{32,48},{40,56},{48,32},{56,40},{64,80... | collective-permute-start | bytes 393224 | tf_op jit(solution)/shard_map/ppermute | solution.py:510
  152.4 6.9 %collective-permute-start.38 = (bf16[256,256]{1,0:T(8,128)(2,1)S(1)}, bf16[256,256]{1,0:T(8,128)(2,1)S(1)}, u32[]{:S(2)}, u32[]{:S(2)}) collective-permute-start(bf16[256,256]{1,0:T(8,128)(2,1)S(1)} %get-tuple-element.79), channel_id=1, source_target_pairs={{0,24},{8,0},{16,8},{24,16},{32,56},{40,32},{48,40},{56,48},{64,88... | collective-permute-start | bytes 393224 | tf_op jit(solution)/shard_map/ppermute | solution.py:510
  (13 other events, 38.2 us)

commit v7 on v6

--- a/solution.py
+++ b/solution.py
@@ -29,6 +29,10 @@
     after, before = (lax.ppermute(array, axis, axis_perm(-r)) for r in (1, SIDE - 1))
     across = lax.ppermute(after, axis, axis_perm(-1))
     return [array, after, across, before]
+
+
+def fetched_direct(array, axis_perm):
+    return [array] + [lax.ppermute(array, "sp", axis_perm(-r)) for r in range(1, SIDE)]
 
 
 def dot_nt(a, b):
@@ -319,9 +323,13 @@
 
 
 def query_kernel(*refs):
-    parts, (low_ref, grad_ref) = refs[:8], refs[8:]
-    for h in range(2):
-        total = sum(ref[...].astype(jnp.float32) for ref in parts[SIDE * h : SIDE * (h + 1)])
+    parts, (low_ref, grad_ref, own, sems) = refs[:8], refs[8:]
+    begin = copy_list(sems)
+    wait_all([begin(parts[SIDE * h], own.at[h]) for h in range(2)])
+    for h in range(2):
+        total = own[h]
+        for ref in parts[SIDE * h + 1 : SIDE * (h + 1)]:
+            total = total + ref[...].astype(jnp.float32)
         cut = slice(h * HEAD, (h + 1) * HEAD)
         low_ref[cut, :] = total.astype(jnp.bfloat16)
         grad_ref[:, cut] = total.T
@@ -444,8 +452,12 @@
             jax.ShapeDtypeStruct((2 * rows, span), jnp.bfloat16),
             jax.ShapeDtypeStruct((span, 2 * rows), jnp.float32),
         ],
-        in_specs=[VM] * 8,
+        in_specs=[ANY, VM, VM, VM] * 2,
         out_specs=[VM] * 2,
+        scratch_shapes=[
+            pltpu.VMEM((2, rows, span), jnp.float32),
+            pltpu.SemaphoreType.DMA((2,)),
+        ],
         compiler_params=pltpu.CompilerParams(vmem_limit_bytes=16 << 20),
         cost_estimate=pl.CostEstimate(flops=10**6, bytes_accessed=2 << 20, transcendentals=0),
         name="query_sums",
@@ -513,7 +525,7 @@
     dq_0, dq_1 = arrived(dq_0, along_z), arrived(dq_1, along_x)
     low, query_grad = query_call(dq_0, dq_1)
     low, dkv_0, dkv_1 = lax.optimization_barrier((low, dkv_0, dkv_1))
-    low_parts = fetched(low, along_z)
+    low_parts = fetched_direct(low, along_z)
     terms = weight_call(low_parts, inputs)
     terms = arrived(terms, along_x)
     weight_grad = sum(part.astype(jnp.float32) for part in terms).T

time: 161 us -> 164 us (1.019)
  starting transfers between devices: 55.1 us -> 60.7 us
  waiting for transfers between devices: 37.6 us -> 34.5 us
    ppermute x0 -> x3, starting transfers between devices: none -> 6.79 us  [fetched_direct(): lax.ppermute(array, 'sp', axis_perm(-r))]
    ppermute x0 -> x3, waiting for transfers between devices: none -> 4.58 us  [fetched_direct(): lax.ppermute(array, 'sp', axis_perm(-r))]
    ppermute x12 -> x10, waiting for transfers between devices: 11.1 us -> 6.74 us  [fetched(): lax.ppermute(array, axis, axis_perm(-r))]
    ppermute x12 -> x10, starting transfers between devices: 21.2 us -> 17 us  [fetched(): lax.ppermute(array, axis, axis_perm(-r))]
    ppermute x15, starting transfers between devices: 13.9 us -> 18.1 us  [arrived(): lax.ppermute(parts[r], 'sp', axis_perm(r))]
    ppermute x15, waiting for transfers between devices: 25.7 us -> 23.1 us  [arrived(): lax.ppermute(parts[r], 'sp', axis_perm(r))]
    ppermute x6 -> x5, starting transfers between devices: 16.3 us -> 15.1 us  [fetched(): across = lax.ppermute(after, axis, axis_perm(-1))]
  transfers between devices with their start and end apart: 39 -> 39, of which waited for: 12 -> 10; matrix products, arithmetic and copies ran while one was open for 0% -> 0% of each run, Pallas kernels for 26% -> 26%
where the time goes in v7:
time: 164 us; the launch traced here: 163 us
  starting transfers between devices  60.7 us (37%)
  Pallas kernels  42.3 us (26%)
  waiting for transfers between devices  34.5 us (21%)
  blocking collectives  18.1 us (11%)
  local copies, waits for them, and re-layouts  6.17 us (4%)
    ppermute x15, waiting for transfers between devices, arrived(): lax.ppermute(parts[r], 'sp', axis_perm(r))  23.1 us
    pallas_call x1, Pallas kernels, grads_call(): pl.pallas_call(grads_kernel, out_shape=shapes(HEAD, span) + shapes(span,...  20.1 us
    ppermute x15, starting transfers between devices, arrived(): lax.ppermute(parts[r], 'sp', axis_perm(r))  18.1 us
    all_to_all x1, blocking collectives, local(): gates = lax.all_to_all(gates, 'sp', 0, 0, tiled=True)  18.1 us
    pallas_call x2, Pallas kernels, stats_call(): pl.pallas_call(functools.partial(stats_kernel, slots, pair_count, pair_of...  17.7 us
    ppermute x10, starting transfers between devices, fetched(): lax.ppermute(array, axis, axis_perm(-r))  17 us
    ppermute x5, starting transfers between devices, fetched(): across = lax.ppermute(after, axis, axis_perm(-1))  15.1 us
    ppermute x3, starting transfers between devices, fetched_direct(): lax.ppermute(array, 'sp', axis_perm(-r))  6.79 us
  transfers between devices with their start and end apart: 39, of which 10 were waited for; matrix products, arithmetic and copies ran while one was open for 0% of the time, Pallas kernels for 26%

profile of v7, /device:TPU:0, one launch (start us, length us, event | category | flops | bytes accessed | tf_op | source)
XLA Modules:
  0.0 162.7 jit_solution(4769208608711663450)
XLA Ops:
  0.7 1.2 fusion.2
  2.1 4.2 %collective-permute-start = (bf16[512,512]{1,0:T(8,128)(2,1)S(1)}, bf16[512,512]{1,0:T(8,128)(2,1)}, u32[]{:S(2)}, u32[]{:S(2)}) collective-permute-start(bf16[512,512]{1,0:T(8,128)(2,1)S(1)} %pad_maximum_fusion.rest_0_), channel_id=1, source_target_pairs={{0,96},{8,104},{16,112},{24,120},{32,0},{40,8},{48,16},{56,24},{64... | collective-permute-start | bytes 1572872 | tf_op jit(solution)/shard_map/ppermute | solution.py:29
  6.4 2.8 %collective-permute-start.2 = (bf16[512,512]{1,0:T(8,128)(2,1)S(1)}, bf16[512,512]{1,0:T(8,128)(2,1)}, u32[]{:S(2)}, u32[]{:S(2)}) collective-permute-start(bf16[512,512]{1,0:T(8,128)(2,1)S(1)} %pad_maximum_fusion.1.rest_3_.rest_4_), channel_id=1, source_target_pairs={{0,24},{8,0},{16,8},{24,16},{32,56},{40,32},{48,40},{56,48},{64,88... | collective-permute-start | bytes 1572872 | tf_op jit(solution)/shard_map/ppermute | solution.py:29
  9.2 1.4 collective-permute-start.27
  10.8 6.7 %collective-permute-done.rest_1_ = bf16[512,512]{1,0:T(8,128)(2,1)} collective-permute-done((bf16[512,512]{1,0:T(8,128)(2,1)S(1)}, bf16[512,512]{1,0:T(8,128)(2,1)}, u32[]{:S(2)}, u32[]{:S(2)}) %collective-permute-start) | collective-permute-done | bytes 524320 | tf_op jit(solution)/shard_map/ppermute | solution.py:29
  17.5 3.8 %collective-permute-start.4 = (bf16[512,512]{1,0:T(8,128)(2,1)}, bf16[512,512]{1,0:T(8,128)(2,1)}, u32[]{:S(2)}, u32[]{:S(2)}) collective-permute-start(bf16[512,512]{1,0:T(8,128)(2,1)} %collective-permute-done.rest_1_), channel_id=1, source_target_pairs={{0,96},{8,104},{16,112},{24,120},{32,0},{40,8},{48,16},{56,24},{64... | collective-permute-start | bytes 1572872 | tf_op jit(solution)/shard_map/ppermute | solution.py:30
  21.3 2.8 %collective-permute-start.5 = (bf16[512,512]{1,0:T(8,128)(2,1)}, bf16[512,512]{1,0:T(8,128)(2,1)}, u32[]{:S(2)}, u32[]{:S(2)}) collective-permute-start(bf16[512,512]{1,0:T(8,128)(2,1)} %collective-permute-done.2.rest_4_.rest_5_), channel_id=1, source_target_pairs={{0,24},{8,0},{16,8},{24,16},{32,56},{40,32},{48,40},{56,48},{64,88... | collective-permute-start | bytes 1572872 | tf_op jit(solution)/shard_map/ppermute | solution.py:30
  24.1 1.7 %collective-permute-start.28 = (bf16[512,512]{1,0:T(8,128)(2,1)}, bf16[512,512]{1,0:T(8,128)(2,1)S(1)}, u32[]{:S(2)}, u32[]{:S(2)}) collective-permute-start(bf16[512,512]{1,0:T(8,128)(2,1)} %collective-permute-done.27), channel_id=1, source_target_pairs={{0,0},{1,1},{2,34},{3,35},{4,68},{5,69},{6,102},{7,103},{8,8},{9,9... | collective-permute-start | bytes 1572872 | tf_op jit(solution)/shard_map/ppermute | solution.py:509
  25.8 18.1 %all_to_all.5.bias_ref = f32[16,2,512]{2,1,0:T(2,128)} all-to-all(f32[16,2,512]{2,1,0:T(2,128)S(1)} %broadcast_in_dim.3), channel_id=1, replica_groups=mesh['sp'=16,'tp'=8] {'sp'}, dimensions={0} | all-to-all | bytes 131072 | tf_op jit(solution)/shard_map/all_to_all | solution.py:488
  43.8 0.8 copy-done.6
  44.6 10.2 %stats.2 = (f32[4,8,512]{2,1,0:T(8,128)}, f32[4,8,512]{2,1,0:T(8,128)}, f32[32,512]{1,0:T(8,128)}) custom-call(f32[16,2,512]{2,1,0:T(2,128)} %all_to_all.5.bias_ref, bf16[512,512]{1,0:T(8,128)(2,1)} %copy-done.4, bf16[512,512]{1,0:T(8,128)(2,1)} %collective-permute-done.rest_1_, bf16[512,512]{1,0:T(8,128)(2,1)} %copy-done.6, bf16[512,512]{1,0:T(8,128)(2,1)} %copy-done.5, ...), custom_call_target="tpu_custom_call" | custom-call | flops 1207959552 | bytes 4194304 | tf_op jit(solution)/shard_map/stats/pallas_call | solution.py:373
  54.9 7.5 %stats.3 = (f32[4,8,512]{2,1,0:T(8,128)}, f32[4,8,512]{2,1,0:T(8,128)}) custom-call(f32[32,512]{1,0:T(8,128)} %get-tuple-element.42.bias_ref, bf16[512,512]{1,0:T(8,128)(2,1)} %copy-done.4, bf16[512,512]{1,0:T(8,128)(2,1)} %collective-permute-done.rest_1_, bf16[512,512]{1,0:T(8,128)(2,1)} %collective-permute-done.4.rest_2_, bf16[512,512]{1,0:T(8,128)(2,1)} %copy-done.6, ...), custom_call_target="tpu_custom_call" | custom-call | flops 939524096 | bytes 4194304 | tf_op jit(solution)/shard_map/stats/pallas_call | solution.py:373
  62.3 3.8 %collective-permute-start.6 = (f32[4,8,512]{2,1,0:T(8,128)}, f32[4,8,512]{2,1,0:T(8,128)S(1)}, u32[]{:S(2)}, u32[]{:S(2)}) collective-permute-start(f32[4,8,512]{2,1,0:T(8,128)} %get-tuple-element.45.rest_8_), channel_id=1, source_target_pairs={{0,96},{8,104},{16,112},{24,120},{32,0},{40,8},{48,16},{56,24},{64... | collective-permute-start | bytes 196616 | tf_op jit(solution)/shard_map/ppermute | solution.py:29
  66.1 2.8 %collective-permute-start.9 = (f32[4,8,512]{2,1,0:T(8,128)}, f32[4,8,512]{2,1,0:T(8,128)S(1)}, u32[]{:S(2)}, u32[]{:S(2)}) collective-permute-start(f32[4,8,512]{2,1,0:T(8,128)} %get-tuple-element.46.rest_12_), channel_id=1, source_target_pairs={{0,24},{8,0},{16,8},{24,16},{32,56},{40,32},{48,40},{56,48},{64,88... | collective-permute-start | bytes 196616 | tf_op jit(solution)/shard_map/ppermute | solution.py:29
  68.9 3.3 %collective-permute-start.7 = (f32[4,8,512]{2,1,0:T(8,128)S(1)}, f32[4,8,512]{2,1,0:T(8,128)S(1)}, u32[]{:S(2)}, u32[]{:S(2)}) collective-permute-start(f32[4,8,512]{2,1,0:T(8,128)S(1)} %collective-permute-done.6.rest_9_), channel_id=1, source_target_pairs={{0,96},{8,104},{16,112},{24,120},{32,0},{40,8},{48,16},{56,24},{64... | collective-permute-start | bytes 196616 | tf_op jit(solution)/shard_map/ppermute | solution.py:30
  72.2 3.2 %collective-permute-start.10 = (f32[4,8,512]{2,1,0:T(8,128)S(1)}, f32[4,8,512]{2,1,0:T(8,128)S(1)}, u32[]{:S(2)}, u32[]{:S(2)}) collective-permute-start(f32[4,8,512]{2,1,0:T(8,128)S(1)} %collective-permute-done.9.rest_13_), channel_id=1, source_target_pairs={{0,24},{8,0},{16,8},{24,16},{32,56},{40,32},{48,40},{56,48},{64,88... | collective-permute-start | bytes 196616 | tf_op jit(solution)/shard_map/ppermute | solution.py:30
  75.4 3.3 %collective-permute-start.29 = (bf16[512,512]{1,0:T(8,128)(2,1)S(1)}, bf16[512,512]{1,0:T(8,128)(2,1)S(1)}, u32[]{:S(2)}, u32[]{:S(2)}) collective-permute-start(bf16[512,512]{1,0:T(8,128)(2,1)S(1)} %collective-permute-done.28.rest_4_), channel_id=1, source_target_pairs={{0,6},{1,7},{2,0},{3,1},{4,2},{5,3},{6,4},{7,5},{8,14},{9,15},{10,... | collective-permute-start | bytes 1572872 | tf_op jit(solution)/shard_map/ppermute | solution.py:29
  78.8 0.6 copy-done.19
  79.4 0.6 copy-done.21
  80.0 20.1 %grads.1 = (f32[128,512]{1,0:T(8,128)}, bf16[128,512]{1,0:T(8,128)(2,1)}, bf16[128,512]{1,0:T(8,128)(2,1)}, bf16[128,512]{1,0:T(8,128)(2,1)}, f32[128,512]{1,0:T...) custom-call(f32[32,512]{1,0:T(8,128)} %get-tuple-element.42.bias_ref, ...), custom_call_target="tpu_custom_call" | custom-call | flops 5704253440 | bytes 8388608 | tf_op jit(solution)/shard_map/grads/pallas_call | solution.py:396
  100.2 1.5 collective-permute-start.13
  101.7 2.1 %collective-permute-start.30 = (bf16[512,512]{1,0:T(8,128)(2,1)S(1)}, bf16[512,512]{1,0:T(8,128)(2,1)S(1)}, u32[]{:S(2)}, u32[]{:S(2)}) collective-permute-start(bf16[512,512]{1,0:T(8,128)(2,1)S(1)} %collective-permute-done.29.rest_5_), channel_id=1, source_target_pairs={{0,6},{1,7},{2,0},{3,1},{4,2},{5,3},{6,4},{7,5},{8,14},{9,15},{10,... | collective-permute-start | bytes 1572872 | tf_op jit(solution)/shard_map/ppermute | solution.py:30
  103.8 4.2 %collective-permute-done.12.refs_1_ = bf16[128,512]{1,0:T(8,128)(2,1)S(1)} collective-permute-done((bf16[128,512]{1,0:T(8,128)(2,1)}, bf16[128,512]{1,0:T(8,128)(2,1)S(1)}, u32[]{:S(2)}, u32[]{:S(2)}) %collective-permute-start.12) | collective-permute-done | bytes 131104 | tf_op jit(solution)/shard_map/ppermute | solution.py:522
  108.0 5.2 %collective-permute-done.14.refs_3_ = bf16[128,512]{1,0:T(8,128)(2,1)S(1)} collective-permute-done((bf16[128,512]{1,0:T(8,128)(2,1)}, bf16[128,512]{1,0:T(8,128)(2,1)S(1)}, u32[]{:S(2)}, u32[]{:S(2)}) %collective-permute-start.14) | collective-permute-done | bytes 131104 | tf_op jit(solution)/shard_map/ppermute | solution.py:522
  113.1 2.6 %collective-permute-done.15.refs_5_ = bf16[128,512]{1,0:T(8,128)(2,1)S(1)} collective-permute-done((bf16[128,512]{1,0:T(8,128)(2,1)}, bf16[128,512]{1,0:T(8,128)(2,1)S(1)}, u32[]{:S(2)}, u32[]{:S(2)}) %collective-permute-start.15) | collective-permute-done | bytes 131104 | tf_op jit(solution)/shard_map/ppermute | solution.py:522
  115.8 4.1 %collective-permute-done.16.refs_6_ = bf16[128,512]{1,0:T(8,128)(2,1)S(1)} collective-permute-done((bf16[128,512]{1,0:T(8,128)(2,1)}, bf16[128,512]{1,0:T(8,128)(2,1)S(1)}, u32[]{:S(2)}, u32[]{:S(2)}) %collective-permute-start.16) | collective-permute-done | bytes 131104 | tf_op jit(solution)/shard_map/ppermute | solution.py:522
  119.8 1.1 collective-permute-done.17.refs_7_
  120.9 0.9 copy-done.2
  121.9 0.9 copy-done.3
  122.9 1.1 query_sums.1
  124.0 2.1 %collective-permute-start.26 = (bf16[256,512]{1,0:T(8,128)(2,1)S(1)}, bf16[256,512]{1,0:T(8,128)(2,1)S(1)}, u32[]{:S(2)}, u32[]{:S(2)}) collective-permute-start(bf16[256,512]{1,0:T(8,128)(2,1)S(1)} %get-tuple-element.75.rest_0_), channel_id=1, source_target_pairs={{0,32},{8,40},{16,48},{24,56},{32,64},{40,72},{48,80},{56,88},{64,... | collective-permute-start | bytes 786440 | tf_op jit(solution)/shard_map/ppermute | solution.py:35
  126.7 5.1 %collective-permute-done.18.refs_1_ = bf16[512,256]{1,0:T(8,128)(2,1)S(1)} collective-permute-done((bf16[512,256]{1,0:T(8,128)(2,1)}, bf16[512,256]{1,0:T(8,128)(2,1)S(1)}, u32[]{:S(2)}, u32[]{:S(2)}) %collective-permute-start.18) | collective-permute-done | bytes 262176 | tf_op jit(solution)/shard_map/ppermute | solution.py:522
  131.8 0.5 collective-permute-start.25
  132.3 4.2 %collective-permute-start.24 = (bf16[256,512]{1,0:T(8,128)(2,1)S(1)}, bf16[256,512]{1,0:T(8,128)(2,1)S(1)}, u32[]{:S(2)}, u32[]{:S(2)}) collective-permute-start(bf16[256,512]{1,0:T(8,128)(2,1)S(1)} %get-tuple-element.75.rest_0_), channel_id=1, source_target_pairs={{0,96},{8,104},{16,112},{24,120},{32,0},{40,8},{48,16},{56,24},{64... | collective-permute-start | bytes 786440 | tf_op jit(solution)/shard_map/ppermute | solution.py:35
  136.5 3.2 %collective-permute-done.25.rest_2_ = bf16[256,512]{1,0:T(8,128)(2,1)S(1)} collective-permute-done((bf16[256,512]{1,0:T(8,128)(2,1)S(1)}, bf16[256,512]{1,0:T(8,128)(2,1)S(1)}, u32[]{:S(2)}, u32[]{:S(2)}) %collective-permute-start.25) | collective-permute-done | bytes 262176 | tf_op jit(solution)/shard_map/ppermute | solution.py:35
  139.7 0.9 collective-permute-start.19
  140.6 1.4 collective-permute-done.24.rest_1_
  142.0 2.2 %collective-permute-start.20 = (bf16[512,256]{1,0:T(8,128)(2,1)S(1)}, bf16[512,256]{1,0:T(8,128)(2,1)S(1)}, u32[]{:S(2)}, u32[]{:S(2)}) collective-permute-start(bf16[512,256]{1,0:T(8,128)(2,1)S(1)} %copy-done.14), channel_id=1, source_target_pairs={{0,24},{8,0},{16,8},{24,16},{32,56},{40,32},{48,40},{56,48},{64,88... | collective-permute-start | bytes 786440 | tf_op jit(solution)/shard_map/ppermute | solution.py:522
  144.2 1.6 collective-permute-start.21
  145.8 2.5 %collective-permute-start.22 = (bf16[512,256]{1,0:T(8,128)(2,1)S(1)}, bf16[512,256]{1,0:T(8,128)(2,1)S(1)}, u32[]{:S(2)}, u32[]{:S(2)}) collective-permute-start(bf16[512,256]{1,0:T(8,128)(2,1)S(1)} %copy-done.12), channel_id=1, source_target_pairs={{0,64},{8,72},{16,80},{24,88},{32,96},{40,104},{48,112},{56,120},{... | collective-permute-start | bytes 786440 | tf_op jit(solution)/shard_map/ppermute | solution.py:522
  148.3 0.8 collective-permute-start.23
  149.1 1.8 %weight.1 = (f32[256,256]{1,0:T(8,128)S(1)}, bf16[256,256]{1,0:T(8,128)(2,1)S(1)}, bf16[256,256]{1,0:T(8,128)(2,1)S(1)}, bf16[256,256]{1,0:T(8,128)(2,1)S(1)}) custom-call(bf16[256,512]{1,0:T(8,128)(2,1)S(1)} %get-tuple-element.75.rest_0_, bf16[256,512]{1,0:T(8,128)(2,1)S(1)} %collective-permute-done.24.rest_1_, ...), custom_call_target="tpu_custom_call" | custom-call | flops 1073741824 | bytes 6291456 | tf_op jit(solution)/shard_map/weight/pallas_call | solution.py:429
  150.9 1.0 collective-permute-start.36
  152.0 3.5 %collective-permute-start.37 = (bf16[256,256]{1,0:T(8,128)(2,1)S(1)}, bf16[256,256]{1,0:T(8,128)(2,1)S(1)}, u32[]{:S(2)}, u32[]{:S(2)}) collective-permute-start(bf16[256,256]{1,0:T(8,128)(2,1)S(1)} %get-tuple-element.78), channel_id=1, source_target_pairs={{0,16},{8,24},{16,0},{24,8},{32,48},{40,56},{48,32},{56,40},{64,80... | collective-permute-start | bytes 393224 | tf_op jit(solution)/shard_map/ppermute | solution.py:522
  155.5 3.8 %collective-permute-start.38 = (bf16[256,256]{1,0:T(8,128)(2,1)S(1)}, bf16[256,256]{1,0:T(8,128)(2,1)S(1)}, u32[]{:S(2)}, u32[]{:S(2)}) collective-permute-start(bf16[256,256]{1,0:T(8,128)(2,1)S(1)} %get-tuple-element.79), channel_id=1, source_target_pairs={{0,24},{8,0},{16,8},{24,16},{32,56},{40,32},{48,40},{56,48},{64,88... | collective-permute-start | bytes 393224 | tf_op jit(solution)/shard_map/ppermute | solution.py:522
  159.3 1.6 key_sums.1
  161.0 0.9 collective-permute-done.38
  161.9 0.8 copy.10
  (88 shorter events, 1.4 us)
Async XLA Ops:
  2.1 15.4 %collective-permute-start = (bf16[512,512]{1,0:T(8,128)(2,1)S(1)}, bf16[512,512]{1,0:T(8,128)(2,1)}, u32[]{:S(2)}, u32[]{:S(2)}) collective-permute-start(bf16[512,512]{1,0:T(8,128)(2,1)S(1)} %pad_maximum_fusion.rest_0_), channel_id=1, source_target_pairs={{0,96},{8,104},{16,112},{24,120},{32,0},{40,8},{48,16},{56,24},{64... | collective-permute-start | bytes 1572872 | tf_op jit(solution)/shard_map/ppermute | solution.py:29
  6.3 19.4 %copy-start.9 = (f32[512,2]{0,1:T(2,128)S(1)}, f32[512,2]{0,1:T(2,128)}, u32[]{:S(2)}) copy-start(f32[512,2]{0,1:T(2,128)} %param.9) | copy-start | bytes 12292
  6.4 38.3 %copy-start.5 = (bf16[512,512]{1,0:T(8,128)(2,1)}, bf16[512,512]{1,0:T(8,128)(2,1)S(1)}, u32[]{:S(2)}) copy-start(bf16[512,512]{1,0:T(8,128)(2,1)S(1)} %pad_maximum_fusion.1.rest_3_.rest_4_) | copy-start | bytes 1572868
  6.4 14.9 %collective-permute-start.2 = (bf16[512,512]{1,0:T(8,128)(2,1)S(1)}, bf16[512,512]{1,0:T(8,128)(2,1)}, u32[]{:S(2)}, u32[]{:S(2)}) collective-permute-start(bf16[512,512]{1,0:T(8,128)(2,1)S(1)} %pad_maximum_fusion.1.rest_3_.rest_4_), channel_id=1, source_target_pairs={{0,24},{8,0},{16,8},{24,16},{32,56},{40,32},{48,40},{56,48},{64,88... | collective-permute-start | bytes 1572872 | tf_op jit(solution)/shard_map/ppermute | solution.py:29
  9.2 14.8 %collective-permute-start.27 = (bf16[512,512]{1,0:T(8,128)(2,1)S(1)}, bf16[512,512]{1,0:T(8,128)(2,1)}, u32[]{:S(2)}, u32[]{:S(2)}) collective-permute-start(bf16[512,512]{1,0:T(8,128)(2,1)S(1)} %copy-done.10), channel_id=1, source_target_pairs={{0,0},{1,1},{2,2},{3,3},{4,4},{5,5},{6,6},{7,7},{8,8},{9,9},{10,10... | collective-permute-start | bytes 1572872 | tf_op jit(solution)/shard_map/ppermute | solution.py:508
  10.7 33.2 %collective-permute-start.1 = (bf16[512,512]{1,0:T(8,128)(2,1)S(1)}, bf16[512,512]{1,0:T(8,128)(2,1)S(1)}, u32[]{:S(2)}, u32[]{:S(2)}) collective-permute-start(bf16[512,512]{1,0:T(8,128)(2,1)S(1)} %pad_maximum_fusion.rest_0_), channel_id=1, source_target_pairs={{0,32},{8,40},{16,48},{24,56},{32,64},{40,72},{48,80},{56,88},{64,... | collective-permute-start | bytes 1572872 | tf_op jit(solution)/shard_map/ppermute | solution.py:29
  10.8 33.9 %collective-permute-start.3 = (bf16[512,512]{1,0:T(8,128)(2,1)S(1)}, bf16[512,512]{1,0:T(8,128)(2,1)}, u32[]{:S(2)}, u32[]{:S(2)}) collective-permute-start(bf16[512,512]{1,0:T(8,128)(2,1)S(1)} %pad_maximum_fusion.1.rest_3_.rest_4_), channel_id=1, source_target_pairs={{0,8},{8,16},{16,24},{24,0},{32,40},{40,48},{48,56},{56,32},{64,72... | collective-permute-start | bytes 1572872 | tf_op jit(solution)/shard_map/ppermute | solution.py:29
  17.5 37.4 %collective-permute-start.4 = (bf16[512,512]{1,0:T(8,128)(2,1)}, bf16[512,512]{1,0:T(8,128)(2,1)}, u32[]{:S(2)}, u32[]{:S(2)}) collective-permute-start(bf16[512,512]{1,0:T(8,128)(2,1)} %collective-permute-done.rest_1_), channel_id=1, source_target_pairs={{0,96},{8,104},{16,112},{24,120},{32,0},{40,8},{48,16},{56,24},{64... | collective-permute-start | bytes 1572872 | tf_op jit(solution)/shard_map/ppermute | solution.py:30
  21.3 33.6 %collective-permute-start.5 = (bf16[512,512]{1,0:T(8,128)(2,1)}, bf16[512,512]{1,0:T(8,128)(2,1)}, u32[]{:S(2)}, u32[]{:S(2)}) collective-permute-start(bf16[512,512]{1,0:T(8,128)(2,1)} %collective-permute-done.2.rest_4_.rest_5_), channel_id=1, source_target_pairs={{0,24},{8,0},{16,8},{24,16},{32,56},{40,32},{48,40},{56,48},{64,88... | collective-permute-start | bytes 1572872 | tf_op jit(solution)/shard_map/ppermute | solution.py:30
  24.1 51.4 %collective-permute-start.28 = (bf16[512,512]{1,0:T(8,128)(2,1)}, bf16[512,512]{1,0:T(8,128)(2,1)S(1)}, u32[]{:S(2)}, u32[]{:S(2)}) collective-permute-start(bf16[512,512]{1,0:T(8,128)(2,1)} %collective-permute-done.27), channel_id=1, source_target_pairs={{0,0},{1,1},{2,34},{3,35},{4,68},{5,69},{6,102},{7,103},{8,8},{9,9... | collective-permute-start | bytes 1572872 | tf_op jit(solution)/shard_map/ppermute | solution.py:509
  62.3 6.6 %collective-permute-start.6 = (f32[4,8,512]{2,1,0:T(8,128)}, f32[4,8,512]{2,1,0:T(8,128)S(1)}, u32[]{:S(2)}, u32[]{:S(2)}) collective-permute-start(f32[4,8,512]{2,1,0:T(8,128)} %get-tuple-element.45.rest_8_), channel_id=1, source_target_pairs={{0,96},{8,104},{16,112},{24,120},{32,0},{40,8},{48,16},{56,24},{64... | collective-permute-start | bytes 196616 | tf_op jit(solution)/shard_map/ppermute | solution.py:29
  66.1 6.1 %collective-permute-start.9 = (f32[4,8,512]{2,1,0:T(8,128)}, f32[4,8,512]{2,1,0:T(8,128)S(1)}, u32[]{:S(2)}, u32[]{:S(2)}) collective-permute-start(f32[4,8,512]{2,1,0:T(8,128)} %get-tuple-element.46.rest_12_), channel_id=1, source_target_pairs={{0,24},{8,0},{16,8},{24,16},{32,56},{40,32},{48,40},{56,48},{64,88... | collective-permute-start | bytes 196616 | tf_op jit(solution)/shard_map/ppermute | solution.py:29
  68.9 6.5 %collective-permute-start.8 = (f32[4,8,512]{2,1,0:T(8,128)}, f32[4,8,512]{2,1,0:T(8,128)S(1)}, u32[]{:S(2)}, u32[]{:S(2)}) collective-permute-start(f32[4,8,512]{2,1,0:T(8,128)} %get-tuple-element.45.rest_8_), channel_id=1, source_target_pairs={{0,32},{8,40},{16,48},{24,56},{32,64},{40,72},{48,80},{56,88},{64,... | collective-permute-start | bytes 196616 | tf_op jit(solution)/shard_map/ppermute | solution.py:29
  68.9 9.8 %collective-permute-start.11 = (f32[4,8,512]{2,1,0:T(8,128)}, f32[4,8,512]{2,1,0:T(8,128)S(1)}, u32[]{:S(2)}, u32[]{:S(2)}) collective-permute-start(f32[4,8,512]{2,1,0:T(8,128)} %get-tuple-element.46.rest_12_), channel_id=1, source_target_pairs={{0,8},{8,16},{16,24},{24,0},{32,40},{40,48},{48,56},{56,32},{64,72... | collective-permute-start | bytes 196616 | tf_op jit(solution)/shard_map/ppermute | solution.py:29
  68.9 9.8 %collective-permute-start.7 = (f32[4,8,512]{2,1,0:T(8,128)S(1)}, f32[4,8,512]{2,1,0:T(8,128)S(1)}, u32[]{:S(2)}, u32[]{:S(2)}) collective-permute-start(f32[4,8,512]{2,1,0:T(8,128)S(1)} %collective-permute-done.6.rest_9_), channel_id=1, source_target_pairs={{0,96},{8,104},{16,112},{24,120},{32,0},{40,8},{48,16},{56,24},{64... | collective-permute-start | bytes 196616 | tf_op jit(solution)/shard_map/ppermute | solution.py:30
  72.2 6.5 %collective-permute-start.10 = (f32[4,8,512]{2,1,0:T(8,128)S(1)}, f32[4,8,512]{2,1,0:T(8,128)S(1)}, u32[]{:S(2)}, u32[]{:S(2)}) collective-permute-start(f32[4,8,512]{2,1,0:T(8,128)S(1)} %collective-permute-done.9.rest_13_), channel_id=1, source_target_pairs={{0,24},{8,0},{16,8},{24,16},{32,56},{40,32},{48,40},{56,48},{64,88... | collective-permute-start | bytes 196616 | tf_op jit(solution)/shard_map/ppermute | solution.py:30
  75.4 50.7 %collective-permute-start.31 = (bf16[512,512]{1,0:T(8,128)(2,1)S(1)}, bf16[512,512]{1,0:T(8,128)(2,1)S(1)}, u32[]{:S(2)}, u32[]{:S(2)}) collective-permute-start(bf16[512,512]{1,0:T(8,128)(2,1)S(1)} %collective-permute-done.28.rest_4_), channel_id=1, source_target_pairs={{0,2},{1,3},{2,4},{3,5},{4,6},{5,7},{6,0},{7,1},{8,10},{9,11},{10,... | collective-permute-start | bytes 1572872 | tf_op jit(solution)/shard_map/ppermute | solution.py:29
  75.4 26.3 %collective-permute-start.29 = (bf16[512,512]{1,0:T(8,128)(2,1)S(1)}, bf16[512,512]{1,0:T(8,128)(2,1)S(1)}, u32[]{:S(2)}, u32[]{:S(2)}) collective-permute-start(bf16[512,512]{1,0:T(8,128)(2,1)S(1)} %collective-permute-done.28.rest_4_), channel_id=1, source_target_pairs={{0,6},{1,7},{2,0},{3,1},{4,2},{5,3},{6,4},{7,5},{8,14},{9,15},{10,... | collective-permute-start | bytes 1572872 | tf_op jit(solution)/shard_map/ppermute | solution.py:29
  100.1 7.9 %collective-permute-start.12 = (bf16[128,512]{1,0:T(8,128)(2,1)}, bf16[128,512]{1,0:T(8,128)(2,1)S(1)}, u32[]{:S(2)}, u32[]{:S(2)}) collective-permute-start(bf16[128,512]{1,0:T(8,128)(2,1)} %get-tuple-element.48), channel_id=1, source_target_pairs={{0,32},{8,40},{16,48},{24,56},{32,64},{40,72},{48,80},{56,88},{64,... | collective-permute-start | bytes 393224 | tf_op jit(solution)/shard_map/ppermute | solution.py:522
  100.2 7.8 %collective-permute-start.13 = (bf16[128,512]{1,0:T(8,128)(2,1)}, bf16[128,512]{1,0:T(8,128)(2,1)S(1)}, u32[]{:S(2)}, u32[]{:S(2)}) collective-permute-start(bf16[128,512]{1,0:T(8,128)(2,1)} %get-tuple-element.49), channel_id=1, source_target_pairs={{0,64},{8,72},{16,80},{24,88},{32,96},{40,104},{48,112},{56,120},{... | collective-permute-start | bytes 393224 | tf_op jit(solution)/shard_map/ppermute | solution.py:522
  101.7 24.4 %collective-permute-start.32 = (bf16[512,512]{1,0:T(8,128)(2,1)S(1)}, bf16[512,512]{1,0:T(8,128)(2,1)S(1)}, u32[]{:S(2)}, u32[]{:S(2)}) collective-permute-start(bf16[512,512]{1,0:T(8,128)(2,1)S(1)} %collective-permute-done.28.rest_4_), channel_id=1, source_target_pairs={{0,1},{1,0},{2,3},{3,2},{4,5},{5,4},{6,7},{7,6},{8,9},{9,8},{10,11... | collective-permute-start | bytes 1572872 | tf_op jit(solution)/shard_map/ppermute | solution.py:512
  101.7 24.9 %collective-permute-start.30 = (bf16[512,512]{1,0:T(8,128)(2,1)S(1)}, bf16[512,512]{1,0:T(8,128)(2,1)S(1)}, u32[]{:S(2)}, u32[]{:S(2)}) collective-permute-start(bf16[512,512]{1,0:T(8,128)(2,1)S(1)} %collective-permute-done.29.rest_5_), channel_id=1, source_target_pairs={{0,6},{1,7},{2,0},{3,1},{4,2},{5,3},{6,4},{7,5},{8,14},{9,15},{10,... | collective-permute-start | bytes 1572872 | tf_op jit(solution)/shard_map/ppermute | solution.py:30
  108.0 5.2 %collective-permute-start.14 = (bf16[128,512]{1,0:T(8,128)(2,1)}, bf16[128,512]{1,0:T(8,128)(2,1)S(1)}, u32[]{:S(2)}, u32[]{:S(2)}) collective-permute-start(bf16[128,512]{1,0:T(8,128)(2,1)} %get-tuple-element.50), channel_id=1, source_target_pairs={{0,96},{8,104},{16,112},{24,120},{32,0},{40,8},{48,16},{56,24},{64... | collective-permute-start | bytes 393224 | tf_op jit(solution)/shard_map/ppermute | solution.py:522
  108.0 7.8 %collective-permute-start.15 = (bf16[128,512]{1,0:T(8,128)(2,1)}, bf16[128,512]{1,0:T(8,128)(2,1)S(1)}, u32[]{:S(2)}, u32[]{:S(2)}) collective-permute-start(bf16[128,512]{1,0:T(8,128)(2,1)} %get-tuple-element.52), channel_id=1, source_target_pairs={{0,8},{8,16},{16,24},{24,0},{32,40},{40,48},{48,56},{56,32},{64,72... | collective-permute-start | bytes 393224 | tf_op jit(solution)/shard_map/ppermute | solution.py:522
  113.1 6.7 %collective-permute-start.16 = (bf16[128,512]{1,0:T(8,128)(2,1)}, bf16[128,512]{1,0:T(8,128)(2,1)S(1)}, u32[]{:S(2)}, u32[]{:S(2)}) collective-permute-start(bf16[128,512]{1,0:T(8,128)(2,1)} %get-tuple-element.53), channel_id=1, source_target_pairs={{0,16},{8,24},{16,0},{24,8},{32,48},{40,56},{48,32},{56,40},{64,80... | collective-permute-start | bytes 393224 | tf_op jit(solution)/shard_map/ppermute | solution.py:522
  115.8 5.2 %collective-permute-start.17 = (bf16[128,512]{1,0:T(8,128)(2,1)}, bf16[128,512]{1,0:T(8,128)(2,1)S(1)}, u32[]{:S(2)}, u32[]{:S(2)}) collective-permute-start(bf16[128,512]{1,0:T(8,128)(2,1)} %get-tuple-element.54), channel_id=1, source_target_pairs={{0,24},{8,0},{16,8},{24,16},{32,56},{40,32},{48,40},{56,48},{64,88... | collective-permute-start | bytes 393224 | tf_op jit(solution)/shard_map/ppermute | solution.py:522
  122.8 16.8 %copy-start.15 = (bf16[512,256]{1,0:T(8,128)(2,1)S(1)}, bf16[512,256]{1,0:T(8,128)(2,1)}, u32[]{:S(2)}) copy-start(bf16[512,256]{1,0:T(8,128)(2,1)} %get-tuple-element.67) | copy-start | bytes 786436
  122.8 19.2 %copy-start.14 = (bf16[512,256]{1,0:T(8,128)(2,1)S(1)}, bf16[512,256]{1,0:T(8,128)(2,1)}, u32[]{:S(2)}) copy-start(bf16[512,256]{1,0:T(8,128)(2,1)} %get-tuple-element.68) | copy-start | bytes 786436
  122.8 21.4 %copy-start.13 = (bf16[512,256]{1,0:T(8,128)(2,1)S(1)}, bf16[512,256]{1,0:T(8,128)(2,1)}, u32[]{:S(2)}) copy-start(bf16[512,256]{1,0:T(8,128)(2,1)} %get-tuple-element.70) | copy-start | bytes 786436
  122.8 22.9 %copy-start.12 = (bf16[512,256]{1,0:T(8,128)(2,1)S(1)}, bf16[512,256]{1,0:T(8,128)(2,1)}, u32[]{:S(2)}) copy-start(bf16[512,256]{1,0:T(8,128)(2,1)} %get-tuple-element.71) | copy-start | bytes 786436
  122.8 25.5 %copy-start.11 = (bf16[512,256]{1,0:T(8,128)(2,1)S(1)}, bf16[512,256]{1,0:T(8,128)(2,1)}, u32[]{:S(2)}) copy-start(bf16[512,256]{1,0:T(8,128)(2,1)} %get-tuple-element.72) | copy-start | bytes 786436
  123.9 35.4 %copy-start = (f32[512,256]{1,0:T(8,128)S(1)}, f32[512,256]{1,0:T(8,128)}, u32[]{:S(2)}) copy-start(f32[512,256]{1,0:T(8,128)} %get-tuple-element.65.refs_0_) | copy-start | bytes 1572868
  123.9 35.4 %copy-start.1 = (f32[512,256]{1,0:T(8,128)S(1)}, f32[512,256]{1,0:T(8,128)}, u32[]{:S(2)}) copy-start(f32[512,256]{1,0:T(8,128)} %get-tuple-element.69.refs_4_) | copy-start | bytes 1572868
  123.9 7.9 %collective-permute-start.18 = (bf16[512,256]{1,0:T(8,128)(2,1)}, bf16[512,256]{1,0:T(8,128)(2,1)S(1)}, u32[]{:S(2)}, u32[]{:S(2)}) collective-permute-start(bf16[512,256]{1,0:T(8,128)(2,1)} %get-tuple-element.66), channel_id=1, source_target_pairs={{0,8},{8,16},{16,24},{24,0},{32,40},{40,48},{48,56},{56,32},{64,72... | collective-permute-start | bytes 786440 | tf_op jit(solution)/shard_map/ppermute | solution.py:522
  124.0 8.3 %collective-permute-start.26 = (bf16[256,512]{1,0:T(8,128)(2,1)S(1)}, bf16[256,512]{1,0:T(8,128)(2,1)S(1)}, u32[]{:S(2)}, u32[]{:S(2)}) collective-permute-start(bf16[256,512]{1,0:T(8,128)(2,1)S(1)} %get-tuple-element.75.rest_0_), channel_id=1, source_target_pairs={{0,32},{8,40},{16,48},{24,56},{32,64},{40,72},{48,80},{56,88},{64,... | collective-permute-start | bytes 786440 | tf_op jit(solution)/shard_map/ppermute | solution.py:35
  126.1 18.1 %collective-permute-start.35 = (bf16[512,512]{1,0:T(8,128)(2,1)S(1)}, bf16[512,512]{1,0:T(8,128)(2,1)S(1)}, u32[]{:S(2)}, u32[]{:S(2)}) collective-permute-start(bf16[512,512]{1,0:T(8,128)(2,1)S(1)} %collective-permute-done.31.rest_7_), channel_id=1, source_target_pairs={{0,1},{1,0},{2,3},{3,2},{4,5},{5,4},{6,7},{7,6},{8,9},{9,8},{10,11... | collective-permute-start | bytes 1572872 | tf_op jit(solution)/shard_map/ppermute | solution.py:512
  126.1 19.7 %collective-permute-start.33 = (bf16[512,512]{1,0:T(8,128)(2,1)S(1)}, bf16[512,512]{1,0:T(8,128)(2,1)S(1)}, u32[]{:S(2)}, u32[]{:S(2)}) collective-permute-start(bf16[512,512]{1,0:T(8,128)(2,1)S(1)} %collective-permute-done.29.rest_5_), channel_id=1, source_target_pairs={{0,1},{1,0},{2,3},{3,2},{4,5},{5,4},{6,7},{7,6},{8,9},{9,8},{10,11... | collective-permute-start | bytes 1572872 | tf_op jit(solution)/shard_map/ppermute | solution.py:512
  126.6 21.7 %collective-permute-start.34 = (bf16[512,512]{1,0:T(8,128)(2,1)S(1)}, bf16[512,512]{1,0:T(8,128)(2,1)S(1)}, u32[]{:S(2)}, u32[]{:S(2)}) collective-permute-start(bf16[512,512]{1,0:T(8,128)(2,1)S(1)} %collective-permute-done.30.rest_6_), channel_id=1, source_target_pairs={{0,1},{1,0},{2,3},{3,2},{4,5},{5,4},{6,7},{7,6},{8,9},{9,8},{10,11... | collective-permute-start | bytes 1572872 | tf_op jit(solution)/shard_map/ppermute | solution.py:512
  131.8 7.9 %collective-permute-start.25 = (bf16[256,512]{1,0:T(8,128)(2,1)S(1)}, bf16[256,512]{1,0:T(8,128)(2,1)S(1)}, u32[]{:S(2)}, u32[]{:S(2)}) collective-permute-start(bf16[256,512]{1,0:T(8,128)(2,1)S(1)} %get-tuple-element.75.rest_0_), channel_id=1, source_target_pairs={{0,64},{8,72},{16,80},{24,88},{32,96},{40,104},{48,112},{56,120},{... | collective-permute-start | bytes 786440 | tf_op jit(solution)/shard_map/ppermute | solution.py:35
  132.3 9.7 %collective-permute-start.24 = (bf16[256,512]{1,0:T(8,128)(2,1)S(1)}, bf16[256,512]{1,0:T(8,128)(2,1)S(1)}, u32[]{:S(2)}, u32[]{:S(2)}) collective-permute-start(bf16[256,512]{1,0:T(8,128)(2,1)S(1)} %get-tuple-element.75.rest_0_), channel_id=1, source_target_pairs={{0,96},{8,104},{16,112},{24,120},{32,0},{40,8},{48,16},{56,24},{64... | collective-permute-start | bytes 786440 | tf_op jit(solution)/shard_map/ppermute | solution.py:35
  139.7 11.2 %collective-permute-start.19 = (bf16[512,256]{1,0:T(8,128)(2,1)S(1)}, bf16[512,256]{1,0:T(8,128)(2,1)S(1)}, u32[]{:S(2)}, u32[]{:S(2)}) collective-permute-start(bf16[512,256]{1,0:T(8,128)(2,1)S(1)} %copy-done.15), channel_id=1, source_target_pairs={{0,16},{8,24},{16,0},{24,8},{32,48},{40,56},{48,32},{56,40},{64,80... | collective-permute-start | bytes 786440 | tf_op jit(solution)/shard_map/ppermute | solution.py:522
  142.0 9.9 %collective-permute-start.20 = (bf16[512,256]{1,0:T(8,128)(2,1)S(1)}, bf16[512,256]{1,0:T(8,128)(2,1)S(1)}, u32[]{:S(2)}, u32[]{:S(2)}) collective-permute-start(bf16[512,256]{1,0:T(8,128)(2,1)S(1)} %copy-done.14), channel_id=1, source_target_pairs={{0,24},{8,0},{16,8},{24,16},{32,56},{40,32},{48,40},{56,48},{64,88... | collective-permute-start | bytes 786440 | tf_op jit(solution)/shard_map/ppermute | solution.py:522
  144.2 11.3 %collective-permute-start.21 = (bf16[512,256]{1,0:T(8,128)(2,1)S(1)}, bf16[512,256]{1,0:T(8,128)(2,1)S(1)}, u32[]{:S(2)}, u32[]{:S(2)}) collective-permute-start(bf16[512,256]{1,0:T(8,128)(2,1)S(1)} %copy-done.13), channel_id=1, source_target_pairs={{0,32},{8,40},{16,48},{24,56},{32,64},{40,72},{48,80},{56,88},{64,... | collective-permute-start | bytes 786440 | tf_op jit(solution)/shard_map/ppermute | solution.py:522
  145.8 13.5 %collective-permute-start.22 = (bf16[512,256]{1,0:T(8,128)(2,1)S(1)}, bf16[512,256]{1,0:T(8,128)(2,1)S(1)}, u32[]{:S(2)}, u32[]{:S(2)}) collective-permute-start(bf16[512,256]{1,0:T(8,128)(2,1)S(1)} %copy-done.12), channel_id=1, source_target_pairs={{0,64},{8,72},{16,80},{24,88},{32,96},{40,104},{48,112},{56,120},{... | collective-permute-start | bytes 786440 | tf_op jit(solution)/shard_map/ppermute | solution.py:522
  148.3 11.0 %collective-permute-start.23 = (bf16[512,256]{1,0:T(8,128)(2,1)S(1)}, bf16[512,256]{1,0:T(8,128)(2,1)S(1)}, u32[]{:S(2)}, u32[]{:S(2)}) collective-permute-start(bf16[512,256]{1,0:T(8,128)(2,1)S(1)} %copy-done.11), channel_id=1, source_target_pairs={{0,96},{8,104},{16,112},{24,120},{32,0},{40,8},{48,16},{56,24},{64... | collective-permute-start | bytes 786440 | tf_op jit(solution)/shard_map/ppermute | solution.py:522
  150.9 10.0 %collective-permute-start.36 = (bf16[256,256]{1,0:T(8,128)(2,1)S(1)}, bf16[256,256]{1,0:T(8,128)(2,1)S(1)}, u32[]{:S(2)}, u32[]{:S(2)}) collective-permute-start(bf16[256,256]{1,0:T(8,128)(2,1)S(1)} %get-tuple-element.77), channel_id=1, source_target_pairs={{0,8},{8,16},{16,24},{24,0},{32,40},{40,48},{48,56},{56,32},{64,72... | collective-permute-start | bytes 393224 | tf_op jit(solution)/shard_map/ppermute | solution.py:522
  152.0 9.0 %collective-permute-start.37 = (bf16[256,256]{1,0:T(8,128)(2,1)S(1)}, bf16[256,256]{1,0:T(8,128)(2,1)S(1)}, u32[]{:S(2)}, u32[]{:S(2)}) collective-permute-start(bf16[256,256]{1,0:T(8,128)(2,1)S(1)} %get-tuple-element.78), channel_id=1, source_target_pairs={{0,16},{8,24},{16,0},{24,8},{32,48},{40,56},{48,32},{56,40},{64,80... | collective-permute-start | bytes 393224 | tf_op jit(solution)/shard_map/ppermute | solution.py:522
  155.5 6.4 %collective-permute-start.38 = (bf16[256,256]{1,0:T(8,128)(2,1)S(1)}, bf16[256,256]{1,0:T(8,128)(2,1)S(1)}, u32[]{:S(2)}, u32[]{:S(2)}) collective-permute-start(bf16[256,256]{1,0:T(8,128)(2,1)S(1)} %get-tuple-element.79), channel_id=1, source_target_pairs={{0,24},{8,0},{16,8},{24,16},{32,56},{40,32},{48,40},{56,48},{64,88... | collective-permute-start | bytes 393224 | tf_op jit(solution)/shard_map/ppermute | solution.py:522
  (13 other events, 38.2 us)

commit v8 on v6

--- a/solution.py
+++ b/solution.py
@@ -29,6 +29,10 @@
     after, before = (lax.ppermute(array, axis, axis_perm(-r)) for r in (1, SIDE - 1))
     across = lax.ppermute(after, axis, axis_perm(-1))
     return [array, after, across, before]
+
+
+def fetched_direct(array, axis_perm):
+    return [array] + [lax.ppermute(array, "sp", axis_perm(-r)) for r in range(1, SIDE)]
 
 
 def dot_nt(a, b):
@@ -212,8 +216,8 @@
 def grads_kernel(bias_ref, *rest):
     z_refs, x_refs = rest[:4], rest[4:8]
     stat_refs = (rest[8:12], rest[12:16])
-    outs = rest[16:32]
-    bias, qd, kv, bcol, parts, rows, kt, dqt, dkv, dq_send, dkv_send, sems = rest[32:]
+    own_dq, dq_outs, dkv_outs = rest[16], rest[17:23], rest[23:31]
+    bias, qd, kv, bcol, parts, rows, kt, dqt, dkv, dq_send, dkv_send, sems = rest[31:]
     span = qd.shape[2]
     begin = copy_list(sems)
     bias_copy = begin(bias_ref, bias)
@@ -259,7 +263,7 @@
     for h in range(2):
         wait_all(loads[h])
         combine(h)
-        key_outs = outs[8 + SIDE * h : 8 + SIDE * (h + 1)]
+        key_outs = dkv_outs[SIDE * h : SIDE * (h + 1)]
         key_sources = [dkv.at[h, 0]] + [dkv_send.at[h, r] for r in range(1, SIDE)]
         key_stores = [
             pltpu.make_async_copy(source, out, sems.at[40 + SIDE * h + r])
@@ -289,10 +293,10 @@
         lax.fori_loop(0, SIDE, one_key_span, 0)
         stores += key_stores
         dqt[h, 0] = dqt[h, 0] * SCALE
-        stores.append(begin(dqt.at[h, 0], outs[SIDE * h]))
+        stores.append(begin(dqt.at[h, 0], own_dq.at[pl.ds(h * HEAD, HEAD), :]))
         for r in range(1, SIDE):
             dq_send[h, r] = (dqt[h, r] * SCALE).astype(jnp.bfloat16)
-            stores.append(begin(dq_send.at[h, r], outs[SIDE * h + r]))
+            stores.append(begin(dq_send.at[h, r], dq_outs[3 * h + r - 1]))
     wait_all(stores)
 
 
@@ -318,11 +322,13 @@
         outs[r][...] = total.astype(outs[r].dtype)
 
 
-def query_kernel(*refs):
-    parts, (low_ref, grad_ref) = refs[:8], refs[8:]
-    for h in range(2):
-        total = sum(ref[...].astype(jnp.float32) for ref in parts[SIDE * h : SIDE * (h + 1)])
+def query_kernel(own_ref, *refs):
+    parts, (low_ref, grad_ref) = refs[:6], refs[6:]
+    for h in range(2):
         cut = slice(h * HEAD, (h + 1) * HEAD)
+        total = own_ref[cut, :]
+        for ref in parts[3 * h : 3 * (h + 1)]:
+            total = total + ref[...].astype(jnp.float32)
         low_ref[cut, :] = total.astype(jnp.bfloat16)
         grad_ref[:, cut] = total.T
 
@@ -380,16 +386,15 @@
     span = z_parts[0].shape[0]
     pairs = 17 * span * span
 
-    def shapes(*shape):
-        own = jax.ShapeDtypeStruct(shape, jnp.float32)
-        send = jax.ShapeDtypeStruct(shape, jnp.bfloat16)
-        return ([own] + [send] * 3) * 2
-
+    own_dq = jax.ShapeDtypeStruct((2 * HEAD, span), jnp.float32)
+    send_dq = jax.ShapeDtypeStruct((HEAD, span), jnp.bfloat16)
+    own_dkv = jax.ShapeDtypeStruct((span, 2 * HEAD), jnp.float32)
+    send_dkv = jax.ShapeDtypeStruct((span, 2 * HEAD), jnp.bfloat16)
     outs = pl.pallas_call(
         grads_kernel,
-        out_shape=shapes(HEAD, span) + shapes(span, 2 * HEAD),
+        out_shape=[own_dq] + [send_dq] * 6 + ([own_dkv] + [send_dkv] * 3) * 2,
         in_specs=[ANY] * 17,
-        out_specs=[ANY] * 16,
+        out_specs=[ANY] * 15,
         scratch_shapes=[
             pltpu.VMEM(bias.shape, jnp.float32),
             pltpu.VMEM((2, SIDE, span, 2 * HEAD), jnp.bfloat16),
@@ -410,7 +415,7 @@
         ),
         name="grads",
     )(bias, *z_parts, *x_parts, *z_stats, *x_stats)
-    return outs[:4], outs[4:8], outs[8:12], outs[12:]
+    return outs[0], outs[1:4], outs[4:7], outs[7:11], outs[11:]
 
 
 def weight_call(query_grads, inputs):
@@ -436,20 +441,20 @@
     )(*query_grads, *inputs)
 
 
-def query_call(parts_0, parts_1):
-    rows, span = parts_0[0].shape
+def query_call(own, parts_0, parts_1):
+    rows, span = own.shape
     return pl.pallas_call(
         query_kernel,
         out_shape=[
-            jax.ShapeDtypeStruct((2 * rows, span), jnp.bfloat16),
-            jax.ShapeDtypeStruct((span, 2 * rows), jnp.float32),
+            jax.ShapeDtypeStruct((rows, span), jnp.bfloat16),
+            jax.ShapeDtypeStruct((span, rows), jnp.float32),
         ],
-        in_specs=[VM] * 8,
+        in_specs=[VM] * 7,
         out_specs=[VM] * 2,
         compiler_params=pltpu.CompilerParams(vmem_limit_bytes=16 << 20),
         cost_estimate=pl.CostEstimate(flops=10**6, bytes_accessed=2 << 20, transcendentals=0),
         name="query_sums",
-    )(*parts_0, *parts_1)
+    )(own, *parts_0, *parts_1)
 
 
 def keys_call(parts_0, parts_1):
@@ -501,19 +506,20 @@
 
     *known, bias = stats_call(gates, z_parts, x_parts)
     stats_z, stats_x = stats_call(bias, z_parts, x_parts, known)
-    z_stats = fetched(stats_z, along_z)
-    x_stats = fetched(stats_x, along_x)
-    dq_0, dq_1, dkv_0, dkv_1 = grads_call(bias, z_parts, x_parts, z_stats, x_stats)
+    z_stats = fetched_direct(stats_z, along_z)
+    x_stats = fetched_direct(stats_x, along_x)
+    own_dq, dq_0, dq_1, dkv_0, dkv_1 = grads_call(bias, z_parts, x_parts, z_stats, x_stats)
+
+    def sent(parts, axis_perm):
+        return [lax.ppermute(part, "sp", axis_perm(r + 1)) for r, part in enumerate(parts)]
 
     def arrived(parts, axis_perm):
-        return [parts[0]] + [
-            lax.ppermute(parts[r], "sp", axis_perm(r)) for r in range(1, SIDE)
-        ]
-
-    dq_0, dq_1 = arrived(dq_0, along_z), arrived(dq_1, along_x)
-    low, query_grad = query_call(dq_0, dq_1)
+        return [parts[0]] + sent(parts[1:], axis_perm)
+
+    dq_0, dq_1 = sent(dq_0, along_z), sent(dq_1, along_x)
+    low, query_grad = query_call(own_dq, dq_0, dq_1)
     low, dkv_0, dkv_1 = lax.optimization_barrier((low, dkv_0, dkv_1))
-    low_parts = fetched(low, along_z)
+    low_parts = fetched_direct(low, along_z)
     terms = weight_call(low_parts, inputs)
     terms = arrived(terms, along_x)
     weight_grad = sum(part.astype(jnp.float32) for part in terms).T

time: 161 us -> 161 us (level)
  starting transfers between devices: 55.1 us -> 59.2 us
  waiting for transfers between devices: 37.6 us -> 35.1 us
    ppermute x15 -> x24, starting transfers between devices: 13.9 us -> 35.6 us  [the longest x15 21.7 us: sent(): lax.ppermute(part, 'sp', axis_perm(r + 1))]
    ppermute x12 -> x6, starting transfers between devices: 21.2 us -> 10.2 us  [fetched(): lax.ppermute(array, axis, axis_perm(-r))]
    ppermute x6 -> x3, starting transfers between devices: 16.3 us -> 9.32 us  [fetched(): across = lax.ppermute(after, axis, axis_perm(-1))]
    ppermute x12 -> x6, waiting for transfers between devices: 11.1 us -> 6.73 us  [fetched(): lax.ppermute(array, axis, axis_perm(-r))]
    ppermute x15 -> x24, waiting for transfers between devices: 25.7 us -> 28.4 us  [the longest x15 17 us: sent(): lax.ppermute(part, 'sp', axis_perm(r + 1))]
    unnamed x45 -> x43, local copies, waits for them, and re-layouts: 4.87 us -> 4.01 us
  transfers between devices with their start and end apart: 39 -> 39, of which waited for: 12 -> 13; matrix products, arithmetic and copies ran while one was open for 0% -> 0% of each run, Pallas kernels for 26% -> 26%
where the time goes in v8:
time: 161 us
  starting transfers between devices  59.2 us (37%)
  Pallas kernels  42.2 us (26%)
  waiting for transfers between devices  35.1 us (22%)
  blocking collectives  18.1 us (11%)
  local copies, waits for them, and re-layouts  5.3 us (3%)
    ppermute x15, starting transfers between devices, sent(): lax.ppermute(part, 'sp', axis_perm(r + 1))  21.7 us
    pallas_call x1, Pallas kernels, grads_call(): pl.pallas_call(grads_kernel, out_shape=[own_dq] + [send_dq] * 6 + ([own_d...  20.1 us
    all_to_all x1, blocking collectives, local(): gates = lax.all_to_all(gates, 'sp', 0, 0, tiled=True)  18.1 us
    pallas_call x2, Pallas kernels, stats_call(): pl.pallas_call(functools.partial(stats_kernel, slots, pair_count, pair_of...  17.7 us
    ppermute x15, waiting for transfers between devices, sent(): lax.ppermute(part, 'sp', axis_perm(r + 1))  17 us
    ppermute x9, starting transfers between devices, fetched_direct(): lax.ppermute(array, 'sp', axis_perm(-r))  13.9 us
    ppermute x9, waiting for transfers between devices, fetched_direct(): lax.ppermute(array, 'sp', axis_perm(-r))  11.4 us
    ppermute x6, starting transfers between devices, fetched(): lax.ppermute(array, axis, axis_perm(-r))  10.2 us
  transfers between devices with their start and end apart: 39, of which 13 were waited for; matrix products, arithmetic and copies ran while one was open for 0% of the time, Pallas kernels for 26%

profile of v8, /device:TPU:0, one launch (start us, length us, event | category | flops | bytes accessed | tf_op | source)
XLA Modules:
  0.0 161.0 jit_solution(8785203054668735484)
XLA Ops:
  0.7 1.2 fusion.2
  2.1 4.2 %collective-permute-start = (bf16[512,512]{1,0:T(8,128)(2,1)S(1)}, bf16[512,512]{1,0:T(8,128)(2,1)}, u32[]{:S(2)}, u32[]{:S(2)}) collective-permute-start(bf16[512,512]{1,0:T(8,128)(2,1)S(1)} %pad_maximum_fusion.rest_0_), channel_id=1, source_target_pairs={{0,96},{8,104},{16,112},{24,120},{32,0},{40,8},{48,16},{56,24},{64... | collective-permute-start | bytes 1572872 | tf_op jit(solution)/shard_map/ppermute | solution.py:29
  6.4 2.8 %collective-permute-start.2 = (bf16[512,512]{1,0:T(8,128)(2,1)S(1)}, bf16[512,512]{1,0:T(8,128)(2,1)}, u32[]{:S(2)}, u32[]{:S(2)}) collective-permute-start(bf16[512,512]{1,0:T(8,128)(2,1)S(1)} %pad_maximum_fusion.1.rest_3_.rest_4_), channel_id=1, source_target_pairs={{0,24},{8,0},{16,8},{24,16},{32,56},{40,32},{48,40},{56,48},{64,88... | collective-permute-start | bytes 1572872 | tf_op jit(solution)/shard_map/ppermute | solution.py:29
  9.2 1.4 collective-permute-start.27
  10.8 6.7 %collective-permute-done.rest_1_ = bf16[512,512]{1,0:T(8,128)(2,1)} collective-permute-done((bf16[512,512]{1,0:T(8,128)(2,1)S(1)}, bf16[512,512]{1,0:T(8,128)(2,1)}, u32[]{:S(2)}, u32[]{:S(2)}) %collective-permute-start) | collective-permute-done | bytes 524320 | tf_op jit(solution)/shard_map/ppermute | solution.py:29
  17.5 3.8 %collective-permute-start.4 = (bf16[512,512]{1,0:T(8,128)(2,1)}, bf16[512,512]{1,0:T(8,128)(2,1)}, u32[]{:S(2)}, u32[]{:S(2)}) collective-permute-start(bf16[512,512]{1,0:T(8,128)(2,1)} %collective-permute-done.rest_1_), channel_id=1, source_target_pairs={{0,96},{8,104},{16,112},{24,120},{32,0},{40,8},{48,16},{56,24},{64... | collective-permute-start | bytes 1572872 | tf_op jit(solution)/shard_map/ppermute | solution.py:30
  21.3 2.8 %collective-permute-start.5 = (bf16[512,512]{1,0:T(8,128)(2,1)}, bf16[512,512]{1,0:T(8,128)(2,1)}, u32[]{:S(2)}, u32[]{:S(2)}) collective-permute-start(bf16[512,512]{1,0:T(8,128)(2,1)} %collective-permute-done.2.rest_4_.rest_5_), channel_id=1, source_target_pairs={{0,24},{8,0},{16,8},{24,16},{32,56},{40,32},{48,40},{56,48},{64,88... | collective-permute-start | bytes 1572872 | tf_op jit(solution)/shard_map/ppermute | solution.py:30
  24.1 1.7 %collective-permute-start.28 = (bf16[512,512]{1,0:T(8,128)(2,1)}, bf16[512,512]{1,0:T(8,128)(2,1)S(1)}, u32[]{:S(2)}, u32[]{:S(2)}) collective-permute-start(bf16[512,512]{1,0:T(8,128)(2,1)} %collective-permute-done.27), channel_id=1, source_target_pairs={{0,0},{1,1},{2,34},{3,35},{4,68},{5,69},{6,102},{7,103},{8,8},{9,9... | collective-permute-start | bytes 1572872 | tf_op jit(solution)/shard_map/ppermute | solution.py:502
  25.8 18.1 %all_to_all.5.bias_ref = f32[16,2,512]{2,1,0:T(2,128)} all-to-all(f32[16,2,512]{2,1,0:T(2,128)S(1)} %broadcast_in_dim.3), channel_id=1, replica_groups=mesh['sp'=16,'tp'=8] {'sp'}, dimensions={0} | all-to-all | bytes 131072 | tf_op jit(solution)/shard_map/all_to_all | solution.py:481
  43.8 0.8 copy-done.5
  44.6 10.2 %stats.2 = (f32[4,8,512]{2,1,0:T(8,128)}, f32[4,8,512]{2,1,0:T(8,128)}, f32[32,512]{1,0:T(8,128)}) custom-call(f32[16,2,512]{2,1,0:T(2,128)} %all_to_all.5.bias_ref, bf16[512,512]{1,0:T(8,128)(2,1)} %copy-done.3, bf16[512,512]{1,0:T(8,128)(2,1)} %collective-permute-done.rest_1_, bf16[512,512]{1,0:T(8,128)(2,1)} %copy-done.5, bf16[512,512]{1,0:T(8,128)(2,1)} %copy-done.4, ...), custom_call_target="tpu_custom_call" | custom-call | flops 1207959552 | bytes 4194304 | tf_op jit(solution)/shard_map/stats/pallas_call | solution.py:371
  54.9 7.5 %stats.3 = (f32[4,8,512]{2,1,0:T(8,128)}, f32[4,8,512]{2,1,0:T(8,128)}) custom-call(f32[32,512]{1,0:T(8,128)} %get-tuple-element.41.bias_ref, bf16[512,512]{1,0:T(8,128)(2,1)} %copy-done.3, bf16[512,512]{1,0:T(8,128)(2,1)} %collective-permute-done.rest_1_, bf16[512,512]{1,0:T(8,128)(2,1)} %collective-permute-done.4.rest_2_, bf16[512,512]{1,0:T(8,128)(2,1)} %copy-done.5, ...), custom_call_target="tpu_custom_call" | custom-call | flops 939524096 | bytes 4194304 | tf_op jit(solution)/shard_map/stats/pallas_call | solution.py:371
  62.3 1.7 %collective-permute-start.8 = (f32[4,8,512]{2,1,0:T(8,128)}, f32[4,8,512]{2,1,0:T(8,128)S(1)}, u32[]{:S(2)}, u32[]{:S(2)}) collective-permute-start(f32[4,8,512]{2,1,0:T(8,128)} %get-tuple-element.44.rest_8_), channel_id=1, source_target_pairs={{0,32},{8,40},{16,48},{24,56},{32,64},{40,72},{48,80},{56,88},{64,... | collective-permute-start | bytes 196616 | tf_op jit(solution)/shard_map/ppermute | solution.py:35
  64.0 3.6 %collective-permute-start.7 = (f32[4,8,512]{2,1,0:T(8,128)}, f32[4,8,512]{2,1,0:T(8,128)S(1)}, u32[]{:S(2)}, u32[]{:S(2)}) collective-permute-start(f32[4,8,512]{2,1,0:T(8,128)} %get-tuple-element.44.rest_8_), channel_id=1, source_target_pairs={{0,64},{8,72},{16,80},{24,88},{32,96},{40,104},{48,112},{56,120},{... | collective-permute-start | bytes 196616 | tf_op jit(solution)/shard_map/ppermute | solution.py:35
  67.6 1.5 collective-permute-start.11
  69.1 2.7 %collective-permute-start.10 = (f32[4,8,512]{2,1,0:T(8,128)}, f32[4,8,512]{2,1,0:T(8,128)S(1)}, u32[]{:S(2)}, u32[]{:S(2)}) collective-permute-start(f32[4,8,512]{2,1,0:T(8,128)} %get-tuple-element.45.rest_12_), channel_id=1, source_target_pairs={{0,16},{8,24},{16,0},{24,8},{32,48},{40,56},{48,32},{56,40},{64,80... | collective-permute-start | bytes 196616 | tf_op jit(solution)/shard_map/ppermute | solution.py:35
  71.9 1.4 collective-permute-start.9
  73.3 3.0 %collective-permute-start.29 = (bf16[512,512]{1,0:T(8,128)(2,1)S(1)}, bf16[512,512]{1,0:T(8,128)(2,1)S(1)}, u32[]{:S(2)}, u32[]{:S(2)}) collective-permute-start(bf16[512,512]{1,0:T(8,128)(2,1)S(1)} %collective-permute-done.28.rest_4_), channel_id=1, source_target_pairs={{0,6},{1,7},{2,0},{3,1},{4,2},{5,3},{6,4},{7,5},{8,14},{9,15},{10,... | collective-permute-start | bytes 1572872 | tf_op jit(solution)/shard_map/ppermute | solution.py:29
  77.0 0.6 copy-done.20
  77.6 20.1 %grads.1 = (f32[256,512]{1,0:T(8,128)}, bf16[128,512]{1,0:T(8,128)(2,1)}, bf16[128,512]{1,0:T(8,128)(2,1)}, bf16[128,512]{1,0:T(8,128)(2,1)}, bf16[128,512]{1,0:...) custom-call(f32[32,512]{1,0:T(8,128)} %get-tuple-element.41.bias_ref, ...), custom_call_target="tpu_custom_call" | custom-call | flops 5704253440 | bytes 8388608 | tf_op jit(solution)/shard_map/grads/pallas_call | solution.py:393
  97.8 2.1 %collective-permute-start.12 = (bf16[128,512]{1,0:T(8,128)(2,1)}, bf16[128,512]{1,0:T(8,128)(2,1)S(1)}, u32[]{:S(2)}, u32[]{:S(2)}) collective-permute-start(bf16[128,512]{1,0:T(8,128)(2,1)} %get-tuple-element.47), channel_id=1, source_target_pairs={{0,32},{8,40},{16,48},{24,56},{32,64},{40,72},{48,80},{56,88},{64,... | collective-permute-start | bytes 393224 | tf_op jit(solution)/shard_map/ppermute | solution.py:514
  99.9 2.8 %collective-permute-start.14 = (bf16[128,512]{1,0:T(8,128)(2,1)}, bf16[128,512]{1,0:T(8,128)(2,1)S(1)}, u32[]{:S(2)}, u32[]{:S(2)}) collective-permute-start(bf16[128,512]{1,0:T(8,128)(2,1)} %get-tuple-element.49), channel_id=1, source_target_pairs={{0,96},{8,104},{16,112},{24,120},{32,0},{40,8},{48,16},{56,24},{64... | collective-permute-start | bytes 393224 | tf_op jit(solution)/shard_map/ppermute | solution.py:514
  102.6 1.6 collective-permute-done.12.refs_0_
  104.8 1.7 %collective-permute-done.13.refs_1_ = bf16[128,512]{1,0:T(8,128)(2,1)S(1)} collective-permute-done((bf16[128,512]{1,0:T(8,128)(2,1)}, bf16[128,512]{1,0:T(8,128)(2,1)S(1)}, u32[]{:S(2)}, u32[]{:S(2)}) %collective-permute-start.13) | collective-permute-done | bytes 131104 | tf_op jit(solution)/shard_map/ppermute | solution.py:514
  106.5 1.5 collective-permute-start.16
  108.0 1.8 %collective-permute-start.17 = (bf16[128,512]{1,0:T(8,128)(2,1)}, bf16[128,512]{1,0:T(8,128)(2,1)S(1)}, u32[]{:S(2)}, u32[]{:S(2)}) collective-permute-start(bf16[128,512]{1,0:T(8,128)(2,1)} %get-tuple-element.52), channel_id=1, source_target_pairs={{0,24},{8,0},{16,8},{24,16},{32,56},{40,32},{48,40},{56,48},{64,88... | collective-permute-start | bytes 393224 | tf_op jit(solution)/shard_map/ppermute | solution.py:514
  109.8 2.8 %collective-permute-start.30 = (bf16[512,512]{1,0:T(8,128)(2,1)S(1)}, bf16[512,512]{1,0:T(8,128)(2,1)S(1)}, u32[]{:S(2)}, u32[]{:S(2)}) collective-permute-start(bf16[512,512]{1,0:T(8,128)(2,1)S(1)} %collective-permute-done.29.rest_5_), channel_id=1, source_target_pairs={{0,6},{1,7},{2,0},{3,1},{4,2},{5,3},{6,4},{7,5},{8,14},{9,15},{10,... | collective-permute-start | bytes 1572872 | tf_op jit(solution)/shard_map/ppermute | solution.py:30
  112.6 0.7 collective-permute-done.16.refs_4_
  113.2 0.7 collective-permute-done.17.refs_5_
  114.0 1.0 copy-done.2
  115.0 1.0 query_sums.1
  116.0 1.2 collective-permute-start.18
  117.5 2.5 %collective-permute-start.25 = (bf16[256,512]{1,0:T(8,128)(2,1)S(1)}, bf16[256,512]{1,0:T(8,128)(2,1)S(1)}, u32[]{:S(2)}, u32[]{:S(2)}) collective-permute-start(bf16[256,512]{1,0:T(8,128)(2,1)S(1)} %get-tuple-element.73.rest_0_), channel_id=1, source_target_pairs={{0,64},{8,72},{16,80},{24,88},{32,96},{40,104},{48,112},{56,120},{... | collective-permute-start | bytes 786440 | tf_op jit(solution)/shard_map/ppermute | solution.py:35
  120.0 3.9 %collective-permute-done.18.refs_1_ = bf16[512,256]{1,0:T(8,128)(2,1)S(1)} collective-permute-done((bf16[512,256]{1,0:T(8,128)(2,1)}, bf16[512,256]{1,0:T(8,128)(2,1)S(1)}, u32[]{:S(2)}, u32[]{:S(2)}) %collective-permute-start.18) | collective-permute-done | bytes 262176 | tf_op jit(solution)/shard_map/ppermute | solution.py:514
  124.3 3.3 %collective-permute-done.26.rest_3_ = bf16[256,512]{1,0:T(8,128)(2,1)S(1)} collective-permute-done((bf16[256,512]{1,0:T(8,128)(2,1)S(1)}, bf16[256,512]{1,0:T(8,128)(2,1)S(1)}, u32[]{:S(2)}, u32[]{:S(2)}) %collective-permute-start.26) | collective-permute-done | bytes 262176 | tf_op jit(solution)/shard_map/ppermute | solution.py:35
  128.4 8.1 %collective-permute-done.24.rest_1_ = bf16[256,512]{1,0:T(8,128)(2,1)S(1)} collective-permute-done((bf16[256,512]{1,0:T(8,128)(2,1)S(1)}, bf16[256,512]{1,0:T(8,128)(2,1)S(1)}, u32[]{:S(2)}, u32[]{:S(2)}) %collective-permute-start.24) | collective-permute-done | bytes 262176 | tf_op jit(solution)/shard_map/ppermute | solution.py:35
  136.5 2.9 %collective-permute-start.19 = (bf16[512,256]{1,0:T(8,128)(2,1)S(1)}, bf16[512,256]{1,0:T(8,128)(2,1)S(1)}, u32[]{:S(2)}, u32[]{:S(2)}) collective-permute-start(bf16[512,256]{1,0:T(8,128)(2,1)S(1)} %copy-done.14), channel_id=1, source_target_pairs={{0,16},{8,24},{16,0},{24,8},{32,48},{40,56},{48,32},{56,40},{64,80... | collective-permute-start | bytes 786440 | tf_op jit(solution)/shard_map/ppermute | solution.py:514
  139.7 2.9 %collective-permute-start.22 = (bf16[512,256]{1,0:T(8,128)(2,1)S(1)}, bf16[512,256]{1,0:T(8,128)(2,1)S(1)}, u32[]{:S(2)}, u32[]{:S(2)}) collective-permute-start(bf16[512,256]{1,0:T(8,128)(2,1)S(1)} %copy-done.11), channel_id=1, source_target_pairs={{0,64},{8,72},{16,80},{24,88},{32,96},{40,104},{48,112},{56,120},{... | collective-permute-start | bytes 786440 | tf_op jit(solution)/shard_map/ppermute | solution.py:514
  143.3 1.8 %weight.1 = (f32[256,256]{1,0:T(8,128)S(1)}, bf16[256,256]{1,0:T(8,128)(2,1)S(1)}, bf16[256,256]{1,0:T(8,128)(2,1)S(1)}, bf16[256,256]{1,0:T(8,128)(2,1)S(1)}) custom-call(bf16[256,512]{1,0:T(8,128)(2,1)S(1)} %get-tuple-element.73.rest_0_, bf16[256,512]{1,0:T(8,128)(2,1)S(1)} %collective-permute-done.24.rest_1_, ...), custom_call_target="tpu_custom_call" | custom-call | flops 1073741824 | bytes 6291456 | tf_op jit(solution)/shard_map/weight/pallas_call | solution.py:426
  145.4 2.4 %collective-permute-start.36 = (bf16[256,256]{1,0:T(8,128)(2,1)S(1)}, bf16[256,256]{1,0:T(8,128)(2,1)S(1)}, u32[]{:S(2)}, u32[]{:S(2)}) collective-permute-start(bf16[256,256]{1,0:T(8,128)(2,1)S(1)} %get-tuple-element.75), channel_id=1, source_target_pairs={{0,8},{8,16},{16,24},{24,0},{32,40},{40,48},{48,56},{56,32},{64,72... | collective-permute-start | bytes 393224 | tf_op jit(solution)/shard_map/ppermute | solution.py:514
  147.8 2.6 %collective-permute-done.20.refs_3_ = bf16[512,256]{1,0:T(8,128)(2,1)S(1)} collective-permute-done((bf16[512,256]{1,0:T(8,128)(2,1)S(1)}, bf16[512,256]{1,0:T(8,128)(2,1)S(1)}, u32[]{:S(2)}, u32[]{:S(2)}) %collective-permute-start.20) | collective-permute-done | bytes 262176 | tf_op jit(solution)/shard_map/ppermute | solution.py:514
  150.4 1.8 %collective-permute-start.37 = (bf16[256,256]{1,0:T(8,128)(2,1)S(1)}, bf16[256,256]{1,0:T(8,128)(2,1)S(1)}, u32[]{:S(2)}, u32[]{:S(2)}) collective-permute-start(bf16[256,256]{1,0:T(8,128)(2,1)S(1)} %get-tuple-element.76), channel_id=1, source_target_pairs={{0,16},{8,24},{16,0},{24,8},{32,48},{40,56},{48,32},{56,40},{64,80... | collective-permute-start | bytes 393224 | tf_op jit(solution)/shard_map/ppermute | solution.py:514
  152.2 1.2 collective-permute-done.21.refs_5_
  153.4 0.8 collective-permute-start.38
  154.3 1.6 key_sums.1
  155.9 1.0 collective-permute-done.37
  156.9 3.2 %collective-permute-done.38 = bf16[256,256]{1,0:T(8,128)(2,1)S(1)} collective-permute-done((bf16[256,256]{1,0:T(8,128)(2,1)S(1)}, bf16[256,256]{1,0:T(8,128)(2,1)S(1)}, u32[]{:S(2)}, u32[]{:S(2)}) %collective-permute-start.38) | collective-permute-done | bytes 131104 | tf_op jit(solution)/shard_map/ppermute | solution.py:514
  160.1 0.8 copy.10
  (86 shorter events, 4.4 us)
Async XLA Ops:
  2.1 15.4 %collective-permute-start = (bf16[512,512]{1,0:T(8,128)(2,1)S(1)}, bf16[512,512]{1,0:T(8,128)(2,1)}, u32[]{:S(2)}, u32[]{:S(2)}) collective-permute-start(bf16[512,512]{1,0:T(8,128)(2,1)S(1)} %pad_maximum_fusion.rest_0_), channel_id=1, source_target_pairs={{0,96},{8,104},{16,112},{24,120},{32,0},{40,8},{48,16},{56,24},{64... | collective-permute-start | bytes 1572872 | tf_op jit(solution)/shard_map/ppermute | solution.py:29
  6.3 19.4 %copy-start.8 = (f32[512,2]{0,1:T(2,128)S(1)}, f32[512,2]{0,1:T(2,128)}, u32[]{:S(2)}) copy-start(f32[512,2]{0,1:T(2,128)} %param.9) | copy-start | bytes 12292
  6.4 38.3 %copy-start.4 = (bf16[512,512]{1,0:T(8,128)(2,1)}, bf16[512,512]{1,0:T(8,128)(2,1)S(1)}, u32[]{:S(2)}) copy-start(bf16[512,512]{1,0:T(8,128)(2,1)S(1)} %pad_maximum_fusion.1.rest_3_.rest_4_) | copy-start | bytes 1572868
  6.4 14.9 %collective-permute-start.2 = (bf16[512,512]{1,0:T(8,128)(2,1)S(1)}, bf16[512,512]{1,0:T(8,128)(2,1)}, u32[]{:S(2)}, u32[]{:S(2)}) collective-permute-start(bf16[512,512]{1,0:T(8,128)(2,1)S(1)} %pad_maximum_fusion.1.rest_3_.rest_4_), channel_id=1, source_target_pairs={{0,24},{8,0},{16,8},{24,16},{32,56},{40,32},{48,40},{56,48},{64,88... | collective-permute-start | bytes 1572872 | tf_op jit(solution)/shard_map/ppermute | solution.py:29
  9.2 14.8 %collective-permute-start.27 = (bf16[512,512]{1,0:T(8,128)(2,1)S(1)}, bf16[512,512]{1,0:T(8,128)(2,1)}, u32[]{:S(2)}, u32[]{:S(2)}) collective-permute-start(bf16[512,512]{1,0:T(8,128)(2,1)S(1)} %copy-done.9), channel_id=1, source_target_pairs={{0,0},{1,1},{2,2},{3,3},{4,4},{5,5},{6,6},{7,7},{8,8},{9,9},{10,10... | collective-permute-start | bytes 1572872 | tf_op jit(solution)/shard_map/ppermute | solution.py:501
  10.7 33.2 %collective-permute-start.1 = (bf16[512,512]{1,0:T(8,128)(2,1)S(1)}, bf16[512,512]{1,0:T(8,128)(2,1)S(1)}, u32[]{:S(2)}, u32[]{:S(2)}) collective-permute-start(bf16[512,512]{1,0:T(8,128)(2,1)S(1)} %pad_maximum_fusion.rest_0_), channel_id=1, source_target_pairs={{0,32},{8,40},{16,48},{24,56},{32,64},{40,72},{48,80},{56,88},{64,... | collective-permute-start | bytes 1572872 | tf_op jit(solution)/shard_map/ppermute | solution.py:29
  10.8 33.9 %collective-permute-start.3 = (bf16[512,512]{1,0:T(8,128)(2,1)S(1)}, bf16[512,512]{1,0:T(8,128)(2,1)}, u32[]{:S(2)}, u32[]{:S(2)}) collective-permute-start(bf16[512,512]{1,0:T(8,128)(2,1)S(1)} %pad_maximum_fusion.1.rest_3_.rest_4_), channel_id=1, source_target_pairs={{0,8},{8,16},{16,24},{24,0},{32,40},{40,48},{48,56},{56,32},{64,72... | collective-permute-start | bytes 1572872 | tf_op jit(solution)/shard_map/ppermute | solution.py:29
  17.5 37.4 %collective-permute-start.4 = (bf16[512,512]{1,0:T(8,128)(2,1)}, bf16[512,512]{1,0:T(8,128)(2,1)}, u32[]{:S(2)}, u32[]{:S(2)}) collective-permute-start(bf16[512,512]{1,0:T(8,128)(2,1)} %collective-permute-done.rest_1_), channel_id=1, source_target_pairs={{0,96},{8,104},{16,112},{24,120},{32,0},{40,8},{48,16},{56,24},{64... | collective-permute-start | bytes 1572872 | tf_op jit(solution)/shard_map/ppermute | solution.py:30
  21.3 33.6 %collective-permute-start.5 = (bf16[512,512]{1,0:T(8,128)(2,1)}, bf16[512,512]{1,0:T(8,128)(2,1)}, u32[]{:S(2)}, u32[]{:S(2)}) collective-permute-start(bf16[512,512]{1,0:T(8,128)(2,1)} %collective-permute-done.2.rest_4_.rest_5_), channel_id=1, source_target_pairs={{0,24},{8,0},{16,8},{24,16},{32,56},{40,32},{48,40},{56,48},{64,88... | collective-permute-start | bytes 1572872 | tf_op jit(solution)/shard_map/ppermute | solution.py:30
  24.1 45.1 %collective-permute-start.28 = (bf16[512,512]{1,0:T(8,128)(2,1)}, bf16[512,512]{1,0:T(8,128)(2,1)S(1)}, u32[]{:S(2)}, u32[]{:S(2)}) collective-permute-start(bf16[512,512]{1,0:T(8,128)(2,1)} %collective-permute-done.27), channel_id=1, source_target_pairs={{0,0},{1,1},{2,34},{3,35},{4,68},{5,69},{6,102},{7,103},{8,8},{9,9... | collective-permute-start | bytes 1572872 | tf_op jit(solution)/shard_map/ppermute | solution.py:502
  62.3 9.5 %collective-permute-start.8 = (f32[4,8,512]{2,1,0:T(8,128)}, f32[4,8,512]{2,1,0:T(8,128)S(1)}, u32[]{:S(2)}, u32[]{:S(2)}) collective-permute-start(f32[4,8,512]{2,1,0:T(8,128)} %get-tuple-element.44.rest_8_), channel_id=1, source_target_pairs={{0,32},{8,40},{16,48},{24,56},{32,64},{40,72},{48,80},{56,88},{64,... | collective-permute-start | bytes 196616 | tf_op jit(solution)/shard_map/ppermute | solution.py:35
  64.0 9.3 %collective-permute-start.7 = (f32[4,8,512]{2,1,0:T(8,128)}, f32[4,8,512]{2,1,0:T(8,128)S(1)}, u32[]{:S(2)}, u32[]{:S(2)}) collective-permute-start(f32[4,8,512]{2,1,0:T(8,128)} %get-tuple-element.44.rest_8_), channel_id=1, source_target_pairs={{0,64},{8,72},{16,80},{24,88},{32,96},{40,104},{48,112},{56,120},{... | collective-permute-start | bytes 196616 | tf_op jit(solution)/shard_map/ppermute | solution.py:35
  67.6 8.7 %collective-permute-start.6 = (f32[4,8,512]{2,1,0:T(8,128)}, f32[4,8,512]{2,1,0:T(8,128)S(1)}, u32[]{:S(2)}, u32[]{:S(2)}) collective-permute-start(f32[4,8,512]{2,1,0:T(8,128)} %get-tuple-element.44.rest_8_), channel_id=1, source_target_pairs={{0,96},{8,104},{16,112},{24,120},{32,0},{40,8},{48,16},{56,24},{64... | collective-permute-start | bytes 196616 | tf_op jit(solution)/shard_map/ppermute | solution.py:35
  67.6 8.7 %collective-permute-start.11 = (f32[4,8,512]{2,1,0:T(8,128)}, f32[4,8,512]{2,1,0:T(8,128)S(1)}, u32[]{:S(2)}, u32[]{:S(2)}) collective-permute-start(f32[4,8,512]{2,1,0:T(8,128)} %get-tuple-element.45.rest_12_), channel_id=1, source_target_pairs={{0,8},{8,16},{16,24},{24,0},{32,40},{40,48},{48,56},{56,32},{64,72... | collective-permute-start | bytes 196616 | tf_op jit(solution)/shard_map/ppermute | solution.py:35
  69.1 7.2 %collective-permute-start.10 = (f32[4,8,512]{2,1,0:T(8,128)}, f32[4,8,512]{2,1,0:T(8,128)S(1)}, u32[]{:S(2)}, u32[]{:S(2)}) collective-permute-start(f32[4,8,512]{2,1,0:T(8,128)} %get-tuple-element.45.rest_12_), channel_id=1, source_target_pairs={{0,16},{8,24},{16,0},{24,8},{32,48},{40,56},{48,32},{56,40},{64,80... | collective-permute-start | bytes 196616 | tf_op jit(solution)/shard_map/ppermute | solution.py:35
  71.9 4.5 %collective-permute-start.9 = (f32[4,8,512]{2,1,0:T(8,128)}, f32[4,8,512]{2,1,0:T(8,128)S(1)}, u32[]{:S(2)}, u32[]{:S(2)}) collective-permute-start(f32[4,8,512]{2,1,0:T(8,128)} %get-tuple-element.45.rest_12_), channel_id=1, source_target_pairs={{0,24},{8,0},{16,8},{24,16},{32,56},{40,32},{48,40},{56,48},{64,88... | collective-permute-start | bytes 196616 | tf_op jit(solution)/shard_map/ppermute | solution.py:35
  73.3 36.5 %collective-permute-start.29 = (bf16[512,512]{1,0:T(8,128)(2,1)S(1)}, bf16[512,512]{1,0:T(8,128)(2,1)S(1)}, u32[]{:S(2)}, u32[]{:S(2)}) collective-permute-start(bf16[512,512]{1,0:T(8,128)(2,1)S(1)} %collective-permute-done.28.rest_4_), channel_id=1, source_target_pairs={{0,6},{1,7},{2,0},{3,1},{4,2},{5,3},{6,4},{7,5},{8,14},{9,15},{10,... | collective-permute-start | bytes 1572872 | tf_op jit(solution)/shard_map/ppermute | solution.py:29
  97.8 6.5 %collective-permute-start.12 = (bf16[128,512]{1,0:T(8,128)(2,1)}, bf16[128,512]{1,0:T(8,128)(2,1)S(1)}, u32[]{:S(2)}, u32[]{:S(2)}) collective-permute-start(bf16[128,512]{1,0:T(8,128)(2,1)} %get-tuple-element.47), channel_id=1, source_target_pairs={{0,32},{8,40},{16,48},{24,56},{32,64},{40,72},{48,80},{56,88},{64,... | collective-permute-start | bytes 393224 | tf_op jit(solution)/shard_map/ppermute | solution.py:514
  99.8 6.7 %collective-permute-start.13 = (bf16[128,512]{1,0:T(8,128)(2,1)}, bf16[128,512]{1,0:T(8,128)(2,1)S(1)}, u32[]{:S(2)}, u32[]{:S(2)}) collective-permute-start(bf16[128,512]{1,0:T(8,128)(2,1)} %get-tuple-element.48), channel_id=1, source_target_pairs={{0,64},{8,72},{16,80},{24,88},{32,96},{40,104},{48,112},{56,120},{... | collective-permute-start | bytes 393224 | tf_op jit(solution)/shard_map/ppermute | solution.py:514
  99.9 8.1 %collective-permute-start.14 = (bf16[128,512]{1,0:T(8,128)(2,1)}, bf16[128,512]{1,0:T(8,128)(2,1)S(1)}, u32[]{:S(2)}, u32[]{:S(2)}) collective-permute-start(bf16[128,512]{1,0:T(8,128)(2,1)} %get-tuple-element.49), channel_id=1, source_target_pairs={{0,96},{8,104},{16,112},{24,120},{32,0},{40,8},{48,16},{56,24},{64... | collective-permute-start | bytes 393224 | tf_op jit(solution)/shard_map/ppermute | solution.py:514
  102.6 21.2 %collective-permute-start.31 = (bf16[512,512]{1,0:T(8,128)(2,1)S(1)}, bf16[512,512]{1,0:T(8,128)(2,1)S(1)}, u32[]{:S(2)}, u32[]{:S(2)}) collective-permute-start(bf16[512,512]{1,0:T(8,128)(2,1)S(1)} %collective-permute-done.28.rest_4_), channel_id=1, source_target_pairs={{0,2},{1,3},{2,4},{3,5},{4,6},{5,7},{6,0},{7,1},{8,10},{9,11},{10,... | collective-permute-start | bytes 1572872 | tf_op jit(solution)/shard_map/ppermute | solution.py:29
  104.2 8.3 %collective-permute-start.15 = (bf16[128,512]{1,0:T(8,128)(2,1)}, bf16[128,512]{1,0:T(8,128)(2,1)S(1)}, u32[]{:S(2)}, u32[]{:S(2)}) collective-permute-start(bf16[128,512]{1,0:T(8,128)(2,1)} %get-tuple-element.50), channel_id=1, source_target_pairs={{0,8},{8,16},{16,24},{24,0},{32,40},{40,48},{48,56},{56,32},{64,72... | collective-permute-start | bytes 393224 | tf_op jit(solution)/shard_map/ppermute | solution.py:514
  106.5 6.7 %collective-permute-start.16 = (bf16[128,512]{1,0:T(8,128)(2,1)}, bf16[128,512]{1,0:T(8,128)(2,1)S(1)}, u32[]{:S(2)}, u32[]{:S(2)}) collective-permute-start(bf16[128,512]{1,0:T(8,128)(2,1)} %get-tuple-element.51), channel_id=1, source_target_pairs={{0,16},{8,24},{16,0},{24,8},{32,48},{40,56},{48,32},{56,40},{64,80... | collective-permute-start | bytes 393224 | tf_op jit(solution)/shard_map/ppermute | solution.py:514
  108.0 6.0 %collective-permute-start.17 = (bf16[128,512]{1,0:T(8,128)(2,1)}, bf16[128,512]{1,0:T(8,128)(2,1)S(1)}, u32[]{:S(2)}, u32[]{:S(2)}) collective-permute-start(bf16[128,512]{1,0:T(8,128)(2,1)} %get-tuple-element.52), channel_id=1, source_target_pairs={{0,24},{8,0},{16,8},{24,16},{32,56},{40,32},{48,40},{56,48},{64,88... | collective-permute-start | bytes 393224 | tf_op jit(solution)/shard_map/ppermute | solution.py:514
  109.8 17.9 %collective-permute-start.30 = (bf16[512,512]{1,0:T(8,128)(2,1)S(1)}, bf16[512,512]{1,0:T(8,128)(2,1)S(1)}, u32[]{:S(2)}, u32[]{:S(2)}) collective-permute-start(bf16[512,512]{1,0:T(8,128)(2,1)S(1)} %collective-permute-done.29.rest_5_), channel_id=1, source_target_pairs={{0,6},{1,7},{2,0},{3,1},{4,2},{5,3},{6,4},{7,5},{8,14},{9,15},{10,... | collective-permute-start | bytes 1572872 | tf_op jit(solution)/shard_map/ppermute | solution.py:30
  115.0 21.5 %copy-start.14 = (bf16[512,256]{1,0:T(8,128)(2,1)S(1)}, bf16[512,256]{1,0:T(8,128)(2,1)}, u32[]{:S(2)}) copy-start(bf16[512,256]{1,0:T(8,128)(2,1)} %get-tuple-element.65) | copy-start | bytes 786436
  115.0 24.4 %copy-start.13 = (bf16[512,256]{1,0:T(8,128)(2,1)S(1)}, bf16[512,256]{1,0:T(8,128)(2,1)}, u32[]{:S(2)}) copy-start(bf16[512,256]{1,0:T(8,128)(2,1)} %get-tuple-element.66) | copy-start | bytes 786436
  115.0 24.7 %copy-start.12 = (bf16[512,256]{1,0:T(8,128)(2,1)S(1)}, bf16[512,256]{1,0:T(8,128)(2,1)}, u32[]{:S(2)}) copy-start(bf16[512,256]{1,0:T(8,128)(2,1)} %get-tuple-element.68) | copy-start | bytes 786436
  115.0 24.7 %copy-start.11 = (bf16[512,256]{1,0:T(8,128)(2,1)S(1)}, bf16[512,256]{1,0:T(8,128)(2,1)}, u32[]{:S(2)}) copy-start(bf16[512,256]{1,0:T(8,128)(2,1)} %get-tuple-element.69) | copy-start | bytes 786436
  115.0 27.7 %copy-start.10 = (bf16[512,256]{1,0:T(8,128)(2,1)S(1)}, bf16[512,256]{1,0:T(8,128)(2,1)}, u32[]{:S(2)}) copy-start(bf16[512,256]{1,0:T(8,128)(2,1)} %get-tuple-element.70) | copy-start | bytes 786436
  116.0 38.2 %copy-start = (f32[512,256]{1,0:T(8,128)S(1)}, f32[512,256]{1,0:T(8,128)}, u32[]{:S(2)}) copy-start(f32[512,256]{1,0:T(8,128)} %get-tuple-element.63.refs_0_) | copy-start | bytes 1572868
  116.0 38.3 %copy-start.1 = (f32[512,256]{1,0:T(8,128)S(1)}, f32[512,256]{1,0:T(8,128)}, u32[]{:S(2)}) copy-start(f32[512,256]{1,0:T(8,128)} %get-tuple-element.67.refs_4_) | copy-start | bytes 1572868
  116.0 7.8 %collective-permute-start.18 = (bf16[512,256]{1,0:T(8,128)(2,1)}, bf16[512,256]{1,0:T(8,128)(2,1)S(1)}, u32[]{:S(2)}, u32[]{:S(2)}) collective-permute-start(bf16[512,256]{1,0:T(8,128)(2,1)} %get-tuple-element.64), channel_id=1, source_target_pairs={{0,8},{8,16},{16,24},{24,0},{32,40},{40,48},{48,56},{56,32},{64,72... | collective-permute-start | bytes 786440 | tf_op jit(solution)/shard_map/ppermute | solution.py:514
  117.3 10.4 %collective-permute-start.26 = (bf16[256,512]{1,0:T(8,128)(2,1)S(1)}, bf16[256,512]{1,0:T(8,128)(2,1)S(1)}, u32[]{:S(2)}, u32[]{:S(2)}) collective-permute-start(bf16[256,512]{1,0:T(8,128)(2,1)S(1)} %get-tuple-element.73.rest_0_), channel_id=1, source_target_pairs={{0,32},{8,40},{16,48},{24,56},{32,64},{40,72},{48,80},{56,88},{64,... | collective-permute-start | bytes 786440 | tf_op jit(solution)/shard_map/ppermute | solution.py:35
  117.5 10.7 %collective-permute-start.25 = (bf16[256,512]{1,0:T(8,128)(2,1)S(1)}, bf16[256,512]{1,0:T(8,128)(2,1)S(1)}, u32[]{:S(2)}, u32[]{:S(2)}) collective-permute-start(bf16[256,512]{1,0:T(8,128)(2,1)S(1)} %get-tuple-element.73.rest_0_), channel_id=1, source_target_pairs={{0,64},{8,72},{16,80},{24,88},{32,96},{40,104},{48,112},{56,120},{... | collective-permute-start | bytes 786440 | tf_op jit(solution)/shard_map/ppermute | solution.py:35
  123.8 15.5 %collective-permute-start.32 = (bf16[512,512]{1,0:T(8,128)(2,1)S(1)}, bf16[512,512]{1,0:T(8,128)(2,1)S(1)}, u32[]{:S(2)}, u32[]{:S(2)}) collective-permute-start(bf16[512,512]{1,0:T(8,128)(2,1)S(1)} %collective-permute-done.28.rest_4_), channel_id=1, source_target_pairs={{0,1},{1,0},{2,3},{3,2},{4,5},{5,4},{6,7},{7,6},{8,9},{9,8},{10,11... | collective-permute-start | bytes 1572872 | tf_op jit(solution)/shard_map/ppermute | solution.py:505
  123.8 15.9 %collective-permute-start.35 = (bf16[512,512]{1,0:T(8,128)(2,1)S(1)}, bf16[512,512]{1,0:T(8,128)(2,1)S(1)}, u32[]{:S(2)}, u32[]{:S(2)}) collective-permute-start(bf16[512,512]{1,0:T(8,128)(2,1)S(1)} %collective-permute-done.31.rest_7_), channel_id=1, source_target_pairs={{0,1},{1,0},{2,3},{3,2},{4,5},{5,4},{6,7},{7,6},{8,9},{9,8},{10,11... | collective-permute-start | bytes 1572872 | tf_op jit(solution)/shard_map/ppermute | solution.py:505
  127.7 12.1 %collective-permute-start.33 = (bf16[512,512]{1,0:T(8,128)(2,1)S(1)}, bf16[512,512]{1,0:T(8,128)(2,1)S(1)}, u32[]{:S(2)}, u32[]{:S(2)}) collective-permute-start(bf16[512,512]{1,0:T(8,128)(2,1)S(1)} %collective-permute-done.29.rest_5_), channel_id=1, source_target_pairs={{0,1},{1,0},{2,3},{3,2},{4,5},{5,4},{6,7},{7,6},{8,9},{9,8},{10,11... | collective-permute-start | bytes 1572872 | tf_op jit(solution)/shard_map/ppermute | solution.py:505
  127.7 15.0 %collective-permute-start.34 = (bf16[512,512]{1,0:T(8,128)(2,1)S(1)}, bf16[512,512]{1,0:T(8,128)(2,1)S(1)}, u32[]{:S(2)}, u32[]{:S(2)}) collective-permute-start(bf16[512,512]{1,0:T(8,128)(2,1)S(1)} %collective-permute-done.30.rest_6_), channel_id=1, source_target_pairs={{0,1},{1,0},{2,3},{3,2},{4,5},{5,4},{6,7},{7,6},{8,9},{9,8},{10,11... | collective-permute-start | bytes 1572872 | tf_op jit(solution)/shard_map/ppermute | solution.py:505
  128.2 8.3 %collective-permute-start.24 = (bf16[256,512]{1,0:T(8,128)(2,1)S(1)}, bf16[256,512]{1,0:T(8,128)(2,1)S(1)}, u32[]{:S(2)}, u32[]{:S(2)}) collective-permute-start(bf16[256,512]{1,0:T(8,128)(2,1)S(1)} %get-tuple-element.73.rest_0_), channel_id=1, source_target_pairs={{0,96},{8,104},{16,112},{24,120},{32,0},{40,8},{48,16},{56,24},{64... | collective-permute-start | bytes 786440 | tf_op jit(solution)/shard_map/ppermute | solution.py:35
  136.5 8.9 %collective-permute-start.19 = (bf16[512,256]{1,0:T(8,128)(2,1)S(1)}, bf16[512,256]{1,0:T(8,128)(2,1)S(1)}, u32[]{:S(2)}, u32[]{:S(2)}) collective-permute-start(bf16[512,256]{1,0:T(8,128)(2,1)S(1)} %copy-done.14), channel_id=1, source_target_pairs={{0,16},{8,24},{16,0},{24,8},{32,48},{40,56},{48,32},{56,40},{64,80... | collective-permute-start | bytes 786440 | tf_op jit(solution)/shard_map/ppermute | solution.py:514
  139.4 11.0 %collective-permute-start.20 = (bf16[512,256]{1,0:T(8,128)(2,1)S(1)}, bf16[512,256]{1,0:T(8,128)(2,1)S(1)}, u32[]{:S(2)}, u32[]{:S(2)}) collective-permute-start(bf16[512,256]{1,0:T(8,128)(2,1)S(1)} %copy-done.13), channel_id=1, source_target_pairs={{0,24},{8,0},{16,8},{24,16},{32,56},{40,32},{48,40},{56,48},{64,88... | collective-permute-start | bytes 786440 | tf_op jit(solution)/shard_map/ppermute | solution.py:514
  139.7 13.7 %collective-permute-start.21 = (bf16[512,256]{1,0:T(8,128)(2,1)S(1)}, bf16[512,256]{1,0:T(8,128)(2,1)S(1)}, u32[]{:S(2)}, u32[]{:S(2)}) collective-permute-start(bf16[512,256]{1,0:T(8,128)(2,1)S(1)} %copy-done.12), channel_id=1, source_target_pairs={{0,32},{8,40},{16,48},{24,56},{32,64},{40,72},{48,80},{56,88},{64,... | collective-permute-start | bytes 786440 | tf_op jit(solution)/shard_map/ppermute | solution.py:514
  139.7 14.5 %collective-permute-start.22 = (bf16[512,256]{1,0:T(8,128)(2,1)S(1)}, bf16[512,256]{1,0:T(8,128)(2,1)S(1)}, u32[]{:S(2)}, u32[]{:S(2)}) collective-permute-start(bf16[512,256]{1,0:T(8,128)(2,1)S(1)} %copy-done.11), channel_id=1, source_target_pairs={{0,64},{8,72},{16,80},{24,88},{32,96},{40,104},{48,112},{56,120},{... | collective-permute-start | bytes 786440 | tf_op jit(solution)/shard_map/ppermute | solution.py:514
  142.7 11.6 %collective-permute-start.23 = (bf16[512,256]{1,0:T(8,128)(2,1)S(1)}, bf16[512,256]{1,0:T(8,128)(2,1)S(1)}, u32[]{:S(2)}, u32[]{:S(2)}) collective-permute-start(bf16[512,256]{1,0:T(8,128)(2,1)S(1)} %copy-done.10), channel_id=1, source_target_pairs={{0,96},{8,104},{16,112},{24,120},{32,0},{40,8},{48,16},{56,24},{64... | collective-permute-start | bytes 786440 | tf_op jit(solution)/shard_map/ppermute | solution.py:514
  145.4 10.5 %collective-permute-start.36 = (bf16[256,256]{1,0:T(8,128)(2,1)S(1)}, bf16[256,256]{1,0:T(8,128)(2,1)S(1)}, u32[]{:S(2)}, u32[]{:S(2)}) collective-permute-start(bf16[256,256]{1,0:T(8,128)(2,1)S(1)} %get-tuple-element.75), channel_id=1, source_target_pairs={{0,8},{8,16},{16,24},{24,0},{32,40},{40,48},{48,56},{56,32},{64,72... | collective-permute-start | bytes 393224 | tf_op jit(solution)/shard_map/ppermute | solution.py:514
  150.4 6.5 %collective-permute-start.37 = (bf16[256,256]{1,0:T(8,128)(2,1)S(1)}, bf16[256,256]{1,0:T(8,128)(2,1)S(1)}, u32[]{:S(2)}, u32[]{:S(2)}) collective-permute-start(bf16[256,256]{1,0:T(8,128)(2,1)S(1)} %get-tuple-element.76), channel_id=1, source_target_pairs={{0,16},{8,24},{16,0},{24,8},{32,48},{40,56},{48,32},{56,40},{64,80... | collective-permute-start | bytes 393224 | tf_op jit(solution)/shard_map/ppermute | solution.py:514
  153.4 6.6 %collective-permute-start.38 = (bf16[256,256]{1,0:T(8,128)(2,1)S(1)}, bf16[256,256]{1,0:T(8,128)(2,1)S(1)}, u32[]{:S(2)}, u32[]{:S(2)}) collective-permute-start(bf16[256,256]{1,0:T(8,128)(2,1)S(1)} %get-tuple-element.77), channel_id=1, source_target_pairs={{0,24},{8,0},{16,8},{24,16},{32,56},{40,32},{48,40},{56,48},{64,88... | collective-permute-start | bytes 393224 | tf_op jit(solution)/shard_map/ppermute | solution.py:514
  (12 other events, 25.9 us)
